TPU v7x, 32 devices: a whole 2x2x4 slice. The times are simulated.
32 devices in a mesh: grp: 2 (over y), ep: 4 (over z), tp: 4 (over x, core).
Axes of the slice: x: 2, y: 2, z: 4, core: 2. Of those that a mesh axis runs over, the one named last changes fastest.
Arguments:
- queries: bfloat16 [1024, 2048], P(('grp', 'ep'), 'tp'), parts along dimension 0, may hold values from -6 to 6
- keys: bfloat16 [1024, 2048], P(('grp', 'ep'), 'tp'), parts along dimension 0, may hold values from -6 to 6
- values: bfloat16 [1024, 2048], P(('grp', 'ep'), 'tp'), parts along dimension 0, may hold values from -6 to 6
- stop_bias: bfloat16 [1024, 32], P(('grp', 'ep'), 'tp'), parts along dimension 0, may hold values from -20 to 0
- out_weight: bfloat16 [2048, 2048], P('tp'), may hold values from -0.125 to 0.125
- mix_gain: float32 [2048], replicated, may hold values from 0.1 to 1.9
- moe_input: bfloat16 [4096, 2048], P(('grp', 'ep', 'tp')), parts along dimension 0, may hold values from -6 to 6
- ffn_gain: float32 [2048], replicated, may hold values from 0.1 to 1.9
- expert_ids: int32 [4096, 2], P(('grp', 'ep', 'tp')), parts along dimension 0, may hold values from 0 to 3, all different within a row; in each aligned block of 128 rows (0 to 127, 128 to 255, ...) at most 96 rows name the same one
- expert_scores: float32 [4096, 2], P(('grp', 'ep', 'tp')), parts along dimension 0, may hold values from 0.05 to 1
- gate_weight: bfloat16 [4, 2048, 1024], P('ep', None, 'tp'), may hold values from -0.125 to 0.125
- up_weight: bfloat16 [4, 2048, 1024], P('ep', None, 'tp'), may hold values from -0.125 to 0.125
- down_weight: bfloat16 [4, 1024, 2048], P('ep', 'tp'), may hold values from -0.1875 to 0.1875
Outputs:
- mixed: bfloat16 [1024, 2048], P(('grp', 'ep', 'tp')), parts along dimension 0
- experts_mixed: bfloat16 [4096, 2048], P(('grp', 'ep', 'tp')), parts along dimension 0
There are 2 independent parts, one for each index of `grp`. A program takes and returns all parts, laid end to end along the dimension named above; an argument that names none is the same for every part. Nothing has to cross between parts.
Inputs may be any that keep to these rules, and one draw needn't show every extreme that they name: `expert_ids`: each token names 2 different experts. Among the 128 tokens of one device, no expert is named by more than 96 tokens, and in some device's tokens some expert is named by exactly 96.
All inputs are finite; a program needn't handle non-finite values.
Results may differ from a plain program's by a relative error of at most 0.012.
Values may be sent and summed in bfloat16 or wider, within the bound.
No kernel may reach another device: no remote copies, remote signals or barrier semaphores. Data moves between devices by JAX's collectives and lax.ppermute only.
A program may use at most 128 MiB of HBM per device.

v0:
```python
import jax
import jax.numpy as jnp
from jax import lax
from jax.experimental import pallas as pl
from jax.experimental.pallas import tpu as pltpu
from jax.sharding import PartitionSpec as P


def norm_rows(values, gain):
    values = values.astype(jnp.float32)
    scale = lax.rsqrt(jnp.mean(values * values, axis=-1, keepdims=True) + 1e-06)
    return values * scale * gain


def break_terms(query_heads, query_place, key_block, bias_block, first):
    span = key_block.shape[0]
    heads = query_heads.shape[1]
    key_heads = key_block.reshape(span, heads, -1)
    scores = jnp.einsum("qhd,khd->hqk", query_heads, key_heads, preferred_element_type=jnp.float32)
    scores = scores * query_heads.shape[2] ** (-0.5) + bias_block.astype(jnp.float32).T[:, None, :]
    key_place = first + jnp.arange(span)
    past = (key_place[None, :] < query_place[:, None])[None]
    rest = jnp.where(past, jax.nn.log_sigmoid(-scores), 0.0)
    later = lax.cumsum(rest, axis=2, reverse=True)
    return (scores, past, rest, later)


def block_part(scores, past, rest, later, value_block, heads):
    within = later - rest
    local = jnp.where(past, jnp.exp(jax.nn.log_sigmoid(scores) + within), 0.0).astype(jnp.bfloat16)
    span = value_block.shape[0]
    value_heads = value_block.reshape(span, heads, -1)
    part = jnp.einsum("hqk,khd->qhd", local, value_heads, preferred_element_type=jnp.float32)
    return part.reshape(part.shape[0], -1)


def keep(state):
    return state


def dispatch_plan(normed, expert_ids, experts, capacity):
    rows, top = expert_ids.shape
    flat_ids = expert_ids.reshape(rows * top)
    onehot = (flat_ids[:, None] == jnp.arange(experts)[None, :]).astype(jnp.int32)
    earlier = jnp.cumsum(onehot, axis=0) - onehot
    place = jnp.sum(earlier * onehot, axis=1)
    target = flat_ids * capacity + place
    source = (
        jnp.zeros((experts * capacity,), jnp.int32)
        .at[target]
        .set(jnp.arange(rows * top, dtype=jnp.int32) // top + 1)
    )
    padded = jnp.concatenate([jnp.zeros((1, normed.shape[1]), normed.dtype), normed], axis=0)
    return (padded[source].reshape(experts, capacity, normed.shape[1]), target)


def expert_hidden(piece, gate_weight, up_weight):
    flat = piece.reshape(-1, piece.shape[-1])
    gate = jnp.dot(flat, gate_weight[0], preferred_element_type=jnp.float32)
    upward = jnp.dot(flat, up_weight[0], preferred_element_type=jnp.float32)
    hidden = (jax.nn.silu(gate) * upward).astype(jnp.bfloat16)
    return hidden.reshape(piece.shape[0], piece.shape[1], -1)


def send_back(summed):
    return lax.all_to_all(
        summed.astype(jnp.bfloat16), "ep", split_axis=0, concat_axis=0, tiled=True
    )


def return_rows(hidden_all, down_weight, sources):
    flat = hidden_all.reshape(-1, hidden_all.shape[2])
    product = jnp.dot(flat, down_weight[0], preferred_element_type=jnp.float32)
    return send_back(
        lax.psum_scatter(
            product.reshape(sources * lax.axis_size("tp"), hidden_all.shape[1], -1).astype(
                jnp.bfloat16
            ),
            "tp",
            scatter_dimension=0,
            tiled=True,
        ).astype(jnp.float32)
    )


def per_device_wide(
    queries,
    keys,
    values,
    stop_bias,
    out_weight,
    mix_gain,
    moe_input,
    ffn_gain,
    expert_ids,
    expert_scores,
    gate_weight,
    up_weight,
    down_weight,
):
    span = queries.shape[0]
    heads = stop_bias.shape[1]
    width_heads = queries.shape[1]
    blocks = lax.axis_size("ep")
    own_first = lax.axis_index("ep") * span
    query_heads = queries.reshape(span, heads, -1)
    query_place = own_first + jnp.arange(span)

    def piece_rows(piece, index):
        return tuple((lax.dynamic_slice_in_dim(member, index * span, span, 0) for member in piece))

    start_state = (
        jnp.zeros((blocks, heads, span), jnp.float32),
        jnp.zeros((blocks, span, width_heads), jnp.float32),
    )
    piece = (
        lax.all_gather(keys, "ep", axis=0, tiled=True),
        lax.all_gather(values, "ep", axis=0, tiled=True),
        lax.all_gather(stop_bias, "ep", axis=0, tiled=True),
    )

    def one_block(index, state):
        key_block, value_block, bias_block = piece_rows(piece, index)
        first = index * span

        def compute(inner_state):
            totals, parts = inner_state
            scores, past, rest, later = break_terms(
                query_heads, query_place, key_block, bias_block, first
            )
            part = block_part(scores, past, rest, later, value_block, heads)
            number = first // span
            totals = lax.dynamic_update_index_in_dim(totals, later[:, :, 0], number, 0)
            parts = lax.dynamic_update_index_in_dim(parts, part, number, 0)
            return (totals, parts)

        return lax.cond(first <= own_first, compute, keep, state)

    totals, parts = lax.fori_loop(0, piece[0].shape[0] // span, one_block, start_state)
    carried = lax.cumsum(totals, axis=0, reverse=True) - totals
    factor = jnp.exp(carried).transpose(0, 2, 1)[:, :, :, None]
    attended = jnp.sum(factor * parts.reshape(blocks, span, heads, -1), axis=0).reshape(
        span, width_heads
    )
    attended = attended.astype(jnp.bfloat16)
    projected = lax.psum_scatter(
        jnp.dot(attended, out_weight, preferred_element_type=jnp.float32).astype(jnp.bfloat16),
        "tp",
        scatter_dimension=0,
        tiled=True,
    ).astype(jnp.float32)
    mixed = norm_rows(projected, mix_gain).astype(jnp.bfloat16)
    normed = norm_rows(moe_input, ffn_gain).astype(jnp.bfloat16)
    rows, top = expert_ids.shape
    experts = lax.axis_size("ep")
    capacity = 3 * rows * top // (2 * experts)
    weights = expert_scores / jnp.sum(expert_scores, axis=1, keepdims=True)
    outbound, target = dispatch_plan(normed, expert_ids, experts, capacity)
    arrived = lax.all_to_all(outbound, "ep", split_axis=0, concat_axis=0, tiled=True)
    hidden_all = expert_hidden(
        lax.all_gather(arrived, "tp", axis=0, tiled=True), gate_weight, up_weight
    )
    returned = return_rows(hidden_all, down_weight, arrived.shape[0])
    picked = returned.reshape(experts * capacity, -1)[target].reshape(rows, top, -1)
    experts_mixed = jnp.sum(picked.astype(jnp.float32) * weights[:, :, None], axis=1).astype(
        jnp.bfloat16
    )
    return (mixed, experts_mixed)


VMEM = pl.BlockSpec(memory_space=pltpu.VMEM)
SMEM = pl.BlockSpec(memory_space=pltpu.SMEM)
ANY = pl.BlockSpec(memory_space=pl.ANY)


def shape_of(shape, dtype=jnp.bfloat16):
    return jax.ShapeDtypeStruct(shape, dtype)


def call(body, outs, ins, scratch=(), flops=0, limit=24):
    return pl.pallas_call(
        body,
        out_shape=outs,
        in_specs=ins,
        out_specs=jax.tree.map(lambda _: VMEM, outs),
        scratch_shapes=scratch,
        compiler_params=pltpu.CompilerParams(vmem_limit_bytes=limit * 1024 * 1024),
        cost_estimate=pl.CostEstimate(flops=flops, transcendentals=0, bytes_accessed=0),
    )


def selections(place_ref, ids_ref, experts, capacity):
    rows, top = ids_ref.shape
    ids = ids_ref[...]
    lane = lax.broadcasted_iota(jnp.int32, (rows, 128), 1)
    expert = (place_ref[0] + lane) % experts
    chosen = jnp.zeros((rows, 128), jnp.float32)
    for k in range(top):
        chosen = chosen + jnp.where(ids[:, k : k + 1] == expert, 1.0, 0.0)
    chosen = jnp.where(lane < experts, chosen, 0.0)
    below = lax.broadcasted_iota(jnp.int32, (rows, rows), 1) < lax.broadcasted_iota(
        jnp.int32, (rows, rows), 0
    )
    rank = jnp.dot(
        below.astype(jnp.bfloat16), chosen.astype(jnp.bfloat16), preferred_element_type=jnp.float32
    )
    slot = lax.broadcasted_iota(jnp.int32, (rows, capacity), 1).astype(jnp.float32)
    picks = []
    for d in range(experts):
        hit = (rank[:, d : d + 1] == slot) & (chosen[:, d : d + 1] > 0.5)
        picks.append(jnp.where(hit, 1.0, 0.0).astype(jnp.bfloat16))
    return ids, expert, picks


def route_rows(place, moe_input, ffn_gain, expert_ids, experts, capacity):
    rows, width = moe_input.shape

    def body(place_ref, input_ref, gain_ref, ids_ref, *outs):
        normed = norm_rows(input_ref[...], gain_ref[...]).astype(jnp.bfloat16)
        _, _, picks = selections(place_ref, ids_ref, experts, capacity)
        for d in range(experts):
            outs[d][...] = lax.dot_general(
                picks[d], normed, (((0,), (0,)), ((), ())), preferred_element_type=jnp.float32
            ).astype(jnp.bfloat16)

    outs = [shape_of((capacity, width))] * experts
    return call(body, outs, [SMEM, VMEM, VMEM, VMEM], flops=4 * capacity * rows * width * 2)(
        place, moe_input, ffn_gain.reshape(1, width), expert_ids
    )


def combine_rows(place, expert_ids, expert_scores, returned):
    rows = expert_ids.shape[0]
    experts = len(returned)
    capacity, width = returned[0].shape

    def body(place_ref, ids_ref, scores_ref, *refs):
        ids, expert, picks = selections(place_ref, ids_ref, experts, capacity)
        scores = scores_ref[...]
        weights = scores / jnp.sum(scores, axis=1, keepdims=True)
        total = jnp.zeros((rows, width), jnp.float32)
        for d in range(experts):
            weight = jnp.zeros((rows, 1), jnp.float32)
            for k in range(ids.shape[1]):
                weight = weight + jnp.where(
                    ids[:, k : k + 1] == expert[:, d : d + 1], weights[:, k : k + 1], 0.0
                )
            total = total + weight * jnp.dot(
                picks[d], refs[d][...], preferred_element_type=jnp.float32
            )
        refs[-1][...] = total.astype(jnp.bfloat16)

    return call(
        body, shape_of((rows, width)), [SMEM, VMEM, VMEM] + [VMEM] * experts,
        flops=4 * capacity * rows * width * 2,
    )(place, expert_ids, expert_scores, *returned)


def expert_part(rows_in, pieces, carried, last):
    capacity, width = rows_in[0].shape
    count = len(rows_in)
    hidden = sum(piece[0].shape[1] for piece in pieces)
    flat = [array for piece in pieces for array in piece]

    def body(*refs):
        row_refs = refs[:count]
        weight_refs = refs[count : count + len(flat)]
        rest = refs[count + len(flat) :]
        if carried is not None:
            acc_ref, rest = rest[0], rest[1:]
        rows = jnp.concatenate([ref[...] for ref in row_refs], axis=0)
        inner = []
        for p in range(len(pieces)):
            size = weight_refs[3 * p].shape[1]
            both = jnp.concatenate([weight_refs[3 * p][...], weight_refs[3 * p + 1][...]], axis=1)
            product = jnp.dot(rows, both, preferred_element_type=jnp.float32)
            gate, upward = product[:, :size], product[:, size:]
            inner.append((gate / (1.0 + jnp.exp(-gate)) * upward).astype(jnp.bfloat16))
        inner = jnp.concatenate(inner, axis=1)
        down = jnp.concatenate([weight_refs[3 * p + 2][...] for p in range(len(pieces))], axis=0)
        if last:
            for d in range(count):
                some = slice(d * capacity, (d + 1) * capacity)
                out = jnp.dot(inner[some], down, preferred_element_type=jnp.float32)
                rest[d][...] = (out + acc_ref[some]).astype(jnp.bfloat16)
        else:
            out = jnp.dot(inner, down, preferred_element_type=jnp.float32)
            rest[0][...] = out if carried is None else out + acc_ref[...]

    outs = (
        [shape_of((capacity, width))] * count
        if last
        else [shape_of((count * capacity, width), jnp.float32)]
    )
    extra = [] if carried is None else [carried]
    return call(
        body,
        outs,
        [VMEM] * (count + len(flat) + len(extra)),
        flops=6 * count * capacity * width * hidden,
    )(*rows_in, *flat, *extra)


def attend_project(place, queries, own, passed, out_weight, heads, quarters):
    span, width_heads = queries.shape
    size = width_heads // heads
    pair = 2 * size
    width = out_weight.shape[1]
    share = span // quarters
    blocks = 1 + len(passed)
    half = quarters // 2

    def body(place_ref, q_ref, own_ref, *refs):
        kv_refs = (own_ref,) + refs[: len(passed)]
        weight_ref, send_ref, keep_ref, acc, carry, att, proj = refs[len(passed) :]
        row = lax.broadcasted_iota(jnp.int32, (span, span), 0)
        column = lax.broadcasted_iota(jnp.int32, (span, span), 1)
        earlier = column < row
        after = jnp.where(row > column, 1.0, 0.0)
        sums = jnp.concatenate([after, jnp.ones((span, span), jnp.float32)], axis=1)
        sums = jnp.concatenate([sums, sums], axis=0).astype(jnp.bfloat16)
        low = lax.broadcasted_iota(jnp.int32, (span, pair), 1) < size

        def one_block(d):
            for h in range(heads):
                lanes = slice((h // 2) * pair, (h // 2 + 1) * pair)
                query = jnp.where(low if h % 2 == 0 else ~low, q_ref[:, lanes], 0.0).astype(jnp.bfloat16)
                key = kv_refs[d][:span, lanes]
                bias = kv_refs[d][span + h : span + h + 1, :span].astype(jnp.float32)
                z = lax.dot_general(
                    query, key, (((1,), (1,)), ((), ())), preferred_element_type=jnp.float32
                ) * size ** (-0.5) + bias
                rest = -(jnp.maximum(z, 0.0) + jnp.log1p(jnp.exp(-jnp.abs(z))))
                masked = jnp.where(earlier, rest, 0.0) if d == 0 else rest
                top = masked.astype(jnp.bfloat16)
                bottom = (masked - top.astype(jnp.float32)).astype(jnp.bfloat16)
                both = jnp.dot(
                    jnp.concatenate([top, bottom], axis=1), sums, preferred_element_type=jnp.float32
                )
                local = jnp.exp(z + rest + both[:, :span])
                if d == 0:
                    local = jnp.where(earlier, local, 0.0)
                value = kv_refs[d][:span, width_heads + lanes.start : width_heads + lanes.stop]
                part = jnp.dot(local.astype(jnp.bfloat16), value, preferred_element_type=jnp.float32)
                if d == 0:
                    carry[h] = both[:, span:]
                    total = part
                else:
                    before = carry[h]
                    total = jnp.exp(before) * part
                    carry[h] = before + both[:, span:]
                mine = low if h % 2 == 0 else ~low
                if d == 0 and h % 2 == 0:
                    acc[h // 2] = total
                elif d == 0:
                    acc[h // 2] = jnp.where(mine, total, acc[h // 2])
                else:
                    acc[h // 2] = acc[h // 2] + jnp.where(mine, total, 0.0)

        one_block(0)
        for d in range(1, blocks):
            pl.when(place_ref[0] >= d)(lambda d=d: one_block(d))
        for p in range(heads // 2):
            att[:, p * pair : (p + 1) * pair] = acc[p].astype(jnp.bfloat16)
        proj[...] = jnp.dot(att[...], weight_ref[...], preferred_element_type=jnp.float32)
        core = place_ref[1]
        for k in range(half):
            send_ref[k * share : (k + 1) * share, :] = proj[
                pl.ds((2 * k + 1 - core) * share, share), :
            ].astype(jnp.bfloat16)
            keep_ref[k * share : (k + 1) * share, :] = proj[pl.ds((2 * k + core) * share, share), :]

    return call(
        body,
        [shape_of((half * share, width)), shape_of((half * share, width), jnp.float32)],
        [SMEM, VMEM, VMEM] + [VMEM] * len(passed) + [VMEM],
        scratch=(
            pltpu.VMEM((heads // 2, span, pair), jnp.float32),
            pltpu.VMEM((heads, span, span), jnp.float32),
            pltpu.VMEM((span, width_heads), jnp.bfloat16),
            pltpu.VMEM((span, width), jnp.float32),
        ),
        flops=4 * blocks * span * span * width_heads + 2 * span * width_heads * width,
    )(place, queries, own, *passed, out_weight)


def per_device(*arrays):
    return paired_step(*arrays)


def paired_step(
    queries,
    keys,
    values,
    stop_bias,
    out_weight,
    mix_gain,
    moe_input,
    ffn_gain,
    expert_ids,
    expert_scores,
    gate_weight,
    up_weight,
    down_weight,
):
    blocks = lax.axis_size("ep")
    shards = lax.axis_size("tp")
    group = lax.axis_index("grp")
    block = lax.axis_index("ep")
    shard = lax.axis_index("tp")
    place = jnp.stack([block, shard % 2]).astype(jnp.int32)
    heads = stop_bias.shape[1]
    span = queries.shape[0]

    def core(array):
        return lax.ppermute(array, "tp", [(i, i ^ 1) for i in range(shards)])

    def across(array):
        return lax.ppermute(array, "tp", [(i, i ^ 2) for i in range(shards)])

    def beside(array):
        return lax.ppermute(array, "grp", [(0, 1), (1, 0)])

    def turn(array, d):
        return lax.ppermute(array, "ep", [(i, (i + d) % blocks) for i in range(blocks)])

    def upward(array, d):
        return lax.ppermute(array, "ep", [(i, i + 1) for i in range(d - 1, blocks - 1)])

    mine = (gate_weight[0], up_weight[0], down_weight[0])
    part = mine[0].shape[1] // 2
    gate_half = lax.dynamic_slice_in_dim(mine[0], group * part, part, 1)

    rows, top = expert_ids.shape
    capacity = 3 * rows * top // (2 * blocks)
    outbound = route_rows(place, moe_input, ffn_gain, expert_ids, blocks, capacity)
    arrived = [outbound[0]] + [turn(outbound[d], d) for d in range(1, blocks)]

    halves = (
        gate_half,
        lax.dynamic_slice_in_dim(mine[1], group * part, part, 1),
        lax.dynamic_slice_in_dim(mine[2], group * part, part, 0),
    )
    far = tuple(across(array) for array in halves)
    near = tuple(core(array) for array in mine)
    other = tuple(beside(array) for array in far)
    far_near = tuple(core(array) for array in far)
    other_near = tuple(core(array) for array in other)

    own = jnp.concatenate(
        [
            jnp.concatenate([keys, values], axis=1),
            jnp.pad(stop_bias.T, ((0, 0), (0, 2 * keys.shape[1] - span))),
        ],
        axis=0,
    )
    passed = []
    for d in range(1, blocks):
        passed.append(upward(passed[-1] if passed else own, d))

    summed = expert_part(arrived, [mine, near], None, False)[0]
    summed = expert_part(arrived, [far, far_near], summed, False)[0]
    produced = expert_part(arrived, [other, other_near], summed, True)
    returned = [produced[0]] + [turn(produced[d], -d) for d in range(1, blocks)]

    send, kept = attend_project(place, queries, own, passed, out_weight, heads, shards)
    chip = kept + core(send).astype(jnp.float32)
    share = span // shards
    first, second = chip[:share], chip[share:]
    outer = jnp.where(shard < 2, second, first).astype(jnp.bfloat16)
    inner = jnp.where(shard < 2, first, second)
    projected = inner + across(outer).astype(jnp.float32)
    mixed = norm_rows(projected, mix_gain).astype(jnp.bfloat16)

    experts_mixed = combine_rows(place, expert_ids, expert_scores, returned)
    return (mixed, experts_mixed)


def solution(mesh):
    sizes = mesh.shape
    paired = sizes["grp"] == 2 and sizes["tp"] == 4 and sizes["ep"] <= sizes["tp"]
    return jax.shard_map(
        per_device if paired else per_device_wide,
        mesh=mesh,
        in_specs=(
            P(("grp", "ep"), "tp"),
            P(("grp", "ep"), "tp"),
            P(("grp", "ep"), "tp"),
            P(("grp", "ep"), "tp"),
            P("tp", None),
            P(),
            P(("grp", "ep", "tp"), None),
            P(),
            P(("grp", "ep", "tp"), None),
            P(("grp", "ep", "tp"), None),
            P("ep", None, "tp"),
            P("ep", None, "tp"),
            P("ep", "tp", None),
        ),
        out_specs=(P(("grp", "ep", "tp"), None), P(("grp", "ep", "tp"), None)),
        check_vma=False,
    )
```

profile of v0, /device:TPU:0, one launch (start us, length us, event | category | flops | bytes accessed | tf_op | source)
XLA Modules:
  0.0 170.1 jit_solution(15754655322014965745)
XLA Ops:
  0.6 1.0 fusion.1.own_ref
  1.6 5.0 %collective-permute-start = (bf16[136,1024]{1,0:T(8,128)(2,1)S(1)}, bf16[136,1024]{1,0:T(8,128)(2,1)S(1)}, u32[]{:S(2)}, u32[]{:S(2)}) collective-permute-start(bf16[136,1024]{1,0:T(8,128)(2,1)S(1)} %fusion.1.own_ref), channel_id=1, source_target_pairs={{0,4},{4,8},{8,12},{1,5},{5,9},{9,13},{2,6},{6,10},{10,14},{3,7},{... | collective-permute-start | bytes 835592 | tf_op jit(solution)/shard_map/ppermute | solution.py:428
  6.6 0.1 pad_add_fusion.place_ref
  6.7 0.8 copy.16.ids_ref
  7.5 1.0 copy-done.7
  8.5 0.7 copy-done.8
  9.2 2.0 %shard_map.141 = (bf16[96,2048]{1,0:T(8,128)(2,1)S(1)}, bf16[96,2048]{1,0:T(8,128)(2,1)}, bf16[96,2048]{1,0:T(8,128)(2,1)S(1)}, bf16[96,2048]{1,0:T(8,128)(2,1)S(1)}) custom-call(s32[2]{0:T(128)S(1)} %pad_add_fusion.place_ref, bf16[128,2048]{1,0:T(8,128)(2,1)S(1)} %copy-done.7, f32[1,2048]{1,0:T(1,128)S(1)} %bitcast.19, s32[128,2]{1,0:T(8,128)S(1)} %copy.16.ids_ref), custom_call_target="tpu_custom_call" | custom-call | flops 201326592 | tf_op jit(solution)/shard_map/pallas_call | solution.py:227
  11.2 1.6 collective-permute-start.5
  12.8 1.0 collective-permute-start.6
  13.8 2.9 %collective-permute-start.7 = (bf16[96,2048]{1,0:T(8,128)(2,1)S(1)}, bf16[96,2048]{1,0:T(8,128)(2,1)S(1)}, u32[]{:S(2)}, u32[]{:S(2)}) collective-permute-start(bf16[96,2048]{1,0:T(8,128)(2,1)S(1)} %get-tuple-element.17), channel_id=1, source_target_pairs={{0,12},{4,0},{8,4},{12,8},{1,13},{5,1},{9,5},{13,9},{2,14},{6,2},{... | collective-permute-start | bytes 1179656 | tf_op jit(solution)/shard_map/ppermute | solution.py:425
  16.7 1.2 dynamic-slice_bitcast_fusion.2
  18.0 1.6 collective-permute-start.8
  19.5 0.0 collective-permute-done.refs_0_
  19.5 0.7 collective-permute-start.1
  20.2 0.7 copy-done.4
  20.9 4.5 %collective-permute-done.5.refs_1_ = bf16[96,2048]{1,0:T(8,128)(2,1)S(1)} collective-permute-done((bf16[96,2048]{1,0:T(8,128)(2,1)}, bf16[96,2048]{1,0:T(8,128)(2,1)S(1)}, u32[]{:S(2)}, u32[]{:S(2)}) %collective-permute-start.5) | collective-permute-done | bytes 393248 | tf_op jit(solution)/shard_map/ppermute | solution.py:425
  25.4 0.0 collective-permute-start.20
  25.4 15.4 %collective-permute-done.6.refs_2_ = bf16[96,2048]{1,0:T(8,128)(2,1)S(1)} collective-permute-done((bf16[96,2048]{1,0:T(8,128)(2,1)S(1)}, bf16[96,2048]{1,0:T(8,128)(2,1)S(1)}, u32[]{:S(2)}, u32[]{:S(2)}) %collective-permute-start.6) | collective-permute-done | bytes 393248 | tf_op jit(solution)/shard_map/ppermute | solution.py:425
  40.8 0.0 collective-permute-start.21
  40.8 0.5 collective-permute-start.22
  41.3 0.7 collective-permute-start.2
  42.0 1.1 dynamic-slice_bitcast_fusion.1
  43.1 0.0 copy-start
  43.1 1.6 collective-permute-start.10
  44.7 1.1 dynamic-slice_bitcast_fusion
  45.8 0.0 collective-permute-done.2.refs_2_
  45.8 0.6 collective-permute-start.12
  46.4 1.0 copy-done.5
  47.3 0.9 copy-done.6
  48.2 3.7 %shard_map.140 = (bf16[64,2048]{1,0:T(8,128)(2,1)}, f32[64,2048]{1,0:T(8,128)S(1)}) custom-call(s32[2]{0:T(128)S(1)} %pad_add_fusion.place_ref, bf16[128,512]{1,0:T(8,128)(2,1)S(1)} %copy-done.6, bf16[136,1024]{1,0:T(8,128)(2,1)S(1)} %fusion.1.own_ref, bf16[136,1024]{1,0:T(8,128)(2,1)S(1)} %copy-done.5, ...), custom_call_target="tpu_custom_call" | custom-call | flops 402653184 | tf_op jit(solution)/shard_map/pallas_call | solution.py:373
  51.9 6.1 %collective-permute-done.10.refs_5_ = bf16[2048,128]{1,0:T(8,128)(2,1)} collective-permute-done((bf16[2048,128]{1,0:T(8,128)(2,1)S(1)}, bf16[2048,128]{1,0:T(8,128)(2,1)}, u32[]{:S(2)}, u32[]{:S(2)}) %collective-permute-start.10) | collective-permute-done | bytes 524320 | tf_op jit(solution)/shard_map/ppermute | solution.py:419
  58.1 0.0 collective-permute-start.3
  58.1 10.3 %collective-permute-done.12.refs_6_ = bf16[128,2048]{1,0:T(8,128)(2,1)} collective-permute-done((bf16[128,2048]{1,0:T(8,128)(2,1)S(1)}, bf16[128,2048]{1,0:T(8,128)(2,1)}, u32[]{:S(2)}, u32[]{:S(2)}) %collective-permute-start.12) | collective-permute-done | bytes 524320 | tf_op jit(solution)/shard_map/ppermute | solution.py:419
  68.4 0.1 copy.17.scores_ref
  68.5 1.6 collective-permute-start.9
  70.1 0.0 collective-permute-done.21.refs_8_
  70.1 0.2 collective-permute-start.18
  70.3 0.5 collective-permute-start.11
  70.8 1.5 collective-permute-start.13
  72.3 1.0 convert_add_fusion
  73.3 0.1 collective-permute-start.19
  73.5 10.1 %collective-permute-done.9.refs_4_ = bf16[2048,128]{1,0:T(8,128)(2,1)S(1)} collective-permute-done((bf16[2048,128]{1,0:T(8,128)(2,1)}, bf16[2048,128]{1,0:T(8,128)(2,1)S(1)}, u32[]{:S(2)}, u32[]{:S(2)}) %collective-permute-start.9) | collective-permute-done | bytes 524320 | tf_op jit(solution)/shard_map/ppermute | solution.py:422
  83.6 0.0 collective-permute-start.14
  83.6 11.2 %collective-permute-done.11.refs_5_ = bf16[2048,128]{1,0:T(8,128)(2,1)S(1)} collective-permute-done((bf16[2048,128]{1,0:T(8,128)(2,1)}, bf16[2048,128]{1,0:T(8,128)(2,1)S(1)}, u32[]{:S(2)}, u32[]{:S(2)}) %collective-permute-start.11) | collective-permute-done | bytes 524320 | tf_op jit(solution)/shard_map/ppermute | solution.py:422
  94.8 10.8 %collective-permute-done.13.refs_6_ = bf16[128,2048]{1,0:T(8,128)(2,1)S(1)} collective-permute-done((bf16[128,2048]{1,0:T(8,128)(2,1)}, bf16[128,2048]{1,0:T(8,128)(2,1)S(1)}, u32[]{:S(2)}, u32[]{:S(2)}) %collective-permute-start.13) | collective-permute-done | bytes 524320 | tf_op jit(solution)/shard_map/ppermute | solution.py:422
  105.6 0.0 collective-permute-start.16
  105.6 0.0 collective-permute-done.18.refs_8_
  105.6 1.5 collective-permute-start.4
  107.1 1.2 copy-done.1
  108.3 1.2 copy-done.2
  109.5 4.5 %shard_map.142.refs_10_ = f32[384,2048]{1,0:T(8,128)S(1)} custom-call(bf16[96,2048]{1,0:T(8,128)(2,1)S(1)} %get-tuple-element.14.refs_0_, bf16[96,2048]{1,0:T(8,128)(2,1)S(1)} %collective-permute-done.5.refs_1_, bf16[96,2048]{1,0:T(8,128)(2,1)S(1)} %collective-permute-done.6.refs_2_, bf16[96,2048]{1,0:T(8,128)(2,1)S(1)} %collective-permute-done.7.refs_3_, ...), custom_call_target="tpu_custom_call" | custom-call | flops 2415919104 | tf_op jit(solution)/shard_map/pallas_call | solution.py:296
  114.0 3.0 %shard_map.143.refs_10_ = f32[384,2048]{1,0:T(8,128)S(1)} custom-call(bf16[96,2048]{1,0:T(8,128)(2,1)S(1)} %get-tuple-element.14.refs_0_, bf16[96,2048]{1,0:T(8,128)(2,1)S(1)} %collective-permute-done.5.refs_1_, bf16[96,2048]{1,0:T(8,128)(2,1)S(1)} %collective-permute-done.6.refs_2_, bf16[96,2048]{1,0:T(8,128)(2,1)S(1)} %collective-permute-done.7.refs_3_, ...), custom_call_target="tpu_custom_call" | custom-call | flops 1207959552 | tf_op jit(solution)/shard_map/pallas_call | solution.py:296
  117.0 0.2 multiply_reduce_fusion
  117.2 0.0 collective-permute-done.15.refs_8_
  117.2 0.0 collective-permute-done.16.refs_9_
  117.2 1.7 shard_map.144
  118.9 12.1 %collective-permute-start.23 = (bf16[96,2048]{1,0:T(8,128)(2,1)S(1)}, bf16[96,2048]{1,0:T(8,128)(2,1)S(1)}, u32[]{:S(2)}, u32[]{:S(2)}) collective-permute-start(bf16[96,2048]{1,0:T(8,128)(2,1)S(1)} %get-tuple-element.19), channel_id=1, source_target_pairs={{0,12},{4,0},{8,4},{12,8},{1,13},{5,1},{9,5},{13,9},{2,14},{6,2},{... | collective-permute-start | bytes 1179656 | tf_op jit(solution)/shard_map/ppermute | solution.py:425
  130.9 1.9 %collective-permute-start.24 = (bf16[96,2048]{1,0:T(8,128)(2,1)S(1)}, bf16[96,2048]{1,0:T(8,128)(2,1)S(1)}, u32[]{:S(2)}, u32[]{:S(2)}) collective-permute-start(bf16[96,2048]{1,0:T(8,128)(2,1)S(1)} %get-tuple-element.20), channel_id=1, source_target_pairs={{0,8},{4,12},{8,0},{12,4},{1,9},{5,13},{9,1},{13,5},{2,10},{6,14},... | collective-permute-start | bytes 1179656 | tf_op jit(solution)/shard_map/ppermute | solution.py:425
  132.9 1.9 %collective-permute-start.25 = (bf16[96,2048]{1,0:T(8,128)(2,1)S(1)}, bf16[96,2048]{1,0:T(8,128)(2,1)S(1)}, u32[]{:S(2)}, u32[]{:S(2)}) collective-permute-start(bf16[96,2048]{1,0:T(8,128)(2,1)S(1)} %get-tuple-element.21), channel_id=1, source_target_pairs={{0,4},{4,8},{8,12},{12,0},{1,5},{5,9},{9,13},{13,1},{2,6},{6,10},{... | collective-permute-start | bytes 1179656 | tf_op jit(solution)/shard_map/ppermute | solution.py:425
  134.8 0.7 multiply_convert_fusion
  135.6 5.0 %collective-permute-done.23.refs_1_ = bf16[96,2048]{1,0:T(8,128)(2,1)S(1)} collective-permute-done((bf16[96,2048]{1,0:T(8,128)(2,1)S(1)}, bf16[96,2048]{1,0:T(8,128)(2,1)S(1)}, u32[]{:S(2)}, u32[]{:S(2)}) %collective-permute-start.23) | collective-permute-done | bytes 393248 | tf_op jit(solution)/shard_map/ppermute | solution.py:425
  140.5 27.0 %collective-permute-done.24.refs_2_ = bf16[96,2048]{1,0:T(8,128)(2,1)S(1)} collective-permute-done((bf16[96,2048]{1,0:T(8,128)(2,1)S(1)}, bf16[96,2048]{1,0:T(8,128)(2,1)S(1)}, u32[]{:S(2)}, u32[]{:S(2)}) %collective-permute-start.24) | collective-permute-done | bytes 393248 | tf_op jit(solution)/shard_map/ppermute | solution.py:425
  167.6 0.0 collective-permute-done.25.refs_3_
  167.6 2.5 %shard_map.145 = bf16[128,2048]{1,0:T(8,128)(2,1)} custom-call(s32[2]{0:T(128)S(1)} %pad_add_fusion.place_ref, s32[128,2]{1,0:T(8,128)S(1)} %copy.16.ids_ref, f32[128,2]{1,0:T(8,128)S(1)} %copy.17.scores_ref, bf16[96,2048]{1,0:T(8,128)(2,1)S(1)} %get-tuple-element.18.refs_0_, bf16[96,2048]{1,0:T(8,128)(2,1)S(1)} %collective-permute-done.23.refs_1_, ...), custom_call_target="tpu_custom_call" | custom-call | flops 201326592 | tf_op jit(solution)/shard_map/pallas_call | solution.py:253
  (28 shorter events, 0.1 us)
Async XLA Ops:
  1.6 17.9 %collective-permute-start = (bf16[136,1024]{1,0:T(8,128)(2,1)S(1)}, bf16[136,1024]{1,0:T(8,128)(2,1)S(1)}, u32[]{:S(2)}, u32[]{:S(2)}) collective-permute-start(bf16[136,1024]{1,0:T(8,128)(2,1)S(1)} %fusion.1.own_ref), channel_id=1, source_target_pairs={{0,4},{4,8},{8,12},{1,5},{5,9},{9,13},{2,6},{6,10},{10,14},{3,7},{... | collective-permute-start | bytes 835592 | tf_op jit(solution)/shard_map/ppermute | solution.py:428
  7.5 1.0 copy-start.7
  8.5 0.7 copy-start.8
  11.2 14.1 %collective-permute-start.5 = (bf16[96,2048]{1,0:T(8,128)(2,1)}, bf16[96,2048]{1,0:T(8,128)(2,1)S(1)}, u32[]{:S(2)}, u32[]{:S(2)}) collective-permute-start(bf16[96,2048]{1,0:T(8,128)(2,1)} %get-tuple-element.15), channel_id=1, source_target_pairs={{0,4},{4,8},{8,12},{12,0},{1,5},{5,9},{9,13},{13,1},{2,6},{6,10},{... | collective-permute-start | bytes 1179656 | tf_op jit(solution)/shard_map/ppermute | solution.py:425
  12.8 28.0 %collective-permute-start.6 = (bf16[96,2048]{1,0:T(8,128)(2,1)S(1)}, bf16[96,2048]{1,0:T(8,128)(2,1)S(1)}, u32[]{:S(2)}, u32[]{:S(2)}) collective-permute-start(bf16[96,2048]{1,0:T(8,128)(2,1)S(1)} %get-tuple-element.16), channel_id=1, source_target_pairs={{0,8},{4,12},{8,0},{12,4},{1,9},{5,13},{9,1},{13,5},{2,10},{6,14},... | collective-permute-start | bytes 1179656 | tf_op jit(solution)/shard_map/ppermute | solution.py:425
  13.8 27.0 %collective-permute-start.7 = (bf16[96,2048]{1,0:T(8,128)(2,1)S(1)}, bf16[96,2048]{1,0:T(8,128)(2,1)S(1)}, u32[]{:S(2)}, u32[]{:S(2)}) collective-permute-start(bf16[96,2048]{1,0:T(8,128)(2,1)S(1)} %get-tuple-element.17), channel_id=1, source_target_pairs={{0,12},{4,0},{8,4},{12,8},{1,13},{5,1},{9,5},{13,9},{2,14},{6,2},{... | collective-permute-start | bytes 1179656 | tf_op jit(solution)/shard_map/ppermute | solution.py:425
  16.7 29.6 %copy-start.3 = (bf16[512,2048]{1,0:T(8,128)(2,1)S(1)}, bf16[512,2048]{1,0:T(8,128)(2,1)}, u32[]{:S(2)}) copy-start(bf16[512,2048]{1,0:T(8,128)(2,1)} %refs_3_.1) | copy-start | bytes 6291460
  16.7 51.6 %copy-start.10 = (f32[128,2]{0,1:T(2,128)S(1)}, f32[128,2]{0,1:T(2,128)}, u32[]{:S(2)}) copy-start(f32[128,2]{0,1:T(2,128)} %param.22) | copy-start | bytes 3076
  18.0 25.1 %collective-permute-start.8 = (bf16[2048,128]{1,0:T(8,128)(2,1)S(1)}, bf16[2048,128]{1,0:T(8,128)(2,1)}, u32[]{:S(2)}, u32[]{:S(2)}) collective-permute-start(bf16[2048,128]{1,0:T(8,128)(2,1)S(1)} %dynamic-slice_bitcast_fusion.2), channel_id=1, source_target_pairs={{0,2},{1,3},{2,0},{3,1},{4,6},{5,7},{6,4},{7,5},{8,10},{9,11},{10,... | collective-permute-start | bytes 1572872 | tf_op jit(solution)/shard_map/ppermute | solution.py:419
  19.5 21.8 %collective-permute-start.1 = (bf16[136,1024]{1,0:T(8,128)(2,1)S(1)}, bf16[136,1024]{1,0:T(8,128)(2,1)S(1)}, u32[]{:S(2)}, u32[]{:S(2)}) collective-permute-start(bf16[136,1024]{1,0:T(8,128)(2,1)S(1)} %collective-permute-done.refs_0_), channel_id=1, source_target_pairs={{4,8},{8,12},{5,9},{9,13},{6,10},{10,14},{7,11},{11,15},{20,24},{2... | collective-permute-start | bytes 835592 | tf_op jit(solution)/shard_map/ppermute | solution.py:428
  20.2 0.7 copy-start.4
  25.4 43.1 %collective-permute-start.20 = (bf16[2048,256]{1,0:T(8,128)(2,1)}, bf16[2048,256]{1,0:T(8,128)(2,1)}, u32[]{:S(2)}, u32[]{:S(2)}) collective-permute-start(bf16[2048,256]{1,0:T(8,128)(2,1)} %bitcast.13), channel_id=1, source_target_pairs={{0,1},{1,0},{2,3},{3,2},{4,5},{5,4},{6,7},{7,6},{8,9},{9,8},{10,11... | collective-permute-start | bytes 3145736 | tf_op jit(solution)/shard_map/ppermute | solution.py:416
  40.8 29.3 %collective-permute-start.21 = (bf16[2048,256]{1,0:T(8,128)(2,1)}, bf16[2048,256]{1,0:T(8,128)(2,1)}, u32[]{:S(2)}, u32[]{:S(2)}) collective-permute-start(bf16[2048,256]{1,0:T(8,128)(2,1)} %bitcast.15), channel_id=1, source_target_pairs={{0,1},{1,0},{2,3},{3,2},{4,5},{5,4},{6,7},{7,6},{8,9},{9,8},{10,11... | collective-permute-start | bytes 3145736 | tf_op jit(solution)/shard_map/ppermute | solution.py:416
  40.8 29.5 %collective-permute-start.22 = (bf16[256,2048]{1,0:T(8,128)(2,1)}, bf16[256,2048]{1,0:T(8,128)(2,1)}, u32[]{:S(2)}, u32[]{:S(2)}) collective-permute-start(bf16[256,2048]{1,0:T(8,128)(2,1)} %bitcast.17), channel_id=1, source_target_pairs={{0,1},{1,0},{2,3},{3,2},{4,5},{5,4},{6,7},{7,6},{8,9},{9,8},{10,11... | collective-permute-start | bytes 3145736 | tf_op jit(solution)/shard_map/ppermute | solution.py:416
  41.3 4.4 %collective-permute-start.2 = (bf16[136,1024]{1,0:T(8,128)(2,1)S(1)}, bf16[136,1024]{1,0:T(8,128)(2,1)S(1)}, u32[]{:S(2)}, u32[]{:S(2)}) collective-permute-start(bf16[136,1024]{1,0:T(8,128)(2,1)S(1)} %collective-permute-done.1.refs_1_), channel_id=1, source_target_pairs={{8,12},{9,13},{10,14},{11,15},{24,28},{25,29},{26,30},{27,31}} | collective-permute-start | bytes 835592 | tf_op jit(solution)/shard_map/ppermute | solution.py:428
  43.1 64.0 %copy-start = (bf16[1,2048,256]{2,1,0:T(8,128)(2,1)S(1)}, bf16[1,2048,256]{2,1,0:T(8,128)(2,1)}, u32[]{:S(2)}) copy-start(bf16[1,2048,256]{2,1,0:T(8,128)(2,1)} %param.23) | copy-start | bytes 3145732
  43.1 15.0 %collective-permute-start.10 = (bf16[2048,128]{1,0:T(8,128)(2,1)S(1)}, bf16[2048,128]{1,0:T(8,128)(2,1)}, u32[]{:S(2)}, u32[]{:S(2)}) collective-permute-start(bf16[2048,128]{1,0:T(8,128)(2,1)S(1)} %dynamic-slice_bitcast_fusion.1), channel_id=1, source_target_pairs={{0,2},{1,3},{2,0},{3,1},{4,6},{5,7},{6,4},{7,5},{8,10},{9,11},{10,... | collective-permute-start | bytes 1572872 | tf_op jit(solution)/shard_map/ppermute | solution.py:419
  45.8 22.6 %collective-permute-start.12 = (bf16[128,2048]{1,0:T(8,128)(2,1)S(1)}, bf16[128,2048]{1,0:T(8,128)(2,1)}, u32[]{:S(2)}, u32[]{:S(2)}) collective-permute-start(bf16[128,2048]{1,0:T(8,128)(2,1)S(1)} %dynamic-slice_bitcast_fusion), channel_id=1, source_target_pairs={{0,2},{1,3},{2,0},{3,1},{4,6},{5,7},{6,4},{7,5},{8,10},{9,11},{10,... | collective-permute-start | bytes 1572872 | tf_op jit(solution)/shard_map/ppermute | solution.py:419
  46.4 1.0 copy-start.5
  47.3 0.9 copy-start.6
  58.1 12.7 %collective-permute-start.3 = (bf16[64,2048]{1,0:T(8,128)(2,1)}, bf16[64,2048]{1,0:T(8,128)(2,1)}, u32[]{:S(2)}, u32[]{:S(2)}) collective-permute-start(bf16[64,2048]{1,0:T(8,128)(2,1)} %get-tuple-element.13), channel_id=1, source_target_pairs={{0,1},{1,0},{2,3},{3,2},{4,5},{5,4},{6,7},{7,6},{8,9},{9,8},{10,11... | collective-permute-start | bytes 786440 | tf_op jit(solution)/shard_map/ppermute | solution.py:416
  68.4 5.0 %collective-permute-start.17 = (bf16[2048,128]{1,0:T(8,128)(2,1)}, bf16[2048,128]{1,0:T(8,128)(2,1)}, u32[]{:S(2)}, u32[]{:S(2)}) collective-permute-start(bf16[2048,128]{1,0:T(8,128)(2,1)} %collective-permute-done.8.refs_4_), channel_id=1, source_target_pairs={{0,1},{1,0},{2,3},{3,2},{4,5},{5,4},{6,7},{7,6},{8,9},{9,8},{10,11... | collective-permute-start | bytes 1572872 | tf_op jit(solution)/shard_map/ppermute | solution.py:416
  68.5 15.1 %collective-permute-start.9 = (bf16[2048,128]{1,0:T(8,128)(2,1)}, bf16[2048,128]{1,0:T(8,128)(2,1)S(1)}, u32[]{:S(2)}, u32[]{:S(2)}) collective-permute-start(bf16[2048,128]{1,0:T(8,128)(2,1)} %collective-permute-done.8.refs_4_), channel_id=1, source_target_pairs={{0,16},{16,0},{1,17},{17,1},{2,18},{18,2},{3,19},{19,3},{4,20},{20... | collective-permute-start | bytes 1572872 | tf_op jit(solution)/shard_map/ppermute | solution.py:422
  70.1 35.5 %collective-permute-start.18 = (bf16[2048,128]{1,0:T(8,128)(2,1)}, bf16[2048,128]{1,0:T(8,128)(2,1)S(1)}, u32[]{:S(2)}, u32[]{:S(2)}) collective-permute-start(bf16[2048,128]{1,0:T(8,128)(2,1)} %collective-permute-done.10.refs_5_), channel_id=1, source_target_pairs={{0,1},{1,0},{2,3},{3,2},{4,5},{5,4},{6,7},{7,6},{8,9},{9,8},{10,11... | collective-permute-start | bytes 1572872 | tf_op jit(solution)/shard_map/ppermute | solution.py:416
  70.3 24.5 %collective-permute-start.11 = (bf16[2048,128]{1,0:T(8,128)(2,1)}, bf16[2048,128]{1,0:T(8,128)(2,1)S(1)}, u32[]{:S(2)}, u32[]{:S(2)}) collective-permute-start(bf16[2048,128]{1,0:T(8,128)(2,1)} %collective-permute-done.10.refs_5_), channel_id=1, source_target_pairs={{0,16},{16,0},{1,17},{17,1},{2,18},{18,2},{3,19},{19,3},{4,20},{20... | collective-permute-start | bytes 1572872 | tf_op jit(solution)/shard_map/ppermute | solution.py:422
  70.8 34.8 %collective-permute-start.13 = (bf16[128,2048]{1,0:T(8,128)(2,1)}, bf16[128,2048]{1,0:T(8,128)(2,1)S(1)}, u32[]{:S(2)}, u32[]{:S(2)}) collective-permute-start(bf16[128,2048]{1,0:T(8,128)(2,1)} %collective-permute-done.12.refs_6_), channel_id=1, source_target_pairs={{0,16},{16,0},{1,17},{17,1},{2,18},{18,2},{3,19},{19,3},{4,20},{20... | collective-permute-start | bytes 1572872 | tf_op jit(solution)/shard_map/ppermute | solution.py:422
  73.3 40.6 %collective-permute-start.19 = (bf16[128,2048]{1,0:T(8,128)(2,1)}, bf16[128,2048]{1,0:T(8,128)(2,1)S(1)}, u32[]{:S(2)}, u32[]{:S(2)}) collective-permute-start(bf16[128,2048]{1,0:T(8,128)(2,1)} %collective-permute-done.12.refs_6_), channel_id=1, source_target_pairs={{0,1},{1,0},{2,3},{3,2},{4,5},{5,4},{6,7},{7,6},{8,9},{9,8},{10,11... | collective-permute-start | bytes 1572872 | tf_op jit(solution)/shard_map/ppermute | solution.py:416
  83.6 33.6 %collective-permute-start.14 = (bf16[2048,128]{1,0:T(8,128)(2,1)S(1)}, bf16[2048,128]{1,0:T(8,128)(2,1)S(1)}, u32[]{:S(2)}, u32[]{:S(2)}) collective-permute-start(bf16[2048,128]{1,0:T(8,128)(2,1)S(1)} %collective-permute-done.9.refs_4_), channel_id=1, source_target_pairs={{0,1},{1,0},{2,3},{3,2},{4,5},{5,4},{6,7},{7,6},{8,9},{9,8},{10,11... | collective-permute-start | bytes 1572872 | tf_op jit(solution)/shard_map/ppermute | solution.py:416
  94.8 22.4 %collective-permute-start.15 = (bf16[2048,128]{1,0:T(8,128)(2,1)S(1)}, bf16[2048,128]{1,0:T(8,128)(2,1)S(1)}, u32[]{:S(2)}, u32[]{:S(2)}) collective-permute-start(bf16[2048,128]{1,0:T(8,128)(2,1)S(1)} %collective-permute-done.11.refs_5_), channel_id=1, source_target_pairs={{0,1},{1,0},{2,3},{3,2},{4,5},{5,4},{6,7},{7,6},{8,9},{9,8},{10,11... | collective-permute-start | bytes 1572872 | tf_op jit(solution)/shard_map/ppermute | solution.py:416
  105.6 11.6 %collective-permute-start.16 = (bf16[128,2048]{1,0:T(8,128)(2,1)S(1)}, bf16[128,2048]{1,0:T(8,128)(2,1)S(1)}, u32[]{:S(2)}, u32[]{:S(2)}) collective-permute-start(bf16[128,2048]{1,0:T(8,128)(2,1)S(1)} %collective-permute-done.13.refs_6_), channel_id=1, source_target_pairs={{0,1},{1,0},{2,3},{3,2},{4,5},{5,4},{6,7},{7,6},{8,9},{9,8},{10,11... | collective-permute-start | bytes 1572872 | tf_op jit(solution)/shard_map/ppermute | solution.py:416
  105.6 11.4 %collective-permute-start.4 = (bf16[32,2048]{1,0:T(8,128)(2,1)S(1)}, bf16[32,2048]{1,0:T(8,128)(2,1)S(1)}, u32[]{:S(2)}, u32[]{:S(2)}) collective-permute-start(bf16[32,2048]{1,0:T(8,128)(2,1)S(1)} %select_convert_fusion), channel_id=1, source_target_pairs={{0,2},{1,3},{2,0},{3,1},{4,6},{5,7},{6,4},{7,5},{8,10},{9,11},{10,... | collective-permute-start | bytes 393224 | tf_op jit(solution)/shard_map/ppermute | solution.py:419
  107.1 1.2 copy-start.1
  108.3 1.2 copy-start.2
  117.2 17.6 %copy-start.9 = (f32[2048]{0:T(1024)S(1)}, f32[2048]{0:T(1024)}, u32[]{:S(2)}) copy-start(f32[2048]{0:T(1024)} %param.18) | copy-start | bytes 24580
  118.9 21.6 %collective-permute-start.23 = (bf16[96,2048]{1,0:T(8,128)(2,1)S(1)}, bf16[96,2048]{1,0:T(8,128)(2,1)S(1)}, u32[]{:S(2)}, u32[]{:S(2)}) collective-permute-start(bf16[96,2048]{1,0:T(8,128)(2,1)S(1)} %get-tuple-element.19), channel_id=1, source_target_pairs={{0,12},{4,0},{8,4},{12,8},{1,13},{5,1},{9,5},{13,9},{2,14},{6,2},{... | collective-permute-start | bytes 1179656 | tf_op jit(solution)/shard_map/ppermute | solution.py:425
  130.9 36.6 %collective-permute-start.24 = (bf16[96,2048]{1,0:T(8,128)(2,1)S(1)}, bf16[96,2048]{1,0:T(8,128)(2,1)S(1)}, u32[]{:S(2)}, u32[]{:S(2)}) collective-permute-start(bf16[96,2048]{1,0:T(8,128)(2,1)S(1)} %get-tuple-element.20), channel_id=1, source_target_pairs={{0,8},{4,12},{8,0},{12,4},{1,9},{5,13},{9,1},{13,5},{2,10},{6,14},... | collective-permute-start | bytes 1179656 | tf_op jit(solution)/shard_map/ppermute | solution.py:425
  132.9 34.7 %collective-permute-start.25 = (bf16[96,2048]{1,0:T(8,128)(2,1)S(1)}, bf16[96,2048]{1,0:T(8,128)(2,1)S(1)}, u32[]{:S(2)}, u32[]{:S(2)}) collective-permute-start(bf16[96,2048]{1,0:T(8,128)(2,1)S(1)} %get-tuple-element.21), channel_id=1, source_target_pairs={{0,4},{4,8},{8,12},{12,0},{1,5},{5,9},{9,13},{13,1},{2,6},{6,10},{... | collective-permute-start | bytes 1179656 | tf_op jit(solution)/shard_map/ppermute | solution.py:425
where the time goes:
time: 171 us; the launch traced here: 170 us
  waiting for transfers between devices  100 us (58%)
  starting transfers between devices  37.4 us (22%)
  Pallas kernels  17.4 us (10%)
  local copies, waits for them, and re-layouts  11.1 us (6%)
  other arithmetic  3.02 us (2%)
    ppermute x6, waiting for transfers between devices, turn(): lax.ppermute(array, 'ep', [(i, (i + d) % blocks) for i in range(blocks)])  51.9 us
    ppermute x3, waiting for transfers between devices, beside(): return lax.ppermute(array, 'grp', [(0, 1), (1, 0)])  32.1 us
    ppermute x6, starting transfers between devices, turn(): lax.ppermute(array, 'ep', [(i, (i + d) % blocks) for i in range(blocks)])  21.4 us
    ppermute x4, waiting for transfers between devices, across(): return lax.ppermute(array, 'tp', [(i, i ^ 2) for i in range(shards)])  16.4 us
    pallas_call x3, Pallas kernels, expert_part(): call(body, outs, [VMEM] * (count + len(flat) + len(extra)), flops=6 * cou...  9.13 us
    unnamed x24, local copies, waits for them, and re-layouts  7.66 us
    ppermute x3, starting transfers between devices, upward(): lax.ppermute(array, 'ep', [(i, i + 1) for i in range(d - 1, blocks - 1)])  6.31 us
    ppermute x4, starting transfers between devices, across(): return lax.ppermute(array, 'tp', [(i, i ^ 2) for i in range(shards)])  5.21 us
  transfers between devices with their start and end apart: 26, of which 9 were waited for; matrix products, arithmetic and copies ran while one was open for 4% of the time, Pallas kernels for 8%

commit v1 on v0

--- a/solution.py
+++ b/solution.py
@@ -170,7 +170,7 @@
 
 VMEM = pl.BlockSpec(memory_space=pltpu.VMEM)
 SMEM = pl.BlockSpec(memory_space=pltpu.SMEM)
-ANY = pl.BlockSpec(memory_space=pl.ANY)
+HBM = pl.BlockSpec(memory_space=pltpu.HBM)
 
 
 def shape_of(shape, dtype=jnp.bfloat16):
@@ -190,77 +190,151 @@
 
 
 def selections(place_ref, ids_ref, experts, capacity):
-    rows, top = ids_ref.shape
-    ids = ids_ref[...]
-    lane = lax.broadcasted_iota(jnp.int32, (rows, 128), 1)
-    expert = (place_ref[0] + lane) % experts
-    chosen = jnp.zeros((rows, 128), jnp.float32)
-    for k in range(top):
-        chosen = chosen + jnp.where(ids[:, k : k + 1] == expert, 1.0, 0.0)
-    chosen = jnp.where(lane < experts, chosen, 0.0)
-    below = lax.broadcasted_iota(jnp.int32, (rows, rows), 1) < lax.broadcasted_iota(
-        jnp.int32, (rows, rows), 0
+    top, rows = ids_ref.shape
+    distance = lax.broadcasted_iota(jnp.int32, (8, rows), 0)
+    expert = (place_ref[0] + distance) % experts
+    hits = [ids_ref[k : k + 1, :] == expert for k in range(top)]
+    chosen = jnp.zeros((8, rows), jnp.float32)
+    for hit in hits:
+        chosen = chosen + jnp.where(hit & (distance < experts), 1.0, 0.0)
+    below = lax.broadcasted_iota(jnp.int32, (rows, rows), 0) < lax.broadcasted_iota(
+        jnp.int32, (rows, rows), 1
     )
     rank = jnp.dot(
-        below.astype(jnp.bfloat16), chosen.astype(jnp.bfloat16), preferred_element_type=jnp.float32
-    )
-    slot = lax.broadcasted_iota(jnp.int32, (rows, capacity), 1).astype(jnp.float32)
+        chosen.astype(jnp.bfloat16),
+        jnp.where(below, 1.0, 0.0).astype(jnp.bfloat16),
+        preferred_element_type=jnp.float32,
+    )
+    slot = lax.broadcasted_iota(jnp.int32, (capacity, rows), 0).astype(jnp.float32)
     picks = []
     for d in range(experts):
-        hit = (rank[:, d : d + 1] == slot) & (chosen[:, d : d + 1] > 0.5)
-        picks.append(jnp.where(hit, 1.0, 0.0).astype(jnp.bfloat16))
-    return ids, expert, picks
-
-
-def route_rows(place, moe_input, ffn_gain, expert_ids, experts, capacity):
+        pick = (rank[d : d + 1, :] == slot) & (chosen[d : d + 1, :] > 0.5)
+        picks.append(jnp.where(pick, 1.0, 0.0).astype(jnp.bfloat16))
+    return hits, picks
+
+
+def prepare(place, moe_input, ffn_gain, ids, keys, values, bias, weights, experts, capacity):
     rows, width = moe_input.shape
-
-    def body(place_ref, input_ref, gain_ref, ids_ref, *outs):
-        normed = norm_rows(input_ref[...], gain_ref[...]).astype(jnp.bfloat16)
-        _, _, picks = selections(place_ref, ids_ref, experts, capacity)
+    span, heads_width = keys.shape
+    heads = bias.shape[0]
+    gate, upward, down = weights
+    part = gate.shape[1] // 2
+    deep = gate.shape[0] // 2
+    thin = part // 2
+
+    def body(place_ref, gain_hbm, ids_hbm, bias_hbm, input_hbm, keys_hbm, values_hbm, *refs):
+        gate_hbm, up_hbm, down_hbm = refs[:3]
+        outs = refs[3 : 3 + experts]
+        own_ref, gate_a, gate_b, up_a, up_b, down_a, down_b = refs[3 + experts : 10 + experts]
+        input_v, gain_v, ids_v, bias_v, sems = refs[10 + experts :]
+        begin = pl.multiple_of(place_ref[2] * part, part)
+        columns = pl.ds(begin, part)
+        moves = [
+            (ids_hbm, ids_v),
+            (input_hbm, input_v),
+            (gain_hbm, gain_v),
+            (bias_hbm, bias_v),
+            (gate_hbm.at[pl.ds(0, deep), columns], gate_a),
+            (gate_hbm.at[pl.ds(deep, deep), columns], gate_b),
+            (keys_hbm, own_ref.at[pl.ds(0, span), pl.ds(0, heads_width)]),
+            (values_hbm, own_ref.at[pl.ds(0, span), pl.ds(heads_width, heads_width)]),
+            (up_hbm.at[pl.ds(0, deep), columns], up_a),
+            (up_hbm.at[pl.ds(deep, deep), columns], up_b),
+            (down_hbm.at[pl.ds(begin, thin), :], down_a),
+            (down_hbm.at[pl.ds(pl.multiple_of(begin + thin, thin), thin), :], down_b),
+        ]
+        copies = [
+            pltpu.make_async_copy(source, target, sems.at[k])
+            for k, (source, target) in enumerate(moves)
+        ]
+        for copy in copies:
+            copy.start()
+        own_ref[span:, :] = jnp.zeros((heads, 2 * heads_width), jnp.bfloat16)
+        copies[0].wait()
+        _, picks = selections(place_ref, ids_v, experts, capacity)
+        copies[1].wait()
+        copies[2].wait()
+        normed = norm_rows(input_v[...], gain_v[...]).astype(jnp.bfloat16)
         for d in range(experts):
-            outs[d][...] = lax.dot_general(
-                picks[d], normed, (((0,), (0,)), ((), ())), preferred_element_type=jnp.float32
+            outs[d][...] = jnp.dot(
+                picks[d], normed, preferred_element_type=jnp.float32
             ).astype(jnp.bfloat16)
-
-    outs = [shape_of((capacity, width))] * experts
-    return call(body, outs, [SMEM, VMEM, VMEM, VMEM], flops=4 * capacity * rows * width * 2)(
-        place, moe_input, ffn_gain.reshape(1, width), expert_ids
-    )
-
-
-def combine_rows(place, expert_ids, expert_scores, returned):
-    rows = expert_ids.shape[0]
+        copies[3].wait()
+        own_ref[span:, :span] = bias_v[...]
+        for copy in copies[4:]:
+            copy.wait()
+
+    outs = [shape_of((capacity, width))] * experts + [
+        shape_of((span + heads, 2 * heads_width)),
+        shape_of((deep, part)),
+        shape_of((deep, part)),
+        shape_of((deep, part)),
+        shape_of((deep, part)),
+        shape_of((thin, width)),
+        shape_of((thin, width)),
+    ]
+    return call(
+        body,
+        outs,
+        [SMEM] + [HBM] * 9,
+        scratch=(
+            pltpu.VMEM((rows, width), jnp.bfloat16),
+            pltpu.VMEM((1, width), jnp.float32),
+            pltpu.VMEM(ids.shape, jnp.int32),
+            pltpu.VMEM(bias.shape, jnp.bfloat16),
+            pltpu.SemaphoreType.DMA((12,)),
+        ),
+        flops=2 * experts * capacity * rows * width,
+    )(
+        place,
+        *(
+            pltpu.with_memory_space_constraint(array, pltpu.HBM)
+            for array in (
+                ffn_gain.reshape(1, width),
+                ids,
+                bias,
+                moe_input,
+                keys,
+                values,
+                gate,
+                upward,
+                down,
+            )
+        ),
+    )
+
+
+def combine_rows(place, ids, scores, returned):
+    rows = ids.shape[1]
     experts = len(returned)
     capacity, width = returned[0].shape
 
     def body(place_ref, ids_ref, scores_ref, *refs):
-        ids, expert, picks = selections(place_ref, ids_ref, experts, capacity)
-        scores = scores_ref[...]
-        weights = scores / jnp.sum(scores, axis=1, keepdims=True)
+        hits, picks = selections(place_ref, ids_ref, experts, capacity)
+        shares = scores_ref[...]
+        shares = shares / jnp.sum(shares, axis=0, keepdims=True)
+        weight = jnp.zeros((8, rows), jnp.float32)
+        for k, hit in enumerate(hits):
+            weight = weight + jnp.where(hit, shares[k : k + 1, :], 0.0)
+        weight = weight.T
         total = jnp.zeros((rows, width), jnp.float32)
         for d in range(experts):
-            weight = jnp.zeros((rows, 1), jnp.float32)
-            for k in range(ids.shape[1]):
-                weight = weight + jnp.where(
-                    ids[:, k : k + 1] == expert[:, d : d + 1], weights[:, k : k + 1], 0.0
-                )
-            total = total + weight * jnp.dot(
-                picks[d], refs[d][...], preferred_element_type=jnp.float32
+            total = total + weight[:, d : d + 1] * lax.dot_general(
+                picks[d], refs[d][...], (((0,), (0,)), ((), ())), preferred_element_type=jnp.float32
             )
         refs[-1][...] = total.astype(jnp.bfloat16)
 
     return call(
         body, shape_of((rows, width)), [SMEM, VMEM, VMEM] + [VMEM] * experts,
-        flops=4 * capacity * rows * width * 2,
-    )(place, expert_ids, expert_scores, *returned)
+        flops=2 * experts * capacity * rows * width,
+    )(place, ids, scores, *returned)
 
 
 def expert_part(rows_in, pieces, carried, last):
     capacity, width = rows_in[0].shape
     count = len(rows_in)
-    hidden = sum(piece[0].shape[1] for piece in pieces)
-    flat = [array for piece in pieces for array in piece]
+    hidden = sum(piece[0][0].shape[1] for piece in pieces)
+    flat = [array for piece in pieces for kind in piece for array in kind]
 
     def body(*refs):
         row_refs = refs[:count]
@@ -269,15 +343,22 @@
         if carried is not None:
             acc_ref, rest = rest[0], rest[1:]
         rows = jnp.concatenate([ref[...] for ref in row_refs], axis=0)
-        inner = []
-        for p in range(len(pieces)):
-            size = weight_refs[3 * p].shape[1]
-            both = jnp.concatenate([weight_refs[3 * p][...], weight_refs[3 * p + 1][...]], axis=1)
+        inner, down = [], []
+        at = 0
+        for piece in pieces:
+            kinds = []
+            for kind in piece:
+                chunk = [ref[...] for ref in weight_refs[at : at + len(kind)]]
+                kinds.append(chunk[0] if len(chunk) == 1 else jnp.concatenate(chunk, axis=0))
+                at += len(kind)
+            size = kinds[0].shape[1]
+            both = jnp.concatenate(kinds[:2], axis=1)
+            down.append(kinds[2])
             product = jnp.dot(rows, both, preferred_element_type=jnp.float32)
             gate, upward = product[:, :size], product[:, size:]
             inner.append((gate / (1.0 + jnp.exp(-gate)) * upward).astype(jnp.bfloat16))
         inner = jnp.concatenate(inner, axis=1)
-        down = jnp.concatenate([weight_refs[3 * p + 2][...] for p in range(len(pieces))], axis=0)
+        down = jnp.concatenate(down, axis=0)
         if last:
             for d in range(count):
                 some = slice(d * capacity, (d + 1) * capacity)
@@ -299,6 +380,27 @@
         [VMEM] * (count + len(flat) + len(extra)),
         flops=6 * count * capacity * width * hidden,
     )(*rows_in, *flat, *extra)
+
+
+def pair_sum(place, kept, received):
+    share = kept.shape[0] // 2
+
+    def body(place_ref, kept_ref, received_ref, outer_ref, inner_ref):
+        mine = place_ref[3]
+        for out, half in ((outer_ref, 1 - mine), (inner_ref, mine)):
+            some = pl.ds(pl.multiple_of(half * share, share), share)
+            out[...] = (kept_ref[some, :] + received_ref[some, :].astype(jnp.float32)).astype(out.dtype)
+
+    outs = [shape_of((share, kept.shape[1])), shape_of((share, kept.shape[1]), jnp.float32)]
+    return call(body, outs, [SMEM, VMEM, VMEM])(place, kept, received)
+
+
+def finish(inner, received, gain):
+    def body(inner_ref, received_ref, gain_ref, out_ref):
+        projected = inner_ref[...] + received_ref[...].astype(jnp.float32)
+        out_ref[...] = norm_rows(projected, gain_ref[...]).astype(jnp.bfloat16)
+
+    return call(body, shape_of(inner.shape), [VMEM] * 3)(inner, received, gain.reshape(1, -1))
 
 
 def attend_project(place, queries, own, passed, out_weight, heads, quarters):
@@ -408,9 +510,8 @@
     group = lax.axis_index("grp")
     block = lax.axis_index("ep")
     shard = lax.axis_index("tp")
-    place = jnp.stack([block, shard % 2]).astype(jnp.int32)
+    place = jnp.stack([block, shard % 2, group, shard // 2]).astype(jnp.int32)
     heads = stop_bias.shape[1]
-    span = queries.shape[0]
 
     def core(array):
         return lax.ppermute(array, "tp", [(i, i ^ 1) for i in range(shards)])
@@ -427,52 +528,41 @@
     def upward(array, d):
         return lax.ppermute(array, "ep", [(i, i + 1) for i in range(d - 1, blocks - 1)])
 
-    mine = (gate_weight[0], up_weight[0], down_weight[0])
-    part = mine[0].shape[1] // 2
-    gate_half = lax.dynamic_slice_in_dim(mine[0], group * part, part, 1)
-
     rows, top = expert_ids.shape
     capacity = 3 * rows * top // (2 * blocks)
-    outbound = route_rows(place, moe_input, ffn_gain, expert_ids, blocks, capacity)
+    mine = (gate_weight[0], up_weight[0], down_weight[0])
+    prepared = prepare(
+        place, moe_input, ffn_gain, expert_ids.T, keys, values, stop_bias.T, mine, blocks, capacity
+    )
+    outbound, own, halves = prepared[:blocks], prepared[blocks], prepared[blocks + 1 :]
+
     arrived = [outbound[0]] + [turn(outbound[d], d) for d in range(1, blocks)]
 
-    halves = (
-        gate_half,
-        lax.dynamic_slice_in_dim(mine[1], group * part, part, 1),
-        lax.dynamic_slice_in_dim(mine[2], group * part, part, 0),
-    )
     far = tuple(across(array) for array in halves)
     near = tuple(core(array) for array in mine)
     other = tuple(beside(array) for array in far)
     far_near = tuple(core(array) for array in far)
     other_near = tuple(core(array) for array in other)
 
-    own = jnp.concatenate(
-        [
-            jnp.concatenate([keys, values], axis=1),
-            jnp.pad(stop_bias.T, ((0, 0), (0, 2 * keys.shape[1] - span))),
-        ],
-        axis=0,
-    )
     passed = []
     for d in range(1, blocks):
         passed.append(upward(passed[-1] if passed else own, d))
 
-    summed = expert_part(arrived, [mine, near], None, False)[0]
-    summed = expert_part(arrived, [far, far_near], summed, False)[0]
-    produced = expert_part(arrived, [other, other_near], summed, True)
+    def whole(arrays):
+        return [[array] for array in arrays]
+
+    def chunked(arrays):
+        return [arrays[0:2], arrays[2:4], arrays[4:6]]
+
+    summed = expert_part(arrived, [whole(mine), whole(near)], None, False)[0]
+    summed = expert_part(arrived, [chunked(far), chunked(far_near)], summed, False)[0]
+    produced = expert_part(arrived, [chunked(other), chunked(other_near)], summed, True)
     returned = [produced[0]] + [turn(produced[d], -d) for d in range(1, blocks)]
 
     send, kept = attend_project(place, queries, own, passed, out_weight, heads, shards)
-    chip = kept + core(send).astype(jnp.float32)
-    share = span // shards
-    first, second = chip[:share], chip[share:]
-    outer = jnp.where(shard < 2, second, first).astype(jnp.bfloat16)
-    inner = jnp.where(shard < 2, first, second)
-    projected = inner + across(outer).astype(jnp.float32)
-    mixed = norm_rows(projected, mix_gain).astype(jnp.bfloat16)
-
-    experts_mixed = combine_rows(place, expert_ids, expert_scores, returned)
+    outer, inner = pair_sum(place, kept, core(send))
+    mixed = finish(inner, across(outer), mix_gain)
+    experts_mixed = combine_rows(place, expert_ids.T, expert_scores.T, returned)
     return (mixed, experts_mixed)
 
 

time: 171 us -> 153 us (0.89)
  waiting for transfers between devices: 100 us -> 82.4 us
  starting transfers between devices: 37.4 us -> 52 us
  local copies, waits for them, and re-layouts: 11.1 us -> 1.63 us
  other arithmetic: 3.02 us -> 0.08 us
  Pallas kernels: 17.4 us -> 15.3 us
    ppermute x6, waiting for transfers between devices: 51.9 us -> 38.4 us  [turn(): lax.ppermute(array, 'ep', [(i, (i + d) % blocks) for i in range(blocks)])]
    ppermute x3 -> x6, waiting for transfers between devices: 32.1 us -> 25.3 us  [beside(): return lax.ppermute(array, 'grp', [(0, 1), (1, 0)])]
    unnamed x24 -> x16, local copies, waits for them, and re-layouts: 7.66 us -> 1.63 us
    ppermute x4 -> x7, starting transfers between devices: 5.21 us -> 10.7 us  [across(): return lax.ppermute(array, 'tp', [(i, i ^ 2) for i in range(shards)])]
    ppermute x3 -> x6, starting transfers between devices: 3.62 us -> 8.05 us  [beside(): return lax.ppermute(array, 'grp', [(0, 1), (1, 0)])]
    dynamic_slice x3 -> x0, local copies, waits for them, and re-layouts: 3.39 us -> none  [the longest x1 1.22 us: paired_step(): gate_half = lax.dynamic_slice_in_dim(mine[0], group * part, part, 1)]
    ppermute x6, starting transfers between devices: 21.4 us -> 24.7 us  [turn(): lax.ppermute(array, 'ep', [(i, (i + d) % blocks) for i in range(blocks)])]
    pallas_call x3, Pallas kernels: 9.13 us -> 5.8 us  [expert_part(): call(body, outs, [VMEM] * (count + len(flat) + len(extra)), flops=6 * cou...]
  transfers between devices with their start and end apart: 26 -> 38, of which waited for: 9 -> 17; matrix products, arithmetic and copies ran while one was open for 4% -> 0% of each run, Pallas kernels for 8% -> 7%
where the time goes in v1:
time: 153 us; the launch traced here: 152 us
  waiting for transfers between devices  82.4 us (54%)
  starting transfers between devices  52 us (34%)
  Pallas kernels  15.3 us (10%)
  local copies, waits for them, and re-layouts  1.63 us (1%)
    ppermute x6, waiting for transfers between devices, turn(): lax.ppermute(array, 'ep', [(i, (i + d) % blocks) for i in range(blocks)])  38.4 us
    ppermute x6, waiting for transfers between devices, beside(): return lax.ppermute(array, 'grp', [(0, 1), (1, 0)])  25.3 us
    ppermute x6, starting transfers between devices, turn(): lax.ppermute(array, 'ep', [(i, (i + d) % blocks) for i in range(blocks)])  24.7 us
    ppermute x7, waiting for transfers between devices, across(): return lax.ppermute(array, 'tp', [(i, i ^ 2) for i in range(shards)])  18.7 us
    ppermute x7, starting transfers between devices, across(): return lax.ppermute(array, 'tp', [(i, i ^ 2) for i in range(shards)])  10.7 us
    ppermute x6, starting transfers between devices, beside(): return lax.ppermute(array, 'grp', [(0, 1), (1, 0)])  8.05 us
    pallas_call x3, Pallas kernels, expert_part(): call(body, outs, [VMEM] * (count + len(flat) + len(extra)), flops=6 * cou...  5.8 us
    ppermute x3, starting transfers between devices, upward(): lax.ppermute(array, 'ep', [(i, i + 1) for i in range(d - 1, blocks - 1)])  5.35 us
  transfers between devices with their start and end apart: 38, of which 17 were waited for; matrix products, arithmetic and copies ran while one was open for 0% of the time, Pallas kernels for 7%

profile of v1, /device:TPU:0, one launch (start us, length us, event | category | flops | bytes accessed | tf_op | source)
XLA Modules:
  0.0 152.3 jit_solution(15211350931769627080)
XLA Ops:
  0.6 0.0 copy-start
  0.6 0.0 copy-start.1
  0.7 0.0 copy-start.2
  0.7 0.1 pad_add_fusion.place_ref
  0.8 2.8 %shard_map.140 = (bf16[96,2048]{1,0:T(8,128)(2,1)S(1)}, bf16[96,2048]{1,0:T(8,128)(2,1)S(1)}, bf16[96,2048]{1,0:T(8,128)(2,1)S(1)}, bf16[96,2048]{1,0:T(8,128)(2...) custom-call(s32[4]{0:T(128)S(1)} %pad_add_fusion.place_ref, ...), custom_call_target="tpu_custom_call" | custom-call | flops 201326592 | tf_op jit(solution)/shard_map/pallas_call | solution.py:276
  3.6 3.0 %collective-permute-start.8 = (bf16[1024,128]{1,0:T(8,128)(2,1)S(1)}, bf16[1024,128]{1,0:T(8,128)(2,1)S(1)}, u32[]{:S(2)}, u32[]{:S(2)}) collective-permute-start(bf16[1024,128]{1,0:T(8,128)(2,1)S(1)} %get-tuple-element.30), channel_id=1, source_target_pairs={{0,2},{1,3},{2,0},{3,1},{4,6},{5,7},{6,4},{7,5},{8,10},{9,11},{10,... | collective-permute-start | bytes 786440 | tf_op jit(solution)/shard_map/ppermute | solution.py:520
  6.6 0.1 collective-permute-start.10
  6.7 1.9 %collective-permute-start.12 = (bf16[1024,128]{1,0:T(8,128)(2,1)S(1)}, bf16[1024,128]{1,0:T(8,128)(2,1)S(1)}, u32[]{:S(2)}, u32[]{:S(2)}) collective-permute-start(bf16[1024,128]{1,0:T(8,128)(2,1)S(1)} %get-tuple-element.32), channel_id=1, source_target_pairs={{0,2},{1,3},{2,0},{3,1},{4,6},{5,7},{6,4},{7,5},{8,10},{9,11},{10,... | collective-permute-start | bytes 786440 | tf_op jit(solution)/shard_map/ppermute | solution.py:520
  8.6 0.1 collective-permute-start.14
  8.7 1.9 %collective-permute-start.16 = (bf16[64,2048]{1,0:T(8,128)(2,1)S(1)}, bf16[64,2048]{1,0:T(8,128)(2,1)S(1)}, u32[]{:S(2)}, u32[]{:S(2)}) collective-permute-start(bf16[64,2048]{1,0:T(8,128)(2,1)S(1)} %get-tuple-element.34), channel_id=1, source_target_pairs={{0,2},{1,3},{2,0},{3,1},{4,6},{5,7},{6,4},{7,5},{8,10},{9,11},{10,... | collective-permute-start | bytes 786440 | tf_op jit(solution)/shard_map/ppermute | solution.py:520
  10.6 3.1 %collective-permute-done.8.refs_4_ = bf16[1024,128]{1,0:T(8,128)(2,1)S(1)} collective-permute-done((bf16[1024,128]{1,0:T(8,128)(2,1)S(1)}, bf16[1024,128]{1,0:T(8,128)(2,1)S(1)}, u32[]{:S(2)}, u32[]{:S(2)}) %collective-permute-start.8) | collective-permute-done | bytes 262176 | tf_op jit(solution)/shard_map/ppermute | solution.py:520
  13.7 4.0 %collective-permute-start = (bf16[136,1024]{1,0:T(8,128)(2,1)S(1)}, bf16[136,1024]{1,0:T(8,128)(2,1)S(1)}, u32[]{:S(2)}, u32[]{:S(2)}) collective-permute-start(bf16[136,1024]{1,0:T(8,128)(2,1)S(1)} %get-tuple-element.21.own_ref), channel_id=1, source_target_pairs={{0,4},{4,8},{8,12},{1,5},{5,9},{9,13},{2,6},{6,10},{10,14},{3,7},{... | collective-permute-start | bytes 835592 | tf_op jit(solution)/shard_map/ppermute | solution.py:529
  17.8 1.6 %collective-permute-done.10.refs_5_ = bf16[1024,128]{1,0:T(8,128)(2,1)S(1)} collective-permute-done((bf16[1024,128]{1,0:T(8,128)(2,1)S(1)}, bf16[1024,128]{1,0:T(8,128)(2,1)S(1)}, u32[]{:S(2)}, u32[]{:S(2)}) %collective-permute-start.10) | collective-permute-done | bytes 262176 | tf_op jit(solution)/shard_map/ppermute | solution.py:520
  19.4 2.0 %collective-permute-start.18 = (bf16[64,2048]{1,0:T(8,128)(2,1)S(1)}, bf16[64,2048]{1,0:T(8,128)(2,1)S(1)}, u32[]{:S(2)}, u32[]{:S(2)}) collective-permute-start(bf16[64,2048]{1,0:T(8,128)(2,1)S(1)} %get-tuple-element.35), channel_id=1, source_target_pairs={{0,2},{1,3},{2,0},{3,1},{4,6},{5,7},{6,4},{7,5},{8,10},{9,11},{10,... | collective-permute-start | bytes 786440 | tf_op jit(solution)/shard_map/ppermute | solution.py:520
  21.4 3.6 %collective-permute-done.12.refs_6_ = bf16[1024,128]{1,0:T(8,128)(2,1)S(1)} collective-permute-done((bf16[1024,128]{1,0:T(8,128)(2,1)S(1)}, bf16[1024,128]{1,0:T(8,128)(2,1)S(1)}, u32[]{:S(2)}, u32[]{:S(2)}) %collective-permute-start.12) | collective-permute-done | bytes 262176 | tf_op jit(solution)/shard_map/ppermute | solution.py:520
  25.0 2.1 %collective-permute-start.5 = (bf16[96,2048]{1,0:T(8,128)(2,1)S(1)}, bf16[96,2048]{1,0:T(8,128)(2,1)S(1)}, u32[]{:S(2)}, u32[]{:S(2)}) collective-permute-start(bf16[96,2048]{1,0:T(8,128)(2,1)S(1)} %get-tuple-element.27), channel_id=1, source_target_pairs={{0,4},{4,8},{8,12},{12,0},{1,5},{5,9},{9,13},{13,1},{2,6},{6,10},{... | collective-permute-start | bytes 1179656 | tf_op jit(solution)/shard_map/ppermute | solution.py:526
  27.1 3.5 %collective-permute-done.14.refs_7_ = bf16[1024,128]{1,0:T(8,128)(2,1)S(1)} collective-permute-done((bf16[1024,128]{1,0:T(8,128)(2,1)S(1)}, bf16[1024,128]{1,0:T(8,128)(2,1)S(1)}, u32[]{:S(2)}, u32[]{:S(2)}) %collective-permute-start.14) | collective-permute-done | bytes 262176 | tf_op jit(solution)/shard_map/ppermute | solution.py:520
  30.6 3.1 %collective-permute-start.6 = (bf16[96,2048]{1,0:T(8,128)(2,1)S(1)}, bf16[96,2048]{1,0:T(8,128)(2,1)S(1)}, u32[]{:S(2)}, u32[]{:S(2)}) collective-permute-start(bf16[96,2048]{1,0:T(8,128)(2,1)S(1)} %get-tuple-element.28), channel_id=1, source_target_pairs={{0,8},{4,12},{8,0},{12,4},{1,9},{5,13},{9,1},{13,5},{2,10},{6,14},... | collective-permute-start | bytes 1179656 | tf_op jit(solution)/shard_map/ppermute | solution.py:526
  33.7 2.5 %collective-permute-done.16.refs_8_ = bf16[64,2048]{1,0:T(8,128)(2,1)S(1)} collective-permute-done((bf16[64,2048]{1,0:T(8,128)(2,1)S(1)}, bf16[64,2048]{1,0:T(8,128)(2,1)S(1)}, u32[]{:S(2)}, u32[]{:S(2)}) %collective-permute-start.16) | collective-permute-done | bytes 262176 | tf_op jit(solution)/shard_map/ppermute | solution.py:520
  36.2 4.1 %collective-permute-start.7 = (bf16[96,2048]{1,0:T(8,128)(2,1)S(1)}, bf16[96,2048]{1,0:T(8,128)(2,1)S(1)}, u32[]{:S(2)}, u32[]{:S(2)}) collective-permute-start(bf16[96,2048]{1,0:T(8,128)(2,1)S(1)} %get-tuple-element.29), channel_id=1, source_target_pairs={{0,12},{4,0},{8,4},{12,8},{1,13},{5,1},{9,5},{13,9},{2,14},{6,2},{... | collective-permute-start | bytes 1179656 | tf_op jit(solution)/shard_map/ppermute | solution.py:526
  40.4 0.6 collective-permute-done.18.refs_9_
  41.0 0.5 collective-permute-start.27
  41.5 0.1 collective-permute-start.28
  41.6 11.7 %collective-permute-done.6.refs_2_ = bf16[96,2048]{1,0:T(8,128)(2,1)S(1)} collective-permute-done((bf16[96,2048]{1,0:T(8,128)(2,1)S(1)}, bf16[96,2048]{1,0:T(8,128)(2,1)S(1)}, u32[]{:S(2)}, u32[]{:S(2)}) %collective-permute-start.6) | collective-permute-done | bytes 393248 | tf_op jit(solution)/shard_map/ppermute | solution.py:526
  53.2 1.7 %collective-permute-done.7.refs_3_ = bf16[96,2048]{1,0:T(8,128)(2,1)S(1)} collective-permute-done((bf16[96,2048]{1,0:T(8,128)(2,1)S(1)}, bf16[96,2048]{1,0:T(8,128)(2,1)S(1)}, u32[]{:S(2)}, u32[]{:S(2)}) %collective-permute-start.7) | collective-permute-done | bytes 393248 | tf_op jit(solution)/shard_map/ppermute | solution.py:526
  54.9 0.5 collective-permute-start.31
  55.4 1.5 collective-permute-start.9
  56.9 0.5 collective-permute-start.11
  57.5 1.5 collective-permute-start.13
  59.0 0.5 collective-permute-start.33
  59.5 5.1 %collective-permute-done.9.refs_4_ = bf16[1024,128]{1,0:T(8,128)(2,1)S(1)} collective-permute-done((bf16[1024,128]{1,0:T(8,128)(2,1)S(1)}, bf16[1024,128]{1,0:T(8,128)(2,1)S(1)}, u32[]{:S(2)}, u32[]{:S(2)}) %collective-permute-start.9) | collective-permute-done | bytes 262176 | tf_op jit(solution)/shard_map/ppermute | solution.py:523
  64.6 5.6 %collective-permute-done.11.refs_5_ = bf16[1024,128]{1,0:T(8,128)(2,1)S(1)} collective-permute-done((bf16[1024,128]{1,0:T(8,128)(2,1)S(1)}, bf16[1024,128]{1,0:T(8,128)(2,1)S(1)}, u32[]{:S(2)}, u32[]{:S(2)}) %collective-permute-start.11) | collective-permute-done | bytes 262176 | tf_op jit(solution)/shard_map/ppermute | solution.py:523
  70.2 0.7 collective-permute-start.1
  70.9 4.0 %collective-permute-done.13.refs_6_ = bf16[1024,128]{1,0:T(8,128)(2,1)S(1)} collective-permute-done((bf16[1024,128]{1,0:T(8,128)(2,1)S(1)}, bf16[1024,128]{1,0:T(8,128)(2,1)S(1)}, u32[]{:S(2)}, u32[]{:S(2)}) %collective-permute-start.13) | collective-permute-done | bytes 262176 | tf_op jit(solution)/shard_map/ppermute | solution.py:523
  74.9 1.5 collective-permute-start.15
  76.5 0.7 collective-permute-start.2
  77.1 5.2 %collective-permute-done.15.refs_7_ = bf16[1024,128]{1,0:T(8,128)(2,1)S(1)} collective-permute-done((bf16[1024,128]{1,0:T(8,128)(2,1)S(1)}, bf16[1024,128]{1,0:T(8,128)(2,1)S(1)}, u32[]{:S(2)}, u32[]{:S(2)}) %collective-permute-start.15) | collective-permute-done | bytes 262176 | tf_op jit(solution)/shard_map/ppermute | solution.py:523
  82.4 1.5 collective-permute-start.17
  83.9 5.1 %collective-permute-done.17.refs_8_ = bf16[64,2048]{1,0:T(8,128)(2,1)S(1)} collective-permute-done((bf16[64,2048]{1,0:T(8,128)(2,1)S(1)}, bf16[64,2048]{1,0:T(8,128)(2,1)S(1)}, u32[]{:S(2)}, u32[]{:S(2)}) %collective-permute-start.17) | collective-permute-done | bytes 262176 | tf_op jit(solution)/shard_map/ppermute | solution.py:523
  88.9 1.5 collective-permute-start.19
  90.4 0.0 copy-start.3
  90.5 1.6 %copy-done.3 = bf16[512,2048]{1,0:T(8,128)(2,1)S(1)} copy-done((bf16[512,2048]{1,0:T(8,128)(2,1)S(1)}, bf16[512,2048]{1,0:T(8,128)(2,1)}, u32[]{:S(2)}) %copy-start.3) | copy-done | bytes 2097176
  92.0 3.0 %shard_map.141 = (bf16[64,2048]{1,0:T(8,128)(2,1)S(1)}, f32[64,2048]{1,0:T(8,128)S(1)}) custom-call(s32[4]{0:T(128)S(1)} %pad_add_fusion.place_ref, bf16[128,512]{1,0:T(8,128)(2,1)S(1)} %copy-done.4, bf16[136,1024]{1,0:T(8,128)(2,1)S(1)} %get-tuple-element.21.own_ref, bf16[136,1024]{1,0:T(8,128)(2,1)S(1)} %collective-permute-done.refs_0_, ...), custom_call_target="tpu_custom_call" | custom-call | flops 402653184 | tf_op jit(solution)/shard_map/pallas_call | solution.py:475
  95.1 0.2 collective-permute-done.19.refs_9_
  95.3 0.4 collective-permute-start.21
  95.7 0.1 collective-permute-start.22
  95.8 0.4 collective-permute-start.23
  96.2 0.1 collective-permute-start.24
  96.3 0.4 collective-permute-start.25
  96.7 2.6 %shard_map.144.refs_16_ = f32[384,2048]{1,0:T(8,128)S(1)} custom-call(bf16[96,2048]{1,0:T(8,128)(2,1)S(1)} %get-tuple-element.26.refs_0_, bf16[96,2048]{1,0:T(8,128)(2,1)S(1)} %collective-permute-done.5.refs_1_, bf16[96,2048]{1,0:T(8,128)(2,1)S(1)} %collective-permute-done.6.refs_2_, bf16[96,2048]{1,0:T(8,128)(2,1)S(1)} %collective-permute-done.7.refs_3_, ...), custom_call_target="tpu_custom_call" | custom-call | flops 2415919104 | tf_op jit(solution)/shard_map/pallas_call | solution.py:377
  99.3 1.5 shard_map.145.refs_16_
  100.8 0.0 copy-start.5
  100.8 0.0 copy-start.7
  100.9 0.2 collective-permute-start.3
  101.1 1.7 %shard_map.146 = (bf16[96,2048]{1,0:T(8,128)(2,1)S(1)}, bf16[96,2048]{1,0:T(8,128)(2,1)S(1)}, bf16[96,2048]{1,0:T(8,128)(2,1)S(1)}, bf16[96,2048]{1,0:T(8,128)(2,1)S(1)}) custom-call(bf16[96,2048]{1,0:T(8,128)(2,1)S(1)} %get-tuple-element.26.refs_0_, bf16[96,2048]{1,0:T(8,128)(2,1)S(1)} %collective-permute-done.5.refs_1_, ...), custom_call_target="tpu_custom_call" | custom-call | flops 1207959552 | tf_op jit(solution)/shard_map/pallas_call | solution.py:377
  102.8 14.7 %collective-permute-start.35 = (bf16[96,2048]{1,0:T(8,128)(2,1)S(1)}, bf16[96,2048]{1,0:T(8,128)(2,1)S(1)}, u32[]{:S(2)}, u32[]{:S(2)}) collective-permute-start(bf16[96,2048]{1,0:T(8,128)(2,1)S(1)} %get-tuple-element.37), channel_id=1, source_target_pairs={{0,12},{4,0},{8,4},{12,8},{1,13},{5,1},{9,5},{13,9},{2,14},{6,2},{... | collective-permute-start | bytes 1179656 | tf_op jit(solution)/shard_map/ppermute | solution.py:526
  117.5 0.6 collective-permute-start.37
  118.2 0.6 shard_map.142
  118.8 1.6 %collective-permute-start.4 = (bf16[32,2048]{1,0:T(8,128)(2,1)S(1)}, bf16[32,2048]{1,0:T(8,128)(2,1)S(1)}, u32[]{:S(2)}, u32[]{:S(2)}) collective-permute-start(bf16[32,2048]{1,0:T(8,128)(2,1)S(1)} %get-tuple-element.25), channel_id=1, source_target_pairs={{0,2},{1,3},{2,0},{3,1},{4,6},{5,7},{6,4},{7,5},{8,10},{9,11},{10,... | collective-permute-start | bytes 393224 | tf_op jit(solution)/shard_map/ppermute | solution.py:520
  120.3 3.8 %collective-permute-done.4.received_ref = bf16[32,2048]{1,0:T(8,128)(2,1)S(1)} collective-permute-done((bf16[32,2048]{1,0:T(8,128)(2,1)S(1)}, bf16[32,2048]{1,0:T(8,128)(2,1)S(1)}, u32[]{:S(2)}, u32[]{:S(2)}) %collective-permute-start.4) | collective-permute-done | bytes 131104 | tf_op jit(solution)/shard_map/ppermute | solution.py:520
  124.1 0.8 shard_map.143
  124.9 2.2 %collective-permute-done.35.refs_1_ = bf16[96,2048]{1,0:T(8,128)(2,1)S(1)} collective-permute-done((bf16[96,2048]{1,0:T(8,128)(2,1)S(1)}, bf16[96,2048]{1,0:T(8,128)(2,1)S(1)}, u32[]{:S(2)}, u32[]{:S(2)}) %collective-permute-start.35) | collective-permute-done | bytes 393248 | tf_op jit(solution)/shard_map/ppermute | solution.py:526
  127.1 22.9 %collective-permute-done.36.refs_2_ = bf16[96,2048]{1,0:T(8,128)(2,1)S(1)} collective-permute-done((bf16[96,2048]{1,0:T(8,128)(2,1)S(1)}, bf16[96,2048]{1,0:T(8,128)(2,1)S(1)}, u32[]{:S(2)}, u32[]{:S(2)}) %collective-permute-start.36) | collective-permute-done | bytes 393248 | tf_op jit(solution)/shard_map/ppermute | solution.py:526
  150.0 2.3 %shard_map.147 = bf16[128,2048]{1,0:T(8,128)(2,1)} custom-call(s32[4]{0:T(128)S(1)} %pad_add_fusion.place_ref, s32[2,128]{1,0:T(2,128)S(1)} %bitcast.23, f32[2,128]{1,0:T(2,128)S(1)} %bitcast.24, bf16[96,2048]{1,0:T(8,128)(2,1)S(1)} %get-tuple-element.36.refs_0_, bf16[96,2048]{1,0:T(8,128)(2,1)S(1)} %collective-permute-done.35.refs_1_, ...), custom_call_target="tpu_custom_call" | custom-call | flops 201326592 | tf_op jit(solution)/shard_map/pallas_call | solution.py:327
  (37 shorter events, 0.1 us)
Async XLA Ops:
  0.6 58.3 %copy-start = (bf16[1,2048,256]{2,1,0:T(8,128)(2,1)S(1)}, bf16[1,2048,256]{2,1,0:T(8,128)(2,1)}, u32[]{:S(2)}) copy-start(bf16[1,2048,256]{2,1,0:T(8,128)(2,1)} %param.23) | copy-start | bytes 3145732
  0.6 58.4 %copy-start.1 = (bf16[1,2048,256]{2,1,0:T(8,128)(2,1)S(1)}, bf16[1,2048,256]{2,1,0:T(8,128)(2,1)}, u32[]{:S(2)}) copy-start(bf16[1,2048,256]{2,1,0:T(8,128)(2,1)} %param.24) | copy-start | bytes 3145732
  0.7 64.0 %copy-start.2 = (bf16[1,256,2048]{2,1,0:T(8,128)(2,1)S(1)}, bf16[1,256,2048]{2,1,0:T(8,128)(2,1)}, u32[]{:S(2)}) copy-start(bf16[1,256,2048]{2,1,0:T(8,128)(2,1)} %param.25) | copy-start | bytes 3145732
  0.7 89.8 %copy-start.4 = (bf16[128,512]{1,0:T(8,128)(2,1)S(1)}, bf16[128,512]{1,0:T(8,128)(2,1)}, u32[]{:S(2)}) copy-start(bf16[128,512]{1,0:T(8,128)(2,1)} %q_ref.1) | copy-start | bytes 393220
  3.6 10.2 %collective-permute-start.8 = (bf16[1024,128]{1,0:T(8,128)(2,1)S(1)}, bf16[1024,128]{1,0:T(8,128)(2,1)S(1)}, u32[]{:S(2)}, u32[]{:S(2)}) collective-permute-start(bf16[1024,128]{1,0:T(8,128)(2,1)S(1)} %get-tuple-element.30), channel_id=1, source_target_pairs={{0,2},{1,3},{2,0},{3,1},{4,6},{5,7},{6,4},{7,5},{8,10},{9,11},{10,... | collective-permute-start | bytes 786440 | tf_op jit(solution)/shard_map/ppermute | solution.py:520
  6.6 12.8 %collective-permute-start.10 = (bf16[1024,128]{1,0:T(8,128)(2,1)S(1)}, bf16[1024,128]{1,0:T(8,128)(2,1)S(1)}, u32[]{:S(2)}, u32[]{:S(2)}) collective-permute-start(bf16[1024,128]{1,0:T(8,128)(2,1)S(1)} %get-tuple-element.31), channel_id=1, source_target_pairs={{0,2},{1,3},{2,0},{3,1},{4,6},{5,7},{6,4},{7,5},{8,10},{9,11},{10,... | collective-permute-start | bytes 786440 | tf_op jit(solution)/shard_map/ppermute | solution.py:520
  6.7 18.3 %collective-permute-start.12 = (bf16[1024,128]{1,0:T(8,128)(2,1)S(1)}, bf16[1024,128]{1,0:T(8,128)(2,1)S(1)}, u32[]{:S(2)}, u32[]{:S(2)}) collective-permute-start(bf16[1024,128]{1,0:T(8,128)(2,1)S(1)} %get-tuple-element.32), channel_id=1, source_target_pairs={{0,2},{1,3},{2,0},{3,1},{4,6},{5,7},{6,4},{7,5},{8,10},{9,11},{10,... | collective-permute-start | bytes 786440 | tf_op jit(solution)/shard_map/ppermute | solution.py:520
  8.6 22.0 %collective-permute-start.14 = (bf16[1024,128]{1,0:T(8,128)(2,1)S(1)}, bf16[1024,128]{1,0:T(8,128)(2,1)S(1)}, u32[]{:S(2)}, u32[]{:S(2)}) collective-permute-start(bf16[1024,128]{1,0:T(8,128)(2,1)S(1)} %get-tuple-element.33), channel_id=1, source_target_pairs={{0,2},{1,3},{2,0},{3,1},{4,6},{5,7},{6,4},{7,5},{8,10},{9,11},{10,... | collective-permute-start | bytes 786440 | tf_op jit(solution)/shard_map/ppermute | solution.py:520
  8.7 27.5 %collective-permute-start.16 = (bf16[64,2048]{1,0:T(8,128)(2,1)S(1)}, bf16[64,2048]{1,0:T(8,128)(2,1)S(1)}, u32[]{:S(2)}, u32[]{:S(2)}) collective-permute-start(bf16[64,2048]{1,0:T(8,128)(2,1)S(1)} %get-tuple-element.34), channel_id=1, source_target_pairs={{0,2},{1,3},{2,0},{3,1},{4,6},{5,7},{6,4},{7,5},{8,10},{9,11},{10,... | collective-permute-start | bytes 786440 | tf_op jit(solution)/shard_map/ppermute | solution.py:520
  13.7 27.2 %collective-permute-start = (bf16[136,1024]{1,0:T(8,128)(2,1)S(1)}, bf16[136,1024]{1,0:T(8,128)(2,1)S(1)}, u32[]{:S(2)}, u32[]{:S(2)}) collective-permute-start(bf16[136,1024]{1,0:T(8,128)(2,1)S(1)} %get-tuple-element.21.own_ref), channel_id=1, source_target_pairs={{0,4},{4,8},{8,12},{1,5},{5,9},{9,13},{2,6},{6,10},{10,14},{3,7},{... | collective-permute-start | bytes 835592 | tf_op jit(solution)/shard_map/ppermute | solution.py:529
  19.4 21.6 %collective-permute-start.18 = (bf16[64,2048]{1,0:T(8,128)(2,1)S(1)}, bf16[64,2048]{1,0:T(8,128)(2,1)S(1)}, u32[]{:S(2)}, u32[]{:S(2)}) collective-permute-start(bf16[64,2048]{1,0:T(8,128)(2,1)S(1)} %get-tuple-element.35), channel_id=1, source_target_pairs={{0,2},{1,3},{2,0},{3,1},{4,6},{5,7},{6,4},{7,5},{8,10},{9,11},{10,... | collective-permute-start | bytes 786440 | tf_op jit(solution)/shard_map/ppermute | solution.py:520
  25.0 16.5 %collective-permute-start.5 = (bf16[96,2048]{1,0:T(8,128)(2,1)S(1)}, bf16[96,2048]{1,0:T(8,128)(2,1)S(1)}, u32[]{:S(2)}, u32[]{:S(2)}) collective-permute-start(bf16[96,2048]{1,0:T(8,128)(2,1)S(1)} %get-tuple-element.27), channel_id=1, source_target_pairs={{0,4},{4,8},{8,12},{12,0},{1,5},{5,9},{9,13},{13,1},{2,6},{6,10},{... | collective-permute-start | bytes 1179656 | tf_op jit(solution)/shard_map/ppermute | solution.py:526
  30.6 22.6 %collective-permute-start.6 = (bf16[96,2048]{1,0:T(8,128)(2,1)S(1)}, bf16[96,2048]{1,0:T(8,128)(2,1)S(1)}, u32[]{:S(2)}, u32[]{:S(2)}) collective-permute-start(bf16[96,2048]{1,0:T(8,128)(2,1)S(1)} %get-tuple-element.28), channel_id=1, source_target_pairs={{0,8},{4,12},{8,0},{12,4},{1,9},{5,13},{9,1},{13,5},{2,10},{6,14},... | collective-permute-start | bytes 1179656 | tf_op jit(solution)/shard_map/ppermute | solution.py:526
  36.2 18.7 %collective-permute-start.7 = (bf16[96,2048]{1,0:T(8,128)(2,1)S(1)}, bf16[96,2048]{1,0:T(8,128)(2,1)S(1)}, u32[]{:S(2)}, u32[]{:S(2)}) collective-permute-start(bf16[96,2048]{1,0:T(8,128)(2,1)S(1)} %get-tuple-element.29), channel_id=1, source_target_pairs={{0,12},{4,0},{8,4},{12,8},{1,13},{5,1},{9,5},{13,9},{2,14},{6,2},{... | collective-permute-start | bytes 1179656 | tf_op jit(solution)/shard_map/ppermute | solution.py:526
  41.0 13.9 %collective-permute-start.26 = (bf16[1024,128]{1,0:T(8,128)(2,1)S(1)}, bf16[1024,128]{1,0:T(8,128)(2,1)S(1)}, u32[]{:S(2)}, u32[]{:S(2)}) collective-permute-start(bf16[1024,128]{1,0:T(8,128)(2,1)S(1)} %collective-permute-done.8.refs_4_), channel_id=1, source_target_pairs={{0,1},{1,0},{2,3},{3,2},{4,5},{5,4},{6,7},{7,6},{8,9},{9,8},{10,11... | collective-permute-start | bytes 786440 | tf_op jit(solution)/shard_map/ppermute | solution.py:517
  41.0 14.4 %collective-permute-start.27 = (bf16[1024,128]{1,0:T(8,128)(2,1)S(1)}, bf16[1024,128]{1,0:T(8,128)(2,1)S(1)}, u32[]{:S(2)}, u32[]{:S(2)}) collective-permute-start(bf16[1024,128]{1,0:T(8,128)(2,1)S(1)} %collective-permute-done.10.refs_5_), channel_id=1, source_target_pairs={{0,1},{1,0},{2,3},{3,2},{4,5},{5,4},{6,7},{7,6},{8,9},{9,8},{10,11... | collective-permute-start | bytes 786440 | tf_op jit(solution)/shard_map/ppermute | solution.py:517
  41.5 15.4 %collective-permute-start.28 = (bf16[1024,128]{1,0:T(8,128)(2,1)S(1)}, bf16[1024,128]{1,0:T(8,128)(2,1)S(1)}, u32[]{:S(2)}, u32[]{:S(2)}) collective-permute-start(bf16[1024,128]{1,0:T(8,128)(2,1)S(1)} %collective-permute-done.12.refs_6_), channel_id=1, source_target_pairs={{0,1},{1,0},{2,3},{3,2},{4,5},{5,4},{6,7},{7,6},{8,9},{9,8},{10,11... | collective-permute-start | bytes 786440 | tf_op jit(solution)/shard_map/ppermute | solution.py:517
  53.2 4.2 %collective-permute-start.29 = (bf16[1024,128]{1,0:T(8,128)(2,1)S(1)}, bf16[1024,128]{1,0:T(8,128)(2,1)S(1)}, u32[]{:S(2)}, u32[]{:S(2)}) collective-permute-start(bf16[1024,128]{1,0:T(8,128)(2,1)S(1)} %collective-permute-done.14.refs_7_), channel_id=1, source_target_pairs={{0,1},{1,0},{2,3},{3,2},{4,5},{5,4},{6,7},{7,6},{8,9},{9,8},{10,11... | collective-permute-start | bytes 786440 | tf_op jit(solution)/shard_map/ppermute | solution.py:517
  54.9 4.1 %collective-permute-start.30 = (bf16[64,2048]{1,0:T(8,128)(2,1)S(1)}, bf16[64,2048]{1,0:T(8,128)(2,1)S(1)}, u32[]{:S(2)}, u32[]{:S(2)}) collective-permute-start(bf16[64,2048]{1,0:T(8,128)(2,1)S(1)} %collective-permute-done.16.refs_8_), channel_id=1, source_target_pairs={{0,1},{1,0},{2,3},{3,2},{4,5},{5,4},{6,7},{7,6},{8,9},{9,8},{10,11... | collective-permute-start | bytes 786440 | tf_op jit(solution)/shard_map/ppermute | solution.py:517
  54.9 4.1 %collective-permute-start.31 = (bf16[64,2048]{1,0:T(8,128)(2,1)S(1)}, bf16[64,2048]{1,0:T(8,128)(2,1)S(1)}, u32[]{:S(2)}, u32[]{:S(2)}) collective-permute-start(bf16[64,2048]{1,0:T(8,128)(2,1)S(1)} %collective-permute-done.18.refs_9_), channel_id=1, source_target_pairs={{0,1},{1,0},{2,3},{3,2},{4,5},{5,4},{6,7},{7,6},{8,9},{9,8},{10,11... | collective-permute-start | bytes 786440 | tf_op jit(solution)/shard_map/ppermute | solution.py:517
  55.4 9.2 %collective-permute-start.9 = (bf16[1024,128]{1,0:T(8,128)(2,1)S(1)}, bf16[1024,128]{1,0:T(8,128)(2,1)S(1)}, u32[]{:S(2)}, u32[]{:S(2)}) collective-permute-start(bf16[1024,128]{1,0:T(8,128)(2,1)S(1)} %collective-permute-done.8.refs_4_), channel_id=1, source_target_pairs={{0,16},{16,0},{1,17},{17,1},{2,18},{18,2},{3,19},{19,3},{4,20},{20... | collective-permute-start | bytes 786440 | tf_op jit(solution)/shard_map/ppermute | solution.py:523
  56.9 13.3 %collective-permute-start.11 = (bf16[1024,128]{1,0:T(8,128)(2,1)S(1)}, bf16[1024,128]{1,0:T(8,128)(2,1)S(1)}, u32[]{:S(2)}, u32[]{:S(2)}) collective-permute-start(bf16[1024,128]{1,0:T(8,128)(2,1)S(1)} %collective-permute-done.10.refs_5_), channel_id=1, source_target_pairs={{0,16},{16,0},{1,17},{17,1},{2,18},{18,2},{3,19},{19,3},{4,20},{20... | collective-permute-start | bytes 786440 | tf_op jit(solution)/shard_map/ppermute | solution.py:523
  57.5 17.5 %collective-permute-start.13 = (bf16[1024,128]{1,0:T(8,128)(2,1)S(1)}, bf16[1024,128]{1,0:T(8,128)(2,1)S(1)}, u32[]{:S(2)}, u32[]{:S(2)}) collective-permute-start(bf16[1024,128]{1,0:T(8,128)(2,1)S(1)} %collective-permute-done.12.refs_6_), channel_id=1, source_target_pairs={{0,16},{16,0},{1,17},{17,1},{2,18},{18,2},{3,19},{19,3},{4,20},{20... | collective-permute-start | bytes 786440 | tf_op jit(solution)/shard_map/ppermute | solution.py:523
  59.0 36.8 %collective-permute-start.32 = (bf16[2048,256]{1,0:T(8,128)(2,1)S(1)}, bf16[2048,256]{1,0:T(8,128)(2,1)S(1)}, u32[]{:S(2)}, u32[]{:S(2)}) collective-permute-start(bf16[2048,256]{1,0:T(8,128)(2,1)S(1)} %bitcast.13), channel_id=1, source_target_pairs={{0,1},{1,0},{2,3},{3,2},{4,5},{5,4},{6,7},{7,6},{8,9},{9,8},{10,11... | collective-permute-start | bytes 3145736 | tf_op jit(solution)/shard_map/ppermute | solution.py:517
  59.0 37.2 %collective-permute-start.33 = (bf16[2048,256]{1,0:T(8,128)(2,1)S(1)}, bf16[2048,256]{1,0:T(8,128)(2,1)S(1)}, u32[]{:S(2)}, u32[]{:S(2)}) collective-permute-start(bf16[2048,256]{1,0:T(8,128)(2,1)S(1)} %bitcast.16), channel_id=1, source_target_pairs={{0,1},{1,0},{2,3},{3,2},{4,5},{5,4},{6,7},{7,6},{8,9},{9,8},{10,11... | collective-permute-start | bytes 3145736 | tf_op jit(solution)/shard_map/ppermute | solution.py:517
  64.6 31.7 %collective-permute-start.34 = (bf16[256,2048]{1,0:T(8,128)(2,1)S(1)}, bf16[256,2048]{1,0:T(8,128)(2,1)S(1)}, u32[]{:S(2)}, u32[]{:S(2)}) collective-permute-start(bf16[256,2048]{1,0:T(8,128)(2,1)S(1)} %bitcast.19), channel_id=1, source_target_pairs={{0,1},{1,0},{2,3},{3,2},{4,5},{5,4},{6,7},{7,6},{8,9},{9,8},{10,11... | collective-permute-start | bytes 3145736 | tf_op jit(solution)/shard_map/ppermute | solution.py:517
  70.2 6.2 %collective-permute-start.1 = (bf16[136,1024]{1,0:T(8,128)(2,1)S(1)}, bf16[136,1024]{1,0:T(8,128)(2,1)S(1)}, u32[]{:S(2)}, u32[]{:S(2)}) collective-permute-start(bf16[136,1024]{1,0:T(8,128)(2,1)S(1)} %collective-permute-done.refs_0_), channel_id=1, source_target_pairs={{4,8},{8,12},{5,9},{9,13},{6,10},{10,14},{7,11},{11,15},{20,24},{2... | collective-permute-start | bytes 835592 | tf_op jit(solution)/shard_map/ppermute | solution.py:529
  74.9 7.4 %collective-permute-start.15 = (bf16[1024,128]{1,0:T(8,128)(2,1)S(1)}, bf16[1024,128]{1,0:T(8,128)(2,1)S(1)}, u32[]{:S(2)}, u32[]{:S(2)}) collective-permute-start(bf16[1024,128]{1,0:T(8,128)(2,1)S(1)} %collective-permute-done.14.refs_7_), channel_id=1, source_target_pairs={{0,16},{16,0},{1,17},{17,1},{2,18},{18,2},{3,19},{19,3},{4,20},{20... | collective-permute-start | bytes 786440 | tf_op jit(solution)/shard_map/ppermute | solution.py:523
  76.5 14.0 %collective-permute-start.2 = (bf16[136,1024]{1,0:T(8,128)(2,1)S(1)}, bf16[136,1024]{1,0:T(8,128)(2,1)S(1)}, u32[]{:S(2)}, u32[]{:S(2)}) collective-permute-start(bf16[136,1024]{1,0:T(8,128)(2,1)S(1)} %collective-permute-done.1.refs_1_), channel_id=1, source_target_pairs={{8,12},{9,13},{10,14},{11,15},{24,28},{25,29},{26,30},{27,31}} | collective-permute-start | bytes 835592 | tf_op jit(solution)/shard_map/ppermute | solution.py:529
  82.4 6.6 %collective-permute-start.17 = (bf16[64,2048]{1,0:T(8,128)(2,1)S(1)}, bf16[64,2048]{1,0:T(8,128)(2,1)S(1)}, u32[]{:S(2)}, u32[]{:S(2)}) collective-permute-start(bf16[64,2048]{1,0:T(8,128)(2,1)S(1)} %collective-permute-done.16.refs_8_), channel_id=1, source_target_pairs={{0,16},{16,0},{1,17},{17,1},{2,18},{18,2},{3,19},{19,3},{4,20},{20... | collective-permute-start | bytes 786440 | tf_op jit(solution)/shard_map/ppermute | solution.py:523
  88.9 6.4 %collective-permute-start.19 = (bf16[64,2048]{1,0:T(8,128)(2,1)S(1)}, bf16[64,2048]{1,0:T(8,128)(2,1)S(1)}, u32[]{:S(2)}, u32[]{:S(2)}) collective-permute-start(bf16[64,2048]{1,0:T(8,128)(2,1)S(1)} %collective-permute-done.18.refs_9_), channel_id=1, source_target_pairs={{0,16},{16,0},{1,17},{17,1},{2,18},{18,2},{3,19},{19,3},{4,20},{20... | collective-permute-start | bytes 786440 | tf_op jit(solution)/shard_map/ppermute | solution.py:523
  90.4 5.2 %collective-permute-start.20 = (bf16[1024,128]{1,0:T(8,128)(2,1)S(1)}, bf16[1024,128]{1,0:T(8,128)(2,1)S(1)}, u32[]{:S(2)}, u32[]{:S(2)}) collective-permute-start(bf16[1024,128]{1,0:T(8,128)(2,1)S(1)} %collective-permute-done.9.refs_4_), channel_id=1, source_target_pairs={{0,1},{1,0},{2,3},{3,2},{4,5},{5,4},{6,7},{7,6},{8,9},{9,8},{10,11... | collective-permute-start | bytes 786440 | tf_op jit(solution)/shard_map/ppermute | solution.py:517
  90.4 1.6 %copy-start.3 = (bf16[512,2048]{1,0:T(8,128)(2,1)S(1)}, bf16[512,2048]{1,0:T(8,128)(2,1)}, u32[]{:S(2)}) copy-start(bf16[512,2048]{1,0:T(8,128)(2,1)} %refs_3_.1) | copy-start | bytes 6291460
  95.3 5.5 %collective-permute-start.21 = (bf16[1024,128]{1,0:T(8,128)(2,1)S(1)}, bf16[1024,128]{1,0:T(8,128)(2,1)S(1)}, u32[]{:S(2)}, u32[]{:S(2)}) collective-permute-start(bf16[1024,128]{1,0:T(8,128)(2,1)S(1)} %collective-permute-done.11.refs_5_), channel_id=1, source_target_pairs={{0,1},{1,0},{2,3},{3,2},{4,5},{5,4},{6,7},{7,6},{8,9},{9,8},{10,11... | collective-permute-start | bytes 786440 | tf_op jit(solution)/shard_map/ppermute | solution.py:517
  95.7 5.4 %collective-permute-start.22 = (bf16[1024,128]{1,0:T(8,128)(2,1)S(1)}, bf16[1024,128]{1,0:T(8,128)(2,1)S(1)}, u32[]{:S(2)}, u32[]{:S(2)}) collective-permute-start(bf16[1024,128]{1,0:T(8,128)(2,1)S(1)} %collective-permute-done.13.refs_6_), channel_id=1, source_target_pairs={{0,1},{1,0},{2,3},{3,2},{4,5},{5,4},{6,7},{7,6},{8,9},{9,8},{10,11... | collective-permute-start | bytes 786440 | tf_op jit(solution)/shard_map/ppermute | solution.py:517
  95.8 5.3 %collective-permute-start.23 = (bf16[1024,128]{1,0:T(8,128)(2,1)S(1)}, bf16[1024,128]{1,0:T(8,128)(2,1)S(1)}, u32[]{:S(2)}, u32[]{:S(2)}) collective-permute-start(bf16[1024,128]{1,0:T(8,128)(2,1)S(1)} %collective-permute-done.15.refs_7_), channel_id=1, source_target_pairs={{0,1},{1,0},{2,3},{3,2},{4,5},{5,4},{6,7},{7,6},{8,9},{9,8},{10,11... | collective-permute-start | bytes 786440 | tf_op jit(solution)/shard_map/ppermute | solution.py:517
  96.2 4.9 %collective-permute-start.24 = (bf16[64,2048]{1,0:T(8,128)(2,1)S(1)}, bf16[64,2048]{1,0:T(8,128)(2,1)S(1)}, u32[]{:S(2)}, u32[]{:S(2)}) collective-permute-start(bf16[64,2048]{1,0:T(8,128)(2,1)S(1)} %collective-permute-done.17.refs_8_), channel_id=1, source_target_pairs={{0,1},{1,0},{2,3},{3,2},{4,5},{5,4},{6,7},{7,6},{8,9},{9,8},{10,11... | collective-permute-start | bytes 786440 | tf_op jit(solution)/shard_map/ppermute | solution.py:517
  96.3 4.7 %collective-permute-start.25 = (bf16[64,2048]{1,0:T(8,128)(2,1)S(1)}, bf16[64,2048]{1,0:T(8,128)(2,1)S(1)}, u32[]{:S(2)}, u32[]{:S(2)}) collective-permute-start(bf16[64,2048]{1,0:T(8,128)(2,1)S(1)} %collective-permute-done.19.refs_9_), channel_id=1, source_target_pairs={{0,1},{1,0},{2,3},{3,2},{4,5},{5,4},{6,7},{7,6},{8,9},{9,8},{10,11... | collective-permute-start | bytes 786440 | tf_op jit(solution)/shard_map/ppermute | solution.py:517
  100.8 23.3 %copy-start.5 = (f32[2048]{0:T(1024)S(1)}, f32[2048]{0:T(1024)}, u32[]{:S(2)}) copy-start(f32[2048]{0:T(1024)} %param.18) | copy-start | bytes 24580
  100.8 49.2 %copy-start.6 = (s32[128,2]{0,1:T(2,128)S(1)}, s32[128,2]{0,1:T(2,128)}, u32[]{:S(2)}) copy-start(s32[128,2]{0,1:T(2,128)} %param.21) | copy-start | bytes 3076
  100.8 49.1 %copy-start.7 = (f32[128,2]{0,1:T(2,128)S(1)}, f32[128,2]{0,1:T(2,128)}, u32[]{:S(2)}) copy-start(f32[128,2]{0,1:T(2,128)} %param.22) | copy-start | bytes 3076
  100.9 17.3 %collective-permute-start.3 = (bf16[64,2048]{1,0:T(8,128)(2,1)S(1)}, bf16[64,2048]{1,0:T(8,128)(2,1)S(1)}, u32[]{:S(2)}, u32[]{:S(2)}) collective-permute-start(bf16[64,2048]{1,0:T(8,128)(2,1)S(1)} %get-tuple-element.23), channel_id=1, source_target_pairs={{0,1},{1,0},{2,3},{3,2},{4,5},{5,4},{6,7},{7,6},{8,9},{9,8},{10,11... | collective-permute-start | bytes 786440 | tf_op jit(solution)/shard_map/ppermute | solution.py:517
  102.8 24.3 %collective-permute-start.35 = (bf16[96,2048]{1,0:T(8,128)(2,1)S(1)}, bf16[96,2048]{1,0:T(8,128)(2,1)S(1)}, u32[]{:S(2)}, u32[]{:S(2)}) collective-permute-start(bf16[96,2048]{1,0:T(8,128)(2,1)S(1)} %get-tuple-element.37), channel_id=1, source_target_pairs={{0,12},{4,0},{8,4},{12,8},{1,13},{5,1},{9,5},{13,9},{2,14},{6,2},{... | collective-permute-start | bytes 1179656 | tf_op jit(solution)/shard_map/ppermute | solution.py:526
  117.5 32.5 %collective-permute-start.36 = (bf16[96,2048]{1,0:T(8,128)(2,1)S(1)}, bf16[96,2048]{1,0:T(8,128)(2,1)S(1)}, u32[]{:S(2)}, u32[]{:S(2)}) collective-permute-start(bf16[96,2048]{1,0:T(8,128)(2,1)S(1)} %get-tuple-element.38), channel_id=1, source_target_pairs={{0,8},{4,12},{8,0},{12,4},{1,9},{5,13},{9,1},{13,5},{2,10},{6,14},... | collective-permute-start | bytes 1179656 | tf_op jit(solution)/shard_map/ppermute | solution.py:526
  117.5 32.5 %collective-permute-start.37 = (bf16[96,2048]{1,0:T(8,128)(2,1)S(1)}, bf16[96,2048]{1,0:T(8,128)(2,1)S(1)}, u32[]{:S(2)}, u32[]{:S(2)}) collective-permute-start(bf16[96,2048]{1,0:T(8,128)(2,1)S(1)} %get-tuple-element.39), channel_id=1, source_target_pairs={{0,4},{4,8},{8,12},{12,0},{1,5},{5,9},{9,13},{13,1},{2,6},{6,10},{... | collective-permute-start | bytes 1179656 | tf_op jit(solution)/shard_map/ppermute | solution.py:526
  118.8 5.3 %collective-permute-start.4 = (bf16[32,2048]{1,0:T(8,128)(2,1)S(1)}, bf16[32,2048]{1,0:T(8,128)(2,1)S(1)}, u32[]{:S(2)}, u32[]{:S(2)}) collective-permute-start(bf16[32,2048]{1,0:T(8,128)(2,1)S(1)} %get-tuple-element.25), channel_id=1, source_target_pairs={{0,2},{1,3},{2,0},{3,1},{4,6},{5,7},{6,4},{7,5},{8,10},{9,11},{10,... | collective-permute-start | bytes 393224 | tf_op jit(solution)/shard_map/ppermute | solution.py:520

commit v2 on v1

--- a/solution.py
+++ b/solution.py
@@ -363,7 +363,9 @@
             for d in range(count):
                 some = slice(d * capacity, (d + 1) * capacity)
                 out = jnp.dot(inner[some], down, preferred_element_type=jnp.float32)
-                rest[d][...] = (out + acc_ref[some]).astype(jnp.bfloat16)
+                if carried is not None:
+                    out = out + acc_ref[some]
+                rest[d][...] = out.astype(jnp.bfloat16)
         else:
             out = jnp.dot(inner, down, preferred_element_type=jnp.float32)
             rest[0][...] = out if carried is None else out + acc_ref[...]
@@ -409,12 +411,22 @@
     pair = 2 * size
     width = out_weight.shape[1]
     share = span // quarters
-    blocks = 1 + len(passed)
+    blocks = len(passed)
     half = quarters // 2
 
     def body(place_ref, q_ref, own_ref, *refs):
-        kv_refs = (own_ref,) + refs[: len(passed)]
-        weight_ref, send_ref, keep_ref, acc, carry, att, proj = refs[len(passed) :]
+        first_ref, direct_ref, relay_ref, last_ref = refs[:blocks]
+        weight_ref, send_ref, keep_ref, acc, carry, att, proj, middle = refs[blocks:]
+        kv_refs = (own_ref, first_ref, middle, last_ref)
+
+        @pl.when(place_ref[0] == 2)
+        def _():
+            middle[...] = direct_ref[...]
+
+        @pl.when(place_ref[0] == 3)
+        def _():
+            middle[...] = relay_ref[...]
+
         row = lax.broadcasted_iota(jnp.int32, (span, span), 0)
         column = lax.broadcasted_iota(jnp.int32, (span, span), 1)
         earlier = column < row
@@ -481,6 +493,7 @@
             pltpu.VMEM((heads, span, span), jnp.float32),
             pltpu.VMEM((span, width_heads), jnp.bfloat16),
             pltpu.VMEM((span, width), jnp.float32),
+            pltpu.VMEM(own.shape, jnp.bfloat16),
         ),
         flops=4 * blocks * span * span * width_heads + 2 * span * width_heads * width,
     )(place, queries, own, *passed, out_weight)
@@ -526,7 +539,7 @@
         return lax.ppermute(array, "ep", [(i, (i + d) % blocks) for i in range(blocks)])
 
     def upward(array, d):
-        return lax.ppermute(array, "ep", [(i, i + 1) for i in range(d - 1, blocks - 1)])
+        return lax.ppermute(array, "ep", [(i, i + d) for i in range(blocks - d)])
 
     rows, top = expert_ids.shape
     capacity = 3 * rows * top // (2 * blocks)
@@ -544,9 +557,8 @@
     far_near = tuple(core(array) for array in far)
     other_near = tuple(core(array) for array in other)
 
-    passed = []
-    for d in range(1, blocks):
-        passed.append(upward(passed[-1] if passed else own, d))
+    passed = [upward(own, 1), lax.ppermute(own, "ep", [(0, 2)])]
+    passed += [lax.ppermute(array, "ep", [(2, 3)]) for array in passed]
 
     def whole(arrays):
         return [[array] for array in arrays]
@@ -554,9 +566,19 @@
     def chunked(arrays):
         return [arrays[0:2], arrays[2:4], arrays[4:6]]
 
-    summed = expert_part(arrived, [whole(mine), whole(near)], None, False)[0]
-    summed = expert_part(arrived, [chunked(far), chunked(far_near)], summed, False)[0]
-    produced = expert_part(arrived, [chunked(other), chunked(other_near)], summed, True)
+    early = [k for k in range(blocks) if k % 2 == 0]
+    late = [k for k in range(blocks) if k % 2 == 1]
+    pieces = [
+        [whole(mine), whole(near)],
+        [chunked(far), chunked(far_near)],
+        [chunked(other), chunked(other_near)],
+    ]
+    head = [arrived[k] for k in early]
+    summed = expert_part(head, pieces[0], None, False)[0]
+    summed = expert_part(head, pieces[1], summed, False)[0]
+    done = expert_part(head, pieces[2], summed, True)
+    done += expert_part([arrived[k] for k in late], pieces[0] + pieces[1] + pieces[2], None, True)
+    produced = [done[(early + late).index(k)] for k in range(blocks)]
     returned = [produced[0]] + [turn(produced[d], -d) for d in range(1, blocks)]
 
     send, kept = attend_project(place, queries, own, passed, out_weight, heads, shards)
@@ -568,7 +590,7 @@
 
 def solution(mesh):
     sizes = mesh.shape
-    paired = sizes["grp"] == 2 and sizes["tp"] == 4 and sizes["ep"] <= sizes["tp"]
+    paired = sizes["grp"] == 2 and sizes["tp"] == 4 and sizes["ep"] == sizes["tp"]
     return jax.shard_map(
         per_device if paired else per_device_wide,
         mesh=mesh,

time: 153 us -> 153 us (level)
  waiting for transfers between devices: 82.4 us -> 78.7 us
  starting transfers between devices: 52 us -> 55.3 us
    ppermute x6, waiting for transfers between devices: 38.4 us -> 31 us  [turn(): lax.ppermute(array, 'ep', [(i, (i + d) % blocks) for i in range(blocks)])]
    ppermute x16, waiting for transfers between devices: 0.04 us -> 7.44 us  [core(): return lax.ppermute(array, 'tp', [(i, i ^ 1) for i in range(shards)])]
    ppermute x3 -> x4, starting transfers between devices: 5.35 us -> 10.4 us  [the longest x1 5.02 us: paired_step(): passed = [upward(own, 1), lax.ppermute(own, 'ep', [(0, 2)])]]
    ppermute x7, waiting for transfers between devices: 18.7 us -> 16.5 us  [across(): return lax.ppermute(array, 'tp', [(i, i ^ 2) for i in range(shards)])]
    ppermute x6, waiting for transfers between devices: 25.3 us -> 23.7 us  [beside(): return lax.ppermute(array, 'grp', [(0, 1), (1, 0)])]
    pallas_call x3 -> x4, Pallas kernels: 5.8 us -> 6.52 us  [expert_part(): call(body, outs, [VMEM] * (count + len(flat) + len(extra)), flops=6 * cou...]
  transfers between devices with their start and end apart: 38 -> 39, of which waited for: 17 -> 22; matrix products, arithmetic and copies ran while one was open for 0% -> 0% of each run, Pallas kernels for 7% -> 7%
where the time goes in v2:
time: 153 us; the launch traced here: 152 us
  waiting for transfers between devices  78.7 us (51%)
  starting transfers between devices  55.3 us (36%)
  Pallas kernels  15.8 us (10%)
  local copies, waits for them, and re-layouts  1.62 us (1%)
    ppermute x6, waiting for transfers between devices, turn(): lax.ppermute(array, 'ep', [(i, (i + d) % blocks) for i in range(blocks)])  31 us
    ppermute x6, starting transfers between devices, turn(): lax.ppermute(array, 'ep', [(i, (i + d) % blocks) for i in range(blocks)])  24.7 us
    ppermute x6, waiting for transfers between devices, beside(): return lax.ppermute(array, 'grp', [(0, 1), (1, 0)])  23.7 us
    ppermute x7, waiting for transfers between devices, across(): return lax.ppermute(array, 'tp', [(i, i ^ 2) for i in range(shards)])  16.5 us
    ppermute x7, starting transfers between devices, across(): return lax.ppermute(array, 'tp', [(i, i ^ 2) for i in range(shards)])  10.7 us
    ppermute x16, waiting for transfers between devices, core(): return lax.ppermute(array, 'tp', [(i, i ^ 1) for i in range(shards)])  7.44 us
    ppermute x6, starting transfers between devices, beside(): return lax.ppermute(array, 'grp', [(0, 1), (1, 0)])  7.35 us
    pallas_call x4, Pallas kernels, expert_part(): call(body, outs, [VMEM] * (count + len(flat) + len(extra)), flops=6 * cou...  6.52 us
  transfers between devices with their start and end apart: 39, of which 22 were waited for; matrix products, arithmetic and copies ran while one was open for 0% of the time, Pallas kernels for 7%

profile of v2, /device:TPU:0, one launch (start us, length us, event | category | flops | bytes accessed | tf_op | source)
XLA Modules:
  0.0 152.4 jit_solution(5016799547829687958)
XLA Ops:
  0.6 0.1 pad_add_fusion.place_ref
  0.7 2.8 %shard_map.140 = (bf16[96,2048]{1,0:T(8,128)(2,1)S(1)}, bf16[96,2048]{1,0:T(8,128)(2,1)S(1)}, bf16[96,2048]{1,0:T(8,128)(2,1)S(1)}, bf16[96,2048]{1,0:T(8,128)(2...) custom-call(s32[4]{0:T(128)S(1)} %pad_add_fusion.place_ref, ...), custom_call_target="tpu_custom_call" | custom-call | flops 201326592 | tf_op jit(solution)/shard_map/pallas_call | solution.py:276
  3.5 3.0 %collective-permute-start.7 = (bf16[1024,128]{1,0:T(8,128)(2,1)S(1)}, bf16[1024,128]{1,0:T(8,128)(2,1)S(1)}, u32[]{:S(2)}, u32[]{:S(2)}) collective-permute-start(bf16[1024,128]{1,0:T(8,128)(2,1)S(1)} %get-tuple-element.28), channel_id=1, source_target_pairs={{0,2},{1,3},{2,0},{3,1},{4,6},{5,7},{6,4},{7,5},{8,10},{9,11},{10,... | collective-permute-start | bytes 786440 | tf_op jit(solution)/shard_map/ppermute | solution.py:533
  6.6 0.1 collective-permute-start.9
  6.6 1.9 %collective-permute-start.11 = (bf16[1024,128]{1,0:T(8,128)(2,1)S(1)}, bf16[1024,128]{1,0:T(8,128)(2,1)S(1)}, u32[]{:S(2)}, u32[]{:S(2)}) collective-permute-start(bf16[1024,128]{1,0:T(8,128)(2,1)S(1)} %get-tuple-element.30), channel_id=1, source_target_pairs={{0,2},{1,3},{2,0},{3,1},{4,6},{5,7},{6,4},{7,5},{8,10},{9,11},{10,... | collective-permute-start | bytes 786440 | tf_op jit(solution)/shard_map/ppermute | solution.py:533
  8.6 0.1 collective-permute-start.13
  8.7 1.9 %collective-permute-start.15 = (bf16[64,2048]{1,0:T(8,128)(2,1)S(1)}, bf16[64,2048]{1,0:T(8,128)(2,1)S(1)}, u32[]{:S(2)}, u32[]{:S(2)}) collective-permute-start(bf16[64,2048]{1,0:T(8,128)(2,1)S(1)} %get-tuple-element.32), channel_id=1, source_target_pairs={{0,2},{1,3},{2,0},{3,1},{4,6},{5,7},{6,4},{7,5},{8,10},{9,11},{10,... | collective-permute-start | bytes 786440 | tf_op jit(solution)/shard_map/ppermute | solution.py:533
  10.6 3.1 %collective-permute-done.7.refs_2_.refs_8_ = bf16[1024,128]{1,0:T(8,128)(2,1)S(1)} collective-permute-done((bf16[1024,128]{1,0:T(8,128)(2,1)S(1)}, bf16[1024,128]{1,0:T(8,128)(2,1)S(1)}, u32[]{:S(2)}, u32[]{:S(2)}) %collective-permute-start.7) | collective-permute-done | bytes 262176 | tf_op jit(solution)/shard_map/ppermute | solution.py:533
  13.7 4.0 %collective-permute-start = (bf16[136,1024]{1,0:T(8,128)(2,1)S(1)}, bf16[136,1024]{1,0:T(8,128)(2,1)S(1)}, u32[]{:S(2)}, u32[]{:S(2)}) collective-permute-start(bf16[136,1024]{1,0:T(8,128)(2,1)S(1)} %get-tuple-element.21.own_ref), channel_id=1, source_target_pairs={{0,4},{4,8},{8,12},{1,5},{5,9},{9,13},{2,6},{6,10},{10,14},{3,7},{... | collective-permute-start | bytes 835592 | tf_op jit(solution)/shard_map/ppermute | solution.py:542
  17.7 1.6 %collective-permute-done.9.refs_3_.refs_9_ = bf16[1024,128]{1,0:T(8,128)(2,1)S(1)} collective-permute-done((bf16[1024,128]{1,0:T(8,128)(2,1)S(1)}, bf16[1024,128]{1,0:T(8,128)(2,1)S(1)}, u32[]{:S(2)}, u32[]{:S(2)}) %collective-permute-start.9) | collective-permute-done | bytes 262176 | tf_op jit(solution)/shard_map/ppermute | solution.py:533
  19.3 2.0 %collective-permute-start.17 = (bf16[64,2048]{1,0:T(8,128)(2,1)S(1)}, bf16[64,2048]{1,0:T(8,128)(2,1)S(1)}, u32[]{:S(2)}, u32[]{:S(2)}) collective-permute-start(bf16[64,2048]{1,0:T(8,128)(2,1)S(1)} %get-tuple-element.33), channel_id=1, source_target_pairs={{0,2},{1,3},{2,0},{3,1},{4,6},{5,7},{6,4},{7,5},{8,10},{9,11},{10,... | collective-permute-start | bytes 786440 | tf_op jit(solution)/shard_map/ppermute | solution.py:533
  21.4 3.6 %collective-permute-done.11.refs_4_.refs_10_ = bf16[1024,128]{1,0:T(8,128)(2,1)S(1)} collective-permute-done((bf16[1024,128]{1,0:T(8,128)(2,1)S(1)}, bf16[1024,128]{1,0:T(8,128)(2,1)S(1)}, u32[]{:S(2)}, u32[]{:S(2)}) %collective-permute-start.11) | collective-permute-done | bytes 262176 | tf_op jit(solution)/shard_map/ppermute | solution.py:533
  25.0 5.0 %collective-permute-start.1 = (bf16[136,1024]{1,0:T(8,128)(2,1)S(1)}, bf16[136,1024]{1,0:T(8,128)(2,1)S(1)}, u32[]{:S(2)}, u32[]{:S(2)}) collective-permute-start(bf16[136,1024]{1,0:T(8,128)(2,1)S(1)} %get-tuple-element.21.own_ref), channel_id=1, source_target_pairs={{0,8},{1,9},{2,10},{3,11},{16,24},{17,25},{18,26},{19,27}} | collective-permute-start | bytes 835592 | tf_op jit(solution)/shard_map/ppermute | solution.py:560
  30.0 0.6 collective-permute-done.13.refs_5_.refs_11_
  30.6 2.1 %collective-permute-start.34 = (bf16[96,2048]{1,0:T(8,128)(2,1)S(1)}, bf16[96,2048]{1,0:T(8,128)(2,1)S(1)}, u32[]{:S(2)}, u32[]{:S(2)}) collective-permute-start(bf16[96,2048]{1,0:T(8,128)(2,1)S(1)} %get-tuple-element.35), channel_id=1, source_target_pairs={{0,4},{4,8},{8,12},{12,0},{1,5},{5,9},{9,13},{13,1},{2,6},{6,10},{... | collective-permute-start | bytes 1179656 | tf_op jit(solution)/shard_map/ppermute | solution.py:539
  32.7 3.5 %collective-permute-done.15.refs_6_.refs_12_ = bf16[64,2048]{1,0:T(8,128)(2,1)S(1)} collective-permute-done((bf16[64,2048]{1,0:T(8,128)(2,1)S(1)}, bf16[64,2048]{1,0:T(8,128)(2,1)S(1)}, u32[]{:S(2)}, u32[]{:S(2)}) %collective-permute-start.15) | collective-permute-done | bytes 262176 | tf_op jit(solution)/shard_map/ppermute | solution.py:533
  36.2 4.1 %collective-permute-start.35 = (bf16[96,2048]{1,0:T(8,128)(2,1)S(1)}, bf16[96,2048]{1,0:T(8,128)(2,1)S(1)}, u32[]{:S(2)}, u32[]{:S(2)}) collective-permute-start(bf16[96,2048]{1,0:T(8,128)(2,1)S(1)} %get-tuple-element.36), channel_id=1, source_target_pairs={{0,12},{4,0},{8,4},{12,8},{1,13},{5,1},{9,5},{13,9},{2,14},{6,2},{... | collective-permute-start | bytes 1179656 | tf_op jit(solution)/shard_map/ppermute | solution.py:539
  40.3 0.6 collective-permute-done.17.refs_7_.refs_13_
  40.9 1.8 %collective-permute-start.8 = (bf16[1024,128]{1,0:T(8,128)(2,1)S(1)}, bf16[1024,128]{1,0:T(8,128)(2,1)S(1)}, u32[]{:S(2)}, u32[]{:S(2)}) collective-permute-start(bf16[1024,128]{1,0:T(8,128)(2,1)S(1)} %collective-permute-done.7.refs_2_.refs_8_), channel_id=1, source_target_pairs={{0,16},{16,0},{1,17},{17,1},{2,18},{18,2},{3,19},{19,3},{4,20},{20... | collective-permute-start | bytes 786440 | tf_op jit(solution)/shard_map/ppermute | solution.py:536
  42.7 0.3 collective-permute-start.10
  43.0 1.8 %collective-permute-start.12 = (bf16[1024,128]{1,0:T(8,128)(2,1)S(1)}, bf16[1024,128]{1,0:T(8,128)(2,1)S(1)}, u32[]{:S(2)}, u32[]{:S(2)}) collective-permute-start(bf16[1024,128]{1,0:T(8,128)(2,1)S(1)} %collective-permute-done.11.refs_4_.refs_10_), channel_id=1, source_target_pairs={{0,16},{16,0},{1,17},{17,1},{2,18},{18,2},{3,19},{19,3},{4,20},{20... | collective-permute-start | bytes 786440 | tf_op jit(solution)/shard_map/ppermute | solution.py:536
  44.8 0.7 collective-permute-done.34.refs_0_
  45.4 1.5 %collective-permute-start.14 = (bf16[1024,128]{1,0:T(8,128)(2,1)S(1)}, bf16[1024,128]{1,0:T(8,128)(2,1)S(1)}, u32[]{:S(2)}, u32[]{:S(2)}) collective-permute-start(bf16[1024,128]{1,0:T(8,128)(2,1)S(1)} %collective-permute-done.13.refs_5_.refs_11_), channel_id=1, source_target_pairs={{0,16},{16,0},{1,17},{17,1},{2,18},{18,2},{3,19},{19,3},{4,20},{20... | collective-permute-start | bytes 786440 | tf_op jit(solution)/shard_map/ppermute | solution.py:536
  46.9 3.8 %collective-permute-done.35.refs_1_ = bf16[96,2048]{1,0:T(8,128)(2,1)S(1)} collective-permute-done((bf16[96,2048]{1,0:T(8,128)(2,1)S(1)}, bf16[96,2048]{1,0:T(8,128)(2,1)S(1)}, u32[]{:S(2)}, u32[]{:S(2)}) %collective-permute-start.35) | collective-permute-done | bytes 393248 | tf_op jit(solution)/shard_map/ppermute | solution.py:539
  50.7 1.5 collective-permute-start.16
  52.2 0.5 collective-permute-start.18
  52.8 3.0 %collective-permute-done.10.refs_3_.refs_21_ = bf16[1024,128]{1,0:T(8,128)(2,1)S(1)} collective-permute-done((bf16[1024,128]{1,0:T(8,128)(2,1)S(1)}, bf16[1024,128]{1,0:T(8,128)(2,1)S(1)}, u32[]{:S(2)}, u32[]{:S(2)}) %collective-permute-start.10) | collective-permute-done | bytes 262176 | tf_op jit(solution)/shard_map/ppermute | solution.py:536
  55.7 5.6 %collective-permute-done.12.refs_4_.refs_22_ = bf16[1024,128]{1,0:T(8,128)(2,1)S(1)} collective-permute-done((bf16[1024,128]{1,0:T(8,128)(2,1)S(1)}, bf16[1024,128]{1,0:T(8,128)(2,1)S(1)}, u32[]{:S(2)}, u32[]{:S(2)}) %collective-permute-start.12) | collective-permute-done | bytes 262176 | tf_op jit(solution)/shard_map/ppermute | solution.py:536
  61.4 5.6 %collective-permute-done.14.refs_5_.refs_23_ = bf16[1024,128]{1,0:T(8,128)(2,1)S(1)} collective-permute-done((bf16[1024,128]{1,0:T(8,128)(2,1)S(1)}, bf16[1024,128]{1,0:T(8,128)(2,1)S(1)}, u32[]{:S(2)}, u32[]{:S(2)}) %collective-permute-start.14) | collective-permute-done | bytes 262176 | tf_op jit(solution)/shard_map/ppermute | solution.py:536
  67.0 5.6 %collective-permute-done.16.refs_6_.refs_24_ = bf16[64,2048]{1,0:T(8,128)(2,1)S(1)} collective-permute-done((bf16[64,2048]{1,0:T(8,128)(2,1)S(1)}, bf16[64,2048]{1,0:T(8,128)(2,1)S(1)}, u32[]{:S(2)}, u32[]{:S(2)}) %collective-permute-start.16) | collective-permute-done | bytes 262176 | tf_op jit(solution)/shard_map/ppermute | solution.py:536
  72.6 3.9 %collective-permute-done.18.refs_7_.refs_25_ = bf16[64,2048]{1,0:T(8,128)(2,1)S(1)} collective-permute-done((bf16[64,2048]{1,0:T(8,128)(2,1)S(1)}, bf16[64,2048]{1,0:T(8,128)(2,1)S(1)}, u32[]{:S(2)}, u32[]{:S(2)}) %collective-permute-start.18) | collective-permute-done | bytes 262176 | tf_op jit(solution)/shard_map/ppermute | solution.py:536
  76.5 0.5 collective-permute-start.30
  77.0 0.7 collective-permute-start.2
  77.7 0.7 collective-permute-start.3
  78.4 0.1 collective-permute-start.31
  78.5 0.5 collective-permute-start.32
  79.0 0.1 collective-permute-start.33
  79.1 0.4 collective-permute-start.19
  79.5 0.1 collective-permute-start.20
  79.6 4.9 %collective-permute-done.19.refs_8_.refs_26_ = bf16[1024,128]{1,0:T(8,128)(2,1)S(1)} collective-permute-done((bf16[1024,128]{1,0:T(8,128)(2,1)S(1)}, bf16[1024,128]{1,0:T(8,128)(2,1)S(1)}, u32[]{:S(2)}, u32[]{:S(2)}) %collective-permute-start.19) | collective-permute-done | bytes 262176 | tf_op jit(solution)/shard_map/ppermute | solution.py:530
  84.5 0.1 collective-permute-start.21
  84.7 0.2 collective-permute-done.20.refs_9_.refs_27_
  84.9 0.1 collective-permute-start.22
  85.0 1.0 collective-permute-done.21.refs_10_.refs_28_
  86.0 0.1 collective-permute-start.23
  86.2 0.2 collective-permute-done.22.refs_11_.refs_29_
  86.4 0.1 collective-permute-start.24
  86.6 1.0 collective-permute-done.23.refs_12_.refs_30_
  87.6 11.0 %collective-permute-start.6 = (bf16[96,2048]{1,0:T(8,128)(2,1)S(1)}, bf16[96,2048]{1,0:T(8,128)(2,1)S(1)}, u32[]{:S(2)}, u32[]{:S(2)}) collective-permute-start(bf16[96,2048]{1,0:T(8,128)(2,1)S(1)} %get-tuple-element.27), channel_id=1, source_target_pairs={{0,8},{4,12},{8,0},{12,4},{1,9},{5,13},{9,1},{13,5},{2,10},{6,14},... | collective-permute-start | bytes 1179656 | tf_op jit(solution)/shard_map/ppermute | solution.py:539
  98.6 1.6 %copy-done.3 = bf16[512,2048]{1,0:T(8,128)(2,1)S(1)} copy-done((bf16[512,2048]{1,0:T(8,128)(2,1)S(1)}, bf16[512,2048]{1,0:T(8,128)(2,1)}, u32[]{:S(2)}) %copy-start.3) | copy-done | bytes 2097176
  100.2 2.9 %shard_map.141 = (bf16[64,2048]{1,0:T(8,128)(2,1)S(1)}, f32[64,2048]{1,0:T(8,128)S(1)}) custom-call(s32[4]{0:T(128)S(1)} %pad_add_fusion.place_ref, bf16[128,512]{1,0:T(8,128)(2,1)S(1)} %copy-done.4, bf16[136,1024]{1,0:T(8,128)(2,1)S(1)} %get-tuple-element.21.own_ref, bf16[136,1024]{1,0:T(8,128)(2,1)S(1)} %collective-permute-done.refs_0_, ...), custom_call_target="tpu_custom_call" | custom-call | flops 402653184 | tf_op jit(solution)/shard_map/pallas_call | solution.py:487
  103.2 3.2 %shard_map.147 = (bf16[96,2048]{1,0:T(8,128)(2,1)S(1)}, bf16[96,2048]{1,0:T(8,128)(2,1)S(1)}) custom-call(bf16[96,2048]{1,0:T(8,128)(2,1)S(1)} %collective-permute-done.34.refs_0_, bf16[96,2048]{1,0:T(8,128)(2,1)S(1)} %collective-permute-done.35.refs_1_, bf16[2048,256]{1,0:T(8,128)(2,1)S(1)} %bitcast.14, bf16[2048,256]{1,0:T(8,128)(2,1)S(1)} %bitcast.18, ...), custom_call_target="tpu_custom_call" | custom-call | flops 2415919104 | tf_op jit(solution)/shard_map/pallas_call | solution.py:379
  106.3 7.4 %collective-permute-start.36 = (bf16[96,2048]{1,0:T(8,128)(2,1)S(1)}, bf16[96,2048]{1,0:T(8,128)(2,1)S(1)}, u32[]{:S(2)}, u32[]{:S(2)}) collective-permute-start(bf16[96,2048]{1,0:T(8,128)(2,1)S(1)} %get-tuple-element.37), channel_id=1, source_target_pairs={{0,12},{4,0},{8,4},{12,8},{1,13},{5,1},{9,5},{13,9},{2,14},{6,2},{... | collective-permute-start | bytes 1179656 | tf_op jit(solution)/shard_map/ppermute | solution.py:539
  113.7 3.3 %collective-permute-done.6.refs_1_ = bf16[96,2048]{1,0:T(8,128)(2,1)S(1)} collective-permute-done((bf16[96,2048]{1,0:T(8,128)(2,1)S(1)}, bf16[96,2048]{1,0:T(8,128)(2,1)S(1)}, u32[]{:S(2)}, u32[]{:S(2)}) %collective-permute-start.6) | collective-permute-done | bytes 393248 | tf_op jit(solution)/shard_map/ppermute | solution.py:539
  117.0 1.5 shard_map.144.refs_14_
  118.5 0.9 shard_map.145.refs_14_
  119.4 1.0 shard_map.146
  120.5 0.6 shard_map.142
  121.1 1.5 %collective-permute-start.5 = (bf16[32,2048]{1,0:T(8,128)(2,1)S(1)}, bf16[32,2048]{1,0:T(8,128)(2,1)S(1)}, u32[]{:S(2)}, u32[]{:S(2)}) collective-permute-start(bf16[32,2048]{1,0:T(8,128)(2,1)S(1)} %get-tuple-element.25), channel_id=1, source_target_pairs={{0,2},{1,3},{2,0},{3,1},{4,6},{5,7},{6,4},{7,5},{8,10},{9,11},{10,... | collective-permute-start | bytes 393224 | tf_op jit(solution)/shard_map/ppermute | solution.py:533
  122.6 3.5 %collective-permute-done.5.received_ref = bf16[32,2048]{1,0:T(8,128)(2,1)S(1)} collective-permute-done((bf16[32,2048]{1,0:T(8,128)(2,1)S(1)}, bf16[32,2048]{1,0:T(8,128)(2,1)S(1)}, u32[]{:S(2)}, u32[]{:S(2)}) %collective-permute-start.5) | collective-permute-done | bytes 131104 | tf_op jit(solution)/shard_map/ppermute | solution.py:533
  126.1 0.8 shard_map.143
  126.9 6.4 %collective-permute-done.36.refs_1_ = bf16[96,2048]{1,0:T(8,128)(2,1)S(1)} collective-permute-done((bf16[96,2048]{1,0:T(8,128)(2,1)S(1)}, bf16[96,2048]{1,0:T(8,128)(2,1)S(1)}, u32[]{:S(2)}, u32[]{:S(2)}) %collective-permute-start.36) | collective-permute-done | bytes 393248 | tf_op jit(solution)/shard_map/ppermute | solution.py:539
  133.3 16.8 %collective-permute-done.37.refs_2_ = bf16[96,2048]{1,0:T(8,128)(2,1)S(1)} collective-permute-done((bf16[96,2048]{1,0:T(8,128)(2,1)S(1)}, bf16[96,2048]{1,0:T(8,128)(2,1)S(1)}, u32[]{:S(2)}, u32[]{:S(2)}) %collective-permute-start.37) | collective-permute-done | bytes 393248 | tf_op jit(solution)/shard_map/ppermute | solution.py:539
  150.2 2.3 %shard_map.148 = bf16[128,2048]{1,0:T(8,128)(2,1)} custom-call(s32[4]{0:T(128)S(1)} %pad_add_fusion.place_ref, s32[2,128]{1,0:T(2,128)S(1)} %bitcast.26, f32[2,128]{1,0:T(2,128)S(1)} %bitcast.27, bf16[96,2048]{1,0:T(8,128)(2,1)S(1)} %get-tuple-element.34.refs_0_, bf16[96,2048]{1,0:T(8,128)(2,1)S(1)} %collective-permute-done.36.refs_1_, ...), custom_call_target="tpu_custom_call" | custom-call | flops 201326592 | tf_op jit(solution)/shard_map/pallas_call | solution.py:327
  (40 shorter events, 0.2 us)
Async XLA Ops:
  0.7 77.7 %copy-start = (bf16[1,2048,256]{2,1,0:T(8,128)(2,1)S(1)}, bf16[1,2048,256]{2,1,0:T(8,128)(2,1)}, u32[]{:S(2)}) copy-start(bf16[1,2048,256]{2,1,0:T(8,128)(2,1)} %param.23) | copy-start | bytes 3145732
  0.7 77.8 %copy-start.1 = (bf16[1,2048,256]{2,1,0:T(8,128)(2,1)S(1)}, bf16[1,2048,256]{2,1,0:T(8,128)(2,1)}, u32[]{:S(2)}) copy-start(bf16[1,2048,256]{2,1,0:T(8,128)(2,1)} %param.24) | copy-start | bytes 3145732
  0.7 78.3 %copy-start.2 = (bf16[1,256,2048]{2,1,0:T(8,128)(2,1)S(1)}, bf16[1,256,2048]{2,1,0:T(8,128)(2,1)}, u32[]{:S(2)}) copy-start(bf16[1,256,2048]{2,1,0:T(8,128)(2,1)} %param.25) | copy-start | bytes 3145732
  0.7 97.8 %copy-start.4 = (bf16[128,512]{1,0:T(8,128)(2,1)S(1)}, bf16[128,512]{1,0:T(8,128)(2,1)}, u32[]{:S(2)}) copy-start(bf16[128,512]{1,0:T(8,128)(2,1)} %q_ref.1) | copy-start | bytes 393220
  3.5 10.2 %collective-permute-start.7 = (bf16[1024,128]{1,0:T(8,128)(2,1)S(1)}, bf16[1024,128]{1,0:T(8,128)(2,1)S(1)}, u32[]{:S(2)}, u32[]{:S(2)}) collective-permute-start(bf16[1024,128]{1,0:T(8,128)(2,1)S(1)} %get-tuple-element.28), channel_id=1, source_target_pairs={{0,2},{1,3},{2,0},{3,1},{4,6},{5,7},{6,4},{7,5},{8,10},{9,11},{10,... | collective-permute-start | bytes 786440 | tf_op jit(solution)/shard_map/ppermute | solution.py:533
  6.6 12.8 %collective-permute-start.9 = (bf16[1024,128]{1,0:T(8,128)(2,1)S(1)}, bf16[1024,128]{1,0:T(8,128)(2,1)S(1)}, u32[]{:S(2)}, u32[]{:S(2)}) collective-permute-start(bf16[1024,128]{1,0:T(8,128)(2,1)S(1)} %get-tuple-element.29), channel_id=1, source_target_pairs={{0,2},{1,3},{2,0},{3,1},{4,6},{5,7},{6,4},{7,5},{8,10},{9,11},{10,... | collective-permute-start | bytes 786440 | tf_op jit(solution)/shard_map/ppermute | solution.py:533
  6.6 18.3 %collective-permute-start.11 = (bf16[1024,128]{1,0:T(8,128)(2,1)S(1)}, bf16[1024,128]{1,0:T(8,128)(2,1)S(1)}, u32[]{:S(2)}, u32[]{:S(2)}) collective-permute-start(bf16[1024,128]{1,0:T(8,128)(2,1)S(1)} %get-tuple-element.30), channel_id=1, source_target_pairs={{0,2},{1,3},{2,0},{3,1},{4,6},{5,7},{6,4},{7,5},{8,10},{9,11},{10,... | collective-permute-start | bytes 786440 | tf_op jit(solution)/shard_map/ppermute | solution.py:533
  8.6 22.0 %collective-permute-start.13 = (bf16[1024,128]{1,0:T(8,128)(2,1)S(1)}, bf16[1024,128]{1,0:T(8,128)(2,1)S(1)}, u32[]{:S(2)}, u32[]{:S(2)}) collective-permute-start(bf16[1024,128]{1,0:T(8,128)(2,1)S(1)} %get-tuple-element.31), channel_id=1, source_target_pairs={{0,2},{1,3},{2,0},{3,1},{4,6},{5,7},{6,4},{7,5},{8,10},{9,11},{10,... | collective-permute-start | bytes 786440 | tf_op jit(solution)/shard_map/ppermute | solution.py:533
  8.7 27.5 %collective-permute-start.15 = (bf16[64,2048]{1,0:T(8,128)(2,1)S(1)}, bf16[64,2048]{1,0:T(8,128)(2,1)S(1)}, u32[]{:S(2)}, u32[]{:S(2)}) collective-permute-start(bf16[64,2048]{1,0:T(8,128)(2,1)S(1)} %get-tuple-element.32), channel_id=1, source_target_pairs={{0,2},{1,3},{2,0},{3,1},{4,6},{5,7},{6,4},{7,5},{8,10},{9,11},{10,... | collective-permute-start | bytes 786440 | tf_op jit(solution)/shard_map/ppermute | solution.py:533
  13.7 29.0 %collective-permute-start = (bf16[136,1024]{1,0:T(8,128)(2,1)S(1)}, bf16[136,1024]{1,0:T(8,128)(2,1)S(1)}, u32[]{:S(2)}, u32[]{:S(2)}) collective-permute-start(bf16[136,1024]{1,0:T(8,128)(2,1)S(1)} %get-tuple-element.21.own_ref), channel_id=1, source_target_pairs={{0,4},{4,8},{8,12},{1,5},{5,9},{9,13},{2,6},{6,10},{10,14},{3,7},{... | collective-permute-start | bytes 835592 | tf_op jit(solution)/shard_map/ppermute | solution.py:542
  19.3 21.6 %collective-permute-start.17 = (bf16[64,2048]{1,0:T(8,128)(2,1)S(1)}, bf16[64,2048]{1,0:T(8,128)(2,1)S(1)}, u32[]{:S(2)}, u32[]{:S(2)}) collective-permute-start(bf16[64,2048]{1,0:T(8,128)(2,1)S(1)} %get-tuple-element.33), channel_id=1, source_target_pairs={{0,2},{1,3},{2,0},{3,1},{4,6},{5,7},{6,4},{7,5},{8,10},{9,11},{10,... | collective-permute-start | bytes 786440 | tf_op jit(solution)/shard_map/ppermute | solution.py:533
  25.0 18.0 %collective-permute-start.1 = (bf16[136,1024]{1,0:T(8,128)(2,1)S(1)}, bf16[136,1024]{1,0:T(8,128)(2,1)S(1)}, u32[]{:S(2)}, u32[]{:S(2)}) collective-permute-start(bf16[136,1024]{1,0:T(8,128)(2,1)S(1)} %get-tuple-element.21.own_ref), channel_id=1, source_target_pairs={{0,8},{1,9},{2,10},{3,11},{16,24},{17,25},{18,26},{19,27}} | collective-permute-start | bytes 835592 | tf_op jit(solution)/shard_map/ppermute | solution.py:560
  30.6 14.8 %collective-permute-start.34 = (bf16[96,2048]{1,0:T(8,128)(2,1)S(1)}, bf16[96,2048]{1,0:T(8,128)(2,1)S(1)}, u32[]{:S(2)}, u32[]{:S(2)}) collective-permute-start(bf16[96,2048]{1,0:T(8,128)(2,1)S(1)} %get-tuple-element.35), channel_id=1, source_target_pairs={{0,4},{4,8},{8,12},{12,0},{1,5},{5,9},{9,13},{13,1},{2,6},{6,10},{... | collective-permute-start | bytes 1179656 | tf_op jit(solution)/shard_map/ppermute | solution.py:539
  36.2 14.5 %collective-permute-start.35 = (bf16[96,2048]{1,0:T(8,128)(2,1)S(1)}, bf16[96,2048]{1,0:T(8,128)(2,1)S(1)}, u32[]{:S(2)}, u32[]{:S(2)}) collective-permute-start(bf16[96,2048]{1,0:T(8,128)(2,1)S(1)} %get-tuple-element.36), channel_id=1, source_target_pairs={{0,12},{4,0},{8,4},{12,8},{1,13},{5,1},{9,5},{13,9},{2,14},{6,2},{... | collective-permute-start | bytes 1179656 | tf_op jit(solution)/shard_map/ppermute | solution.py:539
  40.9 11.3 %collective-permute-start.8 = (bf16[1024,128]{1,0:T(8,128)(2,1)S(1)}, bf16[1024,128]{1,0:T(8,128)(2,1)S(1)}, u32[]{:S(2)}, u32[]{:S(2)}) collective-permute-start(bf16[1024,128]{1,0:T(8,128)(2,1)S(1)} %collective-permute-done.7.refs_2_.refs_8_), channel_id=1, source_target_pairs={{0,16},{16,0},{1,17},{17,1},{2,18},{18,2},{3,19},{19,3},{4,20},{20... | collective-permute-start | bytes 786440 | tf_op jit(solution)/shard_map/ppermute | solution.py:536
  42.7 13.0 %collective-permute-start.10 = (bf16[1024,128]{1,0:T(8,128)(2,1)S(1)}, bf16[1024,128]{1,0:T(8,128)(2,1)S(1)}, u32[]{:S(2)}, u32[]{:S(2)}) collective-permute-start(bf16[1024,128]{1,0:T(8,128)(2,1)S(1)} %collective-permute-done.9.refs_3_.refs_9_), channel_id=1, source_target_pairs={{0,16},{16,0},{1,17},{17,1},{2,18},{18,2},{3,19},{19,3},{4,20},{20... | collective-permute-start | bytes 786440 | tf_op jit(solution)/shard_map/ppermute | solution.py:536
  43.0 18.4 %collective-permute-start.12 = (bf16[1024,128]{1,0:T(8,128)(2,1)S(1)}, bf16[1024,128]{1,0:T(8,128)(2,1)S(1)}, u32[]{:S(2)}, u32[]{:S(2)}) collective-permute-start(bf16[1024,128]{1,0:T(8,128)(2,1)S(1)} %collective-permute-done.11.refs_4_.refs_10_), channel_id=1, source_target_pairs={{0,16},{16,0},{1,17},{17,1},{2,18},{18,2},{3,19},{19,3},{4,20},{20... | collective-permute-start | bytes 786440 | tf_op jit(solution)/shard_map/ppermute | solution.py:536
  45.4 21.6 %collective-permute-start.14 = (bf16[1024,128]{1,0:T(8,128)(2,1)S(1)}, bf16[1024,128]{1,0:T(8,128)(2,1)S(1)}, u32[]{:S(2)}, u32[]{:S(2)}) collective-permute-start(bf16[1024,128]{1,0:T(8,128)(2,1)S(1)} %collective-permute-done.13.refs_5_.refs_11_), channel_id=1, source_target_pairs={{0,16},{16,0},{1,17},{17,1},{2,18},{18,2},{3,19},{19,3},{4,20},{20... | collective-permute-start | bytes 786440 | tf_op jit(solution)/shard_map/ppermute | solution.py:536
  50.7 21.9 %collective-permute-start.16 = (bf16[64,2048]{1,0:T(8,128)(2,1)S(1)}, bf16[64,2048]{1,0:T(8,128)(2,1)S(1)}, u32[]{:S(2)}, u32[]{:S(2)}) collective-permute-start(bf16[64,2048]{1,0:T(8,128)(2,1)S(1)} %collective-permute-done.15.refs_6_.refs_12_), channel_id=1, source_target_pairs={{0,16},{16,0},{1,17},{17,1},{2,18},{18,2},{3,19},{19,3},{4,20},{20... | collective-permute-start | bytes 786440 | tf_op jit(solution)/shard_map/ppermute | solution.py:536
  52.2 24.3 %collective-permute-start.18 = (bf16[64,2048]{1,0:T(8,128)(2,1)S(1)}, bf16[64,2048]{1,0:T(8,128)(2,1)S(1)}, u32[]{:S(2)}, u32[]{:S(2)}) collective-permute-start(bf16[64,2048]{1,0:T(8,128)(2,1)S(1)} %collective-permute-done.17.refs_7_.refs_13_), channel_id=1, source_target_pairs={{0,16},{16,0},{1,17},{17,1},{2,18},{18,2},{3,19},{19,3},{4,20},{20... | collective-permute-start | bytes 786440 | tf_op jit(solution)/shard_map/ppermute | solution.py:536
  55.7 20.8 %collective-permute-start.25 = (bf16[1024,128]{1,0:T(8,128)(2,1)S(1)}, bf16[1024,128]{1,0:T(8,128)(2,1)S(1)}, u32[]{:S(2)}, u32[]{:S(2)}) collective-permute-start(bf16[1024,128]{1,0:T(8,128)(2,1)S(1)} %collective-permute-done.7.refs_2_.refs_8_), channel_id=1, source_target_pairs={{0,1},{1,0},{2,3},{3,2},{4,5},{5,4},{6,7},{7,6},{8,9},{9,8},{10,11... | collective-permute-start | bytes 786440 | tf_op jit(solution)/shard_map/ppermute | solution.py:530
  61.4 15.7 %collective-permute-start.26 = (bf16[1024,128]{1,0:T(8,128)(2,1)S(1)}, bf16[1024,128]{1,0:T(8,128)(2,1)S(1)}, u32[]{:S(2)}, u32[]{:S(2)}) collective-permute-start(bf16[1024,128]{1,0:T(8,128)(2,1)S(1)} %collective-permute-done.9.refs_3_.refs_9_), channel_id=1, source_target_pairs={{0,1},{1,0},{2,3},{3,2},{4,5},{5,4},{6,7},{7,6},{8,9},{9,8},{10,11... | collective-permute-start | bytes 786440 | tf_op jit(solution)/shard_map/ppermute | solution.py:530
  67.0 10.7 %collective-permute-start.27 = (bf16[1024,128]{1,0:T(8,128)(2,1)S(1)}, bf16[1024,128]{1,0:T(8,128)(2,1)S(1)}, u32[]{:S(2)}, u32[]{:S(2)}) collective-permute-start(bf16[1024,128]{1,0:T(8,128)(2,1)S(1)} %collective-permute-done.11.refs_4_.refs_10_), channel_id=1, source_target_pairs={{0,1},{1,0},{2,3},{3,2},{4,5},{5,4},{6,7},{7,6},{8,9},{9,8},{10,11... | collective-permute-start | bytes 786440 | tf_op jit(solution)/shard_map/ppermute | solution.py:530
  72.6 5.8 %collective-permute-start.28 = (bf16[1024,128]{1,0:T(8,128)(2,1)S(1)}, bf16[1024,128]{1,0:T(8,128)(2,1)S(1)}, u32[]{:S(2)}, u32[]{:S(2)}) collective-permute-start(bf16[1024,128]{1,0:T(8,128)(2,1)S(1)} %collective-permute-done.13.refs_5_.refs_11_), channel_id=1, source_target_pairs={{0,1},{1,0},{2,3},{3,2},{4,5},{5,4},{6,7},{7,6},{8,9},{9,8},{10,11... | collective-permute-start | bytes 786440 | tf_op jit(solution)/shard_map/ppermute | solution.py:530
  76.5 2.0 %collective-permute-start.29 = (bf16[64,2048]{1,0:T(8,128)(2,1)S(1)}, bf16[64,2048]{1,0:T(8,128)(2,1)S(1)}, u32[]{:S(2)}, u32[]{:S(2)}) collective-permute-start(bf16[64,2048]{1,0:T(8,128)(2,1)S(1)} %collective-permute-done.15.refs_6_.refs_12_), channel_id=1, source_target_pairs={{0,1},{1,0},{2,3},{3,2},{4,5},{5,4},{6,7},{7,6},{8,9},{9,8},{10,11... | collective-permute-start | bytes 786440 | tf_op jit(solution)/shard_map/ppermute | solution.py:530
  76.5 2.5 %collective-permute-start.30 = (bf16[64,2048]{1,0:T(8,128)(2,1)S(1)}, bf16[64,2048]{1,0:T(8,128)(2,1)S(1)}, u32[]{:S(2)}, u32[]{:S(2)}) collective-permute-start(bf16[64,2048]{1,0:T(8,128)(2,1)S(1)} %collective-permute-done.17.refs_7_.refs_13_), channel_id=1, source_target_pairs={{0,1},{1,0},{2,3},{3,2},{4,5},{5,4},{6,7},{7,6},{8,9},{9,8},{10,11... | collective-permute-start | bytes 786440 | tf_op jit(solution)/shard_map/ppermute | solution.py:530
  77.0 2.1 %collective-permute-start.2 = (bf16[136,1024]{1,0:T(8,128)(2,1)S(1)}, bf16[136,1024]{1,0:T(8,128)(2,1)S(1)}, u32[]{:S(2)}, u32[]{:S(2)}) collective-permute-start(bf16[136,1024]{1,0:T(8,128)(2,1)S(1)} %collective-permute-done.refs_0_), channel_id=1, source_target_pairs={{8,12},{9,13},{10,14},{11,15},{24,28},{25,29},{26,30},{27,31}} | collective-permute-start | bytes 835592 | tf_op jit(solution)/shard_map/ppermute | solution.py:561
  77.7 1.8 %collective-permute-start.3 = (bf16[136,1024]{1,0:T(8,128)(2,1)S(1)}, bf16[136,1024]{1,0:T(8,128)(2,1)S(1)}, u32[]{:S(2)}, u32[]{:S(2)}) collective-permute-start(bf16[136,1024]{1,0:T(8,128)(2,1)S(1)} %collective-permute-done.1.refs_1_), channel_id=1, source_target_pairs={{8,12},{9,13},{10,14},{11,15},{24,28},{25,29},{26,30},{27,31}} | collective-permute-start | bytes 835592 | tf_op jit(solution)/shard_map/ppermute | solution.py:561
  78.4 24.7 %collective-permute-start.31 = (bf16[2048,256]{1,0:T(8,128)(2,1)S(1)}, bf16[2048,256]{1,0:T(8,128)(2,1)S(1)}, u32[]{:S(2)}, u32[]{:S(2)}) collective-permute-start(bf16[2048,256]{1,0:T(8,128)(2,1)S(1)} %bitcast.13), channel_id=1, source_target_pairs={{0,1},{1,0},{2,3},{3,2},{4,5},{5,4},{6,7},{7,6},{8,9},{9,8},{10,11... | collective-permute-start | bytes 3145736 | tf_op jit(solution)/shard_map/ppermute | solution.py:530
  78.5 24.6 %collective-permute-start.32 = (bf16[2048,256]{1,0:T(8,128)(2,1)S(1)}, bf16[2048,256]{1,0:T(8,128)(2,1)S(1)}, u32[]{:S(2)}, u32[]{:S(2)}) collective-permute-start(bf16[2048,256]{1,0:T(8,128)(2,1)S(1)} %bitcast.17), channel_id=1, source_target_pairs={{0,1},{1,0},{2,3},{3,2},{4,5},{5,4},{6,7},{7,6},{8,9},{9,8},{10,11... | collective-permute-start | bytes 3145736 | tf_op jit(solution)/shard_map/ppermute | solution.py:530
  79.0 24.1 %collective-permute-start.33 = (bf16[256,2048]{1,0:T(8,128)(2,1)S(1)}, bf16[256,2048]{1,0:T(8,128)(2,1)S(1)}, u32[]{:S(2)}, u32[]{:S(2)}) collective-permute-start(bf16[256,2048]{1,0:T(8,128)(2,1)S(1)} %bitcast.21), channel_id=1, source_target_pairs={{0,1},{1,0},{2,3},{3,2},{4,5},{5,4},{6,7},{7,6},{8,9},{9,8},{10,11... | collective-permute-start | bytes 3145736 | tf_op jit(solution)/shard_map/ppermute | solution.py:530
  79.1 5.4 %collective-permute-start.19 = (bf16[1024,128]{1,0:T(8,128)(2,1)S(1)}, bf16[1024,128]{1,0:T(8,128)(2,1)S(1)}, u32[]{:S(2)}, u32[]{:S(2)}) collective-permute-start(bf16[1024,128]{1,0:T(8,128)(2,1)S(1)} %collective-permute-done.8.refs_2_.refs_20_), channel_id=1, source_target_pairs={{0,1},{1,0},{2,3},{3,2},{4,5},{5,4},{6,7},{7,6},{8,9},{9,8},{10,11... | collective-permute-start | bytes 786440 | tf_op jit(solution)/shard_map/ppermute | solution.py:530
  79.5 5.4 %collective-permute-start.20 = (bf16[1024,128]{1,0:T(8,128)(2,1)S(1)}, bf16[1024,128]{1,0:T(8,128)(2,1)S(1)}, u32[]{:S(2)}, u32[]{:S(2)}) collective-permute-start(bf16[1024,128]{1,0:T(8,128)(2,1)S(1)} %collective-permute-done.10.refs_3_.refs_21_), channel_id=1, source_target_pairs={{0,1},{1,0},{2,3},{3,2},{4,5},{5,4},{6,7},{7,6},{8,9},{9,8},{10,11... | collective-permute-start | bytes 786440 | tf_op jit(solution)/shard_map/ppermute | solution.py:530
  84.5 1.5 %collective-permute-start.21 = (bf16[1024,128]{1,0:T(8,128)(2,1)S(1)}, bf16[1024,128]{1,0:T(8,128)(2,1)S(1)}, u32[]{:S(2)}, u32[]{:S(2)}) collective-permute-start(bf16[1024,128]{1,0:T(8,128)(2,1)S(1)} %collective-permute-done.12.refs_4_.refs_22_), channel_id=1, source_target_pairs={{0,1},{1,0},{2,3},{3,2},{4,5},{5,4},{6,7},{7,6},{8,9},{9,8},{10,11... | collective-permute-start | bytes 786440 | tf_op jit(solution)/shard_map/ppermute | solution.py:530
  84.9 1.5 %collective-permute-start.22 = (bf16[1024,128]{1,0:T(8,128)(2,1)S(1)}, bf16[1024,128]{1,0:T(8,128)(2,1)S(1)}, u32[]{:S(2)}, u32[]{:S(2)}) collective-permute-start(bf16[1024,128]{1,0:T(8,128)(2,1)S(1)} %collective-permute-done.14.refs_5_.refs_23_), channel_id=1, source_target_pairs={{0,1},{1,0},{2,3},{3,2},{4,5},{5,4},{6,7},{7,6},{8,9},{9,8},{10,11... | collective-permute-start | bytes 786440 | tf_op jit(solution)/shard_map/ppermute | solution.py:530
  86.0 1.5 %collective-permute-start.23 = (bf16[64,2048]{1,0:T(8,128)(2,1)S(1)}, bf16[64,2048]{1,0:T(8,128)(2,1)S(1)}, u32[]{:S(2)}, u32[]{:S(2)}) collective-permute-start(bf16[64,2048]{1,0:T(8,128)(2,1)S(1)} %collective-permute-done.16.refs_6_.refs_24_), channel_id=1, source_target_pairs={{0,1},{1,0},{2,3},{3,2},{4,5},{5,4},{6,7},{7,6},{8,9},{9,8},{10,11... | collective-permute-start | bytes 786440 | tf_op jit(solution)/shard_map/ppermute | solution.py:530
  86.4 16.6 %collective-permute-start.24 = (bf16[64,2048]{1,0:T(8,128)(2,1)S(1)}, bf16[64,2048]{1,0:T(8,128)(2,1)S(1)}, u32[]{:S(2)}, u32[]{:S(2)}) collective-permute-start(bf16[64,2048]{1,0:T(8,128)(2,1)S(1)} %collective-permute-done.18.refs_7_.refs_25_), channel_id=1, source_target_pairs={{0,1},{1,0},{2,3},{3,2},{4,5},{5,4},{6,7},{7,6},{8,9},{9,8},{10,11... | collective-permute-start | bytes 786440 | tf_op jit(solution)/shard_map/ppermute | solution.py:530
  87.6 29.4 %collective-permute-start.6 = (bf16[96,2048]{1,0:T(8,128)(2,1)S(1)}, bf16[96,2048]{1,0:T(8,128)(2,1)S(1)}, u32[]{:S(2)}, u32[]{:S(2)}) collective-permute-start(bf16[96,2048]{1,0:T(8,128)(2,1)S(1)} %get-tuple-element.27), channel_id=1, source_target_pairs={{0,8},{4,12},{8,0},{12,4},{1,9},{5,13},{9,1},{13,5},{2,10},{6,14},... | collective-permute-start | bytes 1179656 | tf_op jit(solution)/shard_map/ppermute | solution.py:539
  98.6 1.6 %copy-start.3 = (bf16[512,2048]{1,0:T(8,128)(2,1)S(1)}, bf16[512,2048]{1,0:T(8,128)(2,1)}, u32[]{:S(2)}) copy-start(bf16[512,2048]{1,0:T(8,128)(2,1)} %refs_4_.1) | copy-start | bytes 6291460
  103.0 17.4 %collective-permute-start.4 = (bf16[64,2048]{1,0:T(8,128)(2,1)S(1)}, bf16[64,2048]{1,0:T(8,128)(2,1)S(1)}, u32[]{:S(2)}, u32[]{:S(2)}) collective-permute-start(bf16[64,2048]{1,0:T(8,128)(2,1)S(1)} %get-tuple-element.23), channel_id=1, source_target_pairs={{0,1},{1,0},{2,3},{3,2},{4,5},{5,4},{6,7},{7,6},{8,9},{9,8},{10,11... | collective-permute-start | bytes 786440 | tf_op jit(solution)/shard_map/ppermute | solution.py:530
  106.3 27.0 %collective-permute-start.36 = (bf16[96,2048]{1,0:T(8,128)(2,1)S(1)}, bf16[96,2048]{1,0:T(8,128)(2,1)S(1)}, u32[]{:S(2)}, u32[]{:S(2)}) collective-permute-start(bf16[96,2048]{1,0:T(8,128)(2,1)S(1)} %get-tuple-element.37), channel_id=1, source_target_pairs={{0,12},{4,0},{8,4},{12,8},{1,13},{5,1},{9,5},{13,9},{2,14},{6,2},{... | collective-permute-start | bytes 1179656 | tf_op jit(solution)/shard_map/ppermute | solution.py:539
  113.7 19.6 %collective-permute-start.38 = (bf16[96,2048]{1,0:T(8,128)(2,1)S(1)}, bf16[96,2048]{1,0:T(8,128)(2,1)S(1)}, u32[]{:S(2)}, u32[]{:S(2)}) collective-permute-start(bf16[96,2048]{1,0:T(8,128)(2,1)S(1)} %get-tuple-element.39), channel_id=1, source_target_pairs={{0,4},{4,8},{8,12},{12,0},{1,5},{5,9},{9,13},{13,1},{2,6},{6,10},{... | collective-permute-start | bytes 1179656 | tf_op jit(solution)/shard_map/ppermute | solution.py:539
  119.4 6.8 %copy-start.5 = (f32[2048]{0:T(1024)S(1)}, f32[2048]{0:T(1024)}, u32[]{:S(2)}) copy-start(f32[2048]{0:T(1024)} %param.18) | copy-start | bytes 24580
  119.4 30.8 %copy-start.6 = (s32[128,2]{0,1:T(2,128)S(1)}, s32[128,2]{0,1:T(2,128)}, u32[]{:S(2)}) copy-start(s32[128,2]{0,1:T(2,128)} %param.21) | copy-start | bytes 3076
  119.4 30.8 %copy-start.7 = (f32[128,2]{0,1:T(2,128)S(1)}, f32[128,2]{0,1:T(2,128)}, u32[]{:S(2)}) copy-start(f32[128,2]{0,1:T(2,128)} %param.22) | copy-start | bytes 3076
  120.4 29.7 %collective-permute-start.37 = (bf16[96,2048]{1,0:T(8,128)(2,1)S(1)}, bf16[96,2048]{1,0:T(8,128)(2,1)S(1)}, u32[]{:S(2)}, u32[]{:S(2)}) collective-permute-start(bf16[96,2048]{1,0:T(8,128)(2,1)S(1)} %get-tuple-element.38), channel_id=1, source_target_pairs={{0,8},{4,12},{8,0},{12,4},{1,9},{5,13},{9,1},{13,5},{2,10},{6,14},... | collective-permute-start | bytes 1179656 | tf_op jit(solution)/shard_map/ppermute | solution.py:539
  121.1 5.0 %collective-permute-start.5 = (bf16[32,2048]{1,0:T(8,128)(2,1)S(1)}, bf16[32,2048]{1,0:T(8,128)(2,1)S(1)}, u32[]{:S(2)}, u32[]{:S(2)}) collective-permute-start(bf16[32,2048]{1,0:T(8,128)(2,1)S(1)} %get-tuple-element.25), channel_id=1, source_target_pairs={{0,2},{1,3},{2,0},{3,1},{4,6},{5,7},{6,4},{7,5},{8,10},{9,11},{10,... | collective-permute-start | bytes 393224 | tf_op jit(solution)/shard_map/ppermute | solution.py:533

commit v3 on v2

--- a/solution.py
+++ b/solution.py
@@ -221,13 +221,15 @@
     part = gate.shape[1] // 2
     deep = gate.shape[0] // 2
     thin = part // 2
+    slim = part // 4
 
     def body(place_ref, gain_hbm, ids_hbm, bias_hbm, input_hbm, keys_hbm, values_hbm, *refs):
         gate_hbm, up_hbm, down_hbm = refs[:3]
         outs = refs[3 : 3 + experts]
-        own_ref, gate_a, gate_b, up_a, up_b, down_a, down_b = refs[3 + experts : 10 + experts]
-        input_v, gain_v, ids_v, bias_v, sems = refs[10 + experts :]
+        own_ref, gate_a, gate_b, up_a, up_b, down_a, down_b, down_c = refs[3 + experts : 11 + experts]
+        input_v, gain_v, ids_v, bias_v, sems = refs[11 + experts :]
         begin = pl.multiple_of(place_ref[2] * part, part)
+        beyond = pl.multiple_of((1 - place_ref[2]) * part, part)
         columns = pl.ds(begin, part)
         moves = [
             (ids_hbm, ids_v),
@@ -241,7 +243,9 @@
             (up_hbm.at[pl.ds(0, deep), columns], up_a),
             (up_hbm.at[pl.ds(deep, deep), columns], up_b),
             (down_hbm.at[pl.ds(begin, thin), :], down_a),
-            (down_hbm.at[pl.ds(pl.multiple_of(begin + thin, thin), thin), :], down_b),
+            (down_hbm.at[pl.ds(pl.multiple_of(begin + thin, slim), slim), :], down_b),
+            (down_hbm.at[pl.ds(pl.multiple_of(begin + 3 * slim, slim), slim), :], down_c.at[pl.ds(0, slim), :]),
+            (down_hbm.at[pl.ds(pl.multiple_of(beyond + 3 * slim, slim), slim), :], down_c.at[pl.ds(slim, slim), :]),
         ]
         copies = [
             pltpu.make_async_copy(source, target, sems.at[k])
@@ -271,6 +275,7 @@
         shape_of((deep, part)),
         shape_of((deep, part)),
         shape_of((thin, width)),
+        shape_of((slim, width)),
         shape_of((thin, width)),
     ]
     return call(
@@ -282,7 +287,7 @@
             pltpu.VMEM((1, width), jnp.float32),
             pltpu.VMEM(ids.shape, jnp.int32),
             pltpu.VMEM(bias.shape, jnp.bfloat16),
-            pltpu.SemaphoreType.DMA((12,)),
+            pltpu.SemaphoreType.DMA((14,)),
         ),
         flops=2 * experts * capacity * rows * width,
     )(
@@ -304,51 +309,63 @@
     )
 
 
-def combine_rows(place, ids, scores, returned):
+def combine_plan(place, ids, scores, experts, capacity):
     rows = ids.shape[1]
-    experts = len(returned)
-    capacity, width = returned[0].shape
-
-    def body(place_ref, ids_ref, scores_ref, *refs):
+
+    def body(place_ref, ids_ref, scores_ref, high_ref, low_ref):
         hits, picks = selections(place_ref, ids_ref, experts, capacity)
         shares = scores_ref[...]
         shares = shares / jnp.sum(shares, axis=0, keepdims=True)
         weight = jnp.zeros((8, rows), jnp.float32)
         for k, hit in enumerate(hits):
             weight = weight + jnp.where(hit, shares[k : k + 1, :], 0.0)
-        weight = weight.T
-        total = jnp.zeros((rows, width), jnp.float32)
         for d in range(experts):
-            total = total + weight[:, d : d + 1] * lax.dot_general(
-                picks[d], refs[d][...], (((0,), (0,)), ((), ())), preferred_element_type=jnp.float32
-            )
-        refs[-1][...] = total.astype(jnp.bfloat16)
+            exact = picks[d].astype(jnp.float32) * weight[d : d + 1, :]
+            high = exact.astype(jnp.bfloat16)
+            some = slice(d * capacity, (d + 1) * capacity)
+            high_ref[some, :] = high
+            low_ref[some, :] = (exact - high.astype(jnp.float32)).astype(jnp.bfloat16)
+
+    outs = [shape_of((experts * capacity, rows))] * 2
+    return call(body, outs, [SMEM, VMEM, VMEM])(place, ids, scores)
+
+
+def combine_rows(high, low, returned):
+    rows = high.shape[1]
+    width = returned[0].shape[1]
+
+    def body(high_ref, low_ref, *refs):
+        outputs = jnp.concatenate([ref[...] for ref in refs[:-1]], axis=0)
+        weights = jnp.concatenate([high_ref[...], low_ref[...]], axis=1)
+        total = lax.dot_general(
+            weights, outputs, (((0,), (0,)), ((), ())), preferred_element_type=jnp.float32
+        )
+        refs[-1][...] = (total[:rows] + total[rows:]).astype(jnp.bfloat16)
 
     return call(
-        body, shape_of((rows, width)), [SMEM, VMEM, VMEM] + [VMEM] * experts,
-        flops=2 * experts * capacity * rows * width,
-    )(place, ids, scores, *returned)
-
-
-def expert_part(rows_in, pieces, carried, last):
+        body, shape_of((rows, width)), [VMEM] * (2 + len(returned)),
+        flops=4 * high.shape[0] * rows * width,
+    )(high, low, *returned)
+
+
+def expert_rows(rows_in, pieces):
     capacity, width = rows_in[0].shape
     count = len(rows_in)
-    hidden = sum(piece[0][0].shape[1] for piece in pieces)
-    flat = [array for piece in pieces for kind in piece for array in kind]
+    hidden = sum(piece[0][0][0].shape[1] for piece in pieces)
+    flat = [chunk[0] for piece in pieces for kind in piece for chunk in kind]
 
     def body(*refs):
-        row_refs = refs[:count]
         weight_refs = refs[count : count + len(flat)]
-        rest = refs[count + len(flat) :]
-        if carried is not None:
-            acc_ref, rest = rest[0], rest[1:]
-        rows = jnp.concatenate([ref[...] for ref in row_refs], axis=0)
+        outs = refs[count + len(flat) :]
+        rows = jnp.concatenate([ref[...] for ref in refs[:count]], axis=0)
         inner, down = [], []
         at = 0
         for piece in pieces:
             kinds = []
             for kind in piece:
-                chunk = [ref[...] for ref in weight_refs[at : at + len(kind)]]
+                chunk = [
+                    weight_refs[at + k][low:high, :] for k, (_, low, high) in enumerate(kind)
+                ]
                 kinds.append(chunk[0] if len(chunk) == 1 else jnp.concatenate(chunk, axis=0))
                 at += len(kind)
             size = kinds[0].shape[1]
@@ -358,30 +375,16 @@
             gate, upward = product[:, :size], product[:, size:]
             inner.append((gate / (1.0 + jnp.exp(-gate)) * upward).astype(jnp.bfloat16))
         inner = jnp.concatenate(inner, axis=1)
-        down = jnp.concatenate(down, axis=0)
-        if last:
-            for d in range(count):
-                some = slice(d * capacity, (d + 1) * capacity)
-                out = jnp.dot(inner[some], down, preferred_element_type=jnp.float32)
-                if carried is not None:
-                    out = out + acc_ref[some]
-                rest[d][...] = out.astype(jnp.bfloat16)
-        else:
-            out = jnp.dot(inner, down, preferred_element_type=jnp.float32)
-            rest[0][...] = out if carried is None else out + acc_ref[...]
-
-    outs = (
-        [shape_of((capacity, width))] * count
-        if last
-        else [shape_of((count * capacity, width), jnp.float32)]
-    )
-    extra = [] if carried is None else [carried]
+        out = jnp.dot(inner, jnp.concatenate(down, axis=0), preferred_element_type=jnp.float32)
+        for d in range(count):
+            outs[d][...] = out[d * capacity : (d + 1) * capacity].astype(jnp.bfloat16)
+
     return call(
         body,
-        outs,
-        [VMEM] * (count + len(flat) + len(extra)),
+        [shape_of((capacity, width))] * count,
+        [VMEM] * (count + len(flat)),
         flops=6 * count * capacity * width * hidden,
-    )(*rows_in, *flat, *extra)
+    )(*rows_in, *flat)
 
 
 def pair_sum(place, kept, received):
@@ -402,7 +405,9 @@
         projected = inner_ref[...] + received_ref[...].astype(jnp.float32)
         out_ref[...] = norm_rows(projected, gain_ref[...]).astype(jnp.bfloat16)
 
-    return call(body, shape_of(inner.shape), [VMEM] * 3)(inner, received, gain.reshape(1, -1))
+    return call(body, shape_of(inner.shape), [VMEM] * 3)(
+        inner, received, gain.reshape(1, -1)
+    )
 
 
 def attend_project(place, queries, own, passed, out_weight, heads, quarters):
@@ -553,38 +558,44 @@
 
     far = tuple(across(array) for array in halves)
     near = tuple(core(array) for array in mine)
-    other = tuple(beside(array) for array in far)
+    other = tuple(beside(array) for array in far[:-1])
     far_near = tuple(core(array) for array in far)
     other_near = tuple(core(array) for array in other)
 
     passed = [upward(own, 1), lax.ppermute(own, "ep", [(0, 2)])]
     passed += [lax.ppermute(array, "ep", [(2, 3)]) for array in passed]
 
+    def chunk(array, low=0, high=None):
+        return (array, low, array.shape[0] if high is None else high)
+
     def whole(arrays):
-        return [[array] for array in arrays]
-
-    def chunked(arrays):
-        return [arrays[0:2], arrays[2:4], arrays[4:6]]
-
-    early = [k for k in range(blocks) if k % 2 == 0]
-    late = [k for k in range(blocks) if k % 2 == 1]
+        return [[chunk(array)] for array in arrays]
+
+    def chunked(arrays, last, which):
+        slim = last.shape[0] // 2
+        kinds = [[chunk(array) for array in some] for some in (arrays[0:2], arrays[2:4], arrays[4:6])]
+        kinds[2].append(chunk(last, which * slim, (which + 1) * slim))
+        return kinds
+
     pieces = [
-        [whole(mine), whole(near)],
-        [chunked(far), chunked(far_near)],
-        [chunked(other), chunked(other_near)],
+        whole(mine),
+        whole(near),
+        chunked(far, far[6], 0),
+        chunked(far_near, far_near[6], 0),
+        chunked(other, far[6], 1),
+        chunked(other_near, far_near[6], 1),
     ]
-    head = [arrived[k] for k in early]
-    summed = expert_part(head, pieces[0], None, False)[0]
-    summed = expert_part(head, pieces[1], summed, False)[0]
-    done = expert_part(head, pieces[2], summed, True)
-    done += expert_part([arrived[k] for k in late], pieces[0] + pieces[1] + pieces[2], None, True)
-    produced = [done[(early + late).index(k)] for k in range(blocks)]
+    order = (2, 0, 1, 3)
+    done = expert_rows([arrived[k] for k in order[:1]], pieces)
+    done += expert_rows([arrived[k] for k in order[1:]], pieces)
+    produced = [done[order.index(k)] for k in range(blocks)]
     returned = [produced[0]] + [turn(produced[d], -d) for d in range(1, blocks)]
 
     send, kept = attend_project(place, queries, own, passed, out_weight, heads, shards)
     outer, inner = pair_sum(place, kept, core(send))
     mixed = finish(inner, across(outer), mix_gain)
-    experts_mixed = combine_rows(place, expert_ids.T, expert_scores.T, returned)
+    high, low = combine_plan(place, expert_ids.T, expert_scores.T, blocks, capacity)
+    experts_mixed = combine_rows(high, low, returned)
     return (mixed, experts_mixed)
 
 

time: 153 us -> 149 us (0.974)
  waiting for transfers between devices: 78.7 us -> 69.7 us
  starting transfers between devices: 55.3 us -> 61 us
    ppermute x6, waiting for transfers between devices: 31 us -> 14.3 us  [turn(): lax.ppermute(array, 'ep', [(i, (i + d) % blocks) for i in range(blocks)])]
    ppermute x7 -> x8, waiting for transfers between devices: 16.5 us -> 24.6 us  [across(): return lax.ppermute(array, 'tp', [(i, i ^ 2) for i in range(shards)])]
    ppermute x6, starting transfers between devices: 24.7 us -> 30.4 us  [turn(): lax.ppermute(array, 'ep', [(i, (i + d) % blocks) for i in range(blocks)])]
    ppermute x1, waiting for transfers between devices: 0.01 us -> 2.91 us  [paired_step(): passed = [upward(own, 1), lax.ppermute(own, 'ep', [(0, 2)])]]
    ppermute x6, waiting for transfers between devices: 23.7 us -> 20.9 us  [beside(): return lax.ppermute(array, 'grp', [(0, 1), (1, 0)])]
    ppermute x16 -> x17, waiting for transfers between devices: 7.44 us -> 6.91 us  [core(): return lax.ppermute(array, 'tp', [(i, i ^ 1) for i in range(shards)])]
    pallas_call x5 -> x4, Pallas kernels: 8.78 us -> 8.28 us  [the longest x2 6.04 us: expert_rows(): call(body, [shape_of((capacity, width))] * count, [VMEM] * (count + len(f...]
    ppermute x7 -> x8, starting transfers between devices: 10.7 us -> 10.7 us  [across(): return lax.ppermute(array, 'tp', [(i, i ^ 2) for i in range(shards)])]
  transfers between devices with their start and end apart: 39 -> 41, of which waited for: 22 -> 22; matrix products, arithmetic and copies ran while one was open for 0% -> 0% of each run, Pallas kernels for 7% -> 8%
where the time goes in v3:
time: 149 us
  waiting for transfers between devices  69.7 us (47%)
  starting transfers between devices  61 us (41%)
  Pallas kernels  15.5 us (10%)
  local copies, waits for them, and re-layouts  1.63 us (1%)
    ppermute x6, starting transfers between devices, turn(): lax.ppermute(array, 'ep', [(i, (i + d) % blocks) for i in range(blocks)])  30.4 us
    ppermute x8, waiting for transfers between devices, across(): return lax.ppermute(array, 'tp', [(i, i ^ 2) for i in range(shards)])  24.6 us
    ppermute x6, waiting for transfers between devices, beside(): return lax.ppermute(array, 'grp', [(0, 1), (1, 0)])  20.9 us
    ppermute x6, waiting for transfers between devices, turn(): lax.ppermute(array, 'ep', [(i, (i + d) % blocks) for i in range(blocks)])  14.3 us
    ppermute x8, starting transfers between devices, across(): return lax.ppermute(array, 'tp', [(i, i ^ 2) for i in range(shards)])  10.7 us
    ppermute x6, starting transfers between devices, beside(): return lax.ppermute(array, 'grp', [(0, 1), (1, 0)])  7.7 us
    ppermute x17, waiting for transfers between devices, core(): return lax.ppermute(array, 'tp', [(i, i ^ 1) for i in range(shards)])  6.91 us
    pallas_call x2, Pallas kernels, expert_rows(): call(body, [shape_of((capacity, width))] * count, [VMEM] * (count + len(f...  6.04 us
  transfers between devices with their start and end apart: 41, of which 22 were waited for; matrix products, arithmetic and copies ran while one was open for 0% of the time, Pallas kernels for 8%

profile of v3, /device:TPU:0, one launch (start us, length us, event | category | flops | bytes accessed | tf_op | source)
XLA Modules:
  0.0 148.8 jit_solution(11377151925263416526)
XLA Ops:
  0.7 0.1 pad_add_fusion.place_ref
  0.8 2.8 %shard_map.140 = (bf16[96,2048]{1,0:T(8,128)(2,1)S(1)}, bf16[96,2048]{1,0:T(8,128)(2,1)S(1)}, bf16[96,2048]{1,0:T(8,128)(2,1)S(1)}, bf16[96,2048]{1,0:T(8,128)(2...) custom-call(s32[4]{0:T(128)S(1)} %pad_add_fusion.place_ref, ...), custom_call_target="tpu_custom_call" | custom-call | flops 201326592 | tf_op jit(solution)/shard_map/pallas_call | solution.py:281
  3.6 3.0 %collective-permute-start.11 = (bf16[1024,128]{1,0:T(8,128)(2,1)S(1)}, bf16[1024,128]{1,0:T(8,128)(2,1)S(1)}, u32[]{:S(2)}, u32[]{:S(2)}) collective-permute-start(bf16[1024,128]{1,0:T(8,128)(2,1)S(1)} %get-tuple-element.33), channel_id=1, source_target_pairs={{0,2},{1,3},{2,0},{3,1},{4,6},{5,7},{6,4},{7,5},{8,10},{9,11},{10,... | collective-permute-start | bytes 786440 | tf_op jit(solution)/shard_map/ppermute | solution.py:538
  6.6 0.1 collective-permute-start.16
  6.7 1.9 %collective-permute-start.12 = (bf16[1024,128]{1,0:T(8,128)(2,1)S(1)}, bf16[1024,128]{1,0:T(8,128)(2,1)S(1)}, u32[]{:S(2)}, u32[]{:S(2)}) collective-permute-start(bf16[1024,128]{1,0:T(8,128)(2,1)S(1)} %get-tuple-element.34), channel_id=1, source_target_pairs={{0,2},{1,3},{2,0},{3,1},{4,6},{5,7},{6,4},{7,5},{8,10},{9,11},{10,... | collective-permute-start | bytes 786440 | tf_op jit(solution)/shard_map/ppermute | solution.py:538
  8.6 0.1 collective-permute-start.13
  8.7 1.9 %collective-permute-start.14 = (bf16[1024,128]{1,0:T(8,128)(2,1)S(1)}, bf16[1024,128]{1,0:T(8,128)(2,1)S(1)}, u32[]{:S(2)}, u32[]{:S(2)}) collective-permute-start(bf16[1024,128]{1,0:T(8,128)(2,1)S(1)} %get-tuple-element.36), channel_id=1, source_target_pairs={{0,2},{1,3},{2,0},{3,1},{4,6},{5,7},{6,4},{7,5},{8,10},{9,11},{10,... | collective-permute-start | bytes 786440 | tf_op jit(solution)/shard_map/ppermute | solution.py:538
  10.7 5.9 %collective-permute-done.16.refs_14_.refs_12_ = bf16[32,2048]{1,0:T(8,128)(2,1)S(1)} collective-permute-done((bf16[32,2048]{1,0:T(8,128)(2,1)S(1)}, bf16[32,2048]{1,0:T(8,128)(2,1)S(1)}, u32[]{:S(2)}, u32[]{:S(2)}) %collective-permute-start.16) | collective-permute-done | bytes 131104 | tf_op jit(solution)/shard_map/ppermute | solution.py:538
  16.6 2.0 %collective-permute-start.15 = (bf16[64,2048]{1,0:T(8,128)(2,1)S(1)}, bf16[64,2048]{1,0:T(8,128)(2,1)S(1)}, u32[]{:S(2)}, u32[]{:S(2)}) collective-permute-start(bf16[64,2048]{1,0:T(8,128)(2,1)S(1)} %get-tuple-element.37), channel_id=1, source_target_pairs={{0,2},{1,3},{2,0},{3,1},{4,6},{5,7},{6,4},{7,5},{8,10},{9,11},{10,... | collective-permute-start | bytes 786440 | tf_op jit(solution)/shard_map/ppermute | solution.py:538
  18.6 3.6 %collective-permute-done.12.refs_10_.refs_8_ = bf16[1024,128]{1,0:T(8,128)(2,1)S(1)} collective-permute-done((bf16[1024,128]{1,0:T(8,128)(2,1)S(1)}, bf16[1024,128]{1,0:T(8,128)(2,1)S(1)}, u32[]{:S(2)}, u32[]{:S(2)}) %collective-permute-start.12) | collective-permute-done | bytes 262176 | tf_op jit(solution)/shard_map/ppermute | solution.py:538
  22.2 4.0 %collective-permute-start = (bf16[136,1024]{1,0:T(8,128)(2,1)S(1)}, bf16[136,1024]{1,0:T(8,128)(2,1)S(1)}, u32[]{:S(2)}, u32[]{:S(2)}) collective-permute-start(bf16[136,1024]{1,0:T(8,128)(2,1)S(1)} %get-tuple-element.23.own_ref), channel_id=1, source_target_pairs={{0,4},{4,8},{8,12},{1,5},{5,9},{9,13},{2,6},{6,10},{10,14},{3,7},{... | collective-permute-start | bytes 835592 | tf_op jit(solution)/shard_map/ppermute | solution.py:547
  26.2 1.6 %collective-permute-done.13.refs_11_.refs_9_ = bf16[1024,128]{1,0:T(8,128)(2,1)S(1)} collective-permute-done((bf16[1024,128]{1,0:T(8,128)(2,1)S(1)}, bf16[1024,128]{1,0:T(8,128)(2,1)S(1)}, u32[]{:S(2)}, u32[]{:S(2)}) %collective-permute-start.13) | collective-permute-done | bytes 262176 | tf_op jit(solution)/shard_map/ppermute | solution.py:538
  27.8 3.1 %collective-permute-start.38 = (bf16[96,2048]{1,0:T(8,128)(2,1)S(1)}, bf16[96,2048]{1,0:T(8,128)(2,1)S(1)}, u32[]{:S(2)}, u32[]{:S(2)}) collective-permute-start(bf16[96,2048]{1,0:T(8,128)(2,1)S(1)} %get-tuple-element.42), channel_id=1, source_target_pairs={{0,8},{4,12},{8,0},{12,4},{1,9},{5,13},{9,1},{13,5},{2,10},{6,14},... | collective-permute-start | bytes 1179656 | tf_op jit(solution)/shard_map/ppermute | solution.py:544
  30.9 2.5 %collective-permute-done.14.refs_12_.refs_10_ = bf16[1024,128]{1,0:T(8,128)(2,1)S(1)} collective-permute-done((bf16[1024,128]{1,0:T(8,128)(2,1)S(1)}, bf16[1024,128]{1,0:T(8,128)(2,1)S(1)}, u32[]{:S(2)}, u32[]{:S(2)}) %collective-permute-start.14) | collective-permute-done | bytes 262176 | tf_op jit(solution)/shard_map/ppermute | solution.py:538
  33.4 2.1 %collective-permute-start.30 = (bf16[32,2048]{1,0:T(8,128)(2,1)S(1)}, bf16[32,2048]{1,0:T(8,128)(2,1)S(1)}, u32[]{:S(2)}, u32[]{:S(2)}) collective-permute-start(bf16[32,2048]{1,0:T(8,128)(2,1)S(1)} %collective-permute-done.16.refs_14_.refs_12_), channel_id=1, source_target_pairs={{0,16},{16,0},{1,17},{17,1},{2,18},{18,2},{3,19},{19,3},{4,20},{20... | collective-permute-start | bytes 393224 | tf_op jit(solution)/shard_map/ppermute | solution.py:541
  35.5 3.6 %collective-permute-done.15.refs_13_.refs_11_ = bf16[64,2048]{1,0:T(8,128)(2,1)S(1)} collective-permute-done((bf16[64,2048]{1,0:T(8,128)(2,1)S(1)}, bf16[64,2048]{1,0:T(8,128)(2,1)S(1)}, u32[]{:S(2)}, u32[]{:S(2)}) %collective-permute-start.15) | collective-permute-done | bytes 262176 | tf_op jit(solution)/shard_map/ppermute | solution.py:538
  39.0 4.8 %collective-permute-done.17.refs_15_.refs_29_.refs_13_.refs_27_ = bf16[64,2048]{1,0:T(8,128)(2,1)S(1)} collective-permute-done((bf16[64,2048]{1,0:T(8,128)(2,1)S(1)}, bf16[64,2048]{1,0:T(8,128)(2,1)S(1)}, u32[]{:S(2)}, u32[]{:S(2)}) %collective-permute-start.17) | collective-permute-done | bytes 262176 | tf_op jit(solution)/shard_map/ppermute | solution.py:538
  43.8 4.7 %collective-permute-start.1 = (bf16[136,1024]{1,0:T(8,128)(2,1)S(1)}, bf16[136,1024]{1,0:T(8,128)(2,1)S(1)}, u32[]{:S(2)}, u32[]{:S(2)}) collective-permute-start(bf16[136,1024]{1,0:T(8,128)(2,1)S(1)} %get-tuple-element.23.own_ref), channel_id=1, source_target_pairs={{0,8},{1,9},{2,10},{3,11},{16,24},{17,25},{18,26},{19,27}} | collective-permute-start | bytes 835592 | tf_op jit(solution)/shard_map/ppermute | solution.py:565
  48.6 1.6 %collective-permute-start.25 = (bf16[1024,128]{1,0:T(8,128)(2,1)S(1)}, bf16[1024,128]{1,0:T(8,128)(2,1)S(1)}, u32[]{:S(2)}, u32[]{:S(2)}) collective-permute-start(bf16[1024,128]{1,0:T(8,128)(2,1)S(1)} %collective-permute-done.11.refs_9_.refs_7_), channel_id=1, source_target_pairs={{0,16},{16,0},{1,17},{17,1},{2,18},{18,2},{3,19},{19,3},{4,20},{20... | collective-permute-start | bytes 786440 | tf_op jit(solution)/shard_map/ppermute | solution.py:541
  50.2 0.5 collective-permute-start.26
  50.7 2.9 %collective-permute-done.1.refs_1_ = bf16[136,1024]{1,0:T(8,128)(2,1)S(1)} collective-permute-done((bf16[136,1024]{1,0:T(8,128)(2,1)S(1)}, bf16[136,1024]{1,0:T(8,128)(2,1)S(1)}, u32[]{:S(2)}, u32[]{:S(2)}) %collective-permute-start.1) | collective-permute-done | bytes 278560 | tf_op jit(solution)/shard_map/ppermute | solution.py:565
  53.6 1.5 %collective-permute-start.27 = (bf16[1024,128]{1,0:T(8,128)(2,1)S(1)}, bf16[1024,128]{1,0:T(8,128)(2,1)S(1)}, u32[]{:S(2)}, u32[]{:S(2)}) collective-permute-start(bf16[1024,128]{1,0:T(8,128)(2,1)S(1)} %collective-permute-done.13.refs_11_.refs_9_), channel_id=1, source_target_pairs={{0,16},{16,0},{1,17},{17,1},{2,18},{18,2},{3,19},{19,3},{4,20},{20... | collective-permute-start | bytes 786440 | tf_op jit(solution)/shard_map/ppermute | solution.py:541
  55.1 0.5 collective-permute-start.28
  55.6 1.5 %collective-permute-start.29 = (bf16[64,2048]{1,0:T(8,128)(2,1)S(1)}, bf16[64,2048]{1,0:T(8,128)(2,1)S(1)}, u32[]{:S(2)}, u32[]{:S(2)}) collective-permute-start(bf16[64,2048]{1,0:T(8,128)(2,1)S(1)} %collective-permute-done.15.refs_13_.refs_11_), channel_id=1, source_target_pairs={{0,16},{16,0},{1,17},{17,1},{2,18},{18,2},{3,19},{19,3},{4,20},{20... | collective-permute-start | bytes 786440 | tf_op jit(solution)/shard_map/ppermute | solution.py:541
  57.2 0.7 collective-permute-done.25.refs_23_.refs_21_
  57.8 5.6 %collective-permute-done.26.refs_24_.refs_22_ = bf16[1024,128]{1,0:T(8,128)(2,1)S(1)} collective-permute-done((bf16[1024,128]{1,0:T(8,128)(2,1)S(1)}, bf16[1024,128]{1,0:T(8,128)(2,1)S(1)}, u32[]{:S(2)}, u32[]{:S(2)}) %collective-permute-start.26) | collective-permute-done | bytes 262176 | tf_op jit(solution)/shard_map/ppermute | solution.py:541
  63.4 5.6 %collective-permute-done.27.refs_25_.refs_23_ = bf16[1024,128]{1,0:T(8,128)(2,1)S(1)} collective-permute-done((bf16[1024,128]{1,0:T(8,128)(2,1)S(1)}, bf16[1024,128]{1,0:T(8,128)(2,1)S(1)}, u32[]{:S(2)}, u32[]{:S(2)}) %collective-permute-start.27) | collective-permute-done | bytes 262176 | tf_op jit(solution)/shard_map/ppermute | solution.py:541
  69.1 5.6 %collective-permute-done.28.refs_26_.refs_24_ = bf16[1024,128]{1,0:T(8,128)(2,1)S(1)} collective-permute-done((bf16[1024,128]{1,0:T(8,128)(2,1)S(1)}, bf16[1024,128]{1,0:T(8,128)(2,1)S(1)}, u32[]{:S(2)}, u32[]{:S(2)}) %collective-permute-start.28) | collective-permute-done | bytes 262176 | tf_op jit(solution)/shard_map/ppermute | solution.py:541
  74.7 3.3 %collective-permute-done.29.refs_27_.refs_25_ = bf16[64,2048]{1,0:T(8,128)(2,1)S(1)} collective-permute-done((bf16[64,2048]{1,0:T(8,128)(2,1)S(1)}, bf16[64,2048]{1,0:T(8,128)(2,1)S(1)}, u32[]{:S(2)}, u32[]{:S(2)}) %collective-permute-start.29) | collective-permute-done | bytes 262176 | tf_op jit(solution)/shard_map/ppermute | solution.py:541
  78.0 0.7 collective-permute-start.2
  78.7 0.1 collective-permute-start.22
  78.8 0.5 collective-permute-start.24
  79.3 0.7 collective-permute-start.3
  80.0 0.2 collective-permute-start.31
  80.1 0.2 collective-permute-done.22.refs_20_.refs_18_
  80.3 0.2 collective-permute-start.10
  80.6 0.1 collective-permute-done.24.refs_22_.refs_36_.refs_20_.refs_34_
  80.7 0.1 collective-permute-start.8
  80.8 0.4 collective-permute-start.9
  81.2 0.1 collective-permute-start.32
  81.4 0.2 collective-permute-done.31.refs_30_.refs_28_
  81.6 0.1 collective-permute-start.33
  81.7 4.7 %collective-permute-done.32.refs_31_.refs_29_ = bf16[1024,128]{1,0:T(8,128)(2,1)S(1)} collective-permute-done((bf16[1024,128]{1,0:T(8,128)(2,1)S(1)}, bf16[1024,128]{1,0:T(8,128)(2,1)S(1)}, u32[]{:S(2)}, u32[]{:S(2)}) %collective-permute-start.32) | collective-permute-done | bytes 262176 | tf_op jit(solution)/shard_map/ppermute | solution.py:535
  86.5 0.1 collective-permute-start.34
  86.6 0.2 collective-permute-done.33.refs_32_.refs_30_
  86.8 0.1 collective-permute-start.35
  87.0 1.0 collective-permute-done.34.refs_33_.refs_31_
  88.0 0.4 collective-permute-done.35.refs_34_.refs_32_
  88.4 7.7 %collective-permute-start.7 = (bf16[96,2048]{1,0:T(8,128)(2,1)S(1)}, bf16[96,2048]{1,0:T(8,128)(2,1)S(1)}, u32[]{:S(2)}, u32[]{:S(2)}) collective-permute-start(bf16[96,2048]{1,0:T(8,128)(2,1)S(1)} %get-tuple-element.32), channel_id=1, source_target_pairs={{0,12},{4,0},{8,4},{12,8},{1,13},{5,1},{9,5},{13,9},{2,14},{6,2},{... | collective-permute-start | bytes 1179656 | tf_op jit(solution)/shard_map/ppermute | solution.py:544
  96.1 1.6 %copy-done.3 = bf16[512,2048]{1,0:T(8,128)(2,1)S(1)} copy-done((bf16[512,2048]{1,0:T(8,128)(2,1)S(1)}, bf16[512,2048]{1,0:T(8,128)(2,1)}, u32[]{:S(2)}) %copy-start.3) | copy-done | bytes 2097176
  97.6 3.1 %shard_map.141 = (bf16[64,2048]{1,0:T(8,128)(2,1)S(1)}, f32[64,2048]{1,0:T(8,128)S(1)}) custom-call(s32[4]{0:T(128)S(1)} %pad_add_fusion.place_ref, bf16[128,512]{1,0:T(8,128)(2,1)S(1)} %copy-done.4, bf16[136,1024]{1,0:T(8,128)(2,1)S(1)} %get-tuple-element.23.own_ref, bf16[136,1024]{1,0:T(8,128)(2,1)S(1)} %collective-permute-done.refs_0_, ...), custom_call_target="tpu_custom_call" | custom-call | flops 402653184 | tf_op jit(solution)/shard_map/pallas_call | solution.py:492
  100.8 2.2 %shard_map.146 = bf16[96,2048]{1,0:T(8,128)(2,1)S(1)} custom-call(bf16[96,2048]{1,0:T(8,128)(2,1)S(1)} %collective-permute-done.38.refs_0_, bf16[2048,256]{1,0:T(8,128)(2,1)S(1)} %bitcast.14, bf16[2048,256]{1,0:T(8,128)(2,1)S(1)} %bitcast.18, bf16[256,2048]{1,0:T(8,128)(2,1)S(1)} %bitcast.22, bf16[2048,256]{1,0:T(8,128)(2,1)S(1)} %collective-permute-done.8.refs_6_.refs_4_, ...), custom_call_target="tpu_custom_call" | custom-call | flops 1207959552 | tf_op jit(solution)/shard_map/pallas_call | solution.py:382
  103.0 3.8 %collective-permute-start.39 = (bf16[96,2048]{1,0:T(8,128)(2,1)S(1)}, bf16[96,2048]{1,0:T(8,128)(2,1)S(1)}, u32[]{:S(2)}, u32[]{:S(2)}) collective-permute-start(bf16[96,2048]{1,0:T(8,128)(2,1)S(1)} %shard_map.146), channel_id=1, source_target_pairs={{0,8},{4,12},{8,0},{12,4},{1,9},{5,13},{9,1},{13,5},{2,10},{6,14},... | collective-permute-start | bytes 1179656 | tf_op jit(solution)/shard_map/ppermute | solution.py:544
  106.8 5.1 %collective-permute-done.7.refs_2_ = bf16[96,2048]{1,0:T(8,128)(2,1)S(1)} collective-permute-done((bf16[96,2048]{1,0:T(8,128)(2,1)S(1)}, bf16[96,2048]{1,0:T(8,128)(2,1)S(1)}, u32[]{:S(2)}, u32[]{:S(2)}) %collective-permute-start.7) | collective-permute-done | bytes 393248 | tf_op jit(solution)/shard_map/ppermute | solution.py:544
  111.9 3.9 %shard_map.145 = (bf16[96,2048]{1,0:T(8,128)(2,1)S(1)}, bf16[96,2048]{1,0:T(8,128)(2,1)S(1)}, bf16[96,2048]{1,0:T(8,128)(2,1)S(1)}) custom-call(bf16[96,2048]{1,0:T(8,128)(2,1)S(1)} %get-tuple-element.30.refs_0_, bf16[96,2048]{1,0:T(8,128)(2,1)S(1)} %collective-permute-done.6.refs_1_, bf16[96,2048]{1,0:T(8,128)(2,1)S(1)} %collective-permute-done.7.refs_2_, ...), custom_call_target="tpu_custom_call" | custom-call | flops 3623878656 | tf_op jit(solution)/shard_map/pallas_call | solution.py:382
  115.8 3.5 %collective-permute-start.37 = (bf16[96,2048]{1,0:T(8,128)(2,1)S(1)}, bf16[96,2048]{1,0:T(8,128)(2,1)S(1)}, u32[]{:S(2)}, u32[]{:S(2)}) collective-permute-start(bf16[96,2048]{1,0:T(8,128)(2,1)S(1)} %get-tuple-element.41), channel_id=1, source_target_pairs={{0,12},{4,0},{8,4},{12,8},{1,13},{5,1},{9,5},{13,9},{2,14},{6,2},{... | collective-permute-start | bytes 1179656 | tf_op jit(solution)/shard_map/ppermute | solution.py:544
  119.2 12.3 %collective-permute-start.40 = (bf16[96,2048]{1,0:T(8,128)(2,1)S(1)}, bf16[96,2048]{1,0:T(8,128)(2,1)S(1)}, u32[]{:S(2)}, u32[]{:S(2)}) collective-permute-start(bf16[96,2048]{1,0:T(8,128)(2,1)S(1)} %get-tuple-element.43), channel_id=1, source_target_pairs={{0,4},{4,8},{8,12},{12,0},{1,5},{5,9},{9,13},{13,1},{2,6},{6,10},{... | collective-permute-start | bytes 1179656 | tf_op jit(solution)/shard_map/ppermute | solution.py:544
  131.6 0.6 shard_map.142
  132.2 1.6 %collective-permute-start.5 = (bf16[32,2048]{1,0:T(8,128)(2,1)S(1)}, bf16[32,2048]{1,0:T(8,128)(2,1)S(1)}, u32[]{:S(2)}, u32[]{:S(2)}) collective-permute-start(bf16[32,2048]{1,0:T(8,128)(2,1)S(1)} %get-tuple-element.27), channel_id=1, source_target_pairs={{0,2},{1,3},{2,0},{3,1},{4,6},{5,7},{6,4},{7,5},{8,10},{9,11},{10,... | collective-permute-start | bytes 393224 | tf_op jit(solution)/shard_map/ppermute | solution.py:538
  133.7 0.7 shard_map.144
  134.5 2.7 %collective-permute-done.5.received_ref = bf16[32,2048]{1,0:T(8,128)(2,1)S(1)} collective-permute-done((bf16[32,2048]{1,0:T(8,128)(2,1)S(1)}, bf16[32,2048]{1,0:T(8,128)(2,1)S(1)}, u32[]{:S(2)}, u32[]{:S(2)}) %collective-permute-start.5) | collective-permute-done | bytes 131104 | tf_op jit(solution)/shard_map/ppermute | solution.py:538
  137.2 0.8 shard_map.143
  138.0 9.2 %collective-permute-done.37.refs_1_ = bf16[96,2048]{1,0:T(8,128)(2,1)S(1)} collective-permute-done((bf16[96,2048]{1,0:T(8,128)(2,1)S(1)}, bf16[96,2048]{1,0:T(8,128)(2,1)S(1)}, u32[]{:S(2)}, u32[]{:S(2)}) %collective-permute-start.37) | collective-permute-done | bytes 393248 | tf_op jit(solution)/shard_map/ppermute | solution.py:544
  147.2 1.5 %shard_map.147 = bf16[128,2048]{1,0:T(8,128)(2,1)} custom-call(bf16[384,128]{1,0:T(8,128)(2,1)S(1)} %get-tuple-element.28.high_ref, bf16[384,128]{1,0:T(8,128)(2,1)S(1)} %get-tuple-element.29.low_ref, bf16[96,2048]{1,0:T(8,128)(2,1)S(1)} %get-tuple-element.40.refs_0_, bf16[96,2048]{1,0:T(8,128)(2,1)S(1)} %collective-permute-done.37.refs_1_, ...), custom_call_target="tpu_custom_call" | custom-call | flops 402653184 | tf_op jit(solution)/shard_map/pallas_call | solution.py:345
  (43 shorter events, 0.2 us)
Async XLA Ops:
  0.6 80.1 %copy-start = (bf16[1,2048,256]{2,1,0:T(8,128)(2,1)S(1)}, bf16[1,2048,256]{2,1,0:T(8,128)(2,1)}, u32[]{:S(2)}) copy-start(bf16[1,2048,256]{2,1,0:T(8,128)(2,1)} %param.23) | copy-start | bytes 3145732
  0.6 80.2 %copy-start.1 = (bf16[1,2048,256]{2,1,0:T(8,128)(2,1)S(1)}, bf16[1,2048,256]{2,1,0:T(8,128)(2,1)}, u32[]{:S(2)}) copy-start(bf16[1,2048,256]{2,1,0:T(8,128)(2,1)} %param.24) | copy-start | bytes 3145732
  0.7 79.7 %copy-start.2 = (bf16[1,256,2048]{2,1,0:T(8,128)(2,1)S(1)}, bf16[1,256,2048]{2,1,0:T(8,128)(2,1)}, u32[]{:S(2)}) copy-start(bf16[1,256,2048]{2,1,0:T(8,128)(2,1)} %param.25) | copy-start | bytes 3145732
  0.7 95.4 %copy-start.4 = (bf16[128,512]{1,0:T(8,128)(2,1)S(1)}, bf16[128,512]{1,0:T(8,128)(2,1)}, u32[]{:S(2)}) copy-start(bf16[128,512]{1,0:T(8,128)(2,1)} %q_ref.1) | copy-start | bytes 393220
  3.6 15.0 %collective-permute-start.11 = (bf16[1024,128]{1,0:T(8,128)(2,1)S(1)}, bf16[1024,128]{1,0:T(8,128)(2,1)S(1)}, u32[]{:S(2)}, u32[]{:S(2)}) collective-permute-start(bf16[1024,128]{1,0:T(8,128)(2,1)S(1)} %get-tuple-element.33), channel_id=1, source_target_pairs={{0,2},{1,3},{2,0},{3,1},{4,6},{5,7},{6,4},{7,5},{8,10},{9,11},{10,... | collective-permute-start | bytes 786440 | tf_op jit(solution)/shard_map/ppermute | solution.py:538
  6.6 10.0 %collective-permute-start.16 = (bf16[32,2048]{1,0:T(8,128)(2,1)S(1)}, bf16[32,2048]{1,0:T(8,128)(2,1)S(1)}, u32[]{:S(2)}, u32[]{:S(2)}) collective-permute-start(bf16[32,2048]{1,0:T(8,128)(2,1)S(1)} %get-tuple-element.38), channel_id=1, source_target_pairs={{0,2},{1,3},{2,0},{3,1},{4,6},{5,7},{6,4},{7,5},{8,10},{9,11},{10,... | collective-permute-start | bytes 393224 | tf_op jit(solution)/shard_map/ppermute | solution.py:538
  6.7 15.5 %collective-permute-start.12 = (bf16[1024,128]{1,0:T(8,128)(2,1)S(1)}, bf16[1024,128]{1,0:T(8,128)(2,1)S(1)}, u32[]{:S(2)}, u32[]{:S(2)}) collective-permute-start(bf16[1024,128]{1,0:T(8,128)(2,1)S(1)} %get-tuple-element.34), channel_id=1, source_target_pairs={{0,2},{1,3},{2,0},{3,1},{4,6},{5,7},{6,4},{7,5},{8,10},{9,11},{10,... | collective-permute-start | bytes 786440 | tf_op jit(solution)/shard_map/ppermute | solution.py:538
  8.6 19.2 %collective-permute-start.13 = (bf16[1024,128]{1,0:T(8,128)(2,1)S(1)}, bf16[1024,128]{1,0:T(8,128)(2,1)S(1)}, u32[]{:S(2)}, u32[]{:S(2)}) collective-permute-start(bf16[1024,128]{1,0:T(8,128)(2,1)S(1)} %get-tuple-element.35), channel_id=1, source_target_pairs={{0,2},{1,3},{2,0},{3,1},{4,6},{5,7},{6,4},{7,5},{8,10},{9,11},{10,... | collective-permute-start | bytes 786440 | tf_op jit(solution)/shard_map/ppermute | solution.py:538
  8.7 24.7 %collective-permute-start.14 = (bf16[1024,128]{1,0:T(8,128)(2,1)S(1)}, bf16[1024,128]{1,0:T(8,128)(2,1)S(1)}, u32[]{:S(2)}, u32[]{:S(2)}) collective-permute-start(bf16[1024,128]{1,0:T(8,128)(2,1)S(1)} %get-tuple-element.36), channel_id=1, source_target_pairs={{0,2},{1,3},{2,0},{3,1},{4,6},{5,7},{6,4},{7,5},{8,10},{9,11},{10,... | collective-permute-start | bytes 786440 | tf_op jit(solution)/shard_map/ppermute | solution.py:538
  16.6 22.5 %collective-permute-start.15 = (bf16[64,2048]{1,0:T(8,128)(2,1)S(1)}, bf16[64,2048]{1,0:T(8,128)(2,1)S(1)}, u32[]{:S(2)}, u32[]{:S(2)}) collective-permute-start(bf16[64,2048]{1,0:T(8,128)(2,1)S(1)} %get-tuple-element.37), channel_id=1, source_target_pairs={{0,2},{1,3},{2,0},{3,1},{4,6},{5,7},{6,4},{7,5},{8,10},{9,11},{10,... | collective-permute-start | bytes 786440 | tf_op jit(solution)/shard_map/ppermute | solution.py:538
  18.6 25.2 %collective-permute-start.17 = (bf16[64,2048]{1,0:T(8,128)(2,1)S(1)}, bf16[64,2048]{1,0:T(8,128)(2,1)S(1)}, u32[]{:S(2)}, u32[]{:S(2)}) collective-permute-start(bf16[64,2048]{1,0:T(8,128)(2,1)S(1)} %get-tuple-element.39), channel_id=1, source_target_pairs={{0,2},{1,3},{2,0},{3,1},{4,6},{5,7},{6,4},{7,5},{8,10},{9,11},{10,... | collective-permute-start | bytes 786440 | tf_op jit(solution)/shard_map/ppermute | solution.py:538
  22.2 28.5 %collective-permute-start = (bf16[136,1024]{1,0:T(8,128)(2,1)S(1)}, bf16[136,1024]{1,0:T(8,128)(2,1)S(1)}, u32[]{:S(2)}, u32[]{:S(2)}) collective-permute-start(bf16[136,1024]{1,0:T(8,128)(2,1)S(1)} %get-tuple-element.23.own_ref), channel_id=1, source_target_pairs={{0,4},{4,8},{8,12},{1,5},{5,9},{9,13},{2,6},{6,10},{10,14},{3,7},{... | collective-permute-start | bytes 835592 | tf_op jit(solution)/shard_map/ppermute | solution.py:547
  27.8 27.8 %collective-permute-start.38 = (bf16[96,2048]{1,0:T(8,128)(2,1)S(1)}, bf16[96,2048]{1,0:T(8,128)(2,1)S(1)}, u32[]{:S(2)}, u32[]{:S(2)}) collective-permute-start(bf16[96,2048]{1,0:T(8,128)(2,1)S(1)} %get-tuple-element.42), channel_id=1, source_target_pairs={{0,8},{4,12},{8,0},{12,4},{1,9},{5,13},{9,1},{13,5},{2,10},{6,14},... | collective-permute-start | bytes 1179656 | tf_op jit(solution)/shard_map/ppermute | solution.py:544
  33.4 15.1 %collective-permute-start.30 = (bf16[32,2048]{1,0:T(8,128)(2,1)S(1)}, bf16[32,2048]{1,0:T(8,128)(2,1)S(1)}, u32[]{:S(2)}, u32[]{:S(2)}) collective-permute-start(bf16[32,2048]{1,0:T(8,128)(2,1)S(1)} %collective-permute-done.16.refs_14_.refs_12_), channel_id=1, source_target_pairs={{0,16},{16,0},{1,17},{17,1},{2,18},{18,2},{3,19},{19,3},{4,20},{20... | collective-permute-start | bytes 393224 | tf_op jit(solution)/shard_map/ppermute | solution.py:541
  39.0 11.1 %collective-permute-start.23 = (bf16[32,2048]{1,0:T(8,128)(2,1)S(1)}, bf16[32,2048]{1,0:T(8,128)(2,1)S(1)}, u32[]{:S(2)}, u32[]{:S(2)}) collective-permute-start(bf16[32,2048]{1,0:T(8,128)(2,1)S(1)} %collective-permute-done.16.refs_14_.refs_12_), channel_id=1, source_target_pairs={{0,1},{1,0},{2,3},{3,2},{4,5},{5,4},{6,7},{7,6},{8,9},{9,8},{10,11... | collective-permute-start | bytes 393224 | tf_op jit(solution)/shard_map/ppermute | solution.py:535
  43.8 9.8 %collective-permute-start.1 = (bf16[136,1024]{1,0:T(8,128)(2,1)S(1)}, bf16[136,1024]{1,0:T(8,128)(2,1)S(1)}, u32[]{:S(2)}, u32[]{:S(2)}) collective-permute-start(bf16[136,1024]{1,0:T(8,128)(2,1)S(1)} %get-tuple-element.23.own_ref), channel_id=1, source_target_pairs={{0,8},{1,9},{2,10},{3,11},{16,24},{17,25},{18,26},{19,27}} | collective-permute-start | bytes 835592 | tf_op jit(solution)/shard_map/ppermute | solution.py:565
  48.6 9.2 %collective-permute-start.25 = (bf16[1024,128]{1,0:T(8,128)(2,1)S(1)}, bf16[1024,128]{1,0:T(8,128)(2,1)S(1)}, u32[]{:S(2)}, u32[]{:S(2)}) collective-permute-start(bf16[1024,128]{1,0:T(8,128)(2,1)S(1)} %collective-permute-done.11.refs_9_.refs_7_), channel_id=1, source_target_pairs={{0,16},{16,0},{1,17},{17,1},{2,18},{18,2},{3,19},{19,3},{4,20},{20... | collective-permute-start | bytes 786440 | tf_op jit(solution)/shard_map/ppermute | solution.py:541
  50.2 13.3 %collective-permute-start.26 = (bf16[1024,128]{1,0:T(8,128)(2,1)S(1)}, bf16[1024,128]{1,0:T(8,128)(2,1)S(1)}, u32[]{:S(2)}, u32[]{:S(2)}) collective-permute-start(bf16[1024,128]{1,0:T(8,128)(2,1)S(1)} %collective-permute-done.12.refs_10_.refs_8_), channel_id=1, source_target_pairs={{0,16},{16,0},{1,17},{17,1},{2,18},{18,2},{3,19},{19,3},{4,20},{20... | collective-permute-start | bytes 786440 | tf_op jit(solution)/shard_map/ppermute | solution.py:541
  50.7 4.4 %collective-permute-start.36 = (bf16[32,2048]{1,0:T(8,128)(2,1)S(1)}, bf16[32,2048]{1,0:T(8,128)(2,1)S(1)}, u32[]{:S(2)}, u32[]{:S(2)}) collective-permute-start(bf16[32,2048]{1,0:T(8,128)(2,1)S(1)} %collective-permute-done.30.refs_28_.refs_26_), channel_id=1, source_target_pairs={{0,1},{1,0},{2,3},{3,2},{4,5},{5,4},{6,7},{7,6},{8,9},{9,8},{10,11... | collective-permute-start | bytes 393224 | tf_op jit(solution)/shard_map/ppermute | solution.py:535
  53.6 15.5 %collective-permute-start.27 = (bf16[1024,128]{1,0:T(8,128)(2,1)S(1)}, bf16[1024,128]{1,0:T(8,128)(2,1)S(1)}, u32[]{:S(2)}, u32[]{:S(2)}) collective-permute-start(bf16[1024,128]{1,0:T(8,128)(2,1)S(1)} %collective-permute-done.13.refs_11_.refs_9_), channel_id=1, source_target_pairs={{0,16},{16,0},{1,17},{17,1},{2,18},{18,2},{3,19},{19,3},{4,20},{20... | collective-permute-start | bytes 786440 | tf_op jit(solution)/shard_map/ppermute | solution.py:541
  55.1 19.6 %collective-permute-start.28 = (bf16[1024,128]{1,0:T(8,128)(2,1)S(1)}, bf16[1024,128]{1,0:T(8,128)(2,1)S(1)}, u32[]{:S(2)}, u32[]{:S(2)}) collective-permute-start(bf16[1024,128]{1,0:T(8,128)(2,1)S(1)} %collective-permute-done.14.refs_12_.refs_10_), channel_id=1, source_target_pairs={{0,16},{16,0},{1,17},{17,1},{2,18},{18,2},{3,19},{19,3},{4,20},{20... | collective-permute-start | bytes 786440 | tf_op jit(solution)/shard_map/ppermute | solution.py:541
  55.6 22.4 %collective-permute-start.29 = (bf16[64,2048]{1,0:T(8,128)(2,1)S(1)}, bf16[64,2048]{1,0:T(8,128)(2,1)S(1)}, u32[]{:S(2)}, u32[]{:S(2)}) collective-permute-start(bf16[64,2048]{1,0:T(8,128)(2,1)S(1)} %collective-permute-done.15.refs_13_.refs_11_), channel_id=1, source_target_pairs={{0,16},{16,0},{1,17},{17,1},{2,18},{18,2},{3,19},{19,3},{4,20},{20... | collective-permute-start | bytes 786440 | tf_op jit(solution)/shard_map/ppermute | solution.py:541
  57.8 20.9 %collective-permute-start.18 = (bf16[1024,128]{1,0:T(8,128)(2,1)S(1)}, bf16[1024,128]{1,0:T(8,128)(2,1)S(1)}, u32[]{:S(2)}, u32[]{:S(2)}) collective-permute-start(bf16[1024,128]{1,0:T(8,128)(2,1)S(1)} %collective-permute-done.11.refs_9_.refs_7_), channel_id=1, source_target_pairs={{0,1},{1,0},{2,3},{3,2},{4,5},{5,4},{6,7},{7,6},{8,9},{9,8},{10,11... | collective-permute-start | bytes 786440 | tf_op jit(solution)/shard_map/ppermute | solution.py:535
  63.4 15.3 %collective-permute-start.19 = (bf16[1024,128]{1,0:T(8,128)(2,1)S(1)}, bf16[1024,128]{1,0:T(8,128)(2,1)S(1)}, u32[]{:S(2)}, u32[]{:S(2)}) collective-permute-start(bf16[1024,128]{1,0:T(8,128)(2,1)S(1)} %collective-permute-done.12.refs_10_.refs_8_), channel_id=1, source_target_pairs={{0,1},{1,0},{2,3},{3,2},{4,5},{5,4},{6,7},{7,6},{8,9},{9,8},{10,11... | collective-permute-start | bytes 786440 | tf_op jit(solution)/shard_map/ppermute | solution.py:535
  69.1 10.2 %collective-permute-start.20 = (bf16[1024,128]{1,0:T(8,128)(2,1)S(1)}, bf16[1024,128]{1,0:T(8,128)(2,1)S(1)}, u32[]{:S(2)}, u32[]{:S(2)}) collective-permute-start(bf16[1024,128]{1,0:T(8,128)(2,1)S(1)} %collective-permute-done.13.refs_11_.refs_9_), channel_id=1, source_target_pairs={{0,1},{1,0},{2,3},{3,2},{4,5},{5,4},{6,7},{7,6},{8,9},{9,8},{10,11... | collective-permute-start | bytes 786440 | tf_op jit(solution)/shard_map/ppermute | solution.py:535
  74.7 5.3 %collective-permute-start.21 = (bf16[1024,128]{1,0:T(8,128)(2,1)S(1)}, bf16[1024,128]{1,0:T(8,128)(2,1)S(1)}, u32[]{:S(2)}, u32[]{:S(2)}) collective-permute-start(bf16[1024,128]{1,0:T(8,128)(2,1)S(1)} %collective-permute-done.14.refs_12_.refs_10_), channel_id=1, source_target_pairs={{0,1},{1,0},{2,3},{3,2},{4,5},{5,4},{6,7},{7,6},{8,9},{9,8},{10,11... | collective-permute-start | bytes 786440 | tf_op jit(solution)/shard_map/ppermute | solution.py:535
  78.0 2.8 %collective-permute-start.2 = (bf16[136,1024]{1,0:T(8,128)(2,1)S(1)}, bf16[136,1024]{1,0:T(8,128)(2,1)S(1)}, u32[]{:S(2)}, u32[]{:S(2)}) collective-permute-start(bf16[136,1024]{1,0:T(8,128)(2,1)S(1)} %collective-permute-done.refs_0_), channel_id=1, source_target_pairs={{8,12},{9,13},{10,14},{11,15},{24,28},{25,29},{26,30},{27,31}} | collective-permute-start | bytes 835592 | tf_op jit(solution)/shard_map/ppermute | solution.py:566
  78.7 1.6 %collective-permute-start.22 = (bf16[64,2048]{1,0:T(8,128)(2,1)S(1)}, bf16[64,2048]{1,0:T(8,128)(2,1)S(1)}, u32[]{:S(2)}, u32[]{:S(2)}) collective-permute-start(bf16[64,2048]{1,0:T(8,128)(2,1)S(1)} %collective-permute-done.15.refs_13_.refs_11_), channel_id=1, source_target_pairs={{0,1},{1,0},{2,3},{3,2},{4,5},{5,4},{6,7},{7,6},{8,9},{9,8},{10,11... | collective-permute-start | bytes 786440 | tf_op jit(solution)/shard_map/ppermute | solution.py:535
  78.8 1.9 %collective-permute-start.24 = (bf16[64,2048]{1,0:T(8,128)(2,1)S(1)}, bf16[64,2048]{1,0:T(8,128)(2,1)S(1)}, u32[]{:S(2)}, u32[]{:S(2)}) collective-permute-start(bf16[64,2048]{1,0:T(8,128)(2,1)S(1)} %collective-permute-done.17.refs_15_.refs_29_.refs_13_.refs_27_), channel_id=1, source_target_pairs={{0,1},{1,0},{2,3},{3,2},{4,5},{5,4},{6,7},{7,6},{8,9},{9,8},{10,11... | collective-permute-start | bytes 786440 | tf_op jit(solution)/shard_map/ppermute | solution.py:535
  79.3 1.9 %collective-permute-start.3 = (bf16[136,1024]{1,0:T(8,128)(2,1)S(1)}, bf16[136,1024]{1,0:T(8,128)(2,1)S(1)}, u32[]{:S(2)}, u32[]{:S(2)}) collective-permute-start(bf16[136,1024]{1,0:T(8,128)(2,1)S(1)} %collective-permute-done.1.refs_1_), channel_id=1, source_target_pairs={{8,12},{9,13},{10,14},{11,15},{24,28},{25,29},{26,30},{27,31}} | collective-permute-start | bytes 835592 | tf_op jit(solution)/shard_map/ppermute | solution.py:566
  80.0 1.6 %collective-permute-start.31 = (bf16[1024,128]{1,0:T(8,128)(2,1)S(1)}, bf16[1024,128]{1,0:T(8,128)(2,1)S(1)}, u32[]{:S(2)}, u32[]{:S(2)}) collective-permute-start(bf16[1024,128]{1,0:T(8,128)(2,1)S(1)} %collective-permute-done.25.refs_23_.refs_21_), channel_id=1, source_target_pairs={{0,1},{1,0},{2,3},{3,2},{4,5},{5,4},{6,7},{7,6},{8,9},{9,8},{10,11... | collective-permute-start | bytes 786440 | tf_op jit(solution)/shard_map/ppermute | solution.py:535
  80.3 20.4 %collective-permute-start.10 = (bf16[256,2048]{1,0:T(8,128)(2,1)S(1)}, bf16[256,2048]{1,0:T(8,128)(2,1)S(1)}, u32[]{:S(2)}, u32[]{:S(2)}) collective-permute-start(bf16[256,2048]{1,0:T(8,128)(2,1)S(1)} %bitcast.21), channel_id=1, source_target_pairs={{0,1},{1,0},{2,3},{3,2},{4,5},{5,4},{6,7},{7,6},{8,9},{9,8},{10,11... | collective-permute-start | bytes 3145736 | tf_op jit(solution)/shard_map/ppermute | solution.py:535
  80.7 20.1 %collective-permute-start.8 = (bf16[2048,256]{1,0:T(8,128)(2,1)S(1)}, bf16[2048,256]{1,0:T(8,128)(2,1)S(1)}, u32[]{:S(2)}, u32[]{:S(2)}) collective-permute-start(bf16[2048,256]{1,0:T(8,128)(2,1)S(1)} %bitcast.13), channel_id=1, source_target_pairs={{0,1},{1,0},{2,3},{3,2},{4,5},{5,4},{6,7},{7,6},{8,9},{9,8},{10,11... | collective-permute-start | bytes 3145736 | tf_op jit(solution)/shard_map/ppermute | solution.py:535
  80.8 20.0 %collective-permute-start.9 = (bf16[2048,256]{1,0:T(8,128)(2,1)S(1)}, bf16[2048,256]{1,0:T(8,128)(2,1)S(1)}, u32[]{:S(2)}, u32[]{:S(2)}) collective-permute-start(bf16[2048,256]{1,0:T(8,128)(2,1)S(1)} %bitcast.17), channel_id=1, source_target_pairs={{0,1},{1,0},{2,3},{3,2},{4,5},{5,4},{6,7},{7,6},{8,9},{9,8},{10,11... | collective-permute-start | bytes 3145736 | tf_op jit(solution)/shard_map/ppermute | solution.py:535
  81.2 5.2 %collective-permute-start.32 = (bf16[1024,128]{1,0:T(8,128)(2,1)S(1)}, bf16[1024,128]{1,0:T(8,128)(2,1)S(1)}, u32[]{:S(2)}, u32[]{:S(2)}) collective-permute-start(bf16[1024,128]{1,0:T(8,128)(2,1)S(1)} %collective-permute-done.26.refs_24_.refs_22_), channel_id=1, source_target_pairs={{0,1},{1,0},{2,3},{3,2},{4,5},{5,4},{6,7},{7,6},{8,9},{9,8},{10,11... | collective-permute-start | bytes 786440 | tf_op jit(solution)/shard_map/ppermute | solution.py:535
  81.6 5.2 %collective-permute-start.33 = (bf16[1024,128]{1,0:T(8,128)(2,1)S(1)}, bf16[1024,128]{1,0:T(8,128)(2,1)S(1)}, u32[]{:S(2)}, u32[]{:S(2)}) collective-permute-start(bf16[1024,128]{1,0:T(8,128)(2,1)S(1)} %collective-permute-done.27.refs_25_.refs_23_), channel_id=1, source_target_pairs={{0,1},{1,0},{2,3},{3,2},{4,5},{5,4},{6,7},{7,6},{8,9},{9,8},{10,11... | collective-permute-start | bytes 786440 | tf_op jit(solution)/shard_map/ppermute | solution.py:535
  86.5 1.5 %collective-permute-start.34 = (bf16[1024,128]{1,0:T(8,128)(2,1)S(1)}, bf16[1024,128]{1,0:T(8,128)(2,1)S(1)}, u32[]{:S(2)}, u32[]{:S(2)}) collective-permute-start(bf16[1024,128]{1,0:T(8,128)(2,1)S(1)} %collective-permute-done.28.refs_26_.refs_24_), channel_id=1, source_target_pairs={{0,1},{1,0},{2,3},{3,2},{4,5},{5,4},{6,7},{7,6},{8,9},{9,8},{10,11... | collective-permute-start | bytes 786440 | tf_op jit(solution)/shard_map/ppermute | solution.py:535
  86.8 1.5 %collective-permute-start.35 = (bf16[64,2048]{1,0:T(8,128)(2,1)S(1)}, bf16[64,2048]{1,0:T(8,128)(2,1)S(1)}, u32[]{:S(2)}, u32[]{:S(2)}) collective-permute-start(bf16[64,2048]{1,0:T(8,128)(2,1)S(1)} %collective-permute-done.29.refs_27_.refs_25_), channel_id=1, source_target_pairs={{0,1},{1,0},{2,3},{3,2},{4,5},{5,4},{6,7},{7,6},{8,9},{9,8},{10,11... | collective-permute-start | bytes 786440 | tf_op jit(solution)/shard_map/ppermute | solution.py:535
  88.0 18.8 %collective-permute-start.6 = (bf16[96,2048]{1,0:T(8,128)(2,1)S(1)}, bf16[96,2048]{1,0:T(8,128)(2,1)S(1)}, u32[]{:S(2)}, u32[]{:S(2)}) collective-permute-start(bf16[96,2048]{1,0:T(8,128)(2,1)S(1)} %get-tuple-element.31), channel_id=1, source_target_pairs={{0,4},{4,8},{8,12},{12,0},{1,5},{5,9},{9,13},{13,1},{2,6},{6,10},{... | collective-permute-start | bytes 1179656 | tf_op jit(solution)/shard_map/ppermute | solution.py:544
  88.4 23.5 %collective-permute-start.7 = (bf16[96,2048]{1,0:T(8,128)(2,1)S(1)}, bf16[96,2048]{1,0:T(8,128)(2,1)S(1)}, u32[]{:S(2)}, u32[]{:S(2)}) collective-permute-start(bf16[96,2048]{1,0:T(8,128)(2,1)S(1)} %get-tuple-element.32), channel_id=1, source_target_pairs={{0,12},{4,0},{8,4},{12,8},{1,13},{5,1},{9,5},{13,9},{2,14},{6,2},{... | collective-permute-start | bytes 1179656 | tf_op jit(solution)/shard_map/ppermute | solution.py:544
  96.1 1.6 %copy-start.3 = (bf16[512,2048]{1,0:T(8,128)(2,1)S(1)}, bf16[512,2048]{1,0:T(8,128)(2,1)}, u32[]{:S(2)}) copy-start(bf16[512,2048]{1,0:T(8,128)(2,1)} %refs_4_.1) | copy-start | bytes 6291460
  100.7 30.8 %collective-permute-start.4 = (bf16[64,2048]{1,0:T(8,128)(2,1)S(1)}, bf16[64,2048]{1,0:T(8,128)(2,1)S(1)}, u32[]{:S(2)}, u32[]{:S(2)}) collective-permute-start(bf16[64,2048]{1,0:T(8,128)(2,1)S(1)} %get-tuple-element.25), channel_id=1, source_target_pairs={{0,1},{1,0},{2,3},{3,2},{4,5},{5,4},{6,7},{7,6},{8,9},{9,8},{10,11... | collective-permute-start | bytes 786440 | tf_op jit(solution)/shard_map/ppermute | solution.py:535
  103.0 35.0 %collective-permute-start.39 = (bf16[96,2048]{1,0:T(8,128)(2,1)S(1)}, bf16[96,2048]{1,0:T(8,128)(2,1)S(1)}, u32[]{:S(2)}, u32[]{:S(2)}) collective-permute-start(bf16[96,2048]{1,0:T(8,128)(2,1)S(1)} %shard_map.146), channel_id=1, source_target_pairs={{0,8},{4,12},{8,0},{12,4},{1,9},{5,13},{9,1},{13,5},{2,10},{6,14},... | collective-permute-start | bytes 1179656 | tf_op jit(solution)/shard_map/ppermute | solution.py:544
  111.9 21.8 %copy-start.6 = (s32[128,2]{0,1:T(2,128)S(1)}, s32[128,2]{0,1:T(2,128)}, u32[]{:S(2)}) copy-start(s32[128,2]{0,1:T(2,128)} %param.21) | copy-start | bytes 3076
  111.9 21.8 %copy-start.7 = (f32[128,2]{0,1:T(2,128)S(1)}, f32[128,2]{0,1:T(2,128)}, u32[]{:S(2)}) copy-start(f32[128,2]{0,1:T(2,128)} %param.22) | copy-start | bytes 3076
  111.9 25.3 %copy-start.5 = (f32[2048]{0:T(1024)S(1)}, f32[2048]{0:T(1024)}, u32[]{:S(2)}) copy-start(f32[2048]{0:T(1024)} %param.18) | copy-start | bytes 24580
  115.8 31.5 %collective-permute-start.37 = (bf16[96,2048]{1,0:T(8,128)(2,1)S(1)}, bf16[96,2048]{1,0:T(8,128)(2,1)S(1)}, u32[]{:S(2)}, u32[]{:S(2)}) collective-permute-start(bf16[96,2048]{1,0:T(8,128)(2,1)S(1)} %get-tuple-element.41), channel_id=1, source_target_pairs={{0,12},{4,0},{8,4},{12,8},{1,13},{5,1},{9,5},{13,9},{2,14},{6,2},{... | collective-permute-start | bytes 1179656 | tf_op jit(solution)/shard_map/ppermute | solution.py:544
  119.2 28.0 %collective-permute-start.40 = (bf16[96,2048]{1,0:T(8,128)(2,1)S(1)}, bf16[96,2048]{1,0:T(8,128)(2,1)S(1)}, u32[]{:S(2)}, u32[]{:S(2)}) collective-permute-start(bf16[96,2048]{1,0:T(8,128)(2,1)S(1)} %get-tuple-element.43), channel_id=1, source_target_pairs={{0,4},{4,8},{8,12},{12,0},{1,5},{5,9},{9,13},{13,1},{2,6},{6,10},{... | collective-permute-start | bytes 1179656 | tf_op jit(solution)/shard_map/ppermute | solution.py:544
  132.2 5.0 %collective-permute-start.5 = (bf16[32,2048]{1,0:T(8,128)(2,1)S(1)}, bf16[32,2048]{1,0:T(8,128)(2,1)S(1)}, u32[]{:S(2)}, u32[]{:S(2)}) collective-permute-start(bf16[32,2048]{1,0:T(8,128)(2,1)S(1)} %get-tuple-element.27), channel_id=1, source_target_pairs={{0,2},{1,3},{2,0},{3,1},{4,6},{5,7},{6,4},{7,5},{8,10},{9,11},{10,... | collective-permute-start | bytes 393224 | tf_op jit(solution)/shard_map/ppermute | solution.py:538

commit v4 on v3

--- a/solution.py
+++ b/solution.py
@@ -213,47 +213,83 @@
     return hits, picks
 
 
-def prepare(place, moe_input, ffn_gain, ids, keys, values, bias, weights, experts, capacity):
-    rows, width = moe_input.shape
+def in_hbm(*arrays):
+    return [pltpu.with_memory_space_constraint(array, pltpu.HBM) for array in arrays]
+
+
+def start_all(moves, sems):
+    copies = [
+        pltpu.make_async_copy(source, target, sems.at[k]) for k, (source, target) in enumerate(moves)
+    ]
+    for copy in copies:
+        copy.start()
+    return copies
+
+
+def pack(place, keys, values, bias, gate):
     span, heads_width = keys.shape
     heads = bias.shape[0]
+    part = gate.shape[1] // 2
+    deep = gate.shape[0] // 2
+
+    def body(place_ref, bias_hbm, keys_hbm, values_hbm, gate_hbm, own_ref, gate_a, bias_v, sems):
+        columns = pl.ds(pl.multiple_of(place_ref[2] * part, part), part)
+        copies = start_all(
+            [
+                (bias_hbm, bias_v),
+                (gate_hbm.at[pl.ds(0, deep), columns], gate_a),
+                (keys_hbm, own_ref.at[pl.ds(0, span), pl.ds(0, heads_width)]),
+                (values_hbm, own_ref.at[pl.ds(0, span), pl.ds(heads_width, heads_width)]),
+            ],
+            sems,
+        )
+        own_ref[span:, :] = jnp.zeros((heads, 2 * heads_width), jnp.bfloat16)
+        copies[0].wait()
+        own_ref[span:, :span] = bias_v[...]
+        for copy in copies[1:]:
+            copy.wait()
+
+    return call(
+        body,
+        [shape_of((span + heads, 2 * heads_width)), shape_of((deep, part))],
+        [SMEM] + [HBM] * 4,
+        scratch=(pltpu.VMEM(bias.shape, jnp.bfloat16), pltpu.SemaphoreType.DMA((4,))),
+    )(place, *in_hbm(bias, keys, values, gate))
+
+
+def route(place, moe_input, ffn_gain, ids, weights, experts, capacity):
+    rows, width = moe_input.shape
     gate, upward, down = weights
     part = gate.shape[1] // 2
     deep = gate.shape[0] // 2
     thin = part // 2
     slim = part // 4
 
-    def body(place_ref, gain_hbm, ids_hbm, bias_hbm, input_hbm, keys_hbm, values_hbm, *refs):
-        gate_hbm, up_hbm, down_hbm = refs[:3]
-        outs = refs[3 : 3 + experts]
-        own_ref, gate_a, gate_b, up_a, up_b, down_a, down_b, down_c = refs[3 + experts : 11 + experts]
-        input_v, gain_v, ids_v, bias_v, sems = refs[11 + experts :]
+    def body(place_ref, gain_hbm, ids_hbm, input_hbm, gate_hbm, up_hbm, down_hbm, *refs):
+        outs = refs[:experts]
+        gate_b, up_a, up_b, down_a, down_b, down_c, input_v, gain_v, ids_v, sems = refs[experts:]
         begin = pl.multiple_of(place_ref[2] * part, part)
         beyond = pl.multiple_of((1 - place_ref[2]) * part, part)
         columns = pl.ds(begin, part)
-        moves = [
-            (ids_hbm, ids_v),
-            (input_hbm, input_v),
-            (gain_hbm, gain_v),
-            (bias_hbm, bias_v),
-            (gate_hbm.at[pl.ds(0, deep), columns], gate_a),
-            (gate_hbm.at[pl.ds(deep, deep), columns], gate_b),
-            (keys_hbm, own_ref.at[pl.ds(0, span), pl.ds(0, heads_width)]),
-            (values_hbm, own_ref.at[pl.ds(0, span), pl.ds(heads_width, heads_width)]),
-            (up_hbm.at[pl.ds(0, deep), columns], up_a),
-            (up_hbm.at[pl.ds(deep, deep), columns], up_b),
-            (down_hbm.at[pl.ds(begin, thin), :], down_a),
-            (down_hbm.at[pl.ds(pl.multiple_of(begin + thin, slim), slim), :], down_b),
-            (down_hbm.at[pl.ds(pl.multiple_of(begin + 3 * slim, slim), slim), :], down_c.at[pl.ds(0, slim), :]),
-            (down_hbm.at[pl.ds(pl.multiple_of(beyond + 3 * slim, slim), slim), :], down_c.at[pl.ds(slim, slim), :]),
-        ]
-        copies = [
-            pltpu.make_async_copy(source, target, sems.at[k])
-            for k, (source, target) in enumerate(moves)
-        ]
-        for copy in copies:
-            copy.start()
-        own_ref[span:, :] = jnp.zeros((heads, 2 * heads_width), jnp.bfloat16)
+
+        def some(first, size):
+            return down_hbm.at[pl.ds(pl.multiple_of(first, slim), size), :]
+
+        copies = start_all(
+            [
+                (ids_hbm, ids_v),
+                (input_hbm, input_v),
+                (gain_hbm, gain_v),
+                (gate_hbm.at[pl.ds(deep, deep), columns], gate_b),
+                (up_hbm.at[pl.ds(0, deep), columns], up_a),
+                (up_hbm.at[pl.ds(deep, deep), columns], up_b),
+                (some(begin, thin), down_a),
+                (some(begin + thin, slim), down_b),
+                (some(begin + 3 * slim, slim), down_c.at[pl.ds(0, slim), :]),
+                (some(beyond + 3 * slim, slim), down_c.at[pl.ds(slim, slim), :]),
+            ],
+            sems,
+        )
         copies[0].wait()
         _, picks = selections(place_ref, ids_v, experts, capacity)
         copies[1].wait()
@@ -263,14 +299,10 @@
             outs[d][...] = jnp.dot(
                 picks[d], normed, preferred_element_type=jnp.float32
             ).astype(jnp.bfloat16)
-        copies[3].wait()
-        own_ref[span:, :span] = bias_v[...]
-        for copy in copies[4:]:
+        for copy in copies[3:]:
             copy.wait()
 
     outs = [shape_of((capacity, width))] * experts + [
-        shape_of((span + heads, 2 * heads_width)),
-        shape_of((deep, part)),
         shape_of((deep, part)),
         shape_of((deep, part)),
         shape_of((deep, part)),
@@ -281,32 +313,15 @@
     return call(
         body,
         outs,
-        [SMEM] + [HBM] * 9,
+        [SMEM] + [HBM] * 6,
         scratch=(
             pltpu.VMEM((rows, width), jnp.bfloat16),
             pltpu.VMEM((1, width), jnp.float32),
             pltpu.VMEM(ids.shape, jnp.int32),
-            pltpu.VMEM(bias.shape, jnp.bfloat16),
-            pltpu.SemaphoreType.DMA((14,)),
+            pltpu.SemaphoreType.DMA((10,)),
         ),
         flops=2 * experts * capacity * rows * width,
-    )(
-        place,
-        *(
-            pltpu.with_memory_space_constraint(array, pltpu.HBM)
-            for array in (
-                ffn_gain.reshape(1, width),
-                ids,
-                bias,
-                moe_input,
-                keys,
-                values,
-                gate,
-                upward,
-                down,
-            )
-        ),
-    )
+    )(place, *in_hbm(ffn_gain.reshape(1, width), ids, moe_input, gate, upward, down))
 
 
 def combine_plan(place, ids, scores, experts, capacity):
@@ -549,10 +564,9 @@
     rows, top = expert_ids.shape
     capacity = 3 * rows * top // (2 * blocks)
     mine = (gate_weight[0], up_weight[0], down_weight[0])
-    prepared = prepare(
-        place, moe_input, ffn_gain, expert_ids.T, keys, values, stop_bias.T, mine, blocks, capacity
-    )
-    outbound, own, halves = prepared[:blocks], prepared[blocks], prepared[blocks + 1 :]
+    own, first_half = pack(place, keys, values, stop_bias.T, mine[0])
+    routed = route(place, moe_input, ffn_gain, expert_ids.T, mine, blocks, capacity)
+    outbound, halves = routed[:blocks], [first_half, *routed[blocks:]]
 
     arrived = [outbound[0]] + [turn(outbound[d], d) for d in range(1, blocks)]
 

time: 149 us -> 142 us (0.953)
  waiting for transfers between devices: 69.7 us -> 63 us
  starting transfers between devices: 61 us -> 58.8 us
  Pallas kernels: 15.5 us -> 17.1 us
    ppermute x8, waiting for transfers between devices: 24.6 us -> 16.2 us  [across(): return lax.ppermute(array, 'tp', [(i, i ^ 2) for i in range(shards)])]
    ppermute x6, starting transfers between devices: 30.4 us -> 25.9 us  [turn(): lax.ppermute(array, 'ep', [(i, (i + d) % blocks) for i in range(blocks)])]
    ppermute x8, starting transfers between devices: 10.7 us -> 12.7 us  [across(): return lax.ppermute(array, 'tp', [(i, i ^ 2) for i in range(shards)])]
    ppermute x6, waiting for transfers between devices: 20.9 us -> 22.7 us  [beside(): return lax.ppermute(array, 'grp', [(0, 1), (1, 0)])]
    pallas_call x1 -> x2, Pallas kernels: 2.8 us -> 4.37 us  [the longest x1 2.73 us: route(): call(body, outs, [SMEM] + [HBM] * 6, scratch=(pltpu.VMEM((rows, width), j...]
    ppermute x1, waiting for transfers between devices: 2.91 us -> 4.44 us  [paired_step(): passed = [upward(own, 1), lax.ppermute(own, 'ep', [(0, 2)])]]
  transfers between devices with their start and end apart: 41 -> 41, of which waited for: 22 -> 20; matrix products, arithmetic and copies ran while one was open for 0% -> 0% of each run, Pallas kernels for 8% -> 9%
where the time goes in v4:
time: 142 us; the launch traced here: 141 us
  waiting for transfers between devices  63 us (44%)
  starting transfers between devices  58.8 us (41%)
  Pallas kernels  17.1 us (12%)
  local copies, waits for them, and re-layouts  1.62 us (1%)
    ppermute x6, starting transfers between devices, turn(): lax.ppermute(array, 'ep', [(i, (i + d) % blocks) for i in range(blocks)])  25.9 us
    ppermute x6, waiting for transfers between devices, beside(): return lax.ppermute(array, 'grp', [(0, 1), (1, 0)])  22.7 us
    ppermute x8, waiting for transfers between devices, across(): return lax.ppermute(array, 'tp', [(i, i ^ 2) for i in range(shards)])  16.2 us
    ppermute x6, waiting for transfers between devices, turn(): lax.ppermute(array, 'ep', [(i, (i + d) % blocks) for i in range(blocks)])  13 us
    ppermute x8, starting transfers between devices, across(): return lax.ppermute(array, 'tp', [(i, i ^ 2) for i in range(shards)])  12.7 us
    ppermute x6, starting transfers between devices, beside(): return lax.ppermute(array, 'grp', [(0, 1), (1, 0)])  7.76 us
    ppermute x17, waiting for transfers between devices, core(): return lax.ppermute(array, 'tp', [(i, i ^ 1) for i in range(shards)])  6.57 us
    pallas_call x2, Pallas kernels, expert_rows(): call(body, [shape_of((capacity, width))] * count, [VMEM] * (count + len(f...  6.02 us
  transfers between devices with their start and end apart: 41, of which 20 were waited for; matrix products, arithmetic and copies ran while one was open for 0% of the time, Pallas kernels for 9%

profile of v4, /device:TPU:0, one launch (start us, length us, event | category | flops | bytes accessed | tf_op | source)
XLA Modules:
  0.0 141.3 jit_solution(9706119660461829092)
XLA Ops:
  0.6 0.1 pad_add_fusion.place_ref
  0.7 2.7 %shard_map.145 = (bf16[96,2048]{1,0:T(8,128)(2,1)S(1)}, bf16[96,2048]{1,0:T(8,128)(2,1)S(1)}, bf16[96,2048]{1,0:T(8,128)(2,1)S(1)}, bf16[96,2048]{1,0:T(8,128)(2...) custom-call(s32[4]{0:T(128)S(1)} %pad_add_fusion.place_ref, ...), custom_call_target="tpu_custom_call" | custom-call | flops 201326592 | tf_op jit(solution)/shard_map/pallas_call | solution.py:313
  3.5 3.0 %collective-permute-start.16 = (bf16[32,2048]{1,0:T(8,128)(2,1)S(1)}, bf16[32,2048]{1,0:T(8,128)(2,1)S(1)}, u32[]{:S(2)}, u32[]{:S(2)}) collective-permute-start(bf16[32,2048]{1,0:T(8,128)(2,1)S(1)} %get-tuple-element.38), channel_id=1, source_target_pairs={{0,2},{1,3},{2,0},{3,1},{4,6},{5,7},{6,4},{7,5},{8,10},{9,11},{10,... | collective-permute-start | bytes 393224 | tf_op jit(solution)/shard_map/ppermute | solution.py:553
  6.5 0.1 collective-permute-start.12
  6.6 1.9 %collective-permute-start.13 = (bf16[1024,128]{1,0:T(8,128)(2,1)S(1)}, bf16[1024,128]{1,0:T(8,128)(2,1)S(1)}, u32[]{:S(2)}, u32[]{:S(2)}) collective-permute-start(bf16[1024,128]{1,0:T(8,128)(2,1)S(1)} %get-tuple-element.35), channel_id=1, source_target_pairs={{0,2},{1,3},{2,0},{3,1},{4,6},{5,7},{6,4},{7,5},{8,10},{9,11},{10,... | collective-permute-start | bytes 786440 | tf_op jit(solution)/shard_map/ppermute | solution.py:553
  8.5 0.1 collective-permute-start.14
  8.6 1.9 %collective-permute-start.15 = (bf16[64,2048]{1,0:T(8,128)(2,1)S(1)}, bf16[64,2048]{1,0:T(8,128)(2,1)S(1)}, u32[]{:S(2)}, u32[]{:S(2)}) collective-permute-start(bf16[64,2048]{1,0:T(8,128)(2,1)S(1)} %get-tuple-element.37), channel_id=1, source_target_pairs={{0,2},{1,3},{2,0},{3,1},{4,6},{5,7},{6,4},{7,5},{8,10},{9,11},{10,... | collective-permute-start | bytes 786440 | tf_op jit(solution)/shard_map/ppermute | solution.py:553
  10.6 0.3 collective-permute-done.16.refs_14_.refs_12_
  10.9 2.0 %collective-permute-start.17 = (bf16[64,2048]{1,0:T(8,128)(2,1)S(1)}, bf16[64,2048]{1,0:T(8,128)(2,1)S(1)}, u32[]{:S(2)}, u32[]{:S(2)}) collective-permute-start(bf16[64,2048]{1,0:T(8,128)(2,1)S(1)} %get-tuple-element.39), channel_id=1, source_target_pairs={{0,2},{1,3},{2,0},{3,1},{4,6},{5,7},{6,4},{7,5},{8,10},{9,11},{10,... | collective-permute-start | bytes 786440 | tf_op jit(solution)/shard_map/ppermute | solution.py:553
  12.9 1.6 %shard_map.140 = (bf16[136,1024]{1,0:T(8,128)(2,1)S(1)}, bf16[1024,128]{1,0:T(8,128)(2,1)S(1)}) custom-call(s32[4]{0:T(128)S(1)} %pad_add_fusion.place_ref, bf16[8,128]{1,0:T(8,128)(2,1)} %bitcast.30, bf16[128,512]{1,0:T(8,128)(2,1)} %keys_hbm.1, bf16[128,512]{1,0:T(8,128)(2,1)} %values_hbm.1, bf16[2048,256]{1,0:T(8,128)(2,1)} %bitcast.13), custom_call_target="tpu_custom_call" | custom-call | tf_op jit(solution)/shard_map/pallas_call | solution.py:252
  14.5 2.0 %collective-permute-done.12.refs_10_.refs_8_ = bf16[1024,128]{1,0:T(8,128)(2,1)S(1)} collective-permute-done((bf16[1024,128]{1,0:T(8,128)(2,1)S(1)}, bf16[1024,128]{1,0:T(8,128)(2,1)S(1)}, u32[]{:S(2)}, u32[]{:S(2)}) %collective-permute-start.12) | collective-permute-done | bytes 262176 | tf_op jit(solution)/shard_map/ppermute | solution.py:553
  16.5 2.0 %collective-permute-start.11 = (bf16[1024,128]{1,0:T(8,128)(2,1)S(1)}, bf16[1024,128]{1,0:T(8,128)(2,1)S(1)}, u32[]{:S(2)}, u32[]{:S(2)}) collective-permute-start(bf16[1024,128]{1,0:T(8,128)(2,1)S(1)} %get-tuple-element.33), channel_id=1, source_target_pairs={{0,2},{1,3},{2,0},{3,1},{4,6},{5,7},{6,4},{7,5},{8,10},{9,11},{10,... | collective-permute-start | bytes 786440 | tf_op jit(solution)/shard_map/ppermute | solution.py:553
  18.5 3.6 %collective-permute-done.13.refs_11_.refs_9_ = bf16[1024,128]{1,0:T(8,128)(2,1)S(1)} collective-permute-done((bf16[1024,128]{1,0:T(8,128)(2,1)S(1)}, bf16[1024,128]{1,0:T(8,128)(2,1)S(1)}, u32[]{:S(2)}, u32[]{:S(2)}) %collective-permute-start.13) | collective-permute-done | bytes 262176 | tf_op jit(solution)/shard_map/ppermute | solution.py:553
  22.1 2.1 %collective-permute-start.30 = (bf16[32,2048]{1,0:T(8,128)(2,1)S(1)}, bf16[32,2048]{1,0:T(8,128)(2,1)S(1)}, u32[]{:S(2)}, u32[]{:S(2)}) collective-permute-start(bf16[32,2048]{1,0:T(8,128)(2,1)S(1)} %collective-permute-done.16.refs_14_.refs_12_), channel_id=1, source_target_pairs={{0,16},{16,0},{1,17},{17,1},{2,18},{18,2},{3,19},{19,3},{4,20},{20... | collective-permute-start | bytes 393224 | tf_op jit(solution)/shard_map/ppermute | solution.py:556
  24.2 3.6 %collective-permute-done.14.refs_12_.refs_10_ = bf16[1024,128]{1,0:T(8,128)(2,1)S(1)} collective-permute-done((bf16[1024,128]{1,0:T(8,128)(2,1)S(1)}, bf16[1024,128]{1,0:T(8,128)(2,1)S(1)}, u32[]{:S(2)}, u32[]{:S(2)}) %collective-permute-start.14) | collective-permute-done | bytes 262176 | tf_op jit(solution)/shard_map/ppermute | solution.py:553
  27.7 4.0 %collective-permute-start = (bf16[136,1024]{1,0:T(8,128)(2,1)S(1)}, bf16[136,1024]{1,0:T(8,128)(2,1)S(1)}, u32[]{:S(2)}, u32[]{:S(2)}) collective-permute-start(bf16[136,1024]{1,0:T(8,128)(2,1)S(1)} %get-tuple-element.23.own_ref), channel_id=1, source_target_pairs={{0,4},{4,8},{8,12},{1,5},{5,9},{9,13},{2,6},{6,10},{10,14},{3,7},{... | collective-permute-start | bytes 835592 | tf_op jit(solution)/shard_map/ppermute | solution.py:562
  31.7 1.6 %collective-permute-done.15.refs_13_.refs_11_ = bf16[64,2048]{1,0:T(8,128)(2,1)S(1)} collective-permute-done((bf16[64,2048]{1,0:T(8,128)(2,1)S(1)}, bf16[64,2048]{1,0:T(8,128)(2,1)S(1)}, u32[]{:S(2)}, u32[]{:S(2)}) %collective-permute-start.15) | collective-permute-done | bytes 262176 | tf_op jit(solution)/shard_map/ppermute | solution.py:553
  33.3 3.1 %collective-permute-start.38 = (bf16[96,2048]{1,0:T(8,128)(2,1)S(1)}, bf16[96,2048]{1,0:T(8,128)(2,1)S(1)}, u32[]{:S(2)}, u32[]{:S(2)}) collective-permute-start(bf16[96,2048]{1,0:T(8,128)(2,1)S(1)} %get-tuple-element.42), channel_id=1, source_target_pairs={{0,8},{4,12},{8,0},{12,4},{1,9},{5,13},{9,1},{13,5},{2,10},{6,14},... | collective-permute-start | bytes 1179656 | tf_op jit(solution)/shard_map/ppermute | solution.py:559
  36.5 2.5 %collective-permute-done.17.refs_15_.refs_29_.refs_13_.refs_27_ = bf16[64,2048]{1,0:T(8,128)(2,1)S(1)} collective-permute-done((bf16[64,2048]{1,0:T(8,128)(2,1)S(1)}, bf16[64,2048]{1,0:T(8,128)(2,1)S(1)}, u32[]{:S(2)}, u32[]{:S(2)}) %collective-permute-start.17) | collective-permute-done | bytes 262176 | tf_op jit(solution)/shard_map/ppermute | solution.py:553
  39.0 5.0 %collective-permute-start.1 = (bf16[136,1024]{1,0:T(8,128)(2,1)S(1)}, bf16[136,1024]{1,0:T(8,128)(2,1)S(1)}, u32[]{:S(2)}, u32[]{:S(2)}) collective-permute-start(bf16[136,1024]{1,0:T(8,128)(2,1)S(1)} %get-tuple-element.23.own_ref), channel_id=1, source_target_pairs={{0,8},{1,9},{2,10},{3,11},{16,24},{17,25},{18,26},{19,27}} | collective-permute-start | bytes 835592 | tf_op jit(solution)/shard_map/ppermute | solution.py:579
  44.0 1.6 %collective-permute-start.26 = (bf16[1024,128]{1,0:T(8,128)(2,1)S(1)}, bf16[1024,128]{1,0:T(8,128)(2,1)S(1)}, u32[]{:S(2)}, u32[]{:S(2)}) collective-permute-start(bf16[1024,128]{1,0:T(8,128)(2,1)S(1)} %collective-permute-done.12.refs_10_.refs_8_), channel_id=1, source_target_pairs={{0,16},{16,0},{1,17},{17,1},{2,18},{18,2},{3,19},{19,3},{4,20},{20... | collective-permute-start | bytes 786440 | tf_op jit(solution)/shard_map/ppermute | solution.py:556
  45.6 0.0 collective-permute-done.11.refs_9_.refs_7_
  45.6 0.5 collective-permute-start.27
  46.1 4.4 %collective-permute-done.1.refs_1_ = bf16[136,1024]{1,0:T(8,128)(2,1)S(1)} collective-permute-done((bf16[136,1024]{1,0:T(8,128)(2,1)S(1)}, bf16[136,1024]{1,0:T(8,128)(2,1)S(1)}, u32[]{:S(2)}, u32[]{:S(2)}) %collective-permute-start.1) | collective-permute-done | bytes 278560 | tf_op jit(solution)/shard_map/ppermute | solution.py:579
  50.5 1.5 %collective-permute-start.28 = (bf16[1024,128]{1,0:T(8,128)(2,1)S(1)}, bf16[1024,128]{1,0:T(8,128)(2,1)S(1)}, u32[]{:S(2)}, u32[]{:S(2)}) collective-permute-start(bf16[1024,128]{1,0:T(8,128)(2,1)S(1)} %collective-permute-done.14.refs_12_.refs_10_), channel_id=1, source_target_pairs={{0,16},{16,0},{1,17},{17,1},{2,18},{18,2},{3,19},{19,3},{4,20},{20... | collective-permute-start | bytes 786440 | tf_op jit(solution)/shard_map/ppermute | solution.py:556
  52.1 0.5 collective-permute-start.29
  52.6 0.7 collective-permute-done.26.refs_24_.refs_22_
  53.3 5.6 %collective-permute-done.27.refs_25_.refs_23_ = bf16[1024,128]{1,0:T(8,128)(2,1)S(1)} collective-permute-done((bf16[1024,128]{1,0:T(8,128)(2,1)S(1)}, bf16[1024,128]{1,0:T(8,128)(2,1)S(1)}, u32[]{:S(2)}, u32[]{:S(2)}) %collective-permute-start.27) | collective-permute-done | bytes 262176 | tf_op jit(solution)/shard_map/ppermute | solution.py:556
  58.9 5.6 %collective-permute-done.28.refs_26_.refs_24_ = bf16[1024,128]{1,0:T(8,128)(2,1)S(1)} collective-permute-done((bf16[1024,128]{1,0:T(8,128)(2,1)S(1)}, bf16[1024,128]{1,0:T(8,128)(2,1)S(1)}, u32[]{:S(2)}, u32[]{:S(2)}) %collective-permute-start.28) | collective-permute-done | bytes 262176 | tf_op jit(solution)/shard_map/ppermute | solution.py:556
  64.5 4.9 %collective-permute-done.29.refs_27_.refs_25_ = bf16[64,2048]{1,0:T(8,128)(2,1)S(1)} collective-permute-done((bf16[64,2048]{1,0:T(8,128)(2,1)S(1)}, bf16[64,2048]{1,0:T(8,128)(2,1)S(1)}, u32[]{:S(2)}, u32[]{:S(2)}) %collective-permute-start.29) | collective-permute-done | bytes 262176 | tf_op jit(solution)/shard_map/ppermute | solution.py:556
  69.4 0.7 collective-permute-start.2
  70.1 1.6 %collective-permute-start.25 = (bf16[1024,128]{1,0:T(8,128)(2,1)S(1)}, bf16[1024,128]{1,0:T(8,128)(2,1)S(1)}, u32[]{:S(2)}, u32[]{:S(2)}) collective-permute-start(bf16[1024,128]{1,0:T(8,128)(2,1)S(1)} %collective-permute-done.11.refs_9_.refs_7_), channel_id=1, source_target_pairs={{0,16},{16,0},{1,17},{17,1},{2,18},{18,2},{3,19},{19,3},{4,20},{20... | collective-permute-start | bytes 786440 | tf_op jit(solution)/shard_map/ppermute | solution.py:556
  71.6 0.2 collective-permute-start.18
  71.9 0.7 collective-permute-start.3
  72.6 0.3 collective-permute-start.32
  72.9 5.9 %collective-permute-done.25.refs_23_.refs_21_ = bf16[1024,128]{1,0:T(8,128)(2,1)S(1)} collective-permute-done((bf16[1024,128]{1,0:T(8,128)(2,1)S(1)}, bf16[1024,128]{1,0:T(8,128)(2,1)S(1)}, u32[]{:S(2)}, u32[]{:S(2)}) %collective-permute-start.25) | collective-permute-done | bytes 262176 | tf_op jit(solution)/shard_map/ppermute | solution.py:556
  78.9 0.5 collective-permute-start.10
  79.4 0.1 collective-permute-start.9
  79.5 0.4 collective-permute-start.33
  79.9 0.1 collective-permute-start.34
  80.0 4.9 %collective-permute-done.33.refs_32_.refs_30_ = bf16[1024,128]{1,0:T(8,128)(2,1)S(1)} collective-permute-done((bf16[1024,128]{1,0:T(8,128)(2,1)S(1)}, bf16[1024,128]{1,0:T(8,128)(2,1)S(1)}, u32[]{:S(2)}, u32[]{:S(2)}) %collective-permute-start.33) | collective-permute-done | bytes 262176 | tf_op jit(solution)/shard_map/ppermute | solution.py:550
  84.9 0.1 collective-permute-start.35
  85.0 0.2 collective-permute-done.34.refs_33_.refs_31_
  85.3 0.1 collective-permute-start.31
  85.4 1.0 collective-permute-done.35.refs_34_.refs_32_
  86.4 0.4 collective-permute-done.31.refs_30_.refs_28_
  86.8 3.5 %collective-permute-start.7 = (bf16[96,2048]{1,0:T(8,128)(2,1)S(1)}, bf16[96,2048]{1,0:T(8,128)(2,1)S(1)}, u32[]{:S(2)}, u32[]{:S(2)}) collective-permute-start(bf16[96,2048]{1,0:T(8,128)(2,1)S(1)} %get-tuple-element.32), channel_id=1, source_target_pairs={{0,12},{4,0},{8,4},{12,8},{1,13},{5,1},{9,5},{13,9},{2,14},{6,2},{... | collective-permute-start | bytes 1179656 | tf_op jit(solution)/shard_map/ppermute | solution.py:559
  90.2 1.6 %copy-done.3 = bf16[512,2048]{1,0:T(8,128)(2,1)S(1)} copy-done((bf16[512,2048]{1,0:T(8,128)(2,1)S(1)}, bf16[512,2048]{1,0:T(8,128)(2,1)}, u32[]{:S(2)}) %copy-start.3) | copy-done | bytes 2097176
  91.8 3.1 %shard_map.141 = (bf16[64,2048]{1,0:T(8,128)(2,1)S(1)}, f32[64,2048]{1,0:T(8,128)S(1)}) custom-call(s32[4]{0:T(128)S(1)} %pad_add_fusion.place_ref, bf16[128,512]{1,0:T(8,128)(2,1)S(1)} %copy-done.4, bf16[136,1024]{1,0:T(8,128)(2,1)S(1)} %get-tuple-element.23.own_ref, bf16[136,1024]{1,0:T(8,128)(2,1)S(1)} %collective-permute-done.refs_0_, ...), custom_call_target="tpu_custom_call" | custom-call | flops 402653184 | tf_op jit(solution)/shard_map/pallas_call | solution.py:507
  94.9 0.1 collective-permute-start.4
  95.0 2.2 %shard_map.147 = bf16[96,2048]{1,0:T(8,128)(2,1)S(1)} custom-call(bf16[96,2048]{1,0:T(8,128)(2,1)S(1)} %collective-permute-done.38.refs_0_, bf16[2048,256]{1,0:T(8,128)(2,1)S(1)} %bitcast.15, bf16[2048,256]{1,0:T(8,128)(2,1)S(1)} %bitcast.19, bf16[256,2048]{1,0:T(8,128)(2,1)S(1)} %bitcast.23, bf16[2048,256]{1,0:T(8,128)(2,1)S(1)} %collective-permute-done.8.refs_6_.refs_4_, ...), custom_call_target="tpu_custom_call" | custom-call | flops 1207959552 | tf_op jit(solution)/shard_map/pallas_call | solution.py:397
  97.2 3.6 %collective-permute-start.39 = (bf16[96,2048]{1,0:T(8,128)(2,1)S(1)}, bf16[96,2048]{1,0:T(8,128)(2,1)S(1)}, u32[]{:S(2)}, u32[]{:S(2)}) collective-permute-start(bf16[96,2048]{1,0:T(8,128)(2,1)S(1)} %shard_map.147), channel_id=1, source_target_pairs={{0,8},{4,12},{8,0},{12,4},{1,9},{5,13},{9,1},{13,5},{2,10},{6,14},... | collective-permute-start | bytes 1179656 | tf_op jit(solution)/shard_map/ppermute | solution.py:559
  100.8 5.6 %collective-permute-done.7.refs_2_ = bf16[96,2048]{1,0:T(8,128)(2,1)S(1)} collective-permute-done((bf16[96,2048]{1,0:T(8,128)(2,1)S(1)}, bf16[96,2048]{1,0:T(8,128)(2,1)S(1)}, u32[]{:S(2)}, u32[]{:S(2)}) %collective-permute-start.7) | collective-permute-done | bytes 393248 | tf_op jit(solution)/shard_map/ppermute | solution.py:559
  106.4 3.8 %shard_map.146 = (bf16[96,2048]{1,0:T(8,128)(2,1)S(1)}, bf16[96,2048]{1,0:T(8,128)(2,1)S(1)}, bf16[96,2048]{1,0:T(8,128)(2,1)S(1)}) custom-call(bf16[96,2048]{1,0:T(8,128)(2,1)S(1)} %get-tuple-element.30.refs_0_, bf16[96,2048]{1,0:T(8,128)(2,1)S(1)} %collective-permute-done.6.refs_1_, bf16[96,2048]{1,0:T(8,128)(2,1)S(1)} %collective-permute-done.7.refs_2_, ...), custom_call_target="tpu_custom_call" | custom-call | flops 3623878656 | tf_op jit(solution)/shard_map/pallas_call | solution.py:397
  110.2 2.9 %collective-permute-start.37 = (bf16[96,2048]{1,0:T(8,128)(2,1)S(1)}, bf16[96,2048]{1,0:T(8,128)(2,1)S(1)}, u32[]{:S(2)}, u32[]{:S(2)}) collective-permute-start(bf16[96,2048]{1,0:T(8,128)(2,1)S(1)} %get-tuple-element.41), channel_id=1, source_target_pairs={{0,12},{4,0},{8,4},{12,8},{1,13},{5,1},{9,5},{13,9},{2,14},{6,2},{... | collective-permute-start | bytes 1179656 | tf_op jit(solution)/shard_map/ppermute | solution.py:559
  113.2 12.8 %collective-permute-start.40 = (bf16[96,2048]{1,0:T(8,128)(2,1)S(1)}, bf16[96,2048]{1,0:T(8,128)(2,1)S(1)}, u32[]{:S(2)}, u32[]{:S(2)}) collective-permute-start(bf16[96,2048]{1,0:T(8,128)(2,1)S(1)} %get-tuple-element.43), channel_id=1, source_target_pairs={{0,4},{4,8},{8,12},{12,0},{1,5},{5,9},{9,13},{13,1},{2,6},{6,10},{... | collective-permute-start | bytes 1179656 | tf_op jit(solution)/shard_map/ppermute | solution.py:559
  125.9 0.6 shard_map.142
  126.5 1.6 %collective-permute-start.5 = (bf16[32,2048]{1,0:T(8,128)(2,1)S(1)}, bf16[32,2048]{1,0:T(8,128)(2,1)S(1)}, u32[]{:S(2)}, u32[]{:S(2)}) collective-permute-start(bf16[32,2048]{1,0:T(8,128)(2,1)S(1)} %get-tuple-element.27), channel_id=1, source_target_pairs={{0,2},{1,3},{2,0},{3,1},{4,6},{5,7},{6,4},{7,5},{8,10},{9,11},{10,... | collective-permute-start | bytes 393224 | tf_op jit(solution)/shard_map/ppermute | solution.py:553
  128.1 0.7 shard_map.144
  128.9 2.7 %collective-permute-done.5.received_ref = bf16[32,2048]{1,0:T(8,128)(2,1)S(1)} collective-permute-done((bf16[32,2048]{1,0:T(8,128)(2,1)S(1)}, bf16[32,2048]{1,0:T(8,128)(2,1)S(1)}, u32[]{:S(2)}, u32[]{:S(2)}) %collective-permute-start.5) | collective-permute-done | bytes 131104 | tf_op jit(solution)/shard_map/ppermute | solution.py:553
  131.6 0.8 shard_map.143
  132.4 2.2 %collective-permute-done.37.refs_1_ = bf16[96,2048]{1,0:T(8,128)(2,1)S(1)} collective-permute-done((bf16[96,2048]{1,0:T(8,128)(2,1)S(1)}, bf16[96,2048]{1,0:T(8,128)(2,1)S(1)}, u32[]{:S(2)}, u32[]{:S(2)}) %collective-permute-start.37) | collective-permute-done | bytes 393248 | tf_op jit(solution)/shard_map/ppermute | solution.py:559
  134.6 5.2 %collective-permute-done.40.refs_3_ = bf16[96,2048]{1,0:T(8,128)(2,1)S(1)} collective-permute-done((bf16[96,2048]{1,0:T(8,128)(2,1)S(1)}, bf16[96,2048]{1,0:T(8,128)(2,1)S(1)}, u32[]{:S(2)}, u32[]{:S(2)}) %collective-permute-start.40) | collective-permute-done | bytes 393248 | tf_op jit(solution)/shard_map/ppermute | solution.py:559
  139.8 1.5 %shard_map.148 = bf16[128,2048]{1,0:T(8,128)(2,1)} custom-call(bf16[384,128]{1,0:T(8,128)(2,1)S(1)} %get-tuple-element.28.high_ref, bf16[384,128]{1,0:T(8,128)(2,1)S(1)} %get-tuple-element.29.low_ref, bf16[96,2048]{1,0:T(8,128)(2,1)S(1)} %get-tuple-element.40.refs_0_, bf16[96,2048]{1,0:T(8,128)(2,1)S(1)} %collective-permute-done.37.refs_1_, ...), custom_call_target="tpu_custom_call" | custom-call | flops 402653184 | tf_op jit(solution)/shard_map/pallas_call | solution.py:360
  (44 shorter events, 0.1 us)
Async XLA Ops:
  0.7 78.1 %copy-start = (bf16[1,2048,256]{2,1,0:T(8,128)(2,1)S(1)}, bf16[1,2048,256]{2,1,0:T(8,128)(2,1)}, u32[]{:S(2)}) copy-start(bf16[1,2048,256]{2,1,0:T(8,128)(2,1)} %param.23) | copy-start | bytes 3145732
  0.7 78.1 %copy-start.2 = (bf16[1,256,2048]{2,1,0:T(8,128)(2,1)S(1)}, bf16[1,256,2048]{2,1,0:T(8,128)(2,1)}, u32[]{:S(2)}) copy-start(bf16[1,256,2048]{2,1,0:T(8,128)(2,1)} %param.25) | copy-start | bytes 3145732
  0.7 78.6 %copy-start.1 = (bf16[1,2048,256]{2,1,0:T(8,128)(2,1)S(1)}, bf16[1,2048,256]{2,1,0:T(8,128)(2,1)}, u32[]{:S(2)}) copy-start(bf16[1,2048,256]{2,1,0:T(8,128)(2,1)} %param.24) | copy-start | bytes 3145732
  0.7 89.5 %copy-start.4 = (bf16[128,512]{1,0:T(8,128)(2,1)S(1)}, bf16[128,512]{1,0:T(8,128)(2,1)}, u32[]{:S(2)}) copy-start(bf16[128,512]{1,0:T(8,128)(2,1)} %q_ref.1) | copy-start | bytes 393220
  3.5 7.4 %collective-permute-start.16 = (bf16[32,2048]{1,0:T(8,128)(2,1)S(1)}, bf16[32,2048]{1,0:T(8,128)(2,1)S(1)}, u32[]{:S(2)}, u32[]{:S(2)}) collective-permute-start(bf16[32,2048]{1,0:T(8,128)(2,1)S(1)} %get-tuple-element.38), channel_id=1, source_target_pairs={{0,2},{1,3},{2,0},{3,1},{4,6},{5,7},{6,4},{7,5},{8,10},{9,11},{10,... | collective-permute-start | bytes 393224 | tf_op jit(solution)/shard_map/ppermute | solution.py:553
  6.5 10.0 %collective-permute-start.12 = (bf16[1024,128]{1,0:T(8,128)(2,1)S(1)}, bf16[1024,128]{1,0:T(8,128)(2,1)S(1)}, u32[]{:S(2)}, u32[]{:S(2)}) collective-permute-start(bf16[1024,128]{1,0:T(8,128)(2,1)S(1)} %get-tuple-element.34), channel_id=1, source_target_pairs={{0,2},{1,3},{2,0},{3,1},{4,6},{5,7},{6,4},{7,5},{8,10},{9,11},{10,... | collective-permute-start | bytes 786440 | tf_op jit(solution)/shard_map/ppermute | solution.py:553
  6.6 15.5 %collective-permute-start.13 = (bf16[1024,128]{1,0:T(8,128)(2,1)S(1)}, bf16[1024,128]{1,0:T(8,128)(2,1)S(1)}, u32[]{:S(2)}, u32[]{:S(2)}) collective-permute-start(bf16[1024,128]{1,0:T(8,128)(2,1)S(1)} %get-tuple-element.35), channel_id=1, source_target_pairs={{0,2},{1,3},{2,0},{3,1},{4,6},{5,7},{6,4},{7,5},{8,10},{9,11},{10,... | collective-permute-start | bytes 786440 | tf_op jit(solution)/shard_map/ppermute | solution.py:553
  8.5 19.2 %collective-permute-start.14 = (bf16[1024,128]{1,0:T(8,128)(2,1)S(1)}, bf16[1024,128]{1,0:T(8,128)(2,1)S(1)}, u32[]{:S(2)}, u32[]{:S(2)}) collective-permute-start(bf16[1024,128]{1,0:T(8,128)(2,1)S(1)} %get-tuple-element.36), channel_id=1, source_target_pairs={{0,2},{1,3},{2,0},{3,1},{4,6},{5,7},{6,4},{7,5},{8,10},{9,11},{10,... | collective-permute-start | bytes 786440 | tf_op jit(solution)/shard_map/ppermute | solution.py:553
  8.6 24.7 %collective-permute-start.15 = (bf16[64,2048]{1,0:T(8,128)(2,1)S(1)}, bf16[64,2048]{1,0:T(8,128)(2,1)S(1)}, u32[]{:S(2)}, u32[]{:S(2)}) collective-permute-start(bf16[64,2048]{1,0:T(8,128)(2,1)S(1)} %get-tuple-element.37), channel_id=1, source_target_pairs={{0,2},{1,3},{2,0},{3,1},{4,6},{5,7},{6,4},{7,5},{8,10},{9,11},{10,... | collective-permute-start | bytes 786440 | tf_op jit(solution)/shard_map/ppermute | solution.py:553
  10.9 28.1 %collective-permute-start.17 = (bf16[64,2048]{1,0:T(8,128)(2,1)S(1)}, bf16[64,2048]{1,0:T(8,128)(2,1)S(1)}, u32[]{:S(2)}, u32[]{:S(2)}) collective-permute-start(bf16[64,2048]{1,0:T(8,128)(2,1)S(1)} %get-tuple-element.39), channel_id=1, source_target_pairs={{0,2},{1,3},{2,0},{3,1},{4,6},{5,7},{6,4},{7,5},{8,10},{9,11},{10,... | collective-permute-start | bytes 786440 | tf_op jit(solution)/shard_map/ppermute | solution.py:553
  16.5 29.1 %collective-permute-start.11 = (bf16[1024,128]{1,0:T(8,128)(2,1)S(1)}, bf16[1024,128]{1,0:T(8,128)(2,1)S(1)}, u32[]{:S(2)}, u32[]{:S(2)}) collective-permute-start(bf16[1024,128]{1,0:T(8,128)(2,1)S(1)} %get-tuple-element.33), channel_id=1, source_target_pairs={{0,2},{1,3},{2,0},{3,1},{4,6},{5,7},{6,4},{7,5},{8,10},{9,11},{10,... | collective-permute-start | bytes 786440 | tf_op jit(solution)/shard_map/ppermute | solution.py:553
  22.1 16.9 %collective-permute-start.30 = (bf16[32,2048]{1,0:T(8,128)(2,1)S(1)}, bf16[32,2048]{1,0:T(8,128)(2,1)S(1)}, u32[]{:S(2)}, u32[]{:S(2)}) collective-permute-start(bf16[32,2048]{1,0:T(8,128)(2,1)S(1)} %collective-permute-done.16.refs_14_.refs_12_), channel_id=1, source_target_pairs={{0,16},{16,0},{1,17},{17,1},{2,18},{18,2},{3,19},{19,3},{4,20},{20... | collective-permute-start | bytes 393224 | tf_op jit(solution)/shard_map/ppermute | solution.py:556
  27.7 18.4 %collective-permute-start = (bf16[136,1024]{1,0:T(8,128)(2,1)S(1)}, bf16[136,1024]{1,0:T(8,128)(2,1)S(1)}, u32[]{:S(2)}, u32[]{:S(2)}) collective-permute-start(bf16[136,1024]{1,0:T(8,128)(2,1)S(1)} %get-tuple-element.23.own_ref), channel_id=1, source_target_pairs={{0,4},{4,8},{8,12},{1,5},{5,9},{9,13},{2,6},{6,10},{10,14},{3,7},{... | collective-permute-start | bytes 835592 | tf_op jit(solution)/shard_map/ppermute | solution.py:562
  33.3 19.2 %collective-permute-start.38 = (bf16[96,2048]{1,0:T(8,128)(2,1)S(1)}, bf16[96,2048]{1,0:T(8,128)(2,1)S(1)}, u32[]{:S(2)}, u32[]{:S(2)}) collective-permute-start(bf16[96,2048]{1,0:T(8,128)(2,1)S(1)} %get-tuple-element.42), channel_id=1, source_target_pairs={{0,8},{4,12},{8,0},{12,4},{1,9},{5,13},{9,1},{13,5},{2,10},{6,14},... | collective-permute-start | bytes 1179656 | tf_op jit(solution)/shard_map/ppermute | solution.py:559
  39.0 5.0 %collective-permute-start.23 = (bf16[32,2048]{1,0:T(8,128)(2,1)S(1)}, bf16[32,2048]{1,0:T(8,128)(2,1)S(1)}, u32[]{:S(2)}, u32[]{:S(2)}) collective-permute-start(bf16[32,2048]{1,0:T(8,128)(2,1)S(1)} %collective-permute-done.16.refs_14_.refs_12_), channel_id=1, source_target_pairs={{0,1},{1,0},{2,3},{3,2},{4,5},{5,4},{6,7},{7,6},{8,9},{9,8},{10,11... | collective-permute-start | bytes 393224 | tf_op jit(solution)/shard_map/ppermute | solution.py:550
  39.0 11.6 %collective-permute-start.1 = (bf16[136,1024]{1,0:T(8,128)(2,1)S(1)}, bf16[136,1024]{1,0:T(8,128)(2,1)S(1)}, u32[]{:S(2)}, u32[]{:S(2)}) collective-permute-start(bf16[136,1024]{1,0:T(8,128)(2,1)S(1)} %get-tuple-element.23.own_ref), channel_id=1, source_target_pairs={{0,8},{1,9},{2,10},{3,11},{16,24},{17,25},{18,26},{19,27}} | collective-permute-start | bytes 835592 | tf_op jit(solution)/shard_map/ppermute | solution.py:579
  44.0 9.2 %collective-permute-start.26 = (bf16[1024,128]{1,0:T(8,128)(2,1)S(1)}, bf16[1024,128]{1,0:T(8,128)(2,1)S(1)}, u32[]{:S(2)}, u32[]{:S(2)}) collective-permute-start(bf16[1024,128]{1,0:T(8,128)(2,1)S(1)} %collective-permute-done.12.refs_10_.refs_8_), channel_id=1, source_target_pairs={{0,16},{16,0},{1,17},{17,1},{2,18},{18,2},{3,19},{19,3},{4,20},{20... | collective-permute-start | bytes 786440 | tf_op jit(solution)/shard_map/ppermute | solution.py:556
  45.6 13.3 %collective-permute-start.27 = (bf16[1024,128]{1,0:T(8,128)(2,1)S(1)}, bf16[1024,128]{1,0:T(8,128)(2,1)S(1)}, u32[]{:S(2)}, u32[]{:S(2)}) collective-permute-start(bf16[1024,128]{1,0:T(8,128)(2,1)S(1)} %collective-permute-done.13.refs_11_.refs_9_), channel_id=1, source_target_pairs={{0,16},{16,0},{1,17},{17,1},{2,18},{18,2},{3,19},{19,3},{4,20},{20... | collective-permute-start | bytes 786440 | tf_op jit(solution)/shard_map/ppermute | solution.py:556
  46.1 6.0 %collective-permute-start.36 = (bf16[32,2048]{1,0:T(8,128)(2,1)S(1)}, bf16[32,2048]{1,0:T(8,128)(2,1)S(1)}, u32[]{:S(2)}, u32[]{:S(2)}) collective-permute-start(bf16[32,2048]{1,0:T(8,128)(2,1)S(1)} %collective-permute-done.30.refs_28_.refs_26_), channel_id=1, source_target_pairs={{0,1},{1,0},{2,3},{3,2},{4,5},{5,4},{6,7},{7,6},{8,9},{9,8},{10,11... | collective-permute-start | bytes 393224 | tf_op jit(solution)/shard_map/ppermute | solution.py:550
  50.5 13.9 %collective-permute-start.28 = (bf16[1024,128]{1,0:T(8,128)(2,1)S(1)}, bf16[1024,128]{1,0:T(8,128)(2,1)S(1)}, u32[]{:S(2)}, u32[]{:S(2)}) collective-permute-start(bf16[1024,128]{1,0:T(8,128)(2,1)S(1)} %collective-permute-done.14.refs_12_.refs_10_), channel_id=1, source_target_pairs={{0,16},{16,0},{1,17},{17,1},{2,18},{18,2},{3,19},{19,3},{4,20},{20... | collective-permute-start | bytes 786440 | tf_op jit(solution)/shard_map/ppermute | solution.py:556
  52.1 17.3 %collective-permute-start.29 = (bf16[64,2048]{1,0:T(8,128)(2,1)S(1)}, bf16[64,2048]{1,0:T(8,128)(2,1)S(1)}, u32[]{:S(2)}, u32[]{:S(2)}) collective-permute-start(bf16[64,2048]{1,0:T(8,128)(2,1)S(1)} %collective-permute-done.15.refs_13_.refs_11_), channel_id=1, source_target_pairs={{0,16},{16,0},{1,17},{17,1},{2,18},{18,2},{3,19},{19,3},{4,20},{20... | collective-permute-start | bytes 786440 | tf_op jit(solution)/shard_map/ppermute | solution.py:556
  52.6 16.8 %collective-permute-start.19 = (bf16[1024,128]{1,0:T(8,128)(2,1)S(1)}, bf16[1024,128]{1,0:T(8,128)(2,1)S(1)}, u32[]{:S(2)}, u32[]{:S(2)}) collective-permute-start(bf16[1024,128]{1,0:T(8,128)(2,1)S(1)} %collective-permute-done.12.refs_10_.refs_8_), channel_id=1, source_target_pairs={{0,1},{1,0},{2,3},{3,2},{4,5},{5,4},{6,7},{7,6},{8,9},{9,8},{10,11... | collective-permute-start | bytes 786440 | tf_op jit(solution)/shard_map/ppermute | solution.py:550
  53.3 16.8 %collective-permute-start.20 = (bf16[1024,128]{1,0:T(8,128)(2,1)S(1)}, bf16[1024,128]{1,0:T(8,128)(2,1)S(1)}, u32[]{:S(2)}, u32[]{:S(2)}) collective-permute-start(bf16[1024,128]{1,0:T(8,128)(2,1)S(1)} %collective-permute-done.13.refs_11_.refs_9_), channel_id=1, source_target_pairs={{0,1},{1,0},{2,3},{3,2},{4,5},{5,4},{6,7},{7,6},{8,9},{9,8},{10,11... | collective-permute-start | bytes 786440 | tf_op jit(solution)/shard_map/ppermute | solution.py:550
  58.9 12.8 %collective-permute-start.21 = (bf16[1024,128]{1,0:T(8,128)(2,1)S(1)}, bf16[1024,128]{1,0:T(8,128)(2,1)S(1)}, u32[]{:S(2)}, u32[]{:S(2)}) collective-permute-start(bf16[1024,128]{1,0:T(8,128)(2,1)S(1)} %collective-permute-done.14.refs_12_.refs_10_), channel_id=1, source_target_pairs={{0,1},{1,0},{2,3},{3,2},{4,5},{5,4},{6,7},{7,6},{8,9},{9,8},{10,11... | collective-permute-start | bytes 786440 | tf_op jit(solution)/shard_map/ppermute | solution.py:550
  64.5 7.4 %collective-permute-start.22 = (bf16[64,2048]{1,0:T(8,128)(2,1)S(1)}, bf16[64,2048]{1,0:T(8,128)(2,1)S(1)}, u32[]{:S(2)}, u32[]{:S(2)}) collective-permute-start(bf16[64,2048]{1,0:T(8,128)(2,1)S(1)} %collective-permute-done.15.refs_13_.refs_11_), channel_id=1, source_target_pairs={{0,1},{1,0},{2,3},{3,2},{4,5},{5,4},{6,7},{7,6},{8,9},{9,8},{10,11... | collective-permute-start | bytes 786440 | tf_op jit(solution)/shard_map/ppermute | solution.py:550
  69.4 3.2 %collective-permute-start.24 = (bf16[64,2048]{1,0:T(8,128)(2,1)S(1)}, bf16[64,2048]{1,0:T(8,128)(2,1)S(1)}, u32[]{:S(2)}, u32[]{:S(2)}) collective-permute-start(bf16[64,2048]{1,0:T(8,128)(2,1)S(1)} %collective-permute-done.17.refs_15_.refs_29_.refs_13_.refs_27_), channel_id=1, source_target_pairs={{0,1},{1,0},{2,3},{3,2},{4,5},{5,4},{6,7},{7,6},{8,9},{9,8},{10,11... | collective-permute-start | bytes 786440 | tf_op jit(solution)/shard_map/ppermute | solution.py:550
  69.4 10.0 %collective-permute-start.2 = (bf16[136,1024]{1,0:T(8,128)(2,1)S(1)}, bf16[136,1024]{1,0:T(8,128)(2,1)S(1)}, u32[]{:S(2)}, u32[]{:S(2)}) collective-permute-start(bf16[136,1024]{1,0:T(8,128)(2,1)S(1)} %collective-permute-done.refs_0_), channel_id=1, source_target_pairs={{8,12},{9,13},{10,14},{11,15},{24,28},{25,29},{26,30},{27,31}} | collective-permute-start | bytes 835592 | tf_op jit(solution)/shard_map/ppermute | solution.py:580
  70.1 8.8 %collective-permute-start.25 = (bf16[1024,128]{1,0:T(8,128)(2,1)S(1)}, bf16[1024,128]{1,0:T(8,128)(2,1)S(1)}, u32[]{:S(2)}, u32[]{:S(2)}) collective-permute-start(bf16[1024,128]{1,0:T(8,128)(2,1)S(1)} %collective-permute-done.11.refs_9_.refs_7_), channel_id=1, source_target_pairs={{0,16},{16,0},{1,17},{17,1},{2,18},{18,2},{3,19},{19,3},{4,20},{20... | collective-permute-start | bytes 786440 | tf_op jit(solution)/shard_map/ppermute | solution.py:556
  71.6 7.2 %collective-permute-start.18 = (bf16[1024,128]{1,0:T(8,128)(2,1)S(1)}, bf16[1024,128]{1,0:T(8,128)(2,1)S(1)}, u32[]{:S(2)}, u32[]{:S(2)}) collective-permute-start(bf16[1024,128]{1,0:T(8,128)(2,1)S(1)} %collective-permute-done.11.refs_9_.refs_7_), channel_id=1, source_target_pairs={{0,1},{1,0},{2,3},{3,2},{4,5},{5,4},{6,7},{7,6},{8,9},{9,8},{10,11... | collective-permute-start | bytes 786440 | tf_op jit(solution)/shard_map/ppermute | solution.py:550
  71.9 7.6 %collective-permute-start.3 = (bf16[136,1024]{1,0:T(8,128)(2,1)S(1)}, bf16[136,1024]{1,0:T(8,128)(2,1)S(1)}, u32[]{:S(2)}, u32[]{:S(2)}) collective-permute-start(bf16[136,1024]{1,0:T(8,128)(2,1)S(1)} %collective-permute-done.1.refs_1_), channel_id=1, source_target_pairs={{8,12},{9,13},{10,14},{11,15},{24,28},{25,29},{26,30},{27,31}} | collective-permute-start | bytes 835592 | tf_op jit(solution)/shard_map/ppermute | solution.py:580
  72.6 7.3 %collective-permute-start.32 = (bf16[1024,128]{1,0:T(8,128)(2,1)S(1)}, bf16[1024,128]{1,0:T(8,128)(2,1)S(1)}, u32[]{:S(2)}, u32[]{:S(2)}) collective-permute-start(bf16[1024,128]{1,0:T(8,128)(2,1)S(1)} %collective-permute-done.26.refs_24_.refs_22_), channel_id=1, source_target_pairs={{0,1},{1,0},{2,3},{3,2},{4,5},{5,4},{6,7},{7,6},{8,9},{9,8},{10,11... | collective-permute-start | bytes 786440 | tf_op jit(solution)/shard_map/ppermute | solution.py:550
  78.8 16.1 %collective-permute-start.8 = (bf16[2048,256]{1,0:T(8,128)(2,1)S(1)}, bf16[2048,256]{1,0:T(8,128)(2,1)S(1)}, u32[]{:S(2)}, u32[]{:S(2)}) collective-permute-start(bf16[2048,256]{1,0:T(8,128)(2,1)S(1)} %bitcast.14), channel_id=1, source_target_pairs={{0,1},{1,0},{2,3},{3,2},{4,5},{5,4},{6,7},{7,6},{8,9},{9,8},{10,11... | collective-permute-start | bytes 3145736 | tf_op jit(solution)/shard_map/ppermute | solution.py:550
  78.9 16.1 %collective-permute-start.10 = (bf16[256,2048]{1,0:T(8,128)(2,1)S(1)}, bf16[256,2048]{1,0:T(8,128)(2,1)S(1)}, u32[]{:S(2)}, u32[]{:S(2)}) collective-permute-start(bf16[256,2048]{1,0:T(8,128)(2,1)S(1)} %bitcast.22), channel_id=1, source_target_pairs={{0,1},{1,0},{2,3},{3,2},{4,5},{5,4},{6,7},{7,6},{8,9},{9,8},{10,11... | collective-permute-start | bytes 3145736 | tf_op jit(solution)/shard_map/ppermute | solution.py:550
  79.4 15.6 %collective-permute-start.9 = (bf16[2048,256]{1,0:T(8,128)(2,1)S(1)}, bf16[2048,256]{1,0:T(8,128)(2,1)S(1)}, u32[]{:S(2)}, u32[]{:S(2)}) collective-permute-start(bf16[2048,256]{1,0:T(8,128)(2,1)S(1)} %bitcast.18), channel_id=1, source_target_pairs={{0,1},{1,0},{2,3},{3,2},{4,5},{5,4},{6,7},{7,6},{8,9},{9,8},{10,11... | collective-permute-start | bytes 3145736 | tf_op jit(solution)/shard_map/ppermute | solution.py:550
  79.5 5.4 %collective-permute-start.33 = (bf16[1024,128]{1,0:T(8,128)(2,1)S(1)}, bf16[1024,128]{1,0:T(8,128)(2,1)S(1)}, u32[]{:S(2)}, u32[]{:S(2)}) collective-permute-start(bf16[1024,128]{1,0:T(8,128)(2,1)S(1)} %collective-permute-done.27.refs_25_.refs_23_), channel_id=1, source_target_pairs={{0,1},{1,0},{2,3},{3,2},{4,5},{5,4},{6,7},{7,6},{8,9},{9,8},{10,11... | collective-permute-start | bytes 786440 | tf_op jit(solution)/shard_map/ppermute | solution.py:550
  79.9 5.4 %collective-permute-start.34 = (bf16[1024,128]{1,0:T(8,128)(2,1)S(1)}, bf16[1024,128]{1,0:T(8,128)(2,1)S(1)}, u32[]{:S(2)}, u32[]{:S(2)}) collective-permute-start(bf16[1024,128]{1,0:T(8,128)(2,1)S(1)} %collective-permute-done.28.refs_26_.refs_24_), channel_id=1, source_target_pairs={{0,1},{1,0},{2,3},{3,2},{4,5},{5,4},{6,7},{7,6},{8,9},{9,8},{10,11... | collective-permute-start | bytes 786440 | tf_op jit(solution)/shard_map/ppermute | solution.py:550
  84.9 1.5 %collective-permute-start.35 = (bf16[64,2048]{1,0:T(8,128)(2,1)S(1)}, bf16[64,2048]{1,0:T(8,128)(2,1)S(1)}, u32[]{:S(2)}, u32[]{:S(2)}) collective-permute-start(bf16[64,2048]{1,0:T(8,128)(2,1)S(1)} %collective-permute-done.29.refs_27_.refs_25_), channel_id=1, source_target_pairs={{0,1},{1,0},{2,3},{3,2},{4,5},{5,4},{6,7},{7,6},{8,9},{9,8},{10,11... | collective-permute-start | bytes 786440 | tf_op jit(solution)/shard_map/ppermute | solution.py:550
  85.3 1.5 %collective-permute-start.31 = (bf16[1024,128]{1,0:T(8,128)(2,1)S(1)}, bf16[1024,128]{1,0:T(8,128)(2,1)S(1)}, u32[]{:S(2)}, u32[]{:S(2)}) collective-permute-start(bf16[1024,128]{1,0:T(8,128)(2,1)S(1)} %collective-permute-done.25.refs_23_.refs_21_), channel_id=1, source_target_pairs={{0,1},{1,0},{2,3},{3,2},{4,5},{5,4},{6,7},{7,6},{8,9},{9,8},{10,11... | collective-permute-start | bytes 786440 | tf_op jit(solution)/shard_map/ppermute | solution.py:550
  86.4 14.4 %collective-permute-start.6 = (bf16[96,2048]{1,0:T(8,128)(2,1)S(1)}, bf16[96,2048]{1,0:T(8,128)(2,1)S(1)}, u32[]{:S(2)}, u32[]{:S(2)}) collective-permute-start(bf16[96,2048]{1,0:T(8,128)(2,1)S(1)} %get-tuple-element.31), channel_id=1, source_target_pairs={{0,4},{4,8},{8,12},{12,0},{1,5},{5,9},{9,13},{13,1},{2,6},{6,10},{... | collective-permute-start | bytes 1179656 | tf_op jit(solution)/shard_map/ppermute | solution.py:559
  86.8 19.6 %collective-permute-start.7 = (bf16[96,2048]{1,0:T(8,128)(2,1)S(1)}, bf16[96,2048]{1,0:T(8,128)(2,1)S(1)}, u32[]{:S(2)}, u32[]{:S(2)}) collective-permute-start(bf16[96,2048]{1,0:T(8,128)(2,1)S(1)} %get-tuple-element.32), channel_id=1, source_target_pairs={{0,12},{4,0},{8,4},{12,8},{1,13},{5,1},{9,5},{13,9},{2,14},{6,2},{... | collective-permute-start | bytes 1179656 | tf_op jit(solution)/shard_map/ppermute | solution.py:559
  90.2 1.6 %copy-start.3 = (bf16[512,2048]{1,0:T(8,128)(2,1)S(1)}, bf16[512,2048]{1,0:T(8,128)(2,1)}, u32[]{:S(2)}) copy-start(bf16[512,2048]{1,0:T(8,128)(2,1)} %refs_4_.1) | copy-start | bytes 6291460
  94.9 31.0 %collective-permute-start.4 = (bf16[64,2048]{1,0:T(8,128)(2,1)S(1)}, bf16[64,2048]{1,0:T(8,128)(2,1)S(1)}, u32[]{:S(2)}, u32[]{:S(2)}) collective-permute-start(bf16[64,2048]{1,0:T(8,128)(2,1)S(1)} %get-tuple-element.25), channel_id=1, source_target_pairs={{0,1},{1,0},{2,3},{3,2},{4,5},{5,4},{6,7},{7,6},{8,9},{9,8},{10,11... | collective-permute-start | bytes 786440 | tf_op jit(solution)/shard_map/ppermute | solution.py:550
  97.2 35.2 %collective-permute-start.39 = (bf16[96,2048]{1,0:T(8,128)(2,1)S(1)}, bf16[96,2048]{1,0:T(8,128)(2,1)S(1)}, u32[]{:S(2)}, u32[]{:S(2)}) collective-permute-start(bf16[96,2048]{1,0:T(8,128)(2,1)S(1)} %shard_map.147), channel_id=1, source_target_pairs={{0,8},{4,12},{8,0},{12,4},{1,9},{5,13},{9,1},{13,5},{2,10},{6,14},... | collective-permute-start | bytes 1179656 | tf_op jit(solution)/shard_map/ppermute | solution.py:559
  106.4 21.8 %copy-start.6 = (s32[128,2]{0,1:T(2,128)S(1)}, s32[128,2]{0,1:T(2,128)}, u32[]{:S(2)}) copy-start(s32[128,2]{0,1:T(2,128)} %param.21) | copy-start | bytes 3076
  106.4 21.8 %copy-start.7 = (f32[128,2]{0,1:T(2,128)S(1)}, f32[128,2]{0,1:T(2,128)}, u32[]{:S(2)}) copy-start(f32[128,2]{0,1:T(2,128)} %param.22) | copy-start | bytes 3076
  106.4 25.2 %copy-start.5 = (f32[2048]{0:T(1024)S(1)}, f32[2048]{0:T(1024)}, u32[]{:S(2)}) copy-start(f32[2048]{0:T(1024)} %param.18) | copy-start | bytes 24580
  110.2 24.4 %collective-permute-start.37 = (bf16[96,2048]{1,0:T(8,128)(2,1)S(1)}, bf16[96,2048]{1,0:T(8,128)(2,1)S(1)}, u32[]{:S(2)}, u32[]{:S(2)}) collective-permute-start(bf16[96,2048]{1,0:T(8,128)(2,1)S(1)} %get-tuple-element.41), channel_id=1, source_target_pairs={{0,12},{4,0},{8,4},{12,8},{1,13},{5,1},{9,5},{13,9},{2,14},{6,2},{... | collective-permute-start | bytes 1179656 | tf_op jit(solution)/shard_map/ppermute | solution.py:559
  113.2 26.6 %collective-permute-start.40 = (bf16[96,2048]{1,0:T(8,128)(2,1)S(1)}, bf16[96,2048]{1,0:T(8,128)(2,1)S(1)}, u32[]{:S(2)}, u32[]{:S(2)}) collective-permute-start(bf16[96,2048]{1,0:T(8,128)(2,1)S(1)} %get-tuple-element.43), channel_id=1, source_target_pairs={{0,4},{4,8},{8,12},{12,0},{1,5},{5,9},{9,13},{13,1},{2,6},{6,10},{... | collective-permute-start | bytes 1179656 | tf_op jit(solution)/shard_map/ppermute | solution.py:559
  126.5 5.0 %collective-permute-start.5 = (bf16[32,2048]{1,0:T(8,128)(2,1)S(1)}, bf16[32,2048]{1,0:T(8,128)(2,1)S(1)}, u32[]{:S(2)}, u32[]{:S(2)}) collective-permute-start(bf16[32,2048]{1,0:T(8,128)(2,1)S(1)} %get-tuple-element.27), channel_id=1, source_target_pairs={{0,2},{1,3},{2,0},{3,1},{4,6},{5,7},{6,4},{7,5},{8,10},{9,11},{10,... | collective-permute-start | bytes 393224 | tf_op jit(solution)/shard_map/ppermute | solution.py:553

commit v5 on v4

--- a/solution.py
+++ b/solution.py
@@ -263,7 +263,6 @@
     part = gate.shape[1] // 2
     deep = gate.shape[0] // 2
     thin = part // 2
-    slim = part // 4
 
     def body(place_ref, gain_hbm, ids_hbm, input_hbm, gate_hbm, up_hbm, down_hbm, *refs):
         outs = refs[:experts]
@@ -273,7 +272,7 @@
         columns = pl.ds(begin, part)
 
         def some(first, size):
-            return down_hbm.at[pl.ds(pl.multiple_of(first, slim), size), :]
+            return down_hbm.at[pl.ds(pl.multiple_of(first, thin), size), :]
 
         copies = start_all(
             [
@@ -284,9 +283,8 @@
                 (up_hbm.at[pl.ds(0, deep), columns], up_a),
                 (up_hbm.at[pl.ds(deep, deep), columns], up_b),
                 (some(begin, thin), down_a),
-                (some(begin + thin, slim), down_b),
-                (some(begin + 3 * slim, slim), down_c.at[pl.ds(0, slim), :]),
-                (some(beyond + 3 * slim, slim), down_c.at[pl.ds(slim, slim), :]),
+                (some(begin + thin, thin), down_b),
+                (some(beyond + thin, thin), down_c),
             ],
             sems,
         )
@@ -307,7 +305,7 @@
         shape_of((deep, part)),
         shape_of((deep, part)),
         shape_of((thin, width)),
-        shape_of((slim, width)),
+        shape_of((thin, width)),
         shape_of((thin, width)),
     ]
     return call(
@@ -318,7 +316,7 @@
             pltpu.VMEM((rows, width), jnp.bfloat16),
             pltpu.VMEM((1, width), jnp.float32),
             pltpu.VMEM(ids.shape, jnp.int32),
-            pltpu.SemaphoreType.DMA((10,)),
+            pltpu.SemaphoreType.DMA((9,)),
         ),
         flops=2 * experts * capacity * rows * width,
     )(place, *in_hbm(ffn_gain.reshape(1, width), ids, moe_input, gate, upward, down))
@@ -366,8 +364,8 @@
 def expert_rows(rows_in, pieces):
     capacity, width = rows_in[0].shape
     count = len(rows_in)
-    hidden = sum(piece[0][0][0].shape[1] for piece in pieces)
-    flat = [chunk[0] for piece in pieces for kind in piece for chunk in kind]
+    hidden = sum(piece[0][0].shape[1] for piece in pieces)
+    flat = [chunk for piece in pieces for kind in piece for chunk in kind]
 
     def body(*refs):
         weight_refs = refs[count : count + len(flat)]
@@ -378,9 +376,7 @@
         for piece in pieces:
             kinds = []
             for kind in piece:
-                chunk = [
-                    weight_refs[at + k][low:high, :] for k, (_, low, high) in enumerate(kind)
-                ]
+                chunk = [ref[...] for ref in weight_refs[at : at + len(kind)]]
                 kinds.append(chunk[0] if len(chunk) == 1 else jnp.concatenate(chunk, axis=0))
                 at += len(kind)
             size = kinds[0].shape[1]
@@ -420,9 +416,7 @@
         projected = inner_ref[...] + received_ref[...].astype(jnp.float32)
         out_ref[...] = norm_rows(projected, gain_ref[...]).astype(jnp.bfloat16)
 
-    return call(body, shape_of(inner.shape), [VMEM] * 3)(
-        inner, received, gain.reshape(1, -1)
-    )
+    return call(body, shape_of(inner.shape), [VMEM] * 3)(inner, received, gain.reshape(1, -1))
 
 
 def attend_project(place, queries, own, passed, out_weight, heads, quarters):
@@ -572,32 +566,26 @@
 
     far = tuple(across(array) for array in halves)
     near = tuple(core(array) for array in mine)
-    other = tuple(beside(array) for array in far[:-1])
+    other = tuple(beside(array) for array in far[:5])
     far_near = tuple(core(array) for array in far)
     other_near = tuple(core(array) for array in other)
 
     passed = [upward(own, 1), lax.ppermute(own, "ep", [(0, 2)])]
     passed += [lax.ppermute(array, "ep", [(2, 3)]) for array in passed]
 
-    def chunk(array, low=0, high=None):
-        return (array, low, array.shape[0] if high is None else high)
-
     def whole(arrays):
-        return [[chunk(array)] for array in arrays]
-
-    def chunked(arrays, last, which):
-        slim = last.shape[0] // 2
-        kinds = [[chunk(array) for array in some] for some in (arrays[0:2], arrays[2:4], arrays[4:6])]
-        kinds[2].append(chunk(last, which * slim, (which + 1) * slim))
-        return kinds
+        return [[array] for array in arrays]
+
+    def chunked(arrays, last):
+        return [arrays[0:2], arrays[2:4], [arrays[4], last]]
 
     pieces = [
         whole(mine),
         whole(near),
-        chunked(far, far[6], 0),
-        chunked(far_near, far_near[6], 0),
-        chunked(other, far[6], 1),
-        chunked(other_near, far_near[6], 1),
+        chunked(far, far[5]),
+        chunked(far_near, far_near[5]),
+        chunked(other, far[6]),
+        chunked(other_near, far_near[6]),
     ]
     order = (2, 0, 1, 3)
     done = expert_rows([arrived[k] for k in order[:1]], pieces)

time: 142 us -> 142 us (level)
  starting transfers between devices: 58.8 us -> 64.2 us
  waiting for transfers between devices: 63 us -> 58.4 us
    ppermute x6, starting transfers between devices: 25.9 us -> 30.4 us  [turn(): lax.ppermute(array, 'ep', [(i, (i + d) % blocks) for i in range(blocks)])]
    ppermute x1, waiting for transfers between devices: 4.44 us -> 0.01 us  [paired_step(): passed = [upward(own, 1), lax.ppermute(own, 'ep', [(0, 2)])]]
    ppermute x6 -> x5, waiting for transfers between devices: 22.7 us -> 19.6 us  [beside(): return lax.ppermute(array, 'grp', [(0, 1), (1, 0)])]
    ppermute x8, waiting for transfers between devices: 16.2 us -> 18.8 us  [across(): return lax.ppermute(array, 'tp', [(i, i ^ 2) for i in range(shards)])]
    ppermute x17 -> x16, starting transfers between devices: 2.04 us -> 3.03 us  [core(): return lax.ppermute(array, 'tp', [(i, i ^ 1) for i in range(shards)])]
    ppermute x17 -> x16, waiting for transfers between devices: 6.57 us -> 6.2 us  [core(): return lax.ppermute(array, 'tp', [(i, i ^ 1) for i in range(shards)])]
    ppermute x6 -> x5, starting transfers between devices: 7.76 us -> 7.72 us  [beside(): return lax.ppermute(array, 'grp', [(0, 1), (1, 0)])]
  transfers between devices with their start and end apart: 41 -> 39, of which waited for: 20 -> 17; matrix products, arithmetic and copies ran while one was open for 0% -> 0% of each run, Pallas kernels for 9% -> 9%
where the time goes in v5:
time: 142 us
  starting transfers between devices  64.2 us (45%)
  waiting for transfers between devices  58.4 us (41%)
  Pallas kernels  17.1 us (12%)
  local copies, waits for them, and re-layouts  1.62 us (1%)
    ppermute x6, starting transfers between devices, turn(): lax.ppermute(array, 'ep', [(i, (i + d) % blocks) for i in range(blocks)])  30.4 us
    ppermute x5, waiting for transfers between devices, beside(): return lax.ppermute(array, 'grp', [(0, 1), (1, 0)])  19.6 us
    ppermute x8, waiting for transfers between devices, across(): return lax.ppermute(array, 'tp', [(i, i ^ 2) for i in range(shards)])  18.8 us
    ppermute x6, waiting for transfers between devices, turn(): lax.ppermute(array, 'ep', [(i, (i + d) % blocks) for i in range(blocks)])  13.8 us
    ppermute x8, starting transfers between devices, across(): return lax.ppermute(array, 'tp', [(i, i ^ 2) for i in range(shards)])  12.7 us
    ppermute x5, starting transfers between devices, beside(): return lax.ppermute(array, 'grp', [(0, 1), (1, 0)])  7.72 us
    ppermute x16, waiting for transfers between devices, core(): return lax.ppermute(array, 'tp', [(i, i ^ 1) for i in range(shards)])  6.2 us
    pallas_call x2, Pallas kernels, expert_rows(): call(body, [shape_of((capacity, width))] * count, [VMEM] * (count + len(f...  6.05 us
  transfers between devices with their start and end apart: 39, of which 17 were waited for; matrix products, arithmetic and copies ran while one was open for 0% of the time, Pallas kernels for 9%

profile of v5, /device:TPU:0, one launch (start us, length us, event | category | flops | bytes accessed | tf_op | source)
XLA Modules:
  0.0 142.2 jit_solution(7376045366472302623)
XLA Ops:
  0.6 0.1 pad_add_fusion.place_ref
  0.7 2.7 %shard_map.145 = (bf16[96,2048]{1,0:T(8,128)(2,1)S(1)}, bf16[96,2048]{1,0:T(8,128)(2,1)S(1)}, bf16[96,2048]{1,0:T(8,128)(2,1)S(1)}, bf16[96,2048]{1,0:T(8,128)(2...) custom-call(s32[4]{0:T(128)S(1)} %pad_add_fusion.place_ref, ...), custom_call_target="tpu_custom_call" | custom-call | flops 201326592 | tf_op jit(solution)/shard_map/pallas_call | solution.py:311
  3.5 3.0 %collective-permute-start.12 = (bf16[1024,128]{1,0:T(8,128)(2,1)S(1)}, bf16[1024,128]{1,0:T(8,128)(2,1)S(1)}, u32[]{:S(2)}, u32[]{:S(2)}) collective-permute-start(bf16[1024,128]{1,0:T(8,128)(2,1)S(1)} %get-tuple-element.34), channel_id=1, source_target_pairs={{0,2},{1,3},{2,0},{3,1},{4,6},{5,7},{6,4},{7,5},{8,10},{9,11},{10,... | collective-permute-start | bytes 786440 | tf_op jit(solution)/shard_map/ppermute | solution.py:547
  6.5 0.1 collective-permute-start.13
  6.6 1.9 %collective-permute-start.14 = (bf16[1024,128]{1,0:T(8,128)(2,1)S(1)}, bf16[1024,128]{1,0:T(8,128)(2,1)S(1)}, u32[]{:S(2)}, u32[]{:S(2)}) collective-permute-start(bf16[1024,128]{1,0:T(8,128)(2,1)S(1)} %get-tuple-element.36), channel_id=1, source_target_pairs={{0,2},{1,3},{2,0},{3,1},{4,6},{5,7},{6,4},{7,5},{8,10},{9,11},{10,... | collective-permute-start | bytes 786440 | tf_op jit(solution)/shard_map/ppermute | solution.py:547
  8.5 0.1 collective-permute-start.15
  8.6 1.9 %collective-permute-start.16 = (bf16[64,2048]{1,0:T(8,128)(2,1)S(1)}, bf16[64,2048]{1,0:T(8,128)(2,1)S(1)}, u32[]{:S(2)}, u32[]{:S(2)}) collective-permute-start(bf16[64,2048]{1,0:T(8,128)(2,1)S(1)} %get-tuple-element.38), channel_id=1, source_target_pairs={{0,2},{1,3},{2,0},{3,1},{4,6},{5,7},{6,4},{7,5},{8,10},{9,11},{10,... | collective-permute-start | bytes 786440 | tf_op jit(solution)/shard_map/ppermute | solution.py:547
  10.6 1.6 %shard_map.140 = (bf16[136,1024]{1,0:T(8,128)(2,1)S(1)}, bf16[1024,128]{1,0:T(8,128)(2,1)S(1)}) custom-call(s32[4]{0:T(128)S(1)} %pad_add_fusion.place_ref, bf16[8,128]{1,0:T(8,128)(2,1)} %bitcast.30, bf16[128,512]{1,0:T(8,128)(2,1)} %keys_hbm.1, bf16[128,512]{1,0:T(8,128)(2,1)} %values_hbm.1, bf16[2048,256]{1,0:T(8,128)(2,1)} %bitcast.13), custom_call_target="tpu_custom_call" | custom-call | tf_op jit(solution)/shard_map/pallas_call | solution.py:252
  12.2 1.5 %collective-permute-done.12.refs_10_.refs_8_ = bf16[1024,128]{1,0:T(8,128)(2,1)S(1)} collective-permute-done((bf16[1024,128]{1,0:T(8,128)(2,1)S(1)}, bf16[1024,128]{1,0:T(8,128)(2,1)S(1)}, u32[]{:S(2)}, u32[]{:S(2)}) %collective-permute-start.12) | collective-permute-done | bytes 262176 | tf_op jit(solution)/shard_map/ppermute | solution.py:547
  13.7 4.0 %collective-permute-start = (bf16[136,1024]{1,0:T(8,128)(2,1)S(1)}, bf16[136,1024]{1,0:T(8,128)(2,1)S(1)}, u32[]{:S(2)}, u32[]{:S(2)}) collective-permute-start(bf16[136,1024]{1,0:T(8,128)(2,1)S(1)} %get-tuple-element.23.own_ref), channel_id=1, source_target_pairs={{0,4},{4,8},{8,12},{1,5},{5,9},{9,13},{2,6},{6,10},{10,14},{3,7},{... | collective-permute-start | bytes 835592 | tf_op jit(solution)/shard_map/ppermute | solution.py:556
  17.7 1.6 %collective-permute-done.13.refs_11_.refs_9_ = bf16[1024,128]{1,0:T(8,128)(2,1)S(1)} collective-permute-done((bf16[1024,128]{1,0:T(8,128)(2,1)S(1)}, bf16[1024,128]{1,0:T(8,128)(2,1)S(1)}, u32[]{:S(2)}, u32[]{:S(2)}) %collective-permute-start.13) | collective-permute-done | bytes 262176 | tf_op jit(solution)/shard_map/ppermute | solution.py:547
  19.3 2.0 %collective-permute-start.28 = (bf16[64,2048]{1,0:T(8,128)(2,1)S(1)}, bf16[64,2048]{1,0:T(8,128)(2,1)S(1)}, u32[]{:S(2)}, u32[]{:S(2)}) collective-permute-start(bf16[64,2048]{1,0:T(8,128)(2,1)S(1)} %get-tuple-element.39), channel_id=1, source_target_pairs={{0,2},{1,3},{2,0},{3,1},{4,6},{5,7},{6,4},{7,5},{8,10},{9,11},{10,... | collective-permute-start | bytes 786440 | tf_op jit(solution)/shard_map/ppermute | solution.py:547
  21.3 3.6 %collective-permute-done.14.refs_12_.refs_10_ = bf16[1024,128]{1,0:T(8,128)(2,1)S(1)} collective-permute-done((bf16[1024,128]{1,0:T(8,128)(2,1)S(1)}, bf16[1024,128]{1,0:T(8,128)(2,1)S(1)}, u32[]{:S(2)}, u32[]{:S(2)}) %collective-permute-start.14) | collective-permute-done | bytes 262176 | tf_op jit(solution)/shard_map/ppermute | solution.py:547
  24.9 2.0 %collective-permute-start.11 = (bf16[1024,128]{1,0:T(8,128)(2,1)S(1)}, bf16[1024,128]{1,0:T(8,128)(2,1)S(1)}, u32[]{:S(2)}, u32[]{:S(2)}) collective-permute-start(bf16[1024,128]{1,0:T(8,128)(2,1)S(1)} %get-tuple-element.33), channel_id=1, source_target_pairs={{0,2},{1,3},{2,0},{3,1},{4,6},{5,7},{6,4},{7,5},{8,10},{9,11},{10,... | collective-permute-start | bytes 786440 | tf_op jit(solution)/shard_map/ppermute | solution.py:547
  26.9 3.6 %collective-permute-done.15.refs_13_.refs_11_ = bf16[64,2048]{1,0:T(8,128)(2,1)S(1)} collective-permute-done((bf16[64,2048]{1,0:T(8,128)(2,1)S(1)}, bf16[64,2048]{1,0:T(8,128)(2,1)S(1)}, u32[]{:S(2)}, u32[]{:S(2)}) %collective-permute-start.15) | collective-permute-done | bytes 262176 | tf_op jit(solution)/shard_map/ppermute | solution.py:547
  30.5 3.1 %collective-permute-start.36 = (bf16[96,2048]{1,0:T(8,128)(2,1)S(1)}, bf16[96,2048]{1,0:T(8,128)(2,1)S(1)}, u32[]{:S(2)}, u32[]{:S(2)}) collective-permute-start(bf16[96,2048]{1,0:T(8,128)(2,1)S(1)} %get-tuple-element.42), channel_id=1, source_target_pairs={{0,8},{4,12},{8,0},{12,4},{1,9},{5,13},{9,1},{13,5},{2,10},{6,14},... | collective-permute-start | bytes 1179656 | tf_op jit(solution)/shard_map/ppermute | solution.py:553
  33.6 2.5 %collective-permute-done.16.refs_14_.refs_12_ = bf16[64,2048]{1,0:T(8,128)(2,1)S(1)} collective-permute-done((bf16[64,2048]{1,0:T(8,128)(2,1)S(1)}, bf16[64,2048]{1,0:T(8,128)(2,1)S(1)}, u32[]{:S(2)}, u32[]{:S(2)}) %collective-permute-start.16) | collective-permute-done | bytes 262176 | tf_op jit(solution)/shard_map/ppermute | solution.py:547
  36.1 5.0 %collective-permute-start.1 = (bf16[136,1024]{1,0:T(8,128)(2,1)S(1)}, bf16[136,1024]{1,0:T(8,128)(2,1)S(1)}, u32[]{:S(2)}, u32[]{:S(2)}) collective-permute-start(bf16[136,1024]{1,0:T(8,128)(2,1)S(1)} %get-tuple-element.23.own_ref), channel_id=1, source_target_pairs={{0,8},{1,9},{2,10},{3,11},{16,24},{17,25},{18,26},{19,27}} | collective-permute-start | bytes 835592 | tf_op jit(solution)/shard_map/ppermute | solution.py:573
  41.2 0.6 collective-permute-done.28.refs_26_.refs_24_
  41.7 2.1 %collective-permute-start.24 = (bf16[1024,128]{1,0:T(8,128)(2,1)S(1)}, bf16[1024,128]{1,0:T(8,128)(2,1)S(1)}, u32[]{:S(2)}, u32[]{:S(2)}) collective-permute-start(bf16[1024,128]{1,0:T(8,128)(2,1)S(1)} %collective-permute-done.12.refs_10_.refs_8_), channel_id=1, source_target_pairs={{0,16},{16,0},{1,17},{17,1},{2,18},{18,2},{3,19},{19,3},{4,20},{20... | collective-permute-start | bytes 786440 | tf_op jit(solution)/shard_map/ppermute | solution.py:550
  43.8 2.7 %collective-permute-done.11.refs_9_.refs_7_ = bf16[1024,128]{1,0:T(8,128)(2,1)S(1)} collective-permute-done((bf16[1024,128]{1,0:T(8,128)(2,1)S(1)}, bf16[1024,128]{1,0:T(8,128)(2,1)S(1)}, u32[]{:S(2)}, u32[]{:S(2)}) %collective-permute-start.11) | collective-permute-done | bytes 262176 | tf_op jit(solution)/shard_map/ppermute | solution.py:547
  46.5 1.8 %collective-permute-start.25 = (bf16[1024,128]{1,0:T(8,128)(2,1)S(1)}, bf16[1024,128]{1,0:T(8,128)(2,1)S(1)}, u32[]{:S(2)}, u32[]{:S(2)}) collective-permute-start(bf16[1024,128]{1,0:T(8,128)(2,1)S(1)} %collective-permute-done.13.refs_11_.refs_9_), channel_id=1, source_target_pairs={{0,16},{16,0},{1,17},{17,1},{2,18},{18,2},{3,19},{19,3},{4,20},{20... | collective-permute-start | bytes 786440 | tf_op jit(solution)/shard_map/ppermute | solution.py:550
  48.3 0.3 collective-permute-start.26
  48.5 0.0 collective-permute-done.1.refs_1_
  48.6 1.8 %collective-permute-start.27 = (bf16[64,2048]{1,0:T(8,128)(2,1)S(1)}, bf16[64,2048]{1,0:T(8,128)(2,1)S(1)}, u32[]{:S(2)}, u32[]{:S(2)}) collective-permute-start(bf16[64,2048]{1,0:T(8,128)(2,1)S(1)} %collective-permute-done.15.refs_13_.refs_11_), channel_id=1, source_target_pairs={{0,16},{16,0},{1,17},{17,1},{2,18},{18,2},{3,19},{19,3},{4,20},{20... | collective-permute-start | bytes 786440 | tf_op jit(solution)/shard_map/ppermute | solution.py:550
  50.3 0.0 collective-permute-done.36.refs_0_
  50.3 0.0 collective-permute-start.18
  50.3 0.5 collective-permute-start.19
  50.8 4.9 %collective-permute-done.25.refs_23_.refs_21_ = bf16[1024,128]{1,0:T(8,128)(2,1)S(1)} collective-permute-done((bf16[1024,128]{1,0:T(8,128)(2,1)S(1)}, bf16[1024,128]{1,0:T(8,128)(2,1)S(1)}, u32[]{:S(2)}, u32[]{:S(2)}) %collective-permute-start.25) | collective-permute-done | bytes 262176 | tf_op jit(solution)/shard_map/ppermute | solution.py:550
  55.7 5.6 %collective-permute-done.26.refs_24_.refs_22_ = bf16[1024,128]{1,0:T(8,128)(2,1)S(1)} collective-permute-done((bf16[1024,128]{1,0:T(8,128)(2,1)S(1)}, bf16[1024,128]{1,0:T(8,128)(2,1)S(1)}, u32[]{:S(2)}, u32[]{:S(2)}) %collective-permute-start.26) | collective-permute-done | bytes 262176 | tf_op jit(solution)/shard_map/ppermute | solution.py:550
  61.3 3.9 %collective-permute-done.27.refs_25_.refs_23_ = bf16[64,2048]{1,0:T(8,128)(2,1)S(1)} collective-permute-done((bf16[64,2048]{1,0:T(8,128)(2,1)S(1)}, bf16[64,2048]{1,0:T(8,128)(2,1)S(1)}, u32[]{:S(2)}, u32[]{:S(2)}) %collective-permute-start.27) | collective-permute-done | bytes 262176 | tf_op jit(solution)/shard_map/ppermute | solution.py:550
  65.2 0.5 collective-permute-start.34
  65.7 0.7 collective-permute-start.2
  66.4 1.9 %collective-permute-start.23 = (bf16[1024,128]{1,0:T(8,128)(2,1)S(1)}, bf16[1024,128]{1,0:T(8,128)(2,1)S(1)}, u32[]{:S(2)}, u32[]{:S(2)}) collective-permute-start(bf16[1024,128]{1,0:T(8,128)(2,1)S(1)} %collective-permute-done.11.refs_9_.refs_7_), channel_id=1, source_target_pairs={{0,16},{16,0},{1,17},{17,1},{2,18},{18,2},{3,19},{19,3},{4,20},{20... | collective-permute-start | bytes 786440 | tf_op jit(solution)/shard_map/ppermute | solution.py:550
  68.3 0.7 collective-permute-start.3
  69.0 0.6 collective-permute-start.30
  69.6 5.2 %collective-permute-done.23.refs_21_.refs_19_ = bf16[1024,128]{1,0:T(8,128)(2,1)S(1)} collective-permute-done((bf16[1024,128]{1,0:T(8,128)(2,1)S(1)}, bf16[1024,128]{1,0:T(8,128)(2,1)S(1)}, u32[]{:S(2)}, u32[]{:S(2)}) %collective-permute-start.23) | collective-permute-done | bytes 262176 | tf_op jit(solution)/shard_map/ppermute | solution.py:550
  74.8 0.5 collective-permute-start.10
  75.3 0.1 collective-permute-start.9
  75.4 0.4 collective-permute-start.31
  75.8 0.1 collective-permute-start.32
  75.9 4.9 %collective-permute-done.31.refs_29_.refs_27_ = bf16[1024,128]{1,0:T(8,128)(2,1)S(1)} collective-permute-done((bf16[1024,128]{1,0:T(8,128)(2,1)S(1)}, bf16[1024,128]{1,0:T(8,128)(2,1)S(1)}, u32[]{:S(2)}, u32[]{:S(2)}) %collective-permute-start.31) | collective-permute-done | bytes 262176 | tf_op jit(solution)/shard_map/ppermute | solution.py:544
  80.8 0.1 collective-permute-start.33
  81.0 0.2 collective-permute-done.32.refs_30_.refs_28_
  81.2 0.1 collective-permute-start.29
  81.3 1.0 collective-permute-done.33.refs_31_.refs_29_
  82.4 1.8 %collective-permute-start.6 = (bf16[96,2048]{1,0:T(8,128)(2,1)S(1)}, bf16[96,2048]{1,0:T(8,128)(2,1)S(1)}, u32[]{:S(2)}, u32[]{:S(2)}) collective-permute-start(bf16[96,2048]{1,0:T(8,128)(2,1)S(1)} %get-tuple-element.31), channel_id=1, source_target_pairs={{0,4},{4,8},{8,12},{12,0},{1,5},{5,9},{9,13},{13,1},{2,6},{6,10},{... | collective-permute-start | bytes 1179656 | tf_op jit(solution)/shard_map/ppermute | solution.py:553
  84.2 5.3 %collective-permute-start.7 = (bf16[96,2048]{1,0:T(8,128)(2,1)S(1)}, bf16[96,2048]{1,0:T(8,128)(2,1)S(1)}, u32[]{:S(2)}, u32[]{:S(2)}) collective-permute-start(bf16[96,2048]{1,0:T(8,128)(2,1)S(1)} %get-tuple-element.32), channel_id=1, source_target_pairs={{0,12},{4,0},{8,4},{12,8},{1,13},{5,1},{9,5},{13,9},{2,14},{6,2},{... | collective-permute-start | bytes 1179656 | tf_op jit(solution)/shard_map/ppermute | solution.py:553
  89.5 1.6 %copy-done.3 = bf16[512,2048]{1,0:T(8,128)(2,1)S(1)} copy-done((bf16[512,2048]{1,0:T(8,128)(2,1)S(1)}, bf16[512,2048]{1,0:T(8,128)(2,1)}, u32[]{:S(2)}) %copy-start.3) | copy-done | bytes 2097176
  91.1 3.0 %shard_map.141 = (bf16[64,2048]{1,0:T(8,128)(2,1)S(1)}, f32[64,2048]{1,0:T(8,128)S(1)}) custom-call(s32[4]{0:T(128)S(1)} %pad_add_fusion.place_ref, bf16[128,512]{1,0:T(8,128)(2,1)S(1)} %copy-done.4, bf16[136,1024]{1,0:T(8,128)(2,1)S(1)} %get-tuple-element.23.own_ref, bf16[136,1024]{1,0:T(8,128)(2,1)S(1)} %collective-permute-done.refs_0_, ...), custom_call_target="tpu_custom_call" | custom-call | flops 402653184 | tf_op jit(solution)/shard_map/pallas_call | solution.py:501
  94.2 0.1 collective-permute-start.4
  94.3 2.2 %shard_map.147 = bf16[96,2048]{1,0:T(8,128)(2,1)S(1)} custom-call(bf16[96,2048]{1,0:T(8,128)(2,1)S(1)} %collective-permute-done.36.refs_0_, bf16[2048,256]{1,0:T(8,128)(2,1)S(1)} %bitcast.15, bf16[2048,256]{1,0:T(8,128)(2,1)S(1)} %bitcast.19, bf16[256,2048]{1,0:T(8,128)(2,1)S(1)} %bitcast.23, bf16[2048,256]{1,0:T(8,128)(2,1)S(1)} %collective-permute-done.8.refs_6_.refs_4_, ...), custom_call_target="tpu_custom_call" | custom-call | flops 1207959552 | tf_op jit(solution)/shard_map/pallas_call | solution.py:393
  96.4 3.8 %collective-permute-start.37 = (bf16[96,2048]{1,0:T(8,128)(2,1)S(1)}, bf16[96,2048]{1,0:T(8,128)(2,1)S(1)}, u32[]{:S(2)}, u32[]{:S(2)}) collective-permute-start(bf16[96,2048]{1,0:T(8,128)(2,1)S(1)} %shard_map.147), channel_id=1, source_target_pairs={{0,8},{4,12},{8,0},{12,4},{1,9},{5,13},{9,1},{13,5},{2,10},{6,14},... | collective-permute-start | bytes 1179656 | tf_op jit(solution)/shard_map/ppermute | solution.py:553
  100.3 5.5 %collective-permute-done.7.refs_2_ = bf16[96,2048]{1,0:T(8,128)(2,1)S(1)} collective-permute-done((bf16[96,2048]{1,0:T(8,128)(2,1)S(1)}, bf16[96,2048]{1,0:T(8,128)(2,1)S(1)}, u32[]{:S(2)}, u32[]{:S(2)}) %collective-permute-start.7) | collective-permute-done | bytes 393248 | tf_op jit(solution)/shard_map/ppermute | solution.py:553
  105.8 3.9 %shard_map.146 = (bf16[96,2048]{1,0:T(8,128)(2,1)S(1)}, bf16[96,2048]{1,0:T(8,128)(2,1)S(1)}, bf16[96,2048]{1,0:T(8,128)(2,1)S(1)}) custom-call(bf16[96,2048]{1,0:T(8,128)(2,1)S(1)} %get-tuple-element.30.refs_0_, bf16[96,2048]{1,0:T(8,128)(2,1)S(1)} %collective-permute-done.6.refs_1_, bf16[96,2048]{1,0:T(8,128)(2,1)S(1)} %collective-permute-done.7.refs_2_, ...), custom_call_target="tpu_custom_call" | custom-call | flops 3623878656 | tf_op jit(solution)/shard_map/pallas_call | solution.py:393
  109.7 3.0 %collective-permute-start.35 = (bf16[96,2048]{1,0:T(8,128)(2,1)S(1)}, bf16[96,2048]{1,0:T(8,128)(2,1)S(1)}, u32[]{:S(2)}, u32[]{:S(2)}) collective-permute-start(bf16[96,2048]{1,0:T(8,128)(2,1)S(1)} %get-tuple-element.41), channel_id=1, source_target_pairs={{0,12},{4,0},{8,4},{12,8},{1,13},{5,1},{9,5},{13,9},{2,14},{6,2},{... | collective-permute-start | bytes 1179656 | tf_op jit(solution)/shard_map/ppermute | solution.py:553
  112.7 13.3 %collective-permute-start.38 = (bf16[96,2048]{1,0:T(8,128)(2,1)S(1)}, bf16[96,2048]{1,0:T(8,128)(2,1)S(1)}, u32[]{:S(2)}, u32[]{:S(2)}) collective-permute-start(bf16[96,2048]{1,0:T(8,128)(2,1)S(1)} %get-tuple-element.43), channel_id=1, source_target_pairs={{0,4},{4,8},{8,12},{12,0},{1,5},{5,9},{9,13},{13,1},{2,6},{6,10},{... | collective-permute-start | bytes 1179656 | tf_op jit(solution)/shard_map/ppermute | solution.py:553
  126.0 0.6 shard_map.142
  126.6 1.6 %collective-permute-start.5 = (bf16[32,2048]{1,0:T(8,128)(2,1)S(1)}, bf16[32,2048]{1,0:T(8,128)(2,1)S(1)}, u32[]{:S(2)}, u32[]{:S(2)}) collective-permute-start(bf16[32,2048]{1,0:T(8,128)(2,1)S(1)} %get-tuple-element.27), channel_id=1, source_target_pairs={{0,2},{1,3},{2,0},{3,1},{4,6},{5,7},{6,4},{7,5},{8,10},{9,11},{10,... | collective-permute-start | bytes 393224 | tf_op jit(solution)/shard_map/ppermute | solution.py:547
  128.2 0.7 shard_map.144
  128.9 2.7 %collective-permute-done.5.received_ref = bf16[32,2048]{1,0:T(8,128)(2,1)S(1)} collective-permute-done((bf16[32,2048]{1,0:T(8,128)(2,1)S(1)}, bf16[32,2048]{1,0:T(8,128)(2,1)S(1)}, u32[]{:S(2)}, u32[]{:S(2)}) %collective-permute-start.5) | collective-permute-done | bytes 131104 | tf_op jit(solution)/shard_map/ppermute | solution.py:547
  131.6 0.8 shard_map.143
  132.4 8.3 %collective-permute-done.35.refs_1_ = bf16[96,2048]{1,0:T(8,128)(2,1)S(1)} collective-permute-done((bf16[96,2048]{1,0:T(8,128)(2,1)S(1)}, bf16[96,2048]{1,0:T(8,128)(2,1)S(1)}, u32[]{:S(2)}, u32[]{:S(2)}) %collective-permute-start.35) | collective-permute-done | bytes 393248 | tf_op jit(solution)/shard_map/ppermute | solution.py:553
  140.7 1.5 %shard_map.148 = bf16[128,2048]{1,0:T(8,128)(2,1)} custom-call(bf16[384,128]{1,0:T(8,128)(2,1)S(1)} %get-tuple-element.28.high_ref, bf16[384,128]{1,0:T(8,128)(2,1)S(1)} %get-tuple-element.29.low_ref, bf16[96,2048]{1,0:T(8,128)(2,1)S(1)} %get-tuple-element.40.refs_0_, bf16[96,2048]{1,0:T(8,128)(2,1)S(1)} %collective-permute-done.35.refs_1_, ...), custom_call_target="tpu_custom_call" | custom-call | flops 402653184 | tf_op jit(solution)/shard_map/pallas_call | solution.py:358
  (40 shorter events, 0.1 us)
Async XLA Ops:
  0.7 74.1 %copy-start = (bf16[1,2048,256]{2,1,0:T(8,128)(2,1)S(1)}, bf16[1,2048,256]{2,1,0:T(8,128)(2,1)}, u32[]{:S(2)}) copy-start(bf16[1,2048,256]{2,1,0:T(8,128)(2,1)} %param.23) | copy-start | bytes 3145732
  0.7 74.1 %copy-start.2 = (bf16[1,256,2048]{2,1,0:T(8,128)(2,1)S(1)}, bf16[1,256,2048]{2,1,0:T(8,128)(2,1)}, u32[]{:S(2)}) copy-start(bf16[1,256,2048]{2,1,0:T(8,128)(2,1)} %param.25) | copy-start | bytes 3145732
  0.7 74.6 %copy-start.1 = (bf16[1,2048,256]{2,1,0:T(8,128)(2,1)S(1)}, bf16[1,2048,256]{2,1,0:T(8,128)(2,1)}, u32[]{:S(2)}) copy-start(bf16[1,2048,256]{2,1,0:T(8,128)(2,1)} %param.24) | copy-start | bytes 3145732
  0.7 88.8 %copy-start.4 = (bf16[128,512]{1,0:T(8,128)(2,1)S(1)}, bf16[128,512]{1,0:T(8,128)(2,1)}, u32[]{:S(2)}) copy-start(bf16[128,512]{1,0:T(8,128)(2,1)} %q_ref.1) | copy-start | bytes 393220
  3.5 10.2 %collective-permute-start.12 = (bf16[1024,128]{1,0:T(8,128)(2,1)S(1)}, bf16[1024,128]{1,0:T(8,128)(2,1)S(1)}, u32[]{:S(2)}, u32[]{:S(2)}) collective-permute-start(bf16[1024,128]{1,0:T(8,128)(2,1)S(1)} %get-tuple-element.34), channel_id=1, source_target_pairs={{0,2},{1,3},{2,0},{3,1},{4,6},{5,7},{6,4},{7,5},{8,10},{9,11},{10,... | collective-permute-start | bytes 786440 | tf_op jit(solution)/shard_map/ppermute | solution.py:547
  6.5 12.8 %collective-permute-start.13 = (bf16[1024,128]{1,0:T(8,128)(2,1)S(1)}, bf16[1024,128]{1,0:T(8,128)(2,1)S(1)}, u32[]{:S(2)}, u32[]{:S(2)}) collective-permute-start(bf16[1024,128]{1,0:T(8,128)(2,1)S(1)} %get-tuple-element.35), channel_id=1, source_target_pairs={{0,2},{1,3},{2,0},{3,1},{4,6},{5,7},{6,4},{7,5},{8,10},{9,11},{10,... | collective-permute-start | bytes 786440 | tf_op jit(solution)/shard_map/ppermute | solution.py:547
  6.6 18.3 %collective-permute-start.14 = (bf16[1024,128]{1,0:T(8,128)(2,1)S(1)}, bf16[1024,128]{1,0:T(8,128)(2,1)S(1)}, u32[]{:S(2)}, u32[]{:S(2)}) collective-permute-start(bf16[1024,128]{1,0:T(8,128)(2,1)S(1)} %get-tuple-element.36), channel_id=1, source_target_pairs={{0,2},{1,3},{2,0},{3,1},{4,6},{5,7},{6,4},{7,5},{8,10},{9,11},{10,... | collective-permute-start | bytes 786440 | tf_op jit(solution)/shard_map/ppermute | solution.py:547
  8.5 22.0 %collective-permute-start.15 = (bf16[64,2048]{1,0:T(8,128)(2,1)S(1)}, bf16[64,2048]{1,0:T(8,128)(2,1)S(1)}, u32[]{:S(2)}, u32[]{:S(2)}) collective-permute-start(bf16[64,2048]{1,0:T(8,128)(2,1)S(1)} %get-tuple-element.37), channel_id=1, source_target_pairs={{0,2},{1,3},{2,0},{3,1},{4,6},{5,7},{6,4},{7,5},{8,10},{9,11},{10,... | collective-permute-start | bytes 786440 | tf_op jit(solution)/shard_map/ppermute | solution.py:547
  8.6 27.5 %collective-permute-start.16 = (bf16[64,2048]{1,0:T(8,128)(2,1)S(1)}, bf16[64,2048]{1,0:T(8,128)(2,1)S(1)}, u32[]{:S(2)}, u32[]{:S(2)}) collective-permute-start(bf16[64,2048]{1,0:T(8,128)(2,1)S(1)} %get-tuple-element.38), channel_id=1, source_target_pairs={{0,2},{1,3},{2,0},{3,1},{4,6},{5,7},{6,4},{7,5},{8,10},{9,11},{10,... | collective-permute-start | bytes 786440 | tf_op jit(solution)/shard_map/ppermute | solution.py:547
  13.7 34.6 %collective-permute-start = (bf16[136,1024]{1,0:T(8,128)(2,1)S(1)}, bf16[136,1024]{1,0:T(8,128)(2,1)S(1)}, u32[]{:S(2)}, u32[]{:S(2)}) collective-permute-start(bf16[136,1024]{1,0:T(8,128)(2,1)S(1)} %get-tuple-element.23.own_ref), channel_id=1, source_target_pairs={{0,4},{4,8},{8,12},{1,5},{5,9},{9,13},{2,6},{6,10},{10,14},{3,7},{... | collective-permute-start | bytes 835592 | tf_op jit(solution)/shard_map/ppermute | solution.py:556
  19.3 22.5 %collective-permute-start.28 = (bf16[64,2048]{1,0:T(8,128)(2,1)S(1)}, bf16[64,2048]{1,0:T(8,128)(2,1)S(1)}, u32[]{:S(2)}, u32[]{:S(2)}) collective-permute-start(bf16[64,2048]{1,0:T(8,128)(2,1)S(1)} %get-tuple-element.39), channel_id=1, source_target_pairs={{0,2},{1,3},{2,0},{3,1},{4,6},{5,7},{6,4},{7,5},{8,10},{9,11},{10,... | collective-permute-start | bytes 786440 | tf_op jit(solution)/shard_map/ppermute | solution.py:547
  24.9 21.6 %collective-permute-start.11 = (bf16[1024,128]{1,0:T(8,128)(2,1)S(1)}, bf16[1024,128]{1,0:T(8,128)(2,1)S(1)}, u32[]{:S(2)}, u32[]{:S(2)}) collective-permute-start(bf16[1024,128]{1,0:T(8,128)(2,1)S(1)} %get-tuple-element.33), channel_id=1, source_target_pairs={{0,2},{1,3},{2,0},{3,1},{4,6},{5,7},{6,4},{7,5},{8,10},{9,11},{10,... | collective-permute-start | bytes 786440 | tf_op jit(solution)/shard_map/ppermute | solution.py:547
  30.5 19.8 %collective-permute-start.36 = (bf16[96,2048]{1,0:T(8,128)(2,1)S(1)}, bf16[96,2048]{1,0:T(8,128)(2,1)S(1)}, u32[]{:S(2)}, u32[]{:S(2)}) collective-permute-start(bf16[96,2048]{1,0:T(8,128)(2,1)S(1)} %get-tuple-element.42), channel_id=1, source_target_pairs={{0,8},{4,12},{8,0},{12,4},{1,9},{5,13},{9,1},{13,5},{2,10},{6,14},... | collective-permute-start | bytes 1179656 | tf_op jit(solution)/shard_map/ppermute | solution.py:553
  36.1 12.4 %collective-permute-start.1 = (bf16[136,1024]{1,0:T(8,128)(2,1)S(1)}, bf16[136,1024]{1,0:T(8,128)(2,1)S(1)}, u32[]{:S(2)}, u32[]{:S(2)}) collective-permute-start(bf16[136,1024]{1,0:T(8,128)(2,1)S(1)} %get-tuple-element.23.own_ref), channel_id=1, source_target_pairs={{0,8},{1,9},{2,10},{3,11},{16,24},{17,25},{18,26},{19,27}} | collective-permute-start | bytes 835592 | tf_op jit(solution)/shard_map/ppermute | solution.py:573
  41.7 8.6 %collective-permute-start.24 = (bf16[1024,128]{1,0:T(8,128)(2,1)S(1)}, bf16[1024,128]{1,0:T(8,128)(2,1)S(1)}, u32[]{:S(2)}, u32[]{:S(2)}) collective-permute-start(bf16[1024,128]{1,0:T(8,128)(2,1)S(1)} %collective-permute-done.12.refs_10_.refs_8_), channel_id=1, source_target_pairs={{0,16},{16,0},{1,17},{17,1},{2,18},{18,2},{3,19},{19,3},{4,20},{20... | collective-permute-start | bytes 786440 | tf_op jit(solution)/shard_map/ppermute | solution.py:550
  46.5 9.2 %collective-permute-start.25 = (bf16[1024,128]{1,0:T(8,128)(2,1)S(1)}, bf16[1024,128]{1,0:T(8,128)(2,1)S(1)}, u32[]{:S(2)}, u32[]{:S(2)}) collective-permute-start(bf16[1024,128]{1,0:T(8,128)(2,1)S(1)} %collective-permute-done.13.refs_11_.refs_9_), channel_id=1, source_target_pairs={{0,16},{16,0},{1,17},{17,1},{2,18},{18,2},{3,19},{19,3},{4,20},{20... | collective-permute-start | bytes 786440 | tf_op jit(solution)/shard_map/ppermute | solution.py:550
  48.3 13.0 %collective-permute-start.26 = (bf16[1024,128]{1,0:T(8,128)(2,1)S(1)}, bf16[1024,128]{1,0:T(8,128)(2,1)S(1)}, u32[]{:S(2)}, u32[]{:S(2)}) collective-permute-start(bf16[1024,128]{1,0:T(8,128)(2,1)S(1)} %collective-permute-done.14.refs_12_.refs_10_), channel_id=1, source_target_pairs={{0,16},{16,0},{1,17},{17,1},{2,18},{18,2},{3,19},{19,3},{4,20},{20... | collective-permute-start | bytes 786440 | tf_op jit(solution)/shard_map/ppermute | solution.py:550
  48.6 16.7 %collective-permute-start.27 = (bf16[64,2048]{1,0:T(8,128)(2,1)S(1)}, bf16[64,2048]{1,0:T(8,128)(2,1)S(1)}, u32[]{:S(2)}, u32[]{:S(2)}) collective-permute-start(bf16[64,2048]{1,0:T(8,128)(2,1)S(1)} %collective-permute-done.15.refs_13_.refs_11_), channel_id=1, source_target_pairs={{0,16},{16,0},{1,17},{17,1},{2,18},{18,2},{3,19},{19,3},{4,20},{20... | collective-permute-start | bytes 786440 | tf_op jit(solution)/shard_map/ppermute | solution.py:550
  50.3 14.9 %collective-permute-start.18 = (bf16[1024,128]{1,0:T(8,128)(2,1)S(1)}, bf16[1024,128]{1,0:T(8,128)(2,1)S(1)}, u32[]{:S(2)}, u32[]{:S(2)}) collective-permute-start(bf16[1024,128]{1,0:T(8,128)(2,1)S(1)} %collective-permute-done.12.refs_10_.refs_8_), channel_id=1, source_target_pairs={{0,1},{1,0},{2,3},{3,2},{4,5},{5,4},{6,7},{7,6},{8,9},{9,8},{10,11... | collective-permute-start | bytes 786440 | tf_op jit(solution)/shard_map/ppermute | solution.py:544
  50.3 15.4 %collective-permute-start.19 = (bf16[1024,128]{1,0:T(8,128)(2,1)S(1)}, bf16[1024,128]{1,0:T(8,128)(2,1)S(1)}, u32[]{:S(2)}, u32[]{:S(2)}) collective-permute-start(bf16[1024,128]{1,0:T(8,128)(2,1)S(1)} %collective-permute-done.13.refs_11_.refs_9_), channel_id=1, source_target_pairs={{0,1},{1,0},{2,3},{3,2},{4,5},{5,4},{6,7},{7,6},{8,9},{9,8},{10,11... | collective-permute-start | bytes 786440 | tf_op jit(solution)/shard_map/ppermute | solution.py:544
  55.7 10.7 %collective-permute-start.20 = (bf16[1024,128]{1,0:T(8,128)(2,1)S(1)}, bf16[1024,128]{1,0:T(8,128)(2,1)S(1)}, u32[]{:S(2)}, u32[]{:S(2)}) collective-permute-start(bf16[1024,128]{1,0:T(8,128)(2,1)S(1)} %collective-permute-done.14.refs_12_.refs_10_), channel_id=1, source_target_pairs={{0,1},{1,0},{2,3},{3,2},{4,5},{5,4},{6,7},{7,6},{8,9},{9,8},{10,11... | collective-permute-start | bytes 786440 | tf_op jit(solution)/shard_map/ppermute | solution.py:544
  61.3 7.0 %collective-permute-start.21 = (bf16[64,2048]{1,0:T(8,128)(2,1)S(1)}, bf16[64,2048]{1,0:T(8,128)(2,1)S(1)}, u32[]{:S(2)}, u32[]{:S(2)}) collective-permute-start(bf16[64,2048]{1,0:T(8,128)(2,1)S(1)} %collective-permute-done.15.refs_13_.refs_11_), channel_id=1, source_target_pairs={{0,1},{1,0},{2,3},{3,2},{4,5},{5,4},{6,7},{7,6},{8,9},{9,8},{10,11... | collective-permute-start | bytes 786440 | tf_op jit(solution)/shard_map/ppermute | solution.py:544
  65.2 3.1 %collective-permute-start.22 = (bf16[64,2048]{1,0:T(8,128)(2,1)S(1)}, bf16[64,2048]{1,0:T(8,128)(2,1)S(1)}, u32[]{:S(2)}, u32[]{:S(2)}) collective-permute-start(bf16[64,2048]{1,0:T(8,128)(2,1)S(1)} %collective-permute-done.16.refs_14_.refs_12_), channel_id=1, source_target_pairs={{0,1},{1,0},{2,3},{3,2},{4,5},{5,4},{6,7},{7,6},{8,9},{9,8},{10,11... | collective-permute-start | bytes 786440 | tf_op jit(solution)/shard_map/ppermute | solution.py:544
  65.2 3.8 %collective-permute-start.34 = (bf16[64,2048]{1,0:T(8,128)(2,1)S(1)}, bf16[64,2048]{1,0:T(8,128)(2,1)S(1)}, u32[]{:S(2)}, u32[]{:S(2)}) collective-permute-start(bf16[64,2048]{1,0:T(8,128)(2,1)S(1)} %collective-permute-done.28.refs_26_.refs_24_), channel_id=1, source_target_pairs={{0,1},{1,0},{2,3},{3,2},{4,5},{5,4},{6,7},{7,6},{8,9},{9,8},{10,11... | collective-permute-start | bytes 786440 | tf_op jit(solution)/shard_map/ppermute | solution.py:544
  65.7 9.6 %collective-permute-start.2 = (bf16[136,1024]{1,0:T(8,128)(2,1)S(1)}, bf16[136,1024]{1,0:T(8,128)(2,1)S(1)}, u32[]{:S(2)}, u32[]{:S(2)}) collective-permute-start(bf16[136,1024]{1,0:T(8,128)(2,1)S(1)} %collective-permute-done.refs_0_), channel_id=1, source_target_pairs={{8,12},{9,13},{10,14},{11,15},{24,28},{25,29},{26,30},{27,31}} | collective-permute-start | bytes 835592 | tf_op jit(solution)/shard_map/ppermute | solution.py:574
  66.4 8.4 %collective-permute-start.23 = (bf16[1024,128]{1,0:T(8,128)(2,1)S(1)}, bf16[1024,128]{1,0:T(8,128)(2,1)S(1)}, u32[]{:S(2)}, u32[]{:S(2)}) collective-permute-start(bf16[1024,128]{1,0:T(8,128)(2,1)S(1)} %collective-permute-done.11.refs_9_.refs_7_), channel_id=1, source_target_pairs={{0,16},{16,0},{1,17},{17,1},{2,18},{18,2},{3,19},{19,3},{4,20},{20... | collective-permute-start | bytes 786440 | tf_op jit(solution)/shard_map/ppermute | solution.py:550
  68.3 6.5 %collective-permute-start.17 = (bf16[1024,128]{1,0:T(8,128)(2,1)S(1)}, bf16[1024,128]{1,0:T(8,128)(2,1)S(1)}, u32[]{:S(2)}, u32[]{:S(2)}) collective-permute-start(bf16[1024,128]{1,0:T(8,128)(2,1)S(1)} %collective-permute-done.11.refs_9_.refs_7_), channel_id=1, source_target_pairs={{0,1},{1,0},{2,3},{3,2},{4,5},{5,4},{6,7},{7,6},{8,9},{9,8},{10,11... | collective-permute-start | bytes 786440 | tf_op jit(solution)/shard_map/ppermute | solution.py:544
  68.3 7.1 %collective-permute-start.3 = (bf16[136,1024]{1,0:T(8,128)(2,1)S(1)}, bf16[136,1024]{1,0:T(8,128)(2,1)S(1)}, u32[]{:S(2)}, u32[]{:S(2)}) collective-permute-start(bf16[136,1024]{1,0:T(8,128)(2,1)S(1)} %collective-permute-done.1.refs_1_), channel_id=1, source_target_pairs={{8,12},{9,13},{10,14},{11,15},{24,28},{25,29},{26,30},{27,31}} | collective-permute-start | bytes 835592 | tf_op jit(solution)/shard_map/ppermute | solution.py:574
  69.0 6.8 %collective-permute-start.30 = (bf16[1024,128]{1,0:T(8,128)(2,1)S(1)}, bf16[1024,128]{1,0:T(8,128)(2,1)S(1)}, u32[]{:S(2)}, u32[]{:S(2)}) collective-permute-start(bf16[1024,128]{1,0:T(8,128)(2,1)S(1)} %collective-permute-done.24.refs_22_.refs_20_), channel_id=1, source_target_pairs={{0,1},{1,0},{2,3},{3,2},{4,5},{5,4},{6,7},{7,6},{8,9},{9,8},{10,11... | collective-permute-start | bytes 786440 | tf_op jit(solution)/shard_map/ppermute | solution.py:544
  74.8 19.4 %collective-permute-start.8 = (bf16[2048,256]{1,0:T(8,128)(2,1)S(1)}, bf16[2048,256]{1,0:T(8,128)(2,1)S(1)}, u32[]{:S(2)}, u32[]{:S(2)}) collective-permute-start(bf16[2048,256]{1,0:T(8,128)(2,1)S(1)} %bitcast.14), channel_id=1, source_target_pairs={{0,1},{1,0},{2,3},{3,2},{4,5},{5,4},{6,7},{7,6},{8,9},{9,8},{10,11... | collective-permute-start | bytes 3145736 | tf_op jit(solution)/shard_map/ppermute | solution.py:544
  74.8 19.4 %collective-permute-start.10 = (bf16[256,2048]{1,0:T(8,128)(2,1)S(1)}, bf16[256,2048]{1,0:T(8,128)(2,1)S(1)}, u32[]{:S(2)}, u32[]{:S(2)}) collective-permute-start(bf16[256,2048]{1,0:T(8,128)(2,1)S(1)} %bitcast.22), channel_id=1, source_target_pairs={{0,1},{1,0},{2,3},{3,2},{4,5},{5,4},{6,7},{7,6},{8,9},{9,8},{10,11... | collective-permute-start | bytes 3145736 | tf_op jit(solution)/shard_map/ppermute | solution.py:544
  75.3 18.9 %collective-permute-start.9 = (bf16[2048,256]{1,0:T(8,128)(2,1)S(1)}, bf16[2048,256]{1,0:T(8,128)(2,1)S(1)}, u32[]{:S(2)}, u32[]{:S(2)}) collective-permute-start(bf16[2048,256]{1,0:T(8,128)(2,1)S(1)} %bitcast.18), channel_id=1, source_target_pairs={{0,1},{1,0},{2,3},{3,2},{4,5},{5,4},{6,7},{7,6},{8,9},{9,8},{10,11... | collective-permute-start | bytes 3145736 | tf_op jit(solution)/shard_map/ppermute | solution.py:544
  75.4 5.4 %collective-permute-start.31 = (bf16[1024,128]{1,0:T(8,128)(2,1)S(1)}, bf16[1024,128]{1,0:T(8,128)(2,1)S(1)}, u32[]{:S(2)}, u32[]{:S(2)}) collective-permute-start(bf16[1024,128]{1,0:T(8,128)(2,1)S(1)} %collective-permute-done.25.refs_23_.refs_21_), channel_id=1, source_target_pairs={{0,1},{1,0},{2,3},{3,2},{4,5},{5,4},{6,7},{7,6},{8,9},{9,8},{10,11... | collective-permute-start | bytes 786440 | tf_op jit(solution)/shard_map/ppermute | solution.py:544
  75.8 5.4 %collective-permute-start.32 = (bf16[1024,128]{1,0:T(8,128)(2,1)S(1)}, bf16[1024,128]{1,0:T(8,128)(2,1)S(1)}, u32[]{:S(2)}, u32[]{:S(2)}) collective-permute-start(bf16[1024,128]{1,0:T(8,128)(2,1)S(1)} %collective-permute-done.26.refs_24_.refs_22_), channel_id=1, source_target_pairs={{0,1},{1,0},{2,3},{3,2},{4,5},{5,4},{6,7},{7,6},{8,9},{9,8},{10,11... | collective-permute-start | bytes 786440 | tf_op jit(solution)/shard_map/ppermute | solution.py:544
  80.8 1.5 %collective-permute-start.33 = (bf16[64,2048]{1,0:T(8,128)(2,1)S(1)}, bf16[64,2048]{1,0:T(8,128)(2,1)S(1)}, u32[]{:S(2)}, u32[]{:S(2)}) collective-permute-start(bf16[64,2048]{1,0:T(8,128)(2,1)S(1)} %collective-permute-done.27.refs_25_.refs_23_), channel_id=1, source_target_pairs={{0,1},{1,0},{2,3},{3,2},{4,5},{5,4},{6,7},{7,6},{8,9},{9,8},{10,11... | collective-permute-start | bytes 786440 | tf_op jit(solution)/shard_map/ppermute | solution.py:544
  81.2 3.0 %collective-permute-start.29 = (bf16[1024,128]{1,0:T(8,128)(2,1)S(1)}, bf16[1024,128]{1,0:T(8,128)(2,1)S(1)}, u32[]{:S(2)}, u32[]{:S(2)}) collective-permute-start(bf16[1024,128]{1,0:T(8,128)(2,1)S(1)} %collective-permute-done.23.refs_21_.refs_19_), channel_id=1, source_target_pairs={{0,1},{1,0},{2,3},{3,2},{4,5},{5,4},{6,7},{7,6},{8,9},{9,8},{10,11... | collective-permute-start | bytes 786440 | tf_op jit(solution)/shard_map/ppermute | solution.py:544
  82.4 17.9 %collective-permute-start.6 = (bf16[96,2048]{1,0:T(8,128)(2,1)S(1)}, bf16[96,2048]{1,0:T(8,128)(2,1)S(1)}, u32[]{:S(2)}, u32[]{:S(2)}) collective-permute-start(bf16[96,2048]{1,0:T(8,128)(2,1)S(1)} %get-tuple-element.31), channel_id=1, source_target_pairs={{0,4},{4,8},{8,12},{12,0},{1,5},{5,9},{9,13},{13,1},{2,6},{6,10},{... | collective-permute-start | bytes 1179656 | tf_op jit(solution)/shard_map/ppermute | solution.py:553
  84.2 21.7 %collective-permute-start.7 = (bf16[96,2048]{1,0:T(8,128)(2,1)S(1)}, bf16[96,2048]{1,0:T(8,128)(2,1)S(1)}, u32[]{:S(2)}, u32[]{:S(2)}) collective-permute-start(bf16[96,2048]{1,0:T(8,128)(2,1)S(1)} %get-tuple-element.32), channel_id=1, source_target_pairs={{0,12},{4,0},{8,4},{12,8},{1,13},{5,1},{9,5},{13,9},{2,14},{6,2},{... | collective-permute-start | bytes 1179656 | tf_op jit(solution)/shard_map/ppermute | solution.py:553
  89.5 1.6 %copy-start.3 = (bf16[512,2048]{1,0:T(8,128)(2,1)S(1)}, bf16[512,2048]{1,0:T(8,128)(2,1)}, u32[]{:S(2)}) copy-start(bf16[512,2048]{1,0:T(8,128)(2,1)} %refs_4_.1) | copy-start | bytes 6291460
  94.2 31.8 %collective-permute-start.4 = (bf16[64,2048]{1,0:T(8,128)(2,1)S(1)}, bf16[64,2048]{1,0:T(8,128)(2,1)S(1)}, u32[]{:S(2)}, u32[]{:S(2)}) collective-permute-start(bf16[64,2048]{1,0:T(8,128)(2,1)S(1)} %get-tuple-element.25), channel_id=1, source_target_pairs={{0,1},{1,0},{2,3},{3,2},{4,5},{5,4},{6,7},{7,6},{8,9},{9,8},{10,11... | collective-permute-start | bytes 786440 | tf_op jit(solution)/shard_map/ppermute | solution.py:544
  96.4 36.0 %collective-permute-start.37 = (bf16[96,2048]{1,0:T(8,128)(2,1)S(1)}, bf16[96,2048]{1,0:T(8,128)(2,1)S(1)}, u32[]{:S(2)}, u32[]{:S(2)}) collective-permute-start(bf16[96,2048]{1,0:T(8,128)(2,1)S(1)} %shard_map.147), channel_id=1, source_target_pairs={{0,8},{4,12},{8,0},{12,4},{1,9},{5,13},{9,1},{13,5},{2,10},{6,14},... | collective-permute-start | bytes 1179656 | tf_op jit(solution)/shard_map/ppermute | solution.py:553
  105.8 22.3 %copy-start.6 = (s32[128,2]{0,1:T(2,128)S(1)}, s32[128,2]{0,1:T(2,128)}, u32[]{:S(2)}) copy-start(s32[128,2]{0,1:T(2,128)} %param.21) | copy-start | bytes 3076
  105.8 22.3 %copy-start.7 = (f32[128,2]{0,1:T(2,128)S(1)}, f32[128,2]{0,1:T(2,128)}, u32[]{:S(2)}) copy-start(f32[128,2]{0,1:T(2,128)} %param.22) | copy-start | bytes 3076
  105.8 25.8 %copy-start.5 = (f32[2048]{0:T(1024)S(1)}, f32[2048]{0:T(1024)}, u32[]{:S(2)}) copy-start(f32[2048]{0:T(1024)} %param.18) | copy-start | bytes 24580
  109.7 31.0 %collective-permute-start.35 = (bf16[96,2048]{1,0:T(8,128)(2,1)S(1)}, bf16[96,2048]{1,0:T(8,128)(2,1)S(1)}, u32[]{:S(2)}, u32[]{:S(2)}) collective-permute-start(bf16[96,2048]{1,0:T(8,128)(2,1)S(1)} %get-tuple-element.41), channel_id=1, source_target_pairs={{0,12},{4,0},{8,4},{12,8},{1,13},{5,1},{9,5},{13,9},{2,14},{6,2},{... | collective-permute-start | bytes 1179656 | tf_op jit(solution)/shard_map/ppermute | solution.py:553
  112.7 28.0 %collective-permute-start.38 = (bf16[96,2048]{1,0:T(8,128)(2,1)S(1)}, bf16[96,2048]{1,0:T(8,128)(2,1)S(1)}, u32[]{:S(2)}, u32[]{:S(2)}) collective-permute-start(bf16[96,2048]{1,0:T(8,128)(2,1)S(1)} %get-tuple-element.43), channel_id=1, source_target_pairs={{0,4},{4,8},{8,12},{12,0},{1,5},{5,9},{9,13},{13,1},{2,6},{6,10},{... | collective-permute-start | bytes 1179656 | tf_op jit(solution)/shard_map/ppermute | solution.py:553
  126.6 5.0 %collective-permute-start.5 = (bf16[32,2048]{1,0:T(8,128)(2,1)S(1)}, bf16[32,2048]{1,0:T(8,128)(2,1)S(1)}, u32[]{:S(2)}, u32[]{:S(2)}) collective-permute-start(bf16[32,2048]{1,0:T(8,128)(2,1)S(1)} %get-tuple-element.27), channel_id=1, source_target_pairs={{0,2},{1,3},{2,0},{3,1},{4,6},{5,7},{6,4},{7,5},{8,10},{9,11},{10,... | collective-permute-start | bytes 393224 | tf_op jit(solution)/shard_map/ppermute | solution.py:547

commit v6 on v5

--- a/solution.py
+++ b/solution.py
@@ -343,22 +343,29 @@
     return call(body, outs, [SMEM, VMEM, VMEM])(place, ids, scores)
 
 
-def combine_rows(high, low, returned):
+def combine_rows(high, low, returned, chosen, before):
     rows = high.shape[1]
-    width = returned[0].shape[1]
+    capacity, width = returned[0].shape
 
     def body(high_ref, low_ref, *refs):
-        outputs = jnp.concatenate([ref[...] for ref in refs[:-1]], axis=0)
-        weights = jnp.concatenate([high_ref[...], low_ref[...]], axis=1)
+        outputs = jnp.concatenate([ref[...] for ref in refs[: len(chosen)]], axis=0)
+        both = jnp.concatenate([high_ref[...], low_ref[...]], axis=1)
+        weights = jnp.concatenate([both[d * capacity : (d + 1) * capacity] for d in chosen], axis=0)
         total = lax.dot_general(
             weights, outputs, (((0,), (0,)), ((), ())), preferred_element_type=jnp.float32
         )
-        refs[-1][...] = (total[:rows] + total[rows:]).astype(jnp.bfloat16)
-
+        total = total[:rows] + total[rows:]
+        if before is not None:
+            total = total + refs[len(chosen)][...]
+        refs[-1][...] = total.astype(refs[-1].dtype)
+
+    extra = [] if before is None else [before]
     return call(
-        body, shape_of((rows, width)), [VMEM] * (2 + len(returned)),
-        flops=4 * high.shape[0] * rows * width,
-    )(high, low, *returned)
+        body,
+        shape_of((rows, width), jnp.float32 if before is None else jnp.bfloat16),
+        [VMEM] * (2 + len(chosen) + len(extra)),
+        flops=4 * len(chosen) * capacity * rows * width,
+    )(high, low, *(returned[d] for d in chosen), *extra)
 
 
 def expert_rows(rows_in, pieces):
@@ -597,7 +604,8 @@
     outer, inner = pair_sum(place, kept, core(send))
     mixed = finish(inner, across(outer), mix_gain)
     high, low = combine_plan(place, expert_ids.T, expert_scores.T, blocks, capacity)
-    experts_mixed = combine_rows(high, low, returned)
+    partial = combine_rows(high, low, returned, (0, 2), None)
+    experts_mixed = combine_rows(high, low, returned, (1, 3), partial)
     return (mixed, experts_mixed)
 
 

time: 142 us -> 142 us (level)
  no operation moved by 1% of the time
where the time goes in v6:
time: 142 us
  starting transfers between devices  64.2 us (45%)
  waiting for transfers between devices  57.9 us (41%)
  Pallas kernels  17.3 us (12%)
  local copies, waits for them, and re-layouts  1.62 us (1%)
    ppermute x6, starting transfers between devices, turn(): lax.ppermute(array, 'ep', [(i, (i + d) % blocks) for i in range(blocks)])  30.4 us
    ppermute x5, waiting for transfers between devices, beside(): return lax.ppermute(array, 'grp', [(0, 1), (1, 0)])  19.6 us
    ppermute x8, waiting for transfers between devices, across(): return lax.ppermute(array, 'tp', [(i, i ^ 2) for i in range(shards)])  18.8 us
    ppermute x6, waiting for transfers between devices, turn(): lax.ppermute(array, 'ep', [(i, (i + d) % blocks) for i in range(blocks)])  13.3 us
    ppermute x8, starting transfers between devices, across(): return lax.ppermute(array, 'tp', [(i, i ^ 2) for i in range(shards)])  12.7 us
    ppermute x5, starting transfers between devices, beside(): return lax.ppermute(array, 'grp', [(0, 1), (1, 0)])  7.72 us
    ppermute x16, waiting for transfers between devices, core(): return lax.ppermute(array, 'tp', [(i, i ^ 1) for i in range(shards)])  6.2 us
    pallas_call x2, Pallas kernels, expert_rows(): call(body, [shape_of((capacity, width))] * count, [VMEM] * (count + len(f...  6.05 us
  transfers between devices with their start and end apart: 39, of which 17 were waited for; matrix products, arithmetic and copies ran while one was open for 0% of the time, Pallas kernels for 9%

profile of v6, /device:TPU:0, one launch (start us, length us, event | category | flops | bytes accessed | tf_op | source)
XLA Modules:
  0.0 141.9 jit_solution(18152242948309381240)
XLA Ops:
  0.6 0.1 pad_add_fusion.place_ref
  0.7 2.7 %shard_map.145 = (bf16[96,2048]{1,0:T(8,128)(2,1)S(1)}, bf16[96,2048]{1,0:T(8,128)(2,1)S(1)}, bf16[96,2048]{1,0:T(8,128)(2,1)S(1)}, bf16[96,2048]{1,0:T(8,128)(2...) custom-call(s32[4]{0:T(128)S(1)} %pad_add_fusion.place_ref, ...), custom_call_target="tpu_custom_call" | custom-call | flops 201326592 | tf_op jit(solution)/shard_map/pallas_call | solution.py:311
  3.5 3.0 %collective-permute-start.12 = (bf16[1024,128]{1,0:T(8,128)(2,1)S(1)}, bf16[1024,128]{1,0:T(8,128)(2,1)S(1)}, u32[]{:S(2)}, u32[]{:S(2)}) collective-permute-start(bf16[1024,128]{1,0:T(8,128)(2,1)S(1)} %get-tuple-element.34), channel_id=1, source_target_pairs={{0,2},{1,3},{2,0},{3,1},{4,6},{5,7},{6,4},{7,5},{8,10},{9,11},{10,... | collective-permute-start | bytes 786440 | tf_op jit(solution)/shard_map/ppermute | solution.py:554
  6.5 0.1 collective-permute-start.13
  6.6 1.9 %collective-permute-start.14 = (bf16[1024,128]{1,0:T(8,128)(2,1)S(1)}, bf16[1024,128]{1,0:T(8,128)(2,1)S(1)}, u32[]{:S(2)}, u32[]{:S(2)}) collective-permute-start(bf16[1024,128]{1,0:T(8,128)(2,1)S(1)} %get-tuple-element.36), channel_id=1, source_target_pairs={{0,2},{1,3},{2,0},{3,1},{4,6},{5,7},{6,4},{7,5},{8,10},{9,11},{10,... | collective-permute-start | bytes 786440 | tf_op jit(solution)/shard_map/ppermute | solution.py:554
  8.5 0.1 collective-permute-start.15
  8.6 1.9 %collective-permute-start.16 = (bf16[64,2048]{1,0:T(8,128)(2,1)S(1)}, bf16[64,2048]{1,0:T(8,128)(2,1)S(1)}, u32[]{:S(2)}, u32[]{:S(2)}) collective-permute-start(bf16[64,2048]{1,0:T(8,128)(2,1)S(1)} %get-tuple-element.38), channel_id=1, source_target_pairs={{0,2},{1,3},{2,0},{3,1},{4,6},{5,7},{6,4},{7,5},{8,10},{9,11},{10,... | collective-permute-start | bytes 786440 | tf_op jit(solution)/shard_map/ppermute | solution.py:554
  10.6 1.6 %shard_map.140 = (bf16[136,1024]{1,0:T(8,128)(2,1)S(1)}, bf16[1024,128]{1,0:T(8,128)(2,1)S(1)}) custom-call(s32[4]{0:T(128)S(1)} %pad_add_fusion.place_ref, bf16[8,128]{1,0:T(8,128)(2,1)} %bitcast.30, bf16[128,512]{1,0:T(8,128)(2,1)} %keys_hbm.1, bf16[128,512]{1,0:T(8,128)(2,1)} %values_hbm.1, bf16[2048,256]{1,0:T(8,128)(2,1)} %bitcast.13), custom_call_target="tpu_custom_call" | custom-call | tf_op jit(solution)/shard_map/pallas_call | solution.py:252
  12.2 1.5 %collective-permute-done.12.refs_10_.refs_8_ = bf16[1024,128]{1,0:T(8,128)(2,1)S(1)} collective-permute-done((bf16[1024,128]{1,0:T(8,128)(2,1)S(1)}, bf16[1024,128]{1,0:T(8,128)(2,1)S(1)}, u32[]{:S(2)}, u32[]{:S(2)}) %collective-permute-start.12) | collective-permute-done | bytes 262176 | tf_op jit(solution)/shard_map/ppermute | solution.py:554
  13.7 4.0 %collective-permute-start = (bf16[136,1024]{1,0:T(8,128)(2,1)S(1)}, bf16[136,1024]{1,0:T(8,128)(2,1)S(1)}, u32[]{:S(2)}, u32[]{:S(2)}) collective-permute-start(bf16[136,1024]{1,0:T(8,128)(2,1)S(1)} %get-tuple-element.23.own_ref), channel_id=1, source_target_pairs={{0,4},{4,8},{8,12},{1,5},{5,9},{9,13},{2,6},{6,10},{10,14},{3,7},{... | collective-permute-start | bytes 835592 | tf_op jit(solution)/shard_map/ppermute | solution.py:563
  17.7 1.6 %collective-permute-done.13.refs_11_.refs_9_ = bf16[1024,128]{1,0:T(8,128)(2,1)S(1)} collective-permute-done((bf16[1024,128]{1,0:T(8,128)(2,1)S(1)}, bf16[1024,128]{1,0:T(8,128)(2,1)S(1)}, u32[]{:S(2)}, u32[]{:S(2)}) %collective-permute-start.13) | collective-permute-done | bytes 262176 | tf_op jit(solution)/shard_map/ppermute | solution.py:554
  19.3 2.0 %collective-permute-start.28 = (bf16[64,2048]{1,0:T(8,128)(2,1)S(1)}, bf16[64,2048]{1,0:T(8,128)(2,1)S(1)}, u32[]{:S(2)}, u32[]{:S(2)}) collective-permute-start(bf16[64,2048]{1,0:T(8,128)(2,1)S(1)} %get-tuple-element.39), channel_id=1, source_target_pairs={{0,2},{1,3},{2,0},{3,1},{4,6},{5,7},{6,4},{7,5},{8,10},{9,11},{10,... | collective-permute-start | bytes 786440 | tf_op jit(solution)/shard_map/ppermute | solution.py:554
  21.3 3.6 %collective-permute-done.14.refs_12_.refs_10_ = bf16[1024,128]{1,0:T(8,128)(2,1)S(1)} collective-permute-done((bf16[1024,128]{1,0:T(8,128)(2,1)S(1)}, bf16[1024,128]{1,0:T(8,128)(2,1)S(1)}, u32[]{:S(2)}, u32[]{:S(2)}) %collective-permute-start.14) | collective-permute-done | bytes 262176 | tf_op jit(solution)/shard_map/ppermute | solution.py:554
  24.9 2.0 %collective-permute-start.11 = (bf16[1024,128]{1,0:T(8,128)(2,1)S(1)}, bf16[1024,128]{1,0:T(8,128)(2,1)S(1)}, u32[]{:S(2)}, u32[]{:S(2)}) collective-permute-start(bf16[1024,128]{1,0:T(8,128)(2,1)S(1)} %get-tuple-element.33), channel_id=1, source_target_pairs={{0,2},{1,3},{2,0},{3,1},{4,6},{5,7},{6,4},{7,5},{8,10},{9,11},{10,... | collective-permute-start | bytes 786440 | tf_op jit(solution)/shard_map/ppermute | solution.py:554
  26.9 3.6 %collective-permute-done.15.refs_13_.refs_11_ = bf16[64,2048]{1,0:T(8,128)(2,1)S(1)} collective-permute-done((bf16[64,2048]{1,0:T(8,128)(2,1)S(1)}, bf16[64,2048]{1,0:T(8,128)(2,1)S(1)}, u32[]{:S(2)}, u32[]{:S(2)}) %collective-permute-start.15) | collective-permute-done | bytes 262176 | tf_op jit(solution)/shard_map/ppermute | solution.py:554
  30.5 3.1 %collective-permute-start.37 = (bf16[96,2048]{1,0:T(8,128)(2,1)S(1)}, bf16[96,2048]{1,0:T(8,128)(2,1)S(1)}, u32[]{:S(2)}, u32[]{:S(2)}) collective-permute-start(bf16[96,2048]{1,0:T(8,128)(2,1)S(1)} %get-tuple-element.43), channel_id=1, source_target_pairs={{0,8},{4,12},{8,0},{12,4},{1,9},{5,13},{9,1},{13,5},{2,10},{6,14},... | collective-permute-start | bytes 1179656 | tf_op jit(solution)/shard_map/ppermute | solution.py:560
  33.6 2.5 %collective-permute-done.16.refs_14_.refs_12_ = bf16[64,2048]{1,0:T(8,128)(2,1)S(1)} collective-permute-done((bf16[64,2048]{1,0:T(8,128)(2,1)S(1)}, bf16[64,2048]{1,0:T(8,128)(2,1)S(1)}, u32[]{:S(2)}, u32[]{:S(2)}) %collective-permute-start.16) | collective-permute-done | bytes 262176 | tf_op jit(solution)/shard_map/ppermute | solution.py:554
  36.1 5.0 %collective-permute-start.1 = (bf16[136,1024]{1,0:T(8,128)(2,1)S(1)}, bf16[136,1024]{1,0:T(8,128)(2,1)S(1)}, u32[]{:S(2)}, u32[]{:S(2)}) collective-permute-start(bf16[136,1024]{1,0:T(8,128)(2,1)S(1)} %get-tuple-element.23.own_ref), channel_id=1, source_target_pairs={{0,8},{1,9},{2,10},{3,11},{16,24},{17,25},{18,26},{19,27}} | collective-permute-start | bytes 835592 | tf_op jit(solution)/shard_map/ppermute | solution.py:580
  41.2 0.6 collective-permute-done.28.refs_26_.refs_24_
  41.7 2.1 %collective-permute-start.24 = (bf16[1024,128]{1,0:T(8,128)(2,1)S(1)}, bf16[1024,128]{1,0:T(8,128)(2,1)S(1)}, u32[]{:S(2)}, u32[]{:S(2)}) collective-permute-start(bf16[1024,128]{1,0:T(8,128)(2,1)S(1)} %collective-permute-done.12.refs_10_.refs_8_), channel_id=1, source_target_pairs={{0,16},{16,0},{1,17},{17,1},{2,18},{18,2},{3,19},{19,3},{4,20},{20... | collective-permute-start | bytes 786440 | tf_op jit(solution)/shard_map/ppermute | solution.py:557
  43.8 2.7 %collective-permute-done.11.refs_9_.refs_7_ = bf16[1024,128]{1,0:T(8,128)(2,1)S(1)} collective-permute-done((bf16[1024,128]{1,0:T(8,128)(2,1)S(1)}, bf16[1024,128]{1,0:T(8,128)(2,1)S(1)}, u32[]{:S(2)}, u32[]{:S(2)}) %collective-permute-start.11) | collective-permute-done | bytes 262176 | tf_op jit(solution)/shard_map/ppermute | solution.py:554
  46.5 1.8 %collective-permute-start.25 = (bf16[1024,128]{1,0:T(8,128)(2,1)S(1)}, bf16[1024,128]{1,0:T(8,128)(2,1)S(1)}, u32[]{:S(2)}, u32[]{:S(2)}) collective-permute-start(bf16[1024,128]{1,0:T(8,128)(2,1)S(1)} %collective-permute-done.13.refs_11_.refs_9_), channel_id=1, source_target_pairs={{0,16},{16,0},{1,17},{17,1},{2,18},{18,2},{3,19},{19,3},{4,20},{20... | collective-permute-start | bytes 786440 | tf_op jit(solution)/shard_map/ppermute | solution.py:557
  48.3 0.3 collective-permute-start.26
  48.5 0.0 collective-permute-done.1.refs_1_
  48.6 1.8 %collective-permute-start.27 = (bf16[64,2048]{1,0:T(8,128)(2,1)S(1)}, bf16[64,2048]{1,0:T(8,128)(2,1)S(1)}, u32[]{:S(2)}, u32[]{:S(2)}) collective-permute-start(bf16[64,2048]{1,0:T(8,128)(2,1)S(1)} %collective-permute-done.15.refs_13_.refs_11_), channel_id=1, source_target_pairs={{0,16},{16,0},{1,17},{17,1},{2,18},{18,2},{3,19},{19,3},{4,20},{20... | collective-permute-start | bytes 786440 | tf_op jit(solution)/shard_map/ppermute | solution.py:557
  50.3 0.0 collective-permute-done.37.refs_0_
  50.3 0.5 collective-permute-start.19
  50.8 4.9 %collective-permute-done.25.refs_23_.refs_21_ = bf16[1024,128]{1,0:T(8,128)(2,1)S(1)} collective-permute-done((bf16[1024,128]{1,0:T(8,128)(2,1)S(1)}, bf16[1024,128]{1,0:T(8,128)(2,1)S(1)}, u32[]{:S(2)}, u32[]{:S(2)}) %collective-permute-start.25) | collective-permute-done | bytes 262176 | tf_op jit(solution)/shard_map/ppermute | solution.py:557
  55.7 5.6 %collective-permute-done.26.refs_24_.refs_22_ = bf16[1024,128]{1,0:T(8,128)(2,1)S(1)} collective-permute-done((bf16[1024,128]{1,0:T(8,128)(2,1)S(1)}, bf16[1024,128]{1,0:T(8,128)(2,1)S(1)}, u32[]{:S(2)}, u32[]{:S(2)}) %collective-permute-start.26) | collective-permute-done | bytes 262176 | tf_op jit(solution)/shard_map/ppermute | solution.py:557
  61.3 3.9 %collective-permute-done.27.refs_25_.refs_23_ = bf16[64,2048]{1,0:T(8,128)(2,1)S(1)} collective-permute-done((bf16[64,2048]{1,0:T(8,128)(2,1)S(1)}, bf16[64,2048]{1,0:T(8,128)(2,1)S(1)}, u32[]{:S(2)}, u32[]{:S(2)}) %collective-permute-start.27) | collective-permute-done | bytes 262176 | tf_op jit(solution)/shard_map/ppermute | solution.py:557
  65.2 0.5 collective-permute-start.34
  65.7 0.7 collective-permute-start.2
  66.4 1.9 %collective-permute-start.23 = (bf16[1024,128]{1,0:T(8,128)(2,1)S(1)}, bf16[1024,128]{1,0:T(8,128)(2,1)S(1)}, u32[]{:S(2)}, u32[]{:S(2)}) collective-permute-start(bf16[1024,128]{1,0:T(8,128)(2,1)S(1)} %collective-permute-done.11.refs_9_.refs_7_), channel_id=1, source_target_pairs={{0,16},{16,0},{1,17},{17,1},{2,18},{18,2},{3,19},{19,3},{4,20},{20... | collective-permute-start | bytes 786440 | tf_op jit(solution)/shard_map/ppermute | solution.py:557
  68.3 0.7 collective-permute-start.3
  69.0 0.6 collective-permute-start.30
  69.6 5.2 %collective-permute-done.23.refs_21_.refs_19_ = bf16[1024,128]{1,0:T(8,128)(2,1)S(1)} collective-permute-done((bf16[1024,128]{1,0:T(8,128)(2,1)S(1)}, bf16[1024,128]{1,0:T(8,128)(2,1)S(1)}, u32[]{:S(2)}, u32[]{:S(2)}) %collective-permute-start.23) | collective-permute-done | bytes 262176 | tf_op jit(solution)/shard_map/ppermute | solution.py:557
  74.8 0.5 collective-permute-start.10
  75.3 0.1 collective-permute-start.9
  75.4 0.4 collective-permute-start.31
  75.8 0.1 collective-permute-start.32
  75.9 4.9 %collective-permute-done.31.refs_29_.refs_27_ = bf16[1024,128]{1,0:T(8,128)(2,1)S(1)} collective-permute-done((bf16[1024,128]{1,0:T(8,128)(2,1)S(1)}, bf16[1024,128]{1,0:T(8,128)(2,1)S(1)}, u32[]{:S(2)}, u32[]{:S(2)}) %collective-permute-start.31) | collective-permute-done | bytes 262176 | tf_op jit(solution)/shard_map/ppermute | solution.py:551
  80.8 0.1 collective-permute-start.33
  81.0 0.2 collective-permute-done.32.refs_30_.refs_28_
  81.2 0.1 collective-permute-start.29
  81.3 1.0 collective-permute-done.33.refs_31_.refs_29_
  82.4 1.8 %collective-permute-start.6 = (bf16[96,2048]{1,0:T(8,128)(2,1)S(1)}, bf16[96,2048]{1,0:T(8,128)(2,1)S(1)}, u32[]{:S(2)}, u32[]{:S(2)}) collective-permute-start(bf16[96,2048]{1,0:T(8,128)(2,1)S(1)} %get-tuple-element.31), channel_id=1, source_target_pairs={{0,4},{4,8},{8,12},{12,0},{1,5},{5,9},{9,13},{13,1},{2,6},{6,10},{... | collective-permute-start | bytes 1179656 | tf_op jit(solution)/shard_map/ppermute | solution.py:560
  84.2 5.3 %collective-permute-start.7 = (bf16[96,2048]{1,0:T(8,128)(2,1)S(1)}, bf16[96,2048]{1,0:T(8,128)(2,1)S(1)}, u32[]{:S(2)}, u32[]{:S(2)}) collective-permute-start(bf16[96,2048]{1,0:T(8,128)(2,1)S(1)} %get-tuple-element.32), channel_id=1, source_target_pairs={{0,12},{4,0},{8,4},{12,8},{1,13},{5,1},{9,5},{13,9},{2,14},{6,2},{... | collective-permute-start | bytes 1179656 | tf_op jit(solution)/shard_map/ppermute | solution.py:560
  89.5 1.6 %copy-done.3 = bf16[512,2048]{1,0:T(8,128)(2,1)S(1)} copy-done((bf16[512,2048]{1,0:T(8,128)(2,1)S(1)}, bf16[512,2048]{1,0:T(8,128)(2,1)}, u32[]{:S(2)}) %copy-start.3) | copy-done | bytes 2097176
  91.1 3.0 %shard_map.141 = (bf16[64,2048]{1,0:T(8,128)(2,1)S(1)}, f32[64,2048]{1,0:T(8,128)S(1)}) custom-call(s32[4]{0:T(128)S(1)} %pad_add_fusion.place_ref, bf16[128,512]{1,0:T(8,128)(2,1)S(1)} %copy-done.4, bf16[136,1024]{1,0:T(8,128)(2,1)S(1)} %get-tuple-element.23.own_ref, bf16[136,1024]{1,0:T(8,128)(2,1)S(1)} %collective-permute-done.refs_0_, ...), custom_call_target="tpu_custom_call" | custom-call | flops 402653184 | tf_op jit(solution)/shard_map/pallas_call | solution.py:508
  94.2 0.1 collective-permute-start.4
  94.3 2.2 %shard_map.147 = bf16[96,2048]{1,0:T(8,128)(2,1)S(1)} custom-call(bf16[96,2048]{1,0:T(8,128)(2,1)S(1)} %collective-permute-done.37.refs_0_, bf16[2048,256]{1,0:T(8,128)(2,1)S(1)} %bitcast.15, bf16[2048,256]{1,0:T(8,128)(2,1)S(1)} %bitcast.19, bf16[256,2048]{1,0:T(8,128)(2,1)S(1)} %bitcast.23, bf16[2048,256]{1,0:T(8,128)(2,1)S(1)} %collective-permute-done.8.refs_6_.refs_4_, ...), custom_call_target="tpu_custom_call" | custom-call | flops 1207959552 | tf_op jit(solution)/shard_map/pallas_call | solution.py:400
  96.4 3.8 %collective-permute-start.38 = (bf16[96,2048]{1,0:T(8,128)(2,1)S(1)}, bf16[96,2048]{1,0:T(8,128)(2,1)S(1)}, u32[]{:S(2)}, u32[]{:S(2)}) collective-permute-start(bf16[96,2048]{1,0:T(8,128)(2,1)S(1)} %shard_map.147), channel_id=1, source_target_pairs={{0,8},{4,12},{8,0},{12,4},{1,9},{5,13},{9,1},{13,5},{2,10},{6,14},... | collective-permute-start | bytes 1179656 | tf_op jit(solution)/shard_map/ppermute | solution.py:560
  100.3 5.5 %collective-permute-done.7.refs_2_ = bf16[96,2048]{1,0:T(8,128)(2,1)S(1)} collective-permute-done((bf16[96,2048]{1,0:T(8,128)(2,1)S(1)}, bf16[96,2048]{1,0:T(8,128)(2,1)S(1)}, u32[]{:S(2)}, u32[]{:S(2)}) %collective-permute-start.7) | collective-permute-done | bytes 393248 | tf_op jit(solution)/shard_map/ppermute | solution.py:560
  105.8 3.9 %shard_map.146 = (bf16[96,2048]{1,0:T(8,128)(2,1)S(1)}, bf16[96,2048]{1,0:T(8,128)(2,1)S(1)}, bf16[96,2048]{1,0:T(8,128)(2,1)S(1)}) custom-call(bf16[96,2048]{1,0:T(8,128)(2,1)S(1)} %get-tuple-element.30.refs_0_, bf16[96,2048]{1,0:T(8,128)(2,1)S(1)} %collective-permute-done.6.refs_1_, bf16[96,2048]{1,0:T(8,128)(2,1)S(1)} %collective-permute-done.7.refs_2_, ...), custom_call_target="tpu_custom_call" | custom-call | flops 3623878656 | tf_op jit(solution)/shard_map/pallas_call | solution.py:400
  109.7 3.0 %collective-permute-start.35 = (bf16[96,2048]{1,0:T(8,128)(2,1)S(1)}, bf16[96,2048]{1,0:T(8,128)(2,1)S(1)}, u32[]{:S(2)}, u32[]{:S(2)}) collective-permute-start(bf16[96,2048]{1,0:T(8,128)(2,1)S(1)} %get-tuple-element.40), channel_id=1, source_target_pairs={{0,12},{4,0},{8,4},{12,8},{1,13},{5,1},{9,5},{13,9},{2,14},{6,2},{... | collective-permute-start | bytes 1179656 | tf_op jit(solution)/shard_map/ppermute | solution.py:560
  112.7 13.3 %collective-permute-start.36 = (bf16[96,2048]{1,0:T(8,128)(2,1)S(1)}, bf16[96,2048]{1,0:T(8,128)(2,1)S(1)}, u32[]{:S(2)}, u32[]{:S(2)}) collective-permute-start(bf16[96,2048]{1,0:T(8,128)(2,1)S(1)} %get-tuple-element.41), channel_id=1, source_target_pairs={{0,4},{4,8},{8,12},{12,0},{1,5},{5,9},{9,13},{13,1},{2,6},{6,10},{... | collective-permute-start | bytes 1179656 | tf_op jit(solution)/shard_map/ppermute | solution.py:560
  126.0 0.6 shard_map.142
  126.6 1.6 %collective-permute-start.5 = (bf16[32,2048]{1,0:T(8,128)(2,1)S(1)}, bf16[32,2048]{1,0:T(8,128)(2,1)S(1)}, u32[]{:S(2)}, u32[]{:S(2)}) collective-permute-start(bf16[32,2048]{1,0:T(8,128)(2,1)S(1)} %get-tuple-element.27), channel_id=1, source_target_pairs={{0,2},{1,3},{2,0},{3,1},{4,6},{5,7},{6,4},{7,5},{8,10},{9,11},{10,... | collective-permute-start | bytes 393224 | tf_op jit(solution)/shard_map/ppermute | solution.py:554
  128.2 0.7 shard_map.144
  128.9 2.7 %collective-permute-done.5.received_ref = bf16[32,2048]{1,0:T(8,128)(2,1)S(1)} collective-permute-done((bf16[32,2048]{1,0:T(8,128)(2,1)S(1)}, bf16[32,2048]{1,0:T(8,128)(2,1)S(1)}, u32[]{:S(2)}, u32[]{:S(2)}) %collective-permute-start.5) | collective-permute-done | bytes 131104 | tf_op jit(solution)/shard_map/ppermute | solution.py:554
  131.6 0.8 shard_map.143
  132.4 0.4 shard_map.148.refs_2_
  132.9 7.8 %collective-permute-done.35.refs_0_ = bf16[96,2048]{1,0:T(8,128)(2,1)S(1)} collective-permute-done((bf16[96,2048]{1,0:T(8,128)(2,1)S(1)}, bf16[96,2048]{1,0:T(8,128)(2,1)S(1)}, u32[]{:S(2)}, u32[]{:S(2)}) %collective-permute-start.35) | collective-permute-done | bytes 393248 | tf_op jit(solution)/shard_map/ppermute | solution.py:560
  140.7 1.2 shard_map.149
  (41 shorter events, 0.1 us)
Async XLA Ops:
  0.7 74.1 %copy-start = (bf16[1,2048,256]{2,1,0:T(8,128)(2,1)S(1)}, bf16[1,2048,256]{2,1,0:T(8,128)(2,1)}, u32[]{:S(2)}) copy-start(bf16[1,2048,256]{2,1,0:T(8,128)(2,1)} %param.23) | copy-start | bytes 3145732
  0.7 74.1 %copy-start.2 = (bf16[1,256,2048]{2,1,0:T(8,128)(2,1)S(1)}, bf16[1,256,2048]{2,1,0:T(8,128)(2,1)}, u32[]{:S(2)}) copy-start(bf16[1,256,2048]{2,1,0:T(8,128)(2,1)} %param.25) | copy-start | bytes 3145732
  0.7 74.6 %copy-start.1 = (bf16[1,2048,256]{2,1,0:T(8,128)(2,1)S(1)}, bf16[1,2048,256]{2,1,0:T(8,128)(2,1)}, u32[]{:S(2)}) copy-start(bf16[1,2048,256]{2,1,0:T(8,128)(2,1)} %param.24) | copy-start | bytes 3145732
  0.7 88.8 %copy-start.4 = (bf16[128,512]{1,0:T(8,128)(2,1)S(1)}, bf16[128,512]{1,0:T(8,128)(2,1)}, u32[]{:S(2)}) copy-start(bf16[128,512]{1,0:T(8,128)(2,1)} %q_ref.1) | copy-start | bytes 393220
  3.5 10.2 %collective-permute-start.12 = (bf16[1024,128]{1,0:T(8,128)(2,1)S(1)}, bf16[1024,128]{1,0:T(8,128)(2,1)S(1)}, u32[]{:S(2)}, u32[]{:S(2)}) collective-permute-start(bf16[1024,128]{1,0:T(8,128)(2,1)S(1)} %get-tuple-element.34), channel_id=1, source_target_pairs={{0,2},{1,3},{2,0},{3,1},{4,6},{5,7},{6,4},{7,5},{8,10},{9,11},{10,... | collective-permute-start | bytes 786440 | tf_op jit(solution)/shard_map/ppermute | solution.py:554
  6.5 12.8 %collective-permute-start.13 = (bf16[1024,128]{1,0:T(8,128)(2,1)S(1)}, bf16[1024,128]{1,0:T(8,128)(2,1)S(1)}, u32[]{:S(2)}, u32[]{:S(2)}) collective-permute-start(bf16[1024,128]{1,0:T(8,128)(2,1)S(1)} %get-tuple-element.35), channel_id=1, source_target_pairs={{0,2},{1,3},{2,0},{3,1},{4,6},{5,7},{6,4},{7,5},{8,10},{9,11},{10,... | collective-permute-start | bytes 786440 | tf_op jit(solution)/shard_map/ppermute | solution.py:554
  6.6 18.3 %collective-permute-start.14 = (bf16[1024,128]{1,0:T(8,128)(2,1)S(1)}, bf16[1024,128]{1,0:T(8,128)(2,1)S(1)}, u32[]{:S(2)}, u32[]{:S(2)}) collective-permute-start(bf16[1024,128]{1,0:T(8,128)(2,1)S(1)} %get-tuple-element.36), channel_id=1, source_target_pairs={{0,2},{1,3},{2,0},{3,1},{4,6},{5,7},{6,4},{7,5},{8,10},{9,11},{10,... | collective-permute-start | bytes 786440 | tf_op jit(solution)/shard_map/ppermute | solution.py:554
  8.5 22.0 %collective-permute-start.15 = (bf16[64,2048]{1,0:T(8,128)(2,1)S(1)}, bf16[64,2048]{1,0:T(8,128)(2,1)S(1)}, u32[]{:S(2)}, u32[]{:S(2)}) collective-permute-start(bf16[64,2048]{1,0:T(8,128)(2,1)S(1)} %get-tuple-element.37), channel_id=1, source_target_pairs={{0,2},{1,3},{2,0},{3,1},{4,6},{5,7},{6,4},{7,5},{8,10},{9,11},{10,... | collective-permute-start | bytes 786440 | tf_op jit(solution)/shard_map/ppermute | solution.py:554
  8.6 27.5 %collective-permute-start.16 = (bf16[64,2048]{1,0:T(8,128)(2,1)S(1)}, bf16[64,2048]{1,0:T(8,128)(2,1)S(1)}, u32[]{:S(2)}, u32[]{:S(2)}) collective-permute-start(bf16[64,2048]{1,0:T(8,128)(2,1)S(1)} %get-tuple-element.38), channel_id=1, source_target_pairs={{0,2},{1,3},{2,0},{3,1},{4,6},{5,7},{6,4},{7,5},{8,10},{9,11},{10,... | collective-permute-start | bytes 786440 | tf_op jit(solution)/shard_map/ppermute | solution.py:554
  13.7 34.6 %collective-permute-start = (bf16[136,1024]{1,0:T(8,128)(2,1)S(1)}, bf16[136,1024]{1,0:T(8,128)(2,1)S(1)}, u32[]{:S(2)}, u32[]{:S(2)}) collective-permute-start(bf16[136,1024]{1,0:T(8,128)(2,1)S(1)} %get-tuple-element.23.own_ref), channel_id=1, source_target_pairs={{0,4},{4,8},{8,12},{1,5},{5,9},{9,13},{2,6},{6,10},{10,14},{3,7},{... | collective-permute-start | bytes 835592 | tf_op jit(solution)/shard_map/ppermute | solution.py:563
  19.3 22.5 %collective-permute-start.28 = (bf16[64,2048]{1,0:T(8,128)(2,1)S(1)}, bf16[64,2048]{1,0:T(8,128)(2,1)S(1)}, u32[]{:S(2)}, u32[]{:S(2)}) collective-permute-start(bf16[64,2048]{1,0:T(8,128)(2,1)S(1)} %get-tuple-element.39), channel_id=1, source_target_pairs={{0,2},{1,3},{2,0},{3,1},{4,6},{5,7},{6,4},{7,5},{8,10},{9,11},{10,... | collective-permute-start | bytes 786440 | tf_op jit(solution)/shard_map/ppermute | solution.py:554
  24.9 21.6 %collective-permute-start.11 = (bf16[1024,128]{1,0:T(8,128)(2,1)S(1)}, bf16[1024,128]{1,0:T(8,128)(2,1)S(1)}, u32[]{:S(2)}, u32[]{:S(2)}) collective-permute-start(bf16[1024,128]{1,0:T(8,128)(2,1)S(1)} %get-tuple-element.33), channel_id=1, source_target_pairs={{0,2},{1,3},{2,0},{3,1},{4,6},{5,7},{6,4},{7,5},{8,10},{9,11},{10,... | collective-permute-start | bytes 786440 | tf_op jit(solution)/shard_map/ppermute | solution.py:554
  30.5 19.8 %collective-permute-start.37 = (bf16[96,2048]{1,0:T(8,128)(2,1)S(1)}, bf16[96,2048]{1,0:T(8,128)(2,1)S(1)}, u32[]{:S(2)}, u32[]{:S(2)}) collective-permute-start(bf16[96,2048]{1,0:T(8,128)(2,1)S(1)} %get-tuple-element.43), channel_id=1, source_target_pairs={{0,8},{4,12},{8,0},{12,4},{1,9},{5,13},{9,1},{13,5},{2,10},{6,14},... | collective-permute-start | bytes 1179656 | tf_op jit(solution)/shard_map/ppermute | solution.py:560
  36.1 12.4 %collective-permute-start.1 = (bf16[136,1024]{1,0:T(8,128)(2,1)S(1)}, bf16[136,1024]{1,0:T(8,128)(2,1)S(1)}, u32[]{:S(2)}, u32[]{:S(2)}) collective-permute-start(bf16[136,1024]{1,0:T(8,128)(2,1)S(1)} %get-tuple-element.23.own_ref), channel_id=1, source_target_pairs={{0,8},{1,9},{2,10},{3,11},{16,24},{17,25},{18,26},{19,27}} | collective-permute-start | bytes 835592 | tf_op jit(solution)/shard_map/ppermute | solution.py:580
  41.7 8.6 %collective-permute-start.24 = (bf16[1024,128]{1,0:T(8,128)(2,1)S(1)}, bf16[1024,128]{1,0:T(8,128)(2,1)S(1)}, u32[]{:S(2)}, u32[]{:S(2)}) collective-permute-start(bf16[1024,128]{1,0:T(8,128)(2,1)S(1)} %collective-permute-done.12.refs_10_.refs_8_), channel_id=1, source_target_pairs={{0,16},{16,0},{1,17},{17,1},{2,18},{18,2},{3,19},{19,3},{4,20},{20... | collective-permute-start | bytes 786440 | tf_op jit(solution)/shard_map/ppermute | solution.py:557
  46.5 9.2 %collective-permute-start.25 = (bf16[1024,128]{1,0:T(8,128)(2,1)S(1)}, bf16[1024,128]{1,0:T(8,128)(2,1)S(1)}, u32[]{:S(2)}, u32[]{:S(2)}) collective-permute-start(bf16[1024,128]{1,0:T(8,128)(2,1)S(1)} %collective-permute-done.13.refs_11_.refs_9_), channel_id=1, source_target_pairs={{0,16},{16,0},{1,17},{17,1},{2,18},{18,2},{3,19},{19,3},{4,20},{20... | collective-permute-start | bytes 786440 | tf_op jit(solution)/shard_map/ppermute | solution.py:557
  48.3 13.0 %collective-permute-start.26 = (bf16[1024,128]{1,0:T(8,128)(2,1)S(1)}, bf16[1024,128]{1,0:T(8,128)(2,1)S(1)}, u32[]{:S(2)}, u32[]{:S(2)}) collective-permute-start(bf16[1024,128]{1,0:T(8,128)(2,1)S(1)} %collective-permute-done.14.refs_12_.refs_10_), channel_id=1, source_target_pairs={{0,16},{16,0},{1,17},{17,1},{2,18},{18,2},{3,19},{19,3},{4,20},{20... | collective-permute-start | bytes 786440 | tf_op jit(solution)/shard_map/ppermute | solution.py:557
  48.6 16.7 %collective-permute-start.27 = (bf16[64,2048]{1,0:T(8,128)(2,1)S(1)}, bf16[64,2048]{1,0:T(8,128)(2,1)S(1)}, u32[]{:S(2)}, u32[]{:S(2)}) collective-permute-start(bf16[64,2048]{1,0:T(8,128)(2,1)S(1)} %collective-permute-done.15.refs_13_.refs_11_), channel_id=1, source_target_pairs={{0,16},{16,0},{1,17},{17,1},{2,18},{18,2},{3,19},{19,3},{4,20},{20... | collective-permute-start | bytes 786440 | tf_op jit(solution)/shard_map/ppermute | solution.py:557
  50.3 14.9 %collective-permute-start.18 = (bf16[1024,128]{1,0:T(8,128)(2,1)S(1)}, bf16[1024,128]{1,0:T(8,128)(2,1)S(1)}, u32[]{:S(2)}, u32[]{:S(2)}) collective-permute-start(bf16[1024,128]{1,0:T(8,128)(2,1)S(1)} %collective-permute-done.12.refs_10_.refs_8_), channel_id=1, source_target_pairs={{0,1},{1,0},{2,3},{3,2},{4,5},{5,4},{6,7},{7,6},{8,9},{9,8},{10,11... | collective-permute-start | bytes 786440 | tf_op jit(solution)/shard_map/ppermute | solution.py:551
  50.3 15.4 %collective-permute-start.19 = (bf16[1024,128]{1,0:T(8,128)(2,1)S(1)}, bf16[1024,128]{1,0:T(8,128)(2,1)S(1)}, u32[]{:S(2)}, u32[]{:S(2)}) collective-permute-start(bf16[1024,128]{1,0:T(8,128)(2,1)S(1)} %collective-permute-done.13.refs_11_.refs_9_), channel_id=1, source_target_pairs={{0,1},{1,0},{2,3},{3,2},{4,5},{5,4},{6,7},{7,6},{8,9},{9,8},{10,11... | collective-permute-start | bytes 786440 | tf_op jit(solution)/shard_map/ppermute | solution.py:551
  55.7 10.7 %collective-permute-start.20 = (bf16[1024,128]{1,0:T(8,128)(2,1)S(1)}, bf16[1024,128]{1,0:T(8,128)(2,1)S(1)}, u32[]{:S(2)}, u32[]{:S(2)}) collective-permute-start(bf16[1024,128]{1,0:T(8,128)(2,1)S(1)} %collective-permute-done.14.refs_12_.refs_10_), channel_id=1, source_target_pairs={{0,1},{1,0},{2,3},{3,2},{4,5},{5,4},{6,7},{7,6},{8,9},{9,8},{10,11... | collective-permute-start | bytes 786440 | tf_op jit(solution)/shard_map/ppermute | solution.py:551
  61.3 7.0 %collective-permute-start.21 = (bf16[64,2048]{1,0:T(8,128)(2,1)S(1)}, bf16[64,2048]{1,0:T(8,128)(2,1)S(1)}, u32[]{:S(2)}, u32[]{:S(2)}) collective-permute-start(bf16[64,2048]{1,0:T(8,128)(2,1)S(1)} %collective-permute-done.15.refs_13_.refs_11_), channel_id=1, source_target_pairs={{0,1},{1,0},{2,3},{3,2},{4,5},{5,4},{6,7},{7,6},{8,9},{9,8},{10,11... | collective-permute-start | bytes 786440 | tf_op jit(solution)/shard_map/ppermute | solution.py:551
  65.2 3.1 %collective-permute-start.22 = (bf16[64,2048]{1,0:T(8,128)(2,1)S(1)}, bf16[64,2048]{1,0:T(8,128)(2,1)S(1)}, u32[]{:S(2)}, u32[]{:S(2)}) collective-permute-start(bf16[64,2048]{1,0:T(8,128)(2,1)S(1)} %collective-permute-done.16.refs_14_.refs_12_), channel_id=1, source_target_pairs={{0,1},{1,0},{2,3},{3,2},{4,5},{5,4},{6,7},{7,6},{8,9},{9,8},{10,11... | collective-permute-start | bytes 786440 | tf_op jit(solution)/shard_map/ppermute | solution.py:551
  65.2 3.8 %collective-permute-start.34 = (bf16[64,2048]{1,0:T(8,128)(2,1)S(1)}, bf16[64,2048]{1,0:T(8,128)(2,1)S(1)}, u32[]{:S(2)}, u32[]{:S(2)}) collective-permute-start(bf16[64,2048]{1,0:T(8,128)(2,1)S(1)} %collective-permute-done.28.refs_26_.refs_24_), channel_id=1, source_target_pairs={{0,1},{1,0},{2,3},{3,2},{4,5},{5,4},{6,7},{7,6},{8,9},{9,8},{10,11... | collective-permute-start | bytes 786440 | tf_op jit(solution)/shard_map/ppermute | solution.py:551
  65.7 9.6 %collective-permute-start.2 = (bf16[136,1024]{1,0:T(8,128)(2,1)S(1)}, bf16[136,1024]{1,0:T(8,128)(2,1)S(1)}, u32[]{:S(2)}, u32[]{:S(2)}) collective-permute-start(bf16[136,1024]{1,0:T(8,128)(2,1)S(1)} %collective-permute-done.refs_0_), channel_id=1, source_target_pairs={{8,12},{9,13},{10,14},{11,15},{24,28},{25,29},{26,30},{27,31}} | collective-permute-start | bytes 835592 | tf_op jit(solution)/shard_map/ppermute | solution.py:581
  66.4 8.4 %collective-permute-start.23 = (bf16[1024,128]{1,0:T(8,128)(2,1)S(1)}, bf16[1024,128]{1,0:T(8,128)(2,1)S(1)}, u32[]{:S(2)}, u32[]{:S(2)}) collective-permute-start(bf16[1024,128]{1,0:T(8,128)(2,1)S(1)} %collective-permute-done.11.refs_9_.refs_7_), channel_id=1, source_target_pairs={{0,16},{16,0},{1,17},{17,1},{2,18},{18,2},{3,19},{19,3},{4,20},{20... | collective-permute-start | bytes 786440 | tf_op jit(solution)/shard_map/ppermute | solution.py:557
  68.3 6.5 %collective-permute-start.17 = (bf16[1024,128]{1,0:T(8,128)(2,1)S(1)}, bf16[1024,128]{1,0:T(8,128)(2,1)S(1)}, u32[]{:S(2)}, u32[]{:S(2)}) collective-permute-start(bf16[1024,128]{1,0:T(8,128)(2,1)S(1)} %collective-permute-done.11.refs_9_.refs_7_), channel_id=1, source_target_pairs={{0,1},{1,0},{2,3},{3,2},{4,5},{5,4},{6,7},{7,6},{8,9},{9,8},{10,11... | collective-permute-start | bytes 786440 | tf_op jit(solution)/shard_map/ppermute | solution.py:551
  68.3 7.1 %collective-permute-start.3 = (bf16[136,1024]{1,0:T(8,128)(2,1)S(1)}, bf16[136,1024]{1,0:T(8,128)(2,1)S(1)}, u32[]{:S(2)}, u32[]{:S(2)}) collective-permute-start(bf16[136,1024]{1,0:T(8,128)(2,1)S(1)} %collective-permute-done.1.refs_1_), channel_id=1, source_target_pairs={{8,12},{9,13},{10,14},{11,15},{24,28},{25,29},{26,30},{27,31}} | collective-permute-start | bytes 835592 | tf_op jit(solution)/shard_map/ppermute | solution.py:581
  69.0 6.8 %collective-permute-start.30 = (bf16[1024,128]{1,0:T(8,128)(2,1)S(1)}, bf16[1024,128]{1,0:T(8,128)(2,1)S(1)}, u32[]{:S(2)}, u32[]{:S(2)}) collective-permute-start(bf16[1024,128]{1,0:T(8,128)(2,1)S(1)} %collective-permute-done.24.refs_22_.refs_20_), channel_id=1, source_target_pairs={{0,1},{1,0},{2,3},{3,2},{4,5},{5,4},{6,7},{7,6},{8,9},{9,8},{10,11... | collective-permute-start | bytes 786440 | tf_op jit(solution)/shard_map/ppermute | solution.py:551
  74.8 19.4 %collective-permute-start.8 = (bf16[2048,256]{1,0:T(8,128)(2,1)S(1)}, bf16[2048,256]{1,0:T(8,128)(2,1)S(1)}, u32[]{:S(2)}, u32[]{:S(2)}) collective-permute-start(bf16[2048,256]{1,0:T(8,128)(2,1)S(1)} %bitcast.14), channel_id=1, source_target_pairs={{0,1},{1,0},{2,3},{3,2},{4,5},{5,4},{6,7},{7,6},{8,9},{9,8},{10,11... | collective-permute-start | bytes 3145736 | tf_op jit(solution)/shard_map/ppermute | solution.py:551
  74.8 19.4 %collective-permute-start.10 = (bf16[256,2048]{1,0:T(8,128)(2,1)S(1)}, bf16[256,2048]{1,0:T(8,128)(2,1)S(1)}, u32[]{:S(2)}, u32[]{:S(2)}) collective-permute-start(bf16[256,2048]{1,0:T(8,128)(2,1)S(1)} %bitcast.22), channel_id=1, source_target_pairs={{0,1},{1,0},{2,3},{3,2},{4,5},{5,4},{6,7},{7,6},{8,9},{9,8},{10,11... | collective-permute-start | bytes 3145736 | tf_op jit(solution)/shard_map/ppermute | solution.py:551
  75.3 18.9 %collective-permute-start.9 = (bf16[2048,256]{1,0:T(8,128)(2,1)S(1)}, bf16[2048,256]{1,0:T(8,128)(2,1)S(1)}, u32[]{:S(2)}, u32[]{:S(2)}) collective-permute-start(bf16[2048,256]{1,0:T(8,128)(2,1)S(1)} %bitcast.18), channel_id=1, source_target_pairs={{0,1},{1,0},{2,3},{3,2},{4,5},{5,4},{6,7},{7,6},{8,9},{9,8},{10,11... | collective-permute-start | bytes 3145736 | tf_op jit(solution)/shard_map/ppermute | solution.py:551
  75.4 5.4 %collective-permute-start.31 = (bf16[1024,128]{1,0:T(8,128)(2,1)S(1)}, bf16[1024,128]{1,0:T(8,128)(2,1)S(1)}, u32[]{:S(2)}, u32[]{:S(2)}) collective-permute-start(bf16[1024,128]{1,0:T(8,128)(2,1)S(1)} %collective-permute-done.25.refs_23_.refs_21_), channel_id=1, source_target_pairs={{0,1},{1,0},{2,3},{3,2},{4,5},{5,4},{6,7},{7,6},{8,9},{9,8},{10,11... | collective-permute-start | bytes 786440 | tf_op jit(solution)/shard_map/ppermute | solution.py:551
  75.8 5.4 %collective-permute-start.32 = (bf16[1024,128]{1,0:T(8,128)(2,1)S(1)}, bf16[1024,128]{1,0:T(8,128)(2,1)S(1)}, u32[]{:S(2)}, u32[]{:S(2)}) collective-permute-start(bf16[1024,128]{1,0:T(8,128)(2,1)S(1)} %collective-permute-done.26.refs_24_.refs_22_), channel_id=1, source_target_pairs={{0,1},{1,0},{2,3},{3,2},{4,5},{5,4},{6,7},{7,6},{8,9},{9,8},{10,11... | collective-permute-start | bytes 786440 | tf_op jit(solution)/shard_map/ppermute | solution.py:551
  80.8 1.5 %collective-permute-start.33 = (bf16[64,2048]{1,0:T(8,128)(2,1)S(1)}, bf16[64,2048]{1,0:T(8,128)(2,1)S(1)}, u32[]{:S(2)}, u32[]{:S(2)}) collective-permute-start(bf16[64,2048]{1,0:T(8,128)(2,1)S(1)} %collective-permute-done.27.refs_25_.refs_23_), channel_id=1, source_target_pairs={{0,1},{1,0},{2,3},{3,2},{4,5},{5,4},{6,7},{7,6},{8,9},{9,8},{10,11... | collective-permute-start | bytes 786440 | tf_op jit(solution)/shard_map/ppermute | solution.py:551
  81.2 3.0 %collective-permute-start.29 = (bf16[1024,128]{1,0:T(8,128)(2,1)S(1)}, bf16[1024,128]{1,0:T(8,128)(2,1)S(1)}, u32[]{:S(2)}, u32[]{:S(2)}) collective-permute-start(bf16[1024,128]{1,0:T(8,128)(2,1)S(1)} %collective-permute-done.23.refs_21_.refs_19_), channel_id=1, source_target_pairs={{0,1},{1,0},{2,3},{3,2},{4,5},{5,4},{6,7},{7,6},{8,9},{9,8},{10,11... | collective-permute-start | bytes 786440 | tf_op jit(solution)/shard_map/ppermute | solution.py:551
  82.4 17.9 %collective-permute-start.6 = (bf16[96,2048]{1,0:T(8,128)(2,1)S(1)}, bf16[96,2048]{1,0:T(8,128)(2,1)S(1)}, u32[]{:S(2)}, u32[]{:S(2)}) collective-permute-start(bf16[96,2048]{1,0:T(8,128)(2,1)S(1)} %get-tuple-element.31), channel_id=1, source_target_pairs={{0,4},{4,8},{8,12},{12,0},{1,5},{5,9},{9,13},{13,1},{2,6},{6,10},{... | collective-permute-start | bytes 1179656 | tf_op jit(solution)/shard_map/ppermute | solution.py:560
  84.2 21.7 %collective-permute-start.7 = (bf16[96,2048]{1,0:T(8,128)(2,1)S(1)}, bf16[96,2048]{1,0:T(8,128)(2,1)S(1)}, u32[]{:S(2)}, u32[]{:S(2)}) collective-permute-start(bf16[96,2048]{1,0:T(8,128)(2,1)S(1)} %get-tuple-element.32), channel_id=1, source_target_pairs={{0,12},{4,0},{8,4},{12,8},{1,13},{5,1},{9,5},{13,9},{2,14},{6,2},{... | collective-permute-start | bytes 1179656 | tf_op jit(solution)/shard_map/ppermute | solution.py:560
  89.5 1.6 %copy-start.3 = (bf16[512,2048]{1,0:T(8,128)(2,1)S(1)}, bf16[512,2048]{1,0:T(8,128)(2,1)}, u32[]{:S(2)}) copy-start(bf16[512,2048]{1,0:T(8,128)(2,1)} %refs_4_.1) | copy-start | bytes 6291460
  94.2 31.8 %collective-permute-start.4 = (bf16[64,2048]{1,0:T(8,128)(2,1)S(1)}, bf16[64,2048]{1,0:T(8,128)(2,1)S(1)}, u32[]{:S(2)}, u32[]{:S(2)}) collective-permute-start(bf16[64,2048]{1,0:T(8,128)(2,1)S(1)} %get-tuple-element.25), channel_id=1, source_target_pairs={{0,1},{1,0},{2,3},{3,2},{4,5},{5,4},{6,7},{7,6},{8,9},{9,8},{10,11... | collective-permute-start | bytes 786440 | tf_op jit(solution)/shard_map/ppermute | solution.py:551
  96.4 36.0 %collective-permute-start.38 = (bf16[96,2048]{1,0:T(8,128)(2,1)S(1)}, bf16[96,2048]{1,0:T(8,128)(2,1)S(1)}, u32[]{:S(2)}, u32[]{:S(2)}) collective-permute-start(bf16[96,2048]{1,0:T(8,128)(2,1)S(1)} %shard_map.147), channel_id=1, source_target_pairs={{0,8},{4,12},{8,0},{12,4},{1,9},{5,13},{9,1},{13,5},{2,10},{6,14},... | collective-permute-start | bytes 1179656 | tf_op jit(solution)/shard_map/ppermute | solution.py:560
  105.8 22.3 %copy-start.6 = (s32[128,2]{0,1:T(2,128)S(1)}, s32[128,2]{0,1:T(2,128)}, u32[]{:S(2)}) copy-start(s32[128,2]{0,1:T(2,128)} %param.21) | copy-start | bytes 3076
  105.8 22.3 %copy-start.7 = (f32[128,2]{0,1:T(2,128)S(1)}, f32[128,2]{0,1:T(2,128)}, u32[]{:S(2)}) copy-start(f32[128,2]{0,1:T(2,128)} %param.22) | copy-start | bytes 3076
  105.8 25.8 %copy-start.5 = (f32[2048]{0:T(1024)S(1)}, f32[2048]{0:T(1024)}, u32[]{:S(2)}) copy-start(f32[2048]{0:T(1024)} %param.18) | copy-start | bytes 24580
  109.7 31.0 %collective-permute-start.35 = (bf16[96,2048]{1,0:T(8,128)(2,1)S(1)}, bf16[96,2048]{1,0:T(8,128)(2,1)S(1)}, u32[]{:S(2)}, u32[]{:S(2)}) collective-permute-start(bf16[96,2048]{1,0:T(8,128)(2,1)S(1)} %get-tuple-element.40), channel_id=1, source_target_pairs={{0,12},{4,0},{8,4},{12,8},{1,13},{5,1},{9,5},{13,9},{2,14},{6,2},{... | collective-permute-start | bytes 1179656 | tf_op jit(solution)/shard_map/ppermute | solution.py:560
  112.7 28.0 %collective-permute-start.36 = (bf16[96,2048]{1,0:T(8,128)(2,1)S(1)}, bf16[96,2048]{1,0:T(8,128)(2,1)S(1)}, u32[]{:S(2)}, u32[]{:S(2)}) collective-permute-start(bf16[96,2048]{1,0:T(8,128)(2,1)S(1)} %get-tuple-element.41), channel_id=1, source_target_pairs={{0,4},{4,8},{8,12},{12,0},{1,5},{5,9},{9,13},{13,1},{2,6},{6,10},{... | collective-permute-start | bytes 1179656 | tf_op jit(solution)/shard_map/ppermute | solution.py:560
  126.6 5.0 %collective-permute-start.5 = (bf16[32,2048]{1,0:T(8,128)(2,1)S(1)}, bf16[32,2048]{1,0:T(8,128)(2,1)S(1)}, u32[]{:S(2)}, u32[]{:S(2)}) collective-permute-start(bf16[32,2048]{1,0:T(8,128)(2,1)S(1)} %get-tuple-element.27), channel_id=1, source_target_pairs={{0,2},{1,3},{2,0},{3,1},{4,6},{5,7},{6,4},{7,5},{8,10},{9,11},{10,... | collective-permute-start | bytes 393224 | tf_op jit(solution)/shard_map/ppermute | solution.py:554
